TPU v7x, 512 devices: a whole 4x4x16 slice. The times are simulated.
512 devices in a mesh: sp: 128 (over z, x, core), tp: 4 (over y).
Axes of the slice: x: 4, y: 4, z: 16, core: 2. Of those that a mesh axis runs over, the one named last changes fastest.
Arguments:
- tokens: bfloat16 [16384, 2048], P('sp', 'tp'), may hold values from -6 to 6
- conv_value_weight: bfloat16 [2048, 1024], P('sp', 'tp'), may hold values from -0.125 to 0.125
- conv_gate_weight: bfloat16 [2048, 1024], P('sp', 'tp'), may hold values from -0.125 to 0.125
- conv_kernel: bfloat16 [31, 1024], P(None, 'tp'), may hold values from -16 to 16
- conv_norm_gain: float32 [1024], P('tp'), may hold values from 0.1 to 1.9
- query_weight: bfloat16 [2048, 2048], P('sp', 'tp'), may hold values from -0.125 to 0.125
- key_weight: bfloat16 [2048, 2048], P('sp', 'tp'), may hold values from -0.125 to 0.125
- value_weight: bfloat16 [2048, 2048], P('sp', 'tp'), may hold values from -0.125 to 0.125
- input_gate_weight: bfloat16 [2048, 8], P(None, 'tp'), may hold values from -0.125 to 0.125
- forget_gate_weight: bfloat16 [2048, 8], P(None, 'tp'), may hold values from -0.125 to 0.125
- input_offset: float32 [16384, 8], P('sp', 'tp'), may hold values from -4 to 210
- forget_offset: float32 [16384, 8], P('sp', 'tp'), may hold values from 0 to 30
- memory_norm_gain: float32 [2048], P('tp'), may hold values from 0.1 to 1.9
- conv_out_weight: bfloat16 [1024, 2048], P('tp', 'sp'), may hold values from -0.3125 to 0.3125
- memory_out_weight: bfloat16 [2048, 2048], P('tp', 'sp'), may hold values from -0.125 to 0.125
Outputs:
- mixed: bfloat16 [16384, 2048], P('sp', 'tp')
All inputs are finite; a program needn't handle non-finite values.
Results may differ from a plain program's by a relative error of at most 0.03.
Values may be sent and summed in bfloat16 or wider, within the bound.
No kernel may reach another device: no remote copies, remote signals or barrier semaphores. Data moves between devices by JAX's collectives and lax.ppermute only.
A program may use at most 128 MiB of HBM per device.

v0:
```python
import jax
import jax.numpy as jnp
from jax import lax
from jax.sharding import Mesh
from jax.sharding import PartitionSpec as P

BLOCK = 64
SP = ("sp_0", "sp_1", "sp_2")


EPS = 1e-06
LOWEST_LEVEL = -1e30


def in_order(blocks, dim):
    blocks = jnp.moveaxis(blocks, 0, dim)
    lengths = blocks.shape
    return blocks.reshape(*lengths[:dim], lengths[dim] * lengths[dim + 1], *lengths[dim + 2 :])


def copy_for_each(shard, axis):
    copies = jnp.broadcast_to(shard, (lax.axis_size(axis), *shard.shape))
    return lax.all_to_all(copies, axis, split_axis=0, concat_axis=0, tiled=True)


def gather_directly(shard, axis, dim):
    return in_order(copy_for_each(shard, axis), dim)


def sent_together(arrays, axis, dim, along):
    ends, at = ([], 0)
    for a in arrays[:-1]:
        at += a.shape[along]
        ends.append(at)
    both = jnp.concatenate(arrays, axis=along)
    return tuple(jnp.split(lax.all_gather(both, axis, axis=dim, tiled=True), ends, axis=along))


def shifted_2(value, axis, steps):
    count = lax.axis_size(axis)
    leading, last = (max(0, -steps), min(count, count - steps))
    return lax.ppermute(value, axis, [(source, source + steps) for source in range(leading, last)])


def neutral_like(shard, identity):
    return jax.tree.map(
        lambda a, e: jnp.broadcast_to(jnp.asarray(e, a.dtype), a.shape), shard, identity
    )


def entering(shard, axes, combine, identity):
    before = start = neutral_like(shard, identity)
    total = shard
    for axis in reversed(axes):
        devices, position = (lax.axis_size(axis), lax.axis_index(axis))
        pieces = jax.tree.map(
            lambda part, kind: lax.all_gather(part.astype(kind), axis),
            total,
            (jnp.bfloat16, jnp.bfloat16, jnp.bfloat16, jnp.bfloat16),
        )
        inside, total = (start, start)
        for k in range(devices):
            passed = k < position
            total = combine(
                total, jax.tree.map(lambda part, own: part[k].astype(own.dtype), pieces, shard)
            )
            inside = jax.tree.map(lambda new, old: jnp.where(passed, new, old), total, inside)
        before = combine(inside, before)
    return before


def of_everyone(shard, axis):
    return copy_for_each(shard, axis).sum(axis=0)


def turned_gather(arrays, axis, dims):
    turned = [jnp.moveaxis(a, dim, 0) for a, dim in zip(arrays, dims)]
    both = jnp.concatenate([t.reshape(len(t), -1) for t in turned], axis=1)
    out, at, finished = (lax.all_gather(both, axis, axis=0, tiled=True), 0, [])
    for t, dim in zip(turned, dims):
        share = out[:, at : at + t[0].size].reshape(-1, *t.shape[1:])
        finished.append(jnp.moveaxis(share, 0, dim))
        at += t[0].size
    return tuple(finished)


def cut_along(shard, dim, devices):
    before, after = (shard.shape[:dim], shard.shape[dim + 1 :])
    return jnp.moveaxis(shard.reshape(*before, devices, -1, *after), dim, 0)


def sum_at_owner(shard, axis, dim):
    blocks = cut_along(shard, dim, lax.axis_size(axis))
    arrived = lax.all_to_all(blocks, axis, split_axis=0, concat_axis=0, tiled=True)
    return arrived.astype(jnp.float32).sum(axis=0)


def block_step(carry, inputs):
    state, normal, level = carry
    query, key, value, gate_in, forget_log = inputs
    length = gate_in.shape[-1]
    scale = query.shape[-1] ** (-0.5)
    causal = jnp.tril(jnp.ones((length, length), dtype=bool))
    within = jnp.cumsum(forget_log, axis=-1)
    log_weight = within[:, :, None] - within[:, None, :] + gate_in[:, None, :]
    log_weight = jnp.where(causal, log_weight, -jnp.inf)
    carried = within + level[:, None]
    top = jnp.maximum(carried, jnp.max(log_weight, axis=-1))
    weight = jnp.exp(log_weight - top[:, :, None])
    carried_weight = jnp.exp(carried - top) * scale
    scores = jnp.einsum("htd,hsd->hts", query, key, preferred_element_type=jnp.float32) * (
        scale * weight
    )
    numer = jnp.einsum(
        "hts,hse->hte", scores.astype(jnp.bfloat16), value, preferred_element_type=jnp.float32
    )
    numer = numer + carried_weight[:, :, None] * jnp.einsum(
        "hed,htd->hte", state.astype(jnp.bfloat16), query, preferred_element_type=jnp.float32
    )
    denom = jnp.sum(scores, axis=-1) + carried_weight * jnp.einsum(
        "hd,htd->ht", normal.astype(jnp.bfloat16), query, preferred_element_type=jnp.float32
    )
    result = numer / jnp.maximum(jnp.abs(denom), 1.0)[:, :, None]
    last = within[:, -1]
    end_log = last[:, None] - within + gate_in
    new_level = jnp.maximum(last + level, jnp.max(end_log, axis=-1))
    keep = jnp.exp(last + level - new_level)
    fresh = jnp.exp(end_log - new_level[:, None])
    scaled_key = (fresh[:, :, None] * key).astype(jnp.bfloat16)
    new_state = keep[:, None, None] * state + jnp.einsum(
        "hse,hsd->hed", value, scaled_key, preferred_element_type=jnp.float32
    )
    new_normal = keep[:, None] * normal + jnp.sum(scaled_key.astype(jnp.float32), axis=1)
    return ((new_state, new_normal, new_level), result)


def depthwise(extended, kernel):
    taps = kernel.shape[0]
    length = extended.shape[0] - taps + 1
    total = extended[0:length] * kernel[0]
    for index in range(1, taps):
        total = total + extended[index : index + length] * kernel[index]
    return total


def merge_states(first, second):
    first_state, first_normal, first_level, first_total = first
    second_state, second_normal, second_level, second_total = second
    shifted = first_level + second_total
    level = jnp.maximum(shifted, second_level)
    older = jnp.exp(shifted - level)
    newer = jnp.exp(second_level - level)
    state = older[:, None, None] * first_state + newer[:, None, None] * second_state
    normal = older[:, None] * first_normal + newer[:, None] * second_normal
    return (state, normal, level, first_total + second_total)


def on_device(
    tokens,
    conv_value_weight,
    conv_gate_weight,
    conv_kernel,
    conv_norm_gain,
    query_weight,
    key_weight,
    value_weight,
    input_gate_weight,
    forget_gate_weight,
    input_offset,
    forget_offset,
    memory_norm_gain,
    conv_out_weight,
    memory_out_weight,
):
    length = tokens.shape[0]
    heads_here = input_gate_weight.shape[1]
    whole = gather_directly(tokens, "tp", 1)
    gathered = sent_together(
        (conv_value_weight, conv_gate_weight, query_weight, key_weight, value_weight), SP, 0, 1
    )
    folded = tuple(
        (jnp.dot(whole, weight, preferred_element_type=jnp.float32) for weight in gathered)
    )
    conv_value, conv_gate, query_flat, key_flat, value_flat = folded
    gate_pre = jnp.dot(whole, input_gate_weight, preferred_element_type=jnp.float32)
    forget_pre = jnp.dot(whole, forget_gate_weight, preferred_element_type=jnp.float32)
    glu = (conv_value * jax.nn.sigmoid(conv_gate)).astype(jnp.bfloat16)
    taps = conv_kernel.shape[0]
    head_dim = query_flat.shape[1] // heads_here

    def to_heads(flat):
        return flat.astype(jnp.bfloat16).reshape(length, heads_here, head_dim).transpose(1, 0, 2)

    query = to_heads(query_flat)
    key = to_heads(key_flat)
    value = to_heads(value_flat)
    gate_in = (gate_pre + input_offset).T
    forget_log = jax.nn.log_sigmoid(forget_pre + forget_offset).T
    within = jnp.cumsum(forget_log, axis=1)
    total = within[:, -1]
    end_log = total[:, None] - within + gate_in
    local_level = jnp.max(end_log, axis=1)
    fresh = jnp.exp(end_log - local_level[:, None])
    scaled_key = (fresh[:, :, None] * key).astype(jnp.bfloat16)
    local_state = jnp.einsum("hse,hsd->hed", value, scaled_key, preferred_element_type=jnp.float32)
    local_normal = jnp.sum(scaled_key.astype(jnp.float32), axis=1)
    blank_state = (
        jnp.zeros_like(local_state),
        jnp.zeros_like(local_normal),
        jnp.full_like(local_level, LOWEST_LEVEL),
        jnp.zeros_like(total),
    )
    prior = shifted_2(glu[length - (taps - 1) :], SP, 1)
    incoming = entering(
        (local_state, local_normal, local_level, total), SP, merge_states, blank_state
    )
    extended = jnp.concatenate([prior, glu], axis=0).astype(jnp.float32)
    conv = depthwise(extended, conv_kernel.astype(jnp.float32))
    blocks = length // BLOCK

    def split(array):
        return jnp.moveaxis(array.reshape((heads_here, blocks, BLOCK) + array.shape[2:]), 1, 0)

    _, hidden = lax.scan(
        block_step,
        tuple(incoming[:3]),
        (split(query), split(key), split(value), split(gate_in), split(forget_log)),
    )
    hidden = jnp.moveaxis(hidden, 0, 1).reshape(heads_here, length, head_dim)
    hidden_squares = jnp.sum(hidden * hidden, axis=(0, 2))
    channel_sum, channel_squares, memory_squares = (
        of_everyone(jnp.sum(conv, axis=1), "tp"),
        of_everyone(jnp.sum(conv * conv, axis=1), "tp"),
        of_everyone(hidden_squares, "tp"),
    )
    channels = conv.shape[1] * lax.axis_size("tp")
    mean = (channel_sum / channels)[:, None]
    variance = (channel_squares / channels)[:, None] - mean * mean
    conv_branch = jax.nn.silu((conv - mean) * lax.rsqrt(variance + EPS) * conv_norm_gain).astype(
        jnp.bfloat16
    )
    entries = heads_here * head_dim * lax.axis_size("tp")
    memory_scale = lax.rsqrt(memory_squares / entries + EPS)
    hidden = hidden * memory_scale[None, :, None]
    hidden = hidden * memory_norm_gain.reshape(heads_here, 1, head_dim)
    memory_branch = (
        hidden.transpose(1, 0, 2).reshape(length, heads_here * head_dim).astype(jnp.bfloat16)
    )
    conv_columns, memory_columns = turned_gather((conv_out_weight, memory_out_weight), SP, (1, 1))
    contract = (((0,), (1,)), ((), ()))
    summed = sum_at_owner(
        (
            lax.dot_general(conv_columns, conv_branch, contract, preferred_element_type=jnp.float32)
            + lax.dot_general(
                memory_columns, memory_branch, contract, preferred_element_type=jnp.float32
            )
        ).astype(jnp.bfloat16),
        "tp",
        0,
    )
    return summed.T.astype(jnp.bfloat16)


def solution(mesh):
    split = Mesh(mesh.devices.reshape(16, 4, 2, mesh.shape["tp"]), ("sp_0", "sp_1", "sp_2", "tp"))
    in_specs = (
        P(SP, "tp"),
        P(SP, "tp"),
        P(SP, "tp"),
        P(None, "tp"),
        P("tp"),
        P(SP, "tp"),
        P(SP, "tp"),
        P(SP, "tp"),
        P(None, "tp"),
        P(None, "tp"),
        P(SP, "tp"),
        P(SP, "tp"),
        P("tp"),
        P("tp", SP),
        P("tp", SP),
    )
    out_specs = P(SP, "tp")
    return jax.shard_map(
        on_device, mesh=split, in_specs=in_specs, out_specs=out_specs, check_vma=False
    )
```

profile of v0, /device:TPU:1, one launch (start us, length us, event | category | flops | bytes accessed | tf_op | source)
XLA Modules:
  0.0 445.2 jit_solution(18037875826479777491)
XLA Ops:
  12.7 5.0 %all-to-all-start = ((bf16[4,128,512]{1,2,0:T(8,128)(2,1)}), bf16[4,128,512]{1,2,0:T(8,128)(2,1)S(1)}, u32[]{:S(2)}, u32[]{:S(2)}) async-start(bf16[4,128,512]{1,2,0:T(8,128)(2,1)} %broadcast_in_dim.26), calls=%async_computation | async-start | bytes 1048576 | tf_op jit(solution)/shard_map/all_to_all | solution.py:23
  19.6 5.0 %all-to-all-done = bf16[4,128,512]{1,2,0:T(8,128)(2,1)S(1)} async-done(((bf16[4,128,512]{1,2,0:T(8,128)(2,1)}), bf16[4,128,512]{1,2,0:T(8,128)(2,1)S(1)}, u32[]{:S(2)}, u32[]{:S(2)}) %all-to-all-start) | async-done | bytes 524320 | tf_op jit(solution)/shard_map/all_to_all | solution.py:23
  27.7 8.5 %all-reduce.2 = (bf16[4]{0:T(256)(128)(2,1)S(1)}, bf16[4]{0:T(256)(128)(2,1)S(1)}) all-reduce(bf16[4]{0:T(256)(128)(2,1)S(1)} %dynamic-update-slice.1, bf16[4]{0:T(256)(128)(2,1)S(1)} %dynamic-update-slice), channel_id=3, replica_groups=mesh['sp_0'=16,'sp_1'=4,'sp_2'=2,'tp'=4] {'sp_2'}, use_global_device_ids=true, to_apply=%add.1 | all-reduce | flops 8 | bytes 32
  36.3 5.6 %all-gather.4 = bf16[4,1,2]{2,1,0:T(2,128)(2,1)S(1)} all-gather(bf16[1,1,2]{2,1,0:T(2,128)(2,1)S(1)} %get-tuple-element.249), channel_id=1, replica_groups=mesh['sp_0'=16,'sp_1'=4,'sp_2'=2,'tp'=4] {'sp_1'}, dimensions={0}, use_global_device_ids=true | all-gather | bytes 20 | tf_op jit(solution)/shard_map/all_gather | solution.py:57
  41.9 7.2 %all-gather.6 = bf16[4,1,2]{2,1,0:T(2,128)(2,1)S(1)} all-gather(bf16[1,1,2]{2,1,0:T(2,128)(2,1)S(1)} %get-tuple-element.250), channel_id=1, replica_groups=mesh['sp_0'=16,'sp_1'=4,'sp_2'=2,'tp'=4] {'sp_1'}, dimensions={0}, use_global_device_ids=true | all-gather | bytes 20 | tf_op jit(solution)/shard_map/all_gather | solution.py:57
  49.1 26.7 %all-gather.7 = bf16[16,1,2]{2,1,0:T(2,128)(2,1)S(1)} all-gather(bf16[1,1,2]{2,1,0:T(2,128)(2,1)S(1)} %get-tuple-element.238), channel_id=1, replica_groups=mesh['sp_0'=16,'sp_1'=4,'sp_2'=2,'tp'=4] {'sp_0'}, dimensions={0}, use_global_device_ids=true | all-gather | bytes 68 | tf_op jit(solution)/shard_map/all_gather | solution.py:57
  75.8 20.2 %all-gather.5 = bf16[16,1,2]{2,1,0:T(2,128)(2,1)S(1)} all-gather(bf16[1,1,2]{2,1,0:T(2,128)(2,1)S(1)} %get-tuple-element.239), channel_id=1, replica_groups=mesh['sp_0'=16,'sp_1'=4,'sp_2'=2,'tp'=4] {'sp_0'}, dimensions={0}, use_global_device_ids=true | all-gather | bytes 68 | tf_op jit(solution)/shard_map/all_gather | solution.py:57
  96.3 67.5 %all-gather.16.cloned.1.call-done = bf16[2048,2048]{1,0:T(8,128)(2,1)} async-done(((bf16[16,2048]{1,0:T(8,128)(2,1)}), bf16[2048,2048]{1,0:T(8,128)(2,1)}) %all-gather.16.cloned.1.call-update) | async-done | bytes 8388624 | tf_op jit(solution)/shard_map/all_gather | solution.py:36
  166.4 2.4 fusion.37
  172.2 24.1 %all-gather.18.cloned.1.call-done = bf16[4,2,256,256]{3,2,1,0:T(8,128)(2,1)} async-done(((bf16[1,2,256,256]{3,2,1,0:T(8,128)(2,1)}), bf16[4,2,256,256]{3,2,1,0:T(8,128)(2,1)}) %all-gather.18.cloned.1.call-update) | async-done | bytes 1048592 | tf_op jit(solution)/shard_map/all_gather | solution.py:57
  199.8 4.2 all-gather.8
  204.1 6.5 %all_gather.72 = bf16[4,2,256]{2,1,0:T(2,128)(2,1)S(1)} all-gather(bf16[1,2,256]{2,1,0:T(2,128)(2,1)S(1)} %fusion.217), channel_id=1, replica_groups=mesh['sp_0'=16,'sp_1'=4,'sp_2'=2,'tp'=4] {'sp_1'}, dimensions={0}, use_global_device_ids=true | all-gather | bytes 5120 | tf_op jit(solution)/shard_map/all_gather | solution.py:57
  213.7 4.5 %collective-permute-start = (bf16[30,256]{1,0:T(8,128)(2,1)S(1)}, bf16[30,256]{1,0:T(8,128)(2,1)S(1)}, u32[]{:S(2)}, u32[]{:S(2)}) collective-permute-start(bf16[30,256]{1,0:T(8,128)(2,1)S(1)} %slice.672), channel_id=1, source_target_pairs={{0,4},{4,8},{8,12},{12,16},{16,20},{20,24},{24,28},{28,32},{32,36}... | collective-permute-start | bytes 46088 | tf_op jit(solution)/shard_map/ppermute | solution.py:42
  218.2 2.4 fusion.43
  221.9 4.0 all-to-all-start.2
  225.9 25.9 %all_gather.73 = bf16[16,2,256]{2,1,0:T(2,128)(2,1)S(1)} all-gather(bf16[1,2,256]{2,1,0:T(2,128)(2,1)S(1)} %fusion.182), channel_id=1, replica_groups=mesh['sp_0'=16,'sp_1'=4,'sp_2'=2,'tp'=4] {'sp_0'}, dimensions={0}, use_global_device_ids=true | all-gather | bytes 17408 | tf_op jit(solution)/shard_map/all_gather | solution.py:57
  252.3 4.6 %all-to-all-start.1 = ((f32[4,1,128]{2,1,0:T(1,128)}), f32[4,1,128]{2,1,0:T(1,128)S(1)}, u32[]{:S(2)}, u32[]{:S(2)}) async-start(f32[4,1,128]{2,1,0:T(1,128)} %broadcast_in_dim.27), calls=%async_computation.1 | async-start | bytes 4096 | tf_op jit(solution)/shard_map/all_to_all | solution.py:23
  257.3 3.9 all-to-all-done.1
  261.2 9.4 %all-gather.20.cloned.1.call-done = bf16[16,2,256,256]{3,2,1,0:T(8,128)(2,1)} async-done(((bf16[1,2,256,256]{3,2,1,0:T(8,128)(2,1)}), bf16[16,2,256,256]{3,2,1,0:T(8,128)(2,1)}) %all-gather.20.cloned.1.call-update) | async-done | bytes 4194320 | tf_op jit(solution)/shard_map/all_gather | solution.py:57
  270.6 4.5 %fusion.78 = f32[2,256,256]{2,1,0:T(8,128)S(1)} fusion(bf16[16,2,256,256]{3,2,1,0:T(8,128)(2,1)} %all-gather.20.cloned.1.call-done, f32[2]{0:T(128)S(1)} %get-tuple-element.247, f32[2]{0:T(128)S(1)} %get-tuple-element.241, f32[2]{0:T(128)S(1)} %get-tuple-element.246, f32[2]{0:T(128)S(1)} %get-tuple-element.245, f32[2]{0:T(128)S(1)} %get-tuple-element.240, ...), kind=kLoop, calls=%fused_computation.107 | loop fusion | flops 15073280 | bytes 6291878 | tf_op jit(solution)/shard_map/add | solution.py:153
  275.1 4.7 %while.16 = (s32[]{:T(128)}, f32[2,256,256]{2,1,0:T(8,128)S(1)}, f32[2,256]{1,0:T(2,128)S(1)}, f32[2]{0:T(128)S(1)}, f32[2,2,64,256]{3,2,0,1:T(8,128)S(1)}, /*in...) while((s32[]{:T(128)}, f32[2,256,256]{2,1,0:T(8,128)S(1)}, ...), condition=%wide.region_13.14_spmd, body=%wide.region_7.13_spmd.sunk | while | flops 42875268 | bytes 2589965 | solution.py:224
  280.6 4.0 all-to-all-start.3
  284.6 136.1 %all-gather.14.cloned.1.call-done = bf16[2048,768]{1,0:T(8,128)(2,1)} async-done(((bf16[16,768]{1,0:T(8,128)(2,1)}), bf16[2048,768]{1,0:T(8,128)(2,1)}) %all-gather.14.cloned.1.call-update) | async-done | bytes 3145744 | tf_op jit(solution)/shard_map/all_gather | solution.py:79
  425.0 12.8 %all_to_all.28 = bf16[4,512,128]{2,1,0:T(8,128)(2,1)S(1)} all-to-all(bf16[4,512,128]{2,1,0:T(8,128)(2,1)S(1)} %bitcast.981), channel_id=1, replica_groups=mesh['sp_0'=16,'sp_1'=4,'sp_2'=2,'tp'=4] {'tp'}, dimensions={0} | all-to-all | bytes 1048576 | tf_op jit(solution)/shard_map/all_to_all | solution.py:94
  (135 shorter events, 36.2 us)
Async XLA Ops:
  6.5 19.5 %copy-start = (bf16[2048,2]{0,1:T(2,128)(2,1)S(1)}, bf16[2048,2]{0,1:T(2,128)(2,1)}, u32[]{:S(2)}) copy-start(bf16[2048,2]{0,1:T(2,128)(2,1)} %param.25) | copy-start | bytes 24580
  6.5 157.3 %all-gather.16.cloned.1.call-start = ((), (), s32[]{:S(2)}) async-start(), calls=%async_computation.6 | async-start | bytes 8454144 | tf_op jit(solution)/shard_map/all_gather | solution.py:36
  10.1 0.6 copy-start.2
  12.7 11.9 %all-to-all-start = ((bf16[4,128,512]{1,2,0:T(8,128)(2,1)}), bf16[4,128,512]{1,2,0:T(8,128)(2,1)S(1)}, u32[]{:S(2)}, u32[]{:S(2)}) async-start(bf16[4,128,512]{1,2,0:T(8,128)(2,1)} %broadcast_in_dim.26), calls=%async_computation | async-start | bytes 1048576 | tf_op jit(solution)/shard_map/all_to_all | solution.py:23
  17.7 178.6 %all-gather.18.cloned.1.call-start = ((), (), s32[]{:S(2)}) async-start(), calls=%async_computation.7 | async-start | bytes 1310720 | tf_op jit(solution)/shard_map/all_gather | solution.py:57
  166.3 32.3 %copy-start.4 = (bf16[512,16]{0,1:T(8,128)(2,1)S(1)}, bf16[512,16]{0,1:T(8,128)(2,1)}, u32[]{:S(2)}) copy-start(bf16[512,16]{0,1:T(8,128)(2,1)} %param.31) | copy-start | bytes 49156
  166.3 32.3 %copy-start.5 = (bf16[256,16]{0,1:T(8,128)(2,1)S(1)}, bf16[256,16]{0,1:T(8,128)(2,1)}, u32[]{:S(2)}) copy-start(bf16[256,16]{0,1:T(8,128)(2,1)} %param.30) | copy-start | bytes 24580
  166.3 32.9 %copy-start.3 = (bf16[31,256]{1,0:T(8,128)(2,1)S(1)}, bf16[31,256]{1,0:T(8,128)(2,1)}, u32[]{:S(2)}) copy-start(bf16[31,256]{1,0:T(8,128)(2,1)} %param.20) | copy-start | bytes 47620
  166.3 33.0 %copy-start.6 = (f32[512]{0:T(512)S(1)}, f32[512]{0:T(512)}, u32[]{:S(2)}) copy-start(f32[512]{0:T(512)} %param.29) | copy-start | bytes 6148
  172.1 98.4 %all-gather.20.cloned.1.call-start = ((), (), s32[]{:S(2)}) async-start(), calls=%async_computation.8 | async-start | bytes 4456448 | tf_op jit(solution)/shard_map/all_gather | solution.py:57
  198.6 222.1 %all-gather.14.cloned.1.call-start = ((), (), s32[]{:S(2)}) async-start(), calls=%async_computation.5 | async-start | bytes 3170304 | tf_op jit(solution)/shard_map/all_gather | solution.py:79
  213.7 56.9 %copy-start.1 = (bf16[4,2,256,256]{3,2,1,0:T(8,128)(2,1)S(1)}, bf16[4,2,256,256]{3,2,1,0:T(8,128)(2,1)}, u32[]{:S(2)}) copy-start(bf16[4,2,256,256]{3,2,1,0:T(8,128)(2,1)} %all-gather.18.cloned.1.call-done) | copy-start | bytes 3145732
  213.7 7.0 %collective-permute-start = (bf16[30,256]{1,0:T(8,128)(2,1)S(1)}, bf16[30,256]{1,0:T(8,128)(2,1)S(1)}, u32[]{:S(2)}, u32[]{:S(2)}) collective-permute-start(bf16[30,256]{1,0:T(8,128)(2,1)S(1)} %slice.672), channel_id=1, source_target_pairs={{0,4},{4,8},{8,12},{12,16},{16,20},{20,24},{24,28},{28,32},{32,36}... | collective-permute-start | bytes 46088 | tf_op jit(solution)/shard_map/ppermute | solution.py:42
  221.9 29.9 %all-to-all-start.2 = ((f32[4,1,128]{2,1,0:T(1,128)}), f32[4,1,128]{2,1,0:T(1,128)S(1)}, u32[]{:S(2)}, u32[]{:S(2)}) async-start(f32[4,1,128]{2,1,0:T(1,128)} %broadcast_in_dim.28), calls=%async_computation.2 | async-start | bytes 4096 | tf_op jit(solution)/shard_map/all_to_all | solution.py:23
  252.3 8.9 %all-to-all-start.1 = ((f32[4,1,128]{2,1,0:T(1,128)}), f32[4,1,128]{2,1,0:T(1,128)S(1)}, u32[]{:S(2)}, u32[]{:S(2)}) async-start(f32[4,1,128]{2,1,0:T(1,128)} %broadcast_in_dim.27), calls=%async_computation.1 | async-start | bytes 4096 | tf_op jit(solution)/shard_map/all_to_all | solution.py:23
  275.1 145.6 %copy-start.7 = (f32[256]{0:T(256)S(1)}, f32[256]{0:T(256)}, u32[]{:S(2)}) copy-start(f32[256]{0:T(256)} %param.21) | copy-start | bytes 3076
  280.6 141.8 %all-to-all-start.3 = ((f32[4,1,128]{2,1,0:T(1,128)}), f32[4,1,128]{2,1,0:T(1,128)S(1)}, u32[]{:S(2)}, u32[]{:S(2)}) async-start(f32[4,1,128]{2,1,0:T(1,128)} %broadcast_in_dim.33), calls=%async_computation.3 | async-start | bytes 4096 | tf_op jit(solution)/shard_map/all_to_all | solution.py:23
Sparse Core Ops, SparseCore 0:
  10.9 152.9 all-gather.15
  172.3 24.0 all-gather.17
  198.7 71.8 all-gather.19
  273.6 147.0 all-gather.13
where the time goes:
time: 446 us; the launch traced here: 445 us
  waiting for transfers between devices  246 us (55%)
  blocking collectives  120 us (27%)
  starting transfers between devices  22.2 us (5%)
  matrix products  18.6 us (4%)
  between operations  14.1 us (3%)
  other arithmetic  12.5 us (3%)
  local copies, waits for them, and re-layouts  12 us (3%)
    all_gather x1, waiting for transfers between devices, turned_gather(): out, at, finished = (lax.all_gather(both, axis, axis=0, tiled=True), 0, [])  136 us
    all_gather x8, blocking collectives, entering(): lax.all_gather(part.astype(kind), axis)  98.4 us
    all_gather x1, waiting for transfers between devices, sent_together(): lax.all_gather(both, axis, axis=dim, tiled=True)  67.5 us
    all_gather x2, waiting for transfers between devices, entering(): lax.all_gather(part.astype(kind), axis)  33.5 us
    all_to_all x4, starting transfers between devices, copy_for_each(): return lax.all_to_all(copies, axis, split_axis=0, concat_axis=0, tiled=True)  17.6 us
    all_to_all x1, blocking collectives, sum_at_owner(): lax.all_to_all(blocks, axis, split_axis=0, concat_axis=0, tiled=True)  12.8 us
    dot_general x5, matrix products, on_device(): jnp.dot(whole, weight, preferred_element_type=jnp.float32)  10.2 us
  transfers between devices with their start and end apart: 9, of which 6 were waited for; matrix products, arithmetic and copies ran while one was open for 6% of the time, Pallas kernels for 0%

commit v1 on v0

v1 whole, which is shorter than its diff:
```python
import jax
import jax.numpy as jnp
from jax import lax
from jax.experimental import pallas as pl
from jax.experimental.pallas import tpu as pltpu
from jax.sharding import Mesh
from jax.sharding import PartitionSpec as P

AXES = ("zh", "zl", "x", "c", "tp")
Z = ("zh", "zl")
SP = ("zh", "zl", "x", "c")
EPS = 1e-06
LOW = -1e30
F32 = jnp.float32
BF16 = jnp.bfloat16
INTERPRET = False


def size(axis):
    return lax.axis_size(axis)


def exchange(pieces, axes):
    return lax.all_to_all(pieces, axes, split_axis=0, concat_axis=0, tiled=True)


def copies(shard, axes):
    return exchange(jnp.broadcast_to(shard, (lax.axis_size(axes), *shard.shape)), axes)


def swapped(value, axis):
    return lax.ppermute(value, axis, [(0, 1), (1, 0)])


def three(value):
    high = lax.reduce_precision(value, 8, 7)
    rest = value - high
    mid = lax.reduce_precision(rest, 8, 7)
    return high.astype(BF16), mid.astype(BF16), (rest - mid).astype(BF16)


def lane_cumsum(rows):
    lane = lax.broadcasted_iota(jnp.int32, rows.shape, 1)
    step = 1
    while step < rows.shape[1]:
        moved = pltpu.roll(rows, step, 1)
        rows = rows + jnp.where(lane >= step, moved, 0.0)
        step *= 2
    return rows


def columns_of(rows):
    count, length = rows.shape
    square = jnp.concatenate([rows, jnp.zeros((length - count, length), F32)], axis=0)
    return square.T


def dot(a, b, dims):
    return lax.dot_general(a, b, (dims, ((), ())), preferred_element_type=F32)


NN = ((1,), (0,))
NT = ((1,), (1,))
TN = ((0,), (0,))


def joined(parts_ref, start, width, chunk, length):
    picked = [
        parts_ref[j, chunk * length : (chunk + 1) * length, start : start + width]
        for j in range(parts_ref.shape[0])
    ]
    return jnp.concatenate(picked, axis=1)


def slab_kernel(qk_ref, v_ref, gate_ref, out_ref, q_ref, k_ref):
    chunks, length = gate_ref.shape[1], gate_ref.shape[2]
    width = qk_ref.shape[2] // 2
    gate, forget = gate_ref[0], gate_ref[1]
    within = lane_cumsum(forget)
    ends = [within[r : r + 1, length - 1 :] for r in range(chunks)]
    after = [jnp.zeros((1, 1), F32)]
    for r in range(chunks - 1, 0, -1):
        after.insert(0, after[0] + ends[r])
    total = after[0] + ends[0]
    to_end = jnp.concatenate([e + a for e, a in zip(ends, after)], axis=0)
    end_log = to_end - within + gate
    level = jnp.max(jnp.max(end_log, axis=1, keepdims=True), axis=0, keepdims=True)
    fresh = columns_of(jnp.exp(end_log - level))
    state = jnp.zeros((2 * width, width * qk_ref.shape[0]), F32)
    for r in range(chunks):
        q_ref[r * length : (r + 1) * length] = joined(qk_ref, 0, width, r, length)
        key = joined(qk_ref, width, width, r, length)
        k_ref[r * length : (r + 1) * length] = key
        scaled = (fresh[:, r : r + 1] * key.astype(F32)).astype(BF16)
        state = state + dot(v_ref[r * length : (r + 1) * length], scaled, TN)
    rows = out_ref.shape[0]
    kept = state[:rows]
    row = lax.broadcasted_iota(jnp.int32, kept.shape, 0)
    lane = lax.broadcasted_iota(jnp.int32, kept.shape, 1)
    for at, value in ((0, level), (3, total)):
        high = value.astype(BF16).astype(F32)
        mid = (value - high).astype(BF16).astype(F32)
        low = value - high - mid
        for k, part in enumerate((high, mid, low)):
            kept = jnp.where((row == width + 1) & (lane == at + k), part, kept)
    out_ref[...] = kept.astype(BF16)


def cell_kernel(place_ref, in_ref, q_ref, k_ref, v_ref, gate_ref, out_ref):
    chunks, length = gate_ref.shape[1], gate_ref.shape[2]
    members, rows, head = in_ref.shape
    width = out_ref.shape[1]
    scale = head ** (-0.5)
    place = place_ref[0]
    acc = jnp.zeros((1, 1), F32)
    logs = [None] * members
    for j in range(members - 1, -1, -1):
        line = in_ref[j, width + 1 : width + 2, :128].astype(F32)
        level_j = line[:, 0:1] + line[:, 1:2] + line[:, 2:3]
        total_j = line[:, 3:4] + line[:, 4:5] + line[:, 5:6]
        before = j < place
        logs[j] = jnp.where(before, level_j + acc, LOW)
        acc = acc + jnp.where(before, total_j, 0.0)
    level = logs[0]
    for j in range(1, members):
        level = jnp.maximum(level, logs[j])
    state = jnp.zeros((rows, head), F32)
    for j in range(members):
        weight = jnp.where(j < place, jnp.exp(logs[j] - level), 0.0)
        state = state + weight * in_ref[j].astype(F32)
    state = jnp.concatenate([state, jnp.zeros((2 * width - rows, head), F32)], axis=0)
    gate, forget = gate_ref[0], gate_ref[1]
    within = lane_cumsum(forget)
    turned = columns_of(jnp.concatenate([within, gate], axis=0))
    causal = lax.broadcasted_iota(jnp.int32, (length, length), 0) >= lax.broadcasted_iota(
        jnp.int32, (length, length), 1
    )
    for r in range(chunks):
        here = slice(r * length, (r + 1) * length)
        query, key, value = q_ref[here], k_ref[here], v_ref[here]
        within_row, gate_row = within[r : r + 1], gate[r : r + 1]
        within_col = turned[:, r : r + 1]
        gate_col = turned[:, chunks + r : chunks + r + 1]
        log_weight = jnp.where(causal, within_col - within_row + gate_row, -jnp.inf)
        carried = within_col + level
        top = jnp.maximum(carried, jnp.max(log_weight, axis=1, keepdims=True))
        weight = jnp.exp(log_weight - top)
        carried_weight = jnp.exp(carried - top) * scale
        scores = dot(query, key, NT) * (scale * weight)
        older = dot(query, state.astype(BF16), NT)
        numer = dot(scores.astype(BF16), value, NN) + carried_weight * older
        denom = jnp.sum(scores, axis=1, keepdims=True) + carried_weight * older[:, width : width + 1]
        result = numer[:, :width] / jnp.maximum(jnp.abs(denom), 1.0)
        out_ref[here] = result.astype(BF16)
        last = within_row[:, length - 1 :]
        end_row = last - within_row + gate_row
        new_level = jnp.maximum(last + level, jnp.max(end_row, axis=1, keepdims=True))
        keep = jnp.exp(last + level - new_level)
        fresh = jnp.exp(last - within_col + gate_col - new_level)
        scaled = (fresh * key.astype(F32)).astype(BF16)
        state = keep * state + dot(value, scaled, TN)
        level = new_level


def vmem(count):
    return [pl.BlockSpec(memory_space=pltpu.VMEM)] * count


def depthwise(extended, kernel):
    taps = kernel.shape[0]
    length = extended.shape[0] - taps + 1
    total = extended[0:length] * kernel[0]
    for index in range(1, taps):
        total = total + extended[index : index + length] * kernel[index]
    return total


def on_device(
    tokens,
    conv_value_weight,
    conv_gate_weight,
    conv_kernel,
    conv_norm_gain,
    query_weight,
    key_weight,
    value_weight,
    input_gate_weight,
    forget_gate_weight,
    input_offset,
    forget_offset,
    memory_norm_gain,
    conv_out_weight,
    memory_out_weight,
):
    nzh, nzl, nx, nc, ny = (size(a) for a in AXES)
    xi, ci = lax.axis_index("x"), lax.axis_index("c")
    length, part = tokens.shape
    slab = length * nx * nc
    head = query_weight.shape[1] // nc
    width = head // nx
    chan = conv_value_weight.shape[1] // nc // nx
    rows = query_weight.shape[0]
    features = part * ny

    out_rows = jnp.concatenate([memory_out_weight, conv_out_weight], axis=0).T
    turned = lax.ppermute(
        out_rows, ("zh", "tp"), [(a * ny + b, b * ny + a) for a in range(nzh) for b in range(ny)]
    )
    out_weight = lax.all_gather(turned, SP, axis=0, tiled=True).reshape(ny, part, -1)

    def cut(weight, each):
        return weight.reshape(rows, nc, nx, each)

    pieces = jnp.concatenate(
        [cut(w, width) for w in (query_weight, key_weight, value_weight)]
        + [cut(w, chan) for w in (conv_value_weight, conv_gate_weight)],
        axis=3,
    )
    wide = pieces.shape[3]
    pieces = pieces.transpose(2, 1, 0, 3).reshape(nx * nc, rows, wide)
    mine = exchange(pieces, ("x", "c")).reshape(nx * nc * rows, wide)
    mine = copies(mine, "zh").reshape(nzh, nx * nc * rows, wide)
    whole = copies(mine, "zl").reshape(nzl, nzh, nx * nc * rows, wide)
    weight = whole.transpose(1, 0, 2, 3).reshape(features, wide)

    extra = jnp.concatenate(
        [input_offset.T.reshape(-1), forget_offset.T.reshape(-1), conv_norm_gain, memory_norm_gain]
    )
    extra = jnp.concatenate(three(extra))
    extra_rows = -(-extra.shape[0] // part)
    extra_rows = -(-extra_rows // 8) * 8
    extra = jnp.pad(extra, (0, extra_rows * part - extra.shape[0])).reshape(extra_rows, part)
    sent = jnp.concatenate([tokens, extra], axis=0)
    own = copies(sent, ("x", "tp")).reshape(nx, ny, length + extra_rows, part)
    other = swapped(own, "c")
    first = ci == 0
    both = jnp.stack([jnp.where(first, own, other), jnp.where(first, other, own)], axis=1)
    slab_tokens = both[:, :, :, :length].transpose(0, 1, 3, 2, 4).reshape(slab, features)
    split_values = 4 * length + conv_norm_gain.shape[0] + memory_norm_gain.shape[0]
    extras = both[:, :, :, length:].reshape(nx, nc, ny, -1)[..., : 3 * split_values]
    extras = extras.reshape(nx, nc, ny, 3, split_values).astype(F32).sum(axis=3)
    gains = extras[0, 0, :, 4 * length :]
    conv_gain = gains[:, : conv_norm_gain.shape[0]].reshape(-1)
    memory_gain = gains[:, conv_norm_gain.shape[0] :].reshape(-1)
    yi = lax.axis_index("tp")
    offsets = lax.dynamic_index_in_dim(extras[..., : 4 * length], yi, 2, keepdims=False)
    offsets = offsets.reshape(nx * nc, 2, nc, length)
    offsets = lax.dynamic_index_in_dim(offsets, ci, 2, keepdims=False)

    projected = jnp.dot(slab_tokens, weight, preferred_element_type=F32)
    gate_weight = jnp.stack([input_gate_weight, forget_gate_weight], axis=0)
    gate_weight = lax.dynamic_index_in_dim(gate_weight, ci, 2, keepdims=False)
    gate_pre = lax.dot_general(
        gate_weight, slab_tokens, (((1,), (1,)), ((), ())), preferred_element_type=F32
    ).reshape(2, nx * nc, length)
    gates = jnp.stack(
        [gate_pre[0] + offsets[:, 0], jax.nn.log_sigmoid(gate_pre[1] + offsets[:, 1])], axis=0
    )
    qk = projected[:, : 2 * width].astype(BF16)
    value = projected[:, 2 * width : 3 * width].astype(BF16)
    lane = lax.broadcasted_iota(jnp.int32, (slab, width), 1)
    value = jnp.concatenate([value, jnp.where(lane == 0, 1.0, 0.0).astype(BF16)], axis=1)
    conv_value = projected[:, 3 * width : 3 * width + chan]
    conv_gate = projected[:, 3 * width + chan :]
    glu = (conv_value * jax.nn.sigmoid(conv_gate)).astype(BF16)

    taps = conv_kernel.shape[0]
    members = nzh * nzl
    prior = lax.ppermute(glu[slab - (taps - 1) :], Z, [(j, j + 1) for j in range(members - 1)])
    all_qk = copies(qk, "x")

    group = slab // nx
    packed = glu.reshape(nx, group, chan).transpose(1, 0, 2).reshape(group, nx * chan)
    lead = jnp.concatenate([prior, packed[group - (taps - 1) :, : (nx - 1) * chan]], axis=1)
    extended = jnp.concatenate([lead, packed], axis=0).astype(F32)
    own_kernel = lax.dynamic_slice_in_dim(conv_kernel, (ci * nx + xi) * chan, chan, 1).astype(F32)
    conv = depthwise(extended, jnp.tile(own_kernel, (1, nx)))
    conv_high = lax.reduce_precision(conv, 8, 7)
    conv_low = (conv - conv_high).astype(BF16).reshape(group, nx, chan)
    conv_high = conv_high.astype(BF16).reshape(group, nx, chan)
    conv_sent = jnp.concatenate([conv_high, conv_low], axis=2).transpose(1, 0, 2)

    state_rows = width + 8
    packed_state, query, key = pl.pallas_call(
        slab_kernel,
        out_shape=(
            jax.ShapeDtypeStruct((state_rows, head), BF16),
            jax.ShapeDtypeStruct((slab, head), BF16),
            jax.ShapeDtypeStruct((slab, head), BF16),
        ),
        in_specs=vmem(3),
        out_specs=vmem(3),
        interpret=INTERPRET,
        name="slab_state",
    )(all_qk.reshape(nx, slab, 2 * width), value, gates)
    states = copies(packed_state, Z).reshape(members, state_rows, head)
    place = (lax.axis_index("zh") * nzl + lax.axis_index("zl")).reshape(1)
    hidden = pl.pallas_call(
        cell_kernel,
        out_shape=jax.ShapeDtypeStruct((slab, width), BF16),
        in_specs=[pl.BlockSpec(memory_space=pltpu.SMEM)] + vmem(5),
        out_specs=pl.BlockSpec(memory_space=pltpu.VMEM),
        interpret=INTERPRET,
        name="cell",
    )(place, states, query, key, value, gates)

    last = jnp.concatenate([hidden.reshape(nx, group, width), conv_sent], axis=2)
    last = last.reshape(nx, nc, 1, length, width + 2 * chan)
    last = jnp.broadcast_to(last, (nx, nc, ny, length, width + 2 * chan))
    arrived = exchange(last.reshape(nx * nc * ny, length, -1), ("x", "c", "tp"))
    arrived = arrived.reshape(nx, nc, ny, length, -1).transpose(3, 2, 1, 0, 4)
    memory = arrived[..., :width].reshape(length, -1).astype(F32)
    conv = (
        arrived[..., width : width + chan].astype(F32) + arrived[..., width + chan :].astype(F32)
    ).reshape(length, -1)
    mean = jnp.mean(conv, axis=1, keepdims=True)
    variance = jnp.mean(conv * conv, axis=1, keepdims=True) - mean * mean
    conv_branch = jax.nn.silu((conv - mean) * lax.rsqrt(variance + EPS) * conv_gain).astype(BF16)
    memory_scale = lax.rsqrt(jnp.mean(memory * memory, axis=1, keepdims=True) + EPS)
    memory_branch = (memory * memory_scale * memory_gain).astype(BF16)
    heads_part = memory_out_weight.shape[0]
    total = jnp.zeros((length, part), F32)
    conv_part = conv_out_weight.shape[0]
    for b in range(ny):
        total = total + dot(
            memory_branch[:, b * heads_part : (b + 1) * heads_part], out_weight[b, :, :heads_part], NT
        )
        total = total + dot(
            conv_branch[:, b * conv_part : (b + 1) * conv_part], out_weight[b, :, heads_part:], NT
        )
    return total.astype(BF16)


def solution(mesh):
    shape = mesh.shape
    depth = shape["sp"] // 32
    split = Mesh(mesh.devices.reshape(4, depth, 4, 2, shape["tp"]), AXES)
    in_specs = (
        P(SP, "tp"),
        P(SP, "tp"),
        P(SP, "tp"),
        P(None, "tp"),
        P("tp"),
        P(SP, "tp"),
        P(SP, "tp"),
        P(SP, "tp"),
        P(None, "tp"),
        P(None, "tp"),
        P(SP, "tp"),
        P(SP, "tp"),
        P("tp"),
        P("tp", SP),
        P("tp", SP),
    )
    return jax.shard_map(
        on_device, mesh=split, in_specs=in_specs, out_specs=P(SP, "tp"), check_vma=False
    )
```

time: 446 us -> 278 us (0.62)
  waiting for transfers between devices: 246 us -> 102 us
  blocking collectives: 120 us -> 42.9 us
  starting transfers between devices: 22.2 us -> 56.2 us
  local copies, waits for them, and re-layouts: 12 us -> 28.5 us
  Pallas kernels: 0 us -> 9.74 us
  matrix products: 18.6 us -> 9.61 us
    all_gather x4 -> x1, waiting for transfers between devices: 237 us -> 28.1 us  [on_device(): lax.all_gather(turned, SP, axis=0, tiled=True).reshape(ny, part, -1)]
    all_gather x8 -> x0, blocking collectives: 98.4 us -> none  [entering(): lax.all_gather(part.astype(kind), axis)]
    all_to_all x4 -> x5, waiting for transfers between devices: 8.85 us -> 69.6 us  [exchange(): return lax.all_to_all(pieces, axes, split_axis=0, concat_axis=0, tiled=True)]
    all_to_all x1 -> x2, blocking collectives: 12.8 us -> 42.9 us  [exchange(): return lax.all_to_all(pieces, axes, split_axis=0, concat_axis=0, tiled=True)]
    all_to_all x4 -> x5, starting transfers between devices: 17.6 us -> 46.4 us  [exchange(): return lax.all_to_all(pieces, axes, split_axis=0, concat_axis=0, tiled=True)]
    pallas_call x0 -> x2, Pallas kernels: none -> 9.74 us  [the longest x1 6.2 us: on_device(): pl.pallas_call(cell_kernel, out_shape=jax.ShapeDtypeStruct((slab, width),...]
    dot_general x20 -> x10, matrix products: 18.6 us -> 9.61 us  [the longest x8 4.93 us: dot(): return lax.dot_general(a, b, (dims, ((), ())), preferred_element_type=F32)]
    unnamed x1 -> x0, blocking collectives: 8.53 us -> none
  transfers between devices with their start and end apart: 9 -> 9, of which waited for: 6 -> 7; matrix products, arithmetic and copies ran while one was open for 6% -> 13% of each run, Pallas kernels for 0% -> 4%
where the time goes in v1:
time: 278 us; the launch traced here: 276 us
  waiting for transfers between devices  102 us (37%)
  starting transfers between devices  56.2 us (20%)
  blocking collectives  42.9 us (15%)
  local copies, waits for them, and re-layouts  28.5 us (10%)
  between operations  14 us (5%)
  other arithmetic  13.5 us (5%)
  Pallas kernels  9.74 us (4%)
  matrix products  9.61 us (3%)
    all_to_all x5, waiting for transfers between devices, exchange(): return lax.all_to_all(pieces, axes, split_axis=0, concat_axis=0, tiled=True)  69.6 us
    all_to_all x5, starting transfers between devices, exchange(): return lax.all_to_all(pieces, axes, split_axis=0, concat_axis=0, tiled=True)  46.4 us
    all_to_all x2, blocking collectives, exchange(): return lax.all_to_all(pieces, axes, split_axis=0, concat_axis=0, tiled=True)  42.9 us
    all_gather x1, waiting for transfers between devices, on_device(): lax.all_gather(turned, SP, axis=0, tiled=True).reshape(ny, part, -1)  28.1 us
    pallas_call x1, Pallas kernels, on_device(): pl.pallas_call(cell_kernel, out_shape=jax.ShapeDtypeStruct((slab, width),...  6.2 us
    ppermute x1, starting transfers between devices, swapped(): return lax.ppermute(value, axis, [(0, 1), (1, 0)])  5.86 us
  transfers between devices with their start and end apart: 9, of which 7 were waited for; matrix products, arithmetic and copies ran while one was open for 13% of the time, Pallas kernels for 4%

profile of v1, /device:TPU:1, one launch (start us, length us, event | category | flops | bytes accessed | tf_op | source)
XLA Modules:
  0.0 276.4 jit_solution(7460503947080541290)
XLA Ops:
  10.8 14.1 %all_to_all.35 = bf16[8,16,256]{2,1,0:T(8,128)(2,1)S(1)} all-to-all(bf16[8,16,256]{2,1,0:T(8,128)(2,1)S(1)} %bitcast.212), channel_id=1, replica_groups=mesh['zh'=4,'zl'=4,'x'=4,'c'=2,'tp'=4] {'x','c'}, dimensions={0} | all-to-all | bytes 131072 | tf_op jit(solution)/shard_map/all_to_all | solution.py:24
  25.6 11.2 %all-to-all-start.2 = ((bf16[4,128,256]{2,1,0:T(8,128)(2,1)}), bf16[4,128,256]{2,1,0:T(8,128)(2,1)S(1)}, u32[]{:S(2)}, u32[]{:S(2)}) async-start(bf16[4,128,256]{2,1,0:T(8,128)(2,1)} %broadcast_in_dim.34), calls=%async_computation.2 | async-start | bytes 524288 | tf_op jit(solution)/shard_map/all_to_all | solution.py:24
  38.5 12.0 %all-to-all-done.2 = bf16[4,128,256]{2,1,0:T(8,128)(2,1)S(1)} async-done(((bf16[4,128,256]{2,1,0:T(8,128)(2,1)}), bf16[4,128,256]{2,1,0:T(8,128)(2,1)S(1)}, u32[]{:S(2)}, u32[]{:S(2)}) %all-to-all-start.2) | async-done | bytes 262176 | tf_op jit(solution)/shard_map/all_to_all | solution.py:24
  50.7 28.9 %all_to_all.36 = bf16[16,136,512]{2,1,0:T(8,128)(2,1)S(1)} all-to-all(bf16[16,136,512]{2,1,0:T(8,128)(2,1)S(1)} %broadcast_in_dim.33), channel_id=1, replica_groups=mesh['zh'=4,'zl'=4,'x'=4,'c'=2,'tp'=4] {'x','tp'}, dimensions={0} | all-to-all | bytes 4456448 | tf_op jit(solution)/shard_map/all_to_all | solution.py:24
  80.7 11.1 %all-to-all-start.3 = ((bf16[4,4,128,256]{3,2,1,0:T(8,128)(2,1)}), bf16[4,4,128,256]{3,2,1,0:T(8,128)(2,1)S(1)}, u32[]{:S(2)}, u32[]{:S(2)}) async-start(bf16[4,4,128,256]{3,2,1,0:T(8,128)(2,1)} %broadcast_in_dim.35), calls=%async_computation.3 | async-start | bytes 2097152 | tf_op jit(solution)/shard_map/all_to_all | solution.py:24
  91.9 5.9 %collective-permute-start = (bf16[4,4,136,512]{3,2,1,0:T(8,128)(2,1)S(1)}, bf16[4,4,136,512]{3,2,1,0:T(8,128)(2,1)}, u32[]{:S(2)}, u32[]{:S(2)}) collective-permute-start(bf16[4,4,136,512]{3,2,1,0:T(8,128)(2,1)S(1)} %bitcast.191), channel_id=1, source_target_pairs={{0,4},{4,0},{1,5},{5,1},{2,6},{6,2},{3,7},{7,3},{8,12},{12,8},{9,1... | collective-permute-start | bytes 6684680 | tf_op jit(solution)/shard_map/ppermute | solution.py:32
  99.2 18.9 %all-to-all-done.3 = bf16[4,4,128,256]{3,2,1,0:T(8,128)(2,1)S(1)} async-done(((bf16[4,4,128,256]{3,2,1,0:T(8,128)(2,1)}), bf16[4,4,128,256]{3,2,1,0:T(8,128)(2,1)S(1)}, u32[]{:S(2)}, u32[]{:S(2)}) %all-to-all-start.3) | async-done | bytes 1048608 | tf_op jit(solution)/shard_map/all_to_all | solution.py:24
  119.3 1.9 select_bitcast_fusion
  121.2 2.2 fusion.1
  123.8 5.4 %copy.45 = bf16[4,2,128,4,512]{4,3,2,1,0:T(4,128)(2,1)S(1)} copy(bf16[4,2,128,4,512]{4,2,3,0,1:T(8,128)(2,1)} %fusion.1) | data formatting | bytes 8388608 | tf_op jit(solution)/shard_map/transpose | solution.py:238
  134.4 3.5 %all-to-all-start.4 = ((bf16[4,1024,128]{2,1,0:T(8,128)(2,1)}), bf16[4,1024,128]{2,1,0:T(8,128)(2,1)S(1)}, u32[]{:S(2)}, u32[]{:S(2)}) async-start(bf16[4,1024,128]{2,1,0:T(8,128)(2,1)} %broadcast_in_dim.36), calls=%async_computation.4 | async-start | bytes 2097152 | tf_op jit(solution)/shard_map/all_to_all | solution.py:24
  137.9 3.4 %fusion.58 = f32[2,1024]{1,0:T(2,128)S(1)} fusion(bf16[1024,2048]{1,0:T(8,128)(2,1)} %bitcast.189, bf16[2,2048,1]{1,2,0:T(2,128)(2,1)S(1)} %dynamic-slice_maximum_fusion), kind=kOutput, calls=%fused_computation.138 | convolution fusion | flops 8388608 | bytes 4210688 | tf_op jit(solution)/shard_map/dot_general | solution.py:253
  142.7 8.4 %all-to-all-done.4.qk_ref = bf16[4,1024,128]{2,1,0:T(8,128)(2,1)S(1)} async-done(((bf16[4,1024,128]{2,1,0:T(8,128)(2,1)}), bf16[4,1024,128]{2,1,0:T(8,128)(2,1)S(1)}, u32[]{:S(2)}, u32[]{:S(2)}) %all-to-all-start.4) | async-done | bytes 1048608 | tf_op jit(solution)/shard_map/all_to_all | solution.py:24
  152.2 3.5 %slab_state.1 = (bf16[72,256]{1,0:T(8,128)(2,1)}, bf16[1024,256]{1,0:T(8,128)(2,1)}, bf16[1024,256]{1,0:T(8,128)(2,1)}) custom-call(bf16[4,1024,128]{2,1,0:T(8,128)(2,1)} %copy-done.2, bf16[1024,128]{1,0:T(8,128)(2,1)} %pad_maximum_fusion.1.v_ref, f32[2,8,128]{2,1,0:T(8,128)} %pad_maximum_fusion.4.gate_ref), custom_call_target="tpu_custom_call" | custom-call | tf_op jit(solution)/shard_map/slab_state/pallas_call | solution.py:284
  155.7 1.7 broadcast_in_dim.39
  157.4 6.2 %all-to-all-start.5 = ((bf16[16,72,256]{2,1,0:T(8,128)(2,1)}), bf16[16,72,256]{2,1,0:T(8,128)(2,1)S(1)}, u32[]{:S(2)}, u32[]{:S(2)}) async-start(bf16[16,72,256]{2,1,0:T(8,128)(2,1)} %broadcast_in_dim.39), calls=%async_computation.5 | async-start | bytes 1179648 | tf_op jit(solution)/shard_map/all_to_all | solution.py:24
  165.6 3.2 %collective-permute-start.1 = (bf16[30,32]{0,1:T(8,128)(2,1)S(1)}, bf16[30,32]{0,1:T(8,128)(2,1)S(1)}, u32[]{:S(2)}, u32[]{:S(2)}) collective-permute-start(bf16[30,32]{0,1:T(8,128)(2,1)S(1)} %slice.563), channel_id=1, source_target_pairs={{0,32},{32,64},{64,96},{96,128},{128,160},{160,192},{192,224},{224... | collective-permute-start | bytes 5768 | tf_op jit(solution)/shard_map/ppermute | solution.py:269
  170.0 4.1 %collective-permute-done.1 = bf16[30,32]{0,1:T(8,128)(2,1)S(1)} collective-permute-done((bf16[30,32]{0,1:T(8,128)(2,1)S(1)}, bf16[30,32]{0,1:T(8,128)(2,1)S(1)}, u32[]{:S(2)}, u32[]{:S(2)}) %collective-permute-start.1) | collective-permute-done | bytes 1952 | tf_op jit(solution)/shard_map/ppermute | solution.py:269
  174.1 1.8 reduce-precision_convert_fusion
  176.2 12.8 %all-to-all-done.5.in_ref = bf16[16,72,256]{2,1,0:T(8,128)(2,1)S(1)} async-done(((bf16[16,72,256]{2,1,0:T(8,128)(2,1)}), bf16[16,72,256]{2,1,0:T(8,128)(2,1)S(1)}, u32[]{:S(2)}, u32[]{:S(2)}) %all-to-all-start.5) | async-done | bytes 589856 | tf_op jit(solution)/shard_map/all_to_all | solution.py:24
  189.9 6.2 %cell.1 = bf16[1024,64]{1,0:T(8,128)(2,1)} custom-call(s32[1]{0:T(128)} %bitcast.place_ref, bf16[16,72,256]{2,1,0:T(8,128)(2,1)} %copy-done.4, bf16[1024,256]{1,0:T(8,128)(2,1)} %get-tuple-element.9.q_ref, bf16[1024,256]{1,0:T(8,128)(2,1)} %get-tuple-element.10.k_ref, bf16[1024,128]{1,0:T(8,128)(2,1)} %pad_maximum_fusion.1.v_ref, ...), custom_call_target="tpu_custom_call" | custom-call | tf_op jit(solution)/shard_map/cell/pallas_call | solution.py:298
  198.4 14.4 %all-to-all-start.6 = ((bf16[32,128,128]{2,1,0:T(8,128)(2,1)}), bf16[32,128,128]{2,1,0:T(8,128)(2,1)S(1)}, u32[]{:S(2)}, u32[]{:S(2)}) async-start(bf16[32,128,128]{2,1,0:T(8,128)(2,1)} %bitcast.62), calls=%async_computation.6 | async-start | bytes 2097152 | tf_op jit(solution)/shard_map/all_to_all | solution.py:24
  212.9 17.4 %all-to-all-done.6 = bf16[32,128,128]{2,1,0:T(8,128)(2,1)S(1)} async-done(((bf16[32,128,128]{2,1,0:T(8,128)(2,1)}), bf16[32,128,128]{2,1,0:T(8,128)(2,1)S(1)}, u32[]{:S(2)}, u32[]{:S(2)}) %all-to-all-start.6) | async-done | bytes 1048608 | tf_op jit(solution)/shard_map/all_to_all | solution.py:24
  236.1 28.1 %all-gather.2.cloned.1.call-done = bf16[2048,768]{1,0:T(8,128)(2,1)} async-done(((bf16[16,768]{1,0:T(8,128)(2,1)}), bf16[2048,768]{1,0:T(8,128)(2,1)}) %all-gather.2.cloned.1.call-update) | async-done | bytes 3145744 | tf_op jit(solution)/shard_map/all_gather | solution.py:209
  (165 shorter events, 36.0 us)
Async XLA Ops:
  25.6 24.9 %all-to-all-start.2 = ((bf16[4,128,256]{2,1,0:T(8,128)(2,1)}), bf16[4,128,256]{2,1,0:T(8,128)(2,1)S(1)}, u32[]{:S(2)}, u32[]{:S(2)}) async-start(bf16[4,128,256]{2,1,0:T(8,128)(2,1)} %broadcast_in_dim.34), calls=%async_computation.2 | async-start | bytes 524288 | tf_op jit(solution)/shard_map/all_to_all | solution.py:24
  50.7 47.1 %copy-start.7 = (bf16[512,16]{0,1:T(8,128)(2,1)S(1)}, bf16[512,16]{0,1:T(8,128)(2,1)}, u32[]{:S(2)}) copy-start(bf16[512,16]{0,1:T(8,128)(2,1)} %param.29) | copy-start | bytes 49156
  50.7 47.0 %copy-start.8 = (bf16[256,16]{0,1:T(8,128)(2,1)S(1)}, bf16[256,16]{0,1:T(8,128)(2,1)}, u32[]{:S(2)}) copy-start(bf16[256,16]{0,1:T(8,128)(2,1)} %param.28) | copy-start | bytes 24580
  50.7 47.7 %copy-start.9 = (bf16[2048,2]{0,1:T(2,128)(2,1)S(1)}, bf16[2048,2]{0,1:T(2,128)(2,1)}, u32[]{:S(2)}) copy-start(bf16[2048,2]{0,1:T(2,128)(2,1)} %param.24) | copy-start | bytes 24580
  50.7 47.7 %copy-start.10 = (bf16[2048,2]{0,1:T(2,128)(2,1)S(1)}, bf16[2048,2]{0,1:T(2,128)(2,1)}, u32[]{:S(2)}) copy-start(bf16[2048,2]{0,1:T(2,128)(2,1)} %param.23) | copy-start | bytes 24580
  80.7 37.4 %all-to-all-start.3 = ((bf16[4,4,128,256]{3,2,1,0:T(8,128)(2,1)}), bf16[4,4,128,256]{3,2,1,0:T(8,128)(2,1)S(1)}, u32[]{:S(2)}, u32[]{:S(2)}) async-start(bf16[4,4,128,256]{3,2,1,0:T(8,128)(2,1)} %broadcast_in_dim.35), calls=%async_computation.3 | async-start | bytes 2097152 | tf_op jit(solution)/shard_map/all_to_all | solution.py:24
  91.9 172.3 %all-gather.2.cloned.1.call-start = ((), (), s32[]{:S(2)}) async-start(), calls=%async_computation.7 | async-start | bytes 3170304 | tf_op jit(solution)/shard_map/all_gather | solution.py:209
  91.9 27.4 %collective-permute-start = (bf16[4,4,136,512]{3,2,1,0:T(8,128)(2,1)S(1)}, bf16[4,4,136,512]{3,2,1,0:T(8,128)(2,1)}, u32[]{:S(2)}, u32[]{:S(2)}) collective-permute-start(bf16[4,4,136,512]{3,2,1,0:T(8,128)(2,1)S(1)} %bitcast.191), channel_id=1, source_target_pairs={{0,4},{4,0},{1,5},{5,1},{2,6},{6,2},{3,7},{7,3},{8,12},{12,8},{9,1... | collective-permute-start | bytes 6684680 | tf_op jit(solution)/shard_map/ppermute | solution.py:32
  97.8 0.8 collective-permute-start.2
  98.6 0.6 copy-start.6
  129.2 1.4 copy-start.5
  130.6 1.9 copy-start
  134.4 16.8 %all-to-all-start.4 = ((bf16[4,1024,128]{2,1,0:T(8,128)(2,1)}), bf16[4,1024,128]{2,1,0:T(8,128)(2,1)S(1)}, u32[]{:S(2)}, u32[]{:S(2)}) async-start(bf16[4,1024,128]{2,1,0:T(8,128)(2,1)} %broadcast_in_dim.36), calls=%async_computation.4 | async-start | bytes 2097152 | tf_op jit(solution)/shard_map/all_to_all | solution.py:24
  137.9 25.7 %copy-start.11 = (bf16[31,256]{1,0:T(8,128)(2,1)S(1)}, bf16[31,256]{1,0:T(8,128)(2,1)}, u32[]{:S(2)}) copy-start(bf16[31,256]{1,0:T(8,128)(2,1)} %param.18) | copy-start | bytes 47620
  151.2 1.0 copy-start.2
  157.4 31.6 %all-to-all-start.5 = ((bf16[16,72,256]{2,1,0:T(8,128)(2,1)}), bf16[16,72,256]{2,1,0:T(8,128)(2,1)S(1)}, u32[]{:S(2)}, u32[]{:S(2)}) async-start(bf16[16,72,256]{2,1,0:T(8,128)(2,1)} %broadcast_in_dim.39), calls=%async_computation.5 | async-start | bytes 1179648 | tf_op jit(solution)/shard_map/all_to_all | solution.py:24
  165.6 8.4 %collective-permute-start.1 = (bf16[30,32]{0,1:T(8,128)(2,1)S(1)}, bf16[30,32]{0,1:T(8,128)(2,1)S(1)}, u32[]{:S(2)}, u32[]{:S(2)}) collective-permute-start(bf16[30,32]{0,1:T(8,128)(2,1)S(1)} %slice.563), channel_id=1, source_target_pairs={{0,32},{32,64},{64,96},{96,128},{128,160},{160,192},{192,224},{224... | collective-permute-start | bytes 5768 | tf_op jit(solution)/shard_map/ppermute | solution.py:269
  189.0 0.9 copy-start.4
  198.4 31.9 %all-to-all-start.6 = ((bf16[32,128,128]{2,1,0:T(8,128)(2,1)}), bf16[32,128,128]{2,1,0:T(8,128)(2,1)S(1)}, u32[]{:S(2)}, u32[]{:S(2)}) async-start(bf16[32,128,128]{2,1,0:T(8,128)(2,1)} %bitcast.62), calls=%async_computation.6 | async-start | bytes 2097152 | tf_op jit(solution)/shard_map/all_to_all | solution.py:24
  234.4 31.1 %copy-start.1 = (f32[128,4,2,4,64]{0,4,3,2,1:T(8,128)S(1)}, f32[128,4,2,4,64]{0,4,3,2,1:T(8,128)}, u32[]{:S(2)}) copy-start(f32[128,4,2,4,64]{0,4,3,2,1:T(8,128)} %copy.53) | copy-start | bytes 3145732
  264.2 3.0 %copy-start.3 = (bf16[2048,768]{1,0:T(8,128)(2,1)S(1)}, bf16[2048,768]{1,0:T(8,128)(2,1)}, u32[]{:S(2)}) copy-start(bf16[2048,768]{1,0:T(8,128)(2,1)} %all-gather.2.cloned.1.call-done) | copy-start | bytes 9437188
Sparse Core Ops, SparseCore 0:
  99.3 164.7 all-gather.1

commit v2 on v1

v2 whole, which is shorter than its diff:
```python
import jax
import jax.numpy as jnp
from jax import lax
from jax.experimental import pallas as pl
from jax.experimental.pallas import tpu as pltpu
from jax.sharding import Mesh
from jax.sharding import PartitionSpec as P

AXES = ("zh", "zl", "x", "c", "tp")
Z = ("zh", "zl")
SP = ("zh", "zl", "x", "c")
EPS = 1e-06
LOW = -1e30
F32 = jnp.float32
BF16 = jnp.bfloat16
INTERPRET = False


def size(axis):
    return lax.axis_size(axis)


def exchange(pieces, axes):
    return lax.all_to_all(pieces, axes, split_axis=0, concat_axis=0, tiled=True)


def swapped(value, axis):
    return lax.ppermute(value, axis, [(0, 1), (1, 0)])


def lane_cumsum(rows):
    lane = lax.broadcasted_iota(jnp.int32, rows.shape, 1)
    step = 1
    while step < rows.shape[1]:
        moved = pltpu.roll(rows, step, 1)
        rows = rows + jnp.where(lane >= step, moved, 0.0)
        step *= 2
    return rows


def columns_of(rows):
    count, length = rows.shape
    square = jnp.concatenate([rows, jnp.zeros((length - count, length), F32)], axis=0)
    return square.T


def dot(a, b, dims):
    return lax.dot_general(a, b, (dims, ((), ())), preferred_element_type=F32)


NN = ((1,), (0,))
NT = ((1,), (1,))
TN = ((0,), (0,))


def joined(parts_ref, start, width, chunk, length):
    picked = [
        parts_ref[j, chunk * length : (chunk + 1) * length, start : start + width]
        for j in range(parts_ref.shape[0])
    ]
    return jnp.concatenate(picked, axis=1)


def three_parts(value):
    high = value.astype(BF16).astype(F32)
    mid = (value - high).astype(BF16).astype(F32)
    return high, mid, value - high - mid


def pack_kernel(tokens_ref, offsets_ref, conv_gain_ref, memory_gain_ref, out_ref):
    length = tokens_ref.shape[0]
    offsets = three_parts(offsets_ref[...])
    conv_gain = three_parts(conv_gain_ref[...])
    memory_gain = three_parts(memory_gain_ref[...])
    rows = [jnp.concatenate([p[k : k + 1] for k in range(p.shape[0])], axis=1) for p in offsets]
    rows += memory_gain
    rows.append(jnp.concatenate(conv_gain[:2], axis=1))
    rows.append(jnp.concatenate([conv_gain[2], jnp.zeros_like(conv_gain[2])], axis=1))
    extra = jnp.concatenate(rows, axis=0).astype(BF16)
    tokens = tokens_ref[...]
    for j in range(out_ref.shape[0]):
        out_ref[j, :length] = tokens
        out_ref[j, length:] = extra


def piece_kernel(query_ref, key_ref, value_ref, left_ref, right_ref, out_weight_ref, out_ref):
    rows = query_ref.shape[0]
    nx, nc = out_ref.shape[0], out_ref.shape[1]
    wide = out_ref.shape[3]
    chunks = out_weight_ref.shape[1] // wide
    for x in range(nx):
        for c in range(nc):
            at = c * nx + x
            parts = []
            for ref in (query_ref, key_ref, value_ref, left_ref, right_ref):
                width = ref.shape[1] // (nx * nc)
                parts.append(ref[:, at * width : (at + 1) * width])
            out_ref[x, c, :rows] = jnp.concatenate(parts, axis=1)
            for k in range(chunks):
                out_ref[x, c, rows * (k + 1) : rows * (k + 2)] = out_weight_ref[
                    :, k * wide : (k + 1) * wide
                ]


def project_kernel(
    place_ref, own_ref, other_ref, w0_ref, w1_ref, w2_ref, w3_ref, gate_ref,
    qk_ref, v_ref, glu_ref, gates_ref, conv_gain_ref, memory_gain_ref,
):
    nx, ny, _, part = own_ref.shape
    block = w0_ref.shape[1]
    length = glu_ref.shape[1]
    blocks = part * ny // block
    per_part = part // block
    place, core, column = place_ref[0], place_ref[1], place_ref[2]
    groups = ((w0_ref, 0, w1_ref, 1), (w2_ref, 2, w3_ref, blocks - 1))
    tokens_rows = nx * length
    width = qk_ref.shape[4] // 2
    chan = glu_ref.shape[2] // nx
    lane = lax.broadcasted_iota(jnp.int32, (length, width), 1)
    ones = jnp.where(lane == 0, 1.0, 0.0).astype(BF16)
    row = lax.broadcasted_iota(jnp.int32, (2 * nx, length), 0)
    gate_in = jnp.zeros((2 * nx, length), F32)
    forget = jnp.zeros((2 * nx, length), F32)
    for half, ref in enumerate((own_ref, other_ref)):
        home = core if half == 0 else 1 - core
        acc = jnp.zeros((tokens_rows, w0_ref.shape[2]), F32)
        pre = jnp.zeros((tokens_rows, gate_ref.shape[1]), F32)
        for first_ref, first_at, second_ref, second_at in groups:
            for k in range(w0_ref.shape[0]):
                left, right, gate_rows = [], [], []
                for w_ref, at in ((first_ref, first_at), (second_ref, second_at)):
                    kb = lax.rem(place + at + k * (blocks // w0_ref.shape[0]), blocks)
                    lanes = pl.ds(pl.multiple_of(lax.rem(kb, per_part) * block, block), block)
                    left.append(
                        ref[:, lax.div(kb, per_part), :length, lanes].reshape(tokens_rows, block)
                    )
                    right.append(w_ref[k])
                    gate_rows.append(gate_ref[pl.ds(pl.multiple_of(kb * block, block), block)])
                lhs = jnp.concatenate(left, axis=1)
                acc = acc + dot(lhs, jnp.concatenate(right, axis=0), NN)
                pre = pre + dot(lhs, jnp.concatenate(gate_rows, axis=0), NN)
        packed = []
        for x in range(nx):
            here = slice(x * length, (x + 1) * length)
            mine = acc[here]
            qk = mine[:, : 2 * width].astype(BF16)[None]
            for j in range(qk_ref.shape[0]):
                qk_ref[j, x, pl.ds(home, 1)] = qk
            v_ref[x, pl.ds(home, 1)] = jnp.concatenate(
                [mine[:, 2 * width : 3 * width].astype(BF16), ones], axis=1
            )[None]
            left = mine[:, 3 * width : 3 * width + chan]
            right = mine[:, 3 * width + chan :]
            packed.append(left / (1.0 + jnp.exp(-right)))
            turned = pre[here].T
            extra = ref[x, column, length : length + 8].astype(F32)
            values = extra[0:1] + extra[1:2] + extra[2:3]
            offsets = jnp.where(core == 0, values[:, :length], values[:, length : 2 * length])
            offsets_f = jnp.where(
                core == 0, values[:, 2 * length : 3 * length], values[:, 3 * length : 4 * length]
            )
            at = row == 2 * x + home
            gate_pre = jnp.where(core == 0, turned[0:1], turned[1:2])
            forget_pre = jnp.where(core == 0, turned[2:3], turned[3:4])
            gate_in = jnp.where(at, gate_pre + offsets, gate_in)
            forget = jnp.where(at, forget_pre + offsets_f, forget)
        glu_ref[pl.ds(home, 1)] = jnp.concatenate(packed, axis=1).astype(BF16)[None]
    for b in range(ny):
        extra = own_ref[0, b, length : length + 8].astype(F32)
        memory_gain_ref[b : b + 1] = extra[3:4] + extra[4:5] + extra[5:6]
        half = part // 2
        conv_gain_ref[b : b + 1] = extra[6:7, :half] + extra[6:7, half:] + extra[7:8, :half]
    y = jnp.exp(-jnp.abs(forget))
    small = y * (1.0 - y * (1 / 2 - y * (1 / 3 - y * (1 / 4 - y * (1 / 5)))))
    gates_ref[0] = gate_in
    gates_ref[1] = jnp.minimum(forget, 0.0) - jnp.where(y < 0.03, small, jnp.log(1.0 + y))


def finish_kernel(arrived_ref, weight_ref, conv_gain_ref, memory_gain_ref, out_ref):
    nx, nc, ny, length, lanes = arrived_ref.shape
    width = lanes // 2
    chan = width // 2
    rows = weight_ref.shape[2] // 3
    depth = weight_ref.shape[0] // ny
    conv, memory = [], []
    for b in range(ny):
        pairs = [(x, c) for c in range(nc) for x in range(nx)]
        blocks = [arrived_ref[x, c, b].astype(F32) for x, c in pairs]
        memory.append(jnp.concatenate([t[:, :width] for t in blocks], axis=1))
        conv.append(
            jnp.concatenate(
                [t[:, width : width + chan] + t[:, width + chan :] for t in blocks], axis=1
            )
        )
    squares = sum(jnp.sum(m * m, axis=1, keepdims=True) for m in memory)
    scale = lax.rsqrt(squares / (ny * memory[0].shape[1]) + EPS)
    channels = ny * conv[0].shape[1]
    mean = sum(jnp.sum(t, axis=1, keepdims=True) for t in conv) / channels
    second = sum(jnp.sum(t * t, axis=1, keepdims=True) for t in conv) / channels
    spread = lax.rsqrt(second - mean * mean + EPS)
    total = jnp.zeros((length, out_ref.shape[1]), F32)
    for b in range(ny):
        scaled = (memory[b] * scale * memory_gain_ref[b : b + 1]).astype(BF16)
        normed = (conv[b] - mean) * spread * conv_gain_ref[b : b + 1]
        branch = (normed / (1.0 + jnp.exp(-normed))).astype(BF16)
        wide = branch.shape[1]
        for k, lhs in enumerate((scaled[:, :wide], scaled[:, wide:], branch)):
            rhs = weight_ref[b * depth : (b + 1) * depth, :, k * rows : (k + 1) * rows]
            total = total + dot(lhs, rhs.reshape(out_ref.shape[1], wide), NT)
    out_ref[...] = total.astype(BF16)


def convolve(glu_ref, prior_ref, taps_ref, out_ref, core, x_at):
    nc, length, lanes = glu_ref.shape
    nx, chan = out_ref.shape[0], out_ref.shape[2] // 2
    group = nc * length
    glu = glu_ref[...].reshape(group, lanes).astype(F32)
    taps = taps_ref.shape[0]
    hold = 32
    lane = lax.broadcasted_iota(jnp.int32, (hold, lanes), 1)
    before = pltpu.roll(glu[group - hold :], chan, 1)
    prior = jnp.concatenate([prior_ref[...].astype(F32), jnp.zeros((hold, lanes - chan), F32)], axis=1)
    extended = jnp.concatenate([jnp.where(lane < chan, prior, before), glu], axis=0)
    weights = taps_ref[...].astype(F32)
    weights = jnp.where(core == 0, weights[:, :lanes], weights[:, lanes:])
    weights = pltpu.roll(weights, lax.rem(lanes - chan * x_at, lanes), 1)
    weights = jnp.where(lax.broadcasted_iota(jnp.int32, weights.shape, 1) < chan, weights, 0.0)
    weights = sum(pltpu.roll(weights, chan * k, 1) for k in range(1, nx)) + weights
    total = jnp.zeros((group, lanes), F32)
    first = hold - (taps - 1)
    for shift in range(8):
        moved = extended[shift : shift + group + hold - 8] if shift else extended
        for j in range(taps):
            at = first + j
            if at % 8 == shift:
                total = total + moved[at - shift : at - shift + group] * weights[j : j + 1]
    high = total.astype(BF16)
    low = (total - high.astype(F32)).astype(BF16)
    for x in range(nx):
        mine = slice(x * chan, (x + 1) * chan)
        out_ref[x] = jnp.concatenate([high[:, mine], low[:, mine]], axis=1)


def slab_kernel(
    place_ref, qk_ref, v_ref, gate_ref, glu_ref, prior_ref, taps_ref,
    out_ref, q_ref, k_ref, conv_ref,
):
    convolve(glu_ref, prior_ref, taps_ref, conv_ref, place_ref[1], place_ref[3])
    chunks, length = gate_ref.shape[1], gate_ref.shape[2]
    width = qk_ref.shape[2] // 2
    gate, forget = gate_ref[0], gate_ref[1]
    within = lane_cumsum(forget)
    ends = [within[r : r + 1, length - 1 :] for r in range(chunks)]
    after = [jnp.zeros((1, 1), F32)]
    for r in range(chunks - 1, 0, -1):
        after.insert(0, after[0] + ends[r])
    total = after[0] + ends[0]
    to_end = jnp.concatenate([e + a for e, a in zip(ends, after)], axis=0)
    end_log = to_end - within + gate
    level = jnp.max(jnp.max(end_log, axis=1, keepdims=True), axis=0, keepdims=True)
    fresh = columns_of(jnp.exp(end_log - level))
    state = jnp.zeros((2 * width, width * qk_ref.shape[0]), F32)
    for r in range(chunks):
        q_ref[r * length : (r + 1) * length] = joined(qk_ref, 0, width, r, length)
        key = joined(qk_ref, width, width, r, length)
        k_ref[r * length : (r + 1) * length] = key
        scaled = (fresh[:, r : r + 1] * key.astype(F32)).astype(BF16)
        state = state + dot(v_ref[r * length : (r + 1) * length], scaled, TN)
    rows = out_ref.shape[1]
    kept = state[:rows]
    row = lax.broadcasted_iota(jnp.int32, kept.shape, 0)
    lane = lax.broadcasted_iota(jnp.int32, kept.shape, 1)
    for at, value in ((0, level), (3, total)):
        high = value.astype(BF16).astype(F32)
        mid = (value - high).astype(BF16).astype(F32)
        low = value - high - mid
        for k, part in enumerate((high, mid, low)):
            kept = jnp.where((row == width + 1) & (lane == at + k), part, kept)
    kept = kept.astype(BF16)
    for j in range(out_ref.shape[0]):
        out_ref[j] = kept


def cell_kernel(place_ref, in_ref, q_ref, k_ref, v_ref, gate_ref, conv_ref, out_ref):
    chunks, length = gate_ref.shape[1], gate_ref.shape[2]
    members, rows, head = in_ref.shape
    width = out_ref.shape[4] // 2
    nc, ny = out_ref.shape[1], out_ref.shape[2]
    scale = head ** (-0.5)
    place = place_ref[0]
    acc = jnp.zeros((1, 1), F32)
    logs = [None] * members
    for j in range(members - 1, -1, -1):
        line = in_ref[j, width + 1 : width + 2, :128].astype(F32)
        level_j = line[:, 0:1] + line[:, 1:2] + line[:, 2:3]
        total_j = line[:, 3:4] + line[:, 4:5] + line[:, 5:6]
        before = j < place
        logs[j] = jnp.where(before, level_j + acc, LOW)
        acc = acc + jnp.where(before, total_j, 0.0)
    level = logs[0]
    for j in range(1, members):
        level = jnp.maximum(level, logs[j])
    state = jnp.zeros((rows, head), F32)
    for j in range(members):
        weight = jnp.where(j < place, jnp.exp(logs[j] - level), 0.0)
        state = state + weight * in_ref[j].astype(F32)
    state = jnp.concatenate([state, jnp.zeros((2 * width - rows, head), F32)], axis=0)
    gate, forget = gate_ref[0], gate_ref[1]
    within = lane_cumsum(forget)
    turned = columns_of(jnp.concatenate([within, gate], axis=0))
    causal = lax.broadcasted_iota(jnp.int32, (length, length), 0) >= lax.broadcasted_iota(
        jnp.int32, (length, length), 1
    )
    for r in range(chunks):
        here = slice(r * length, (r + 1) * length)
        query, key, value = q_ref[here], k_ref[here], v_ref[here]
        within_row, gate_row = within[r : r + 1], gate[r : r + 1]
        within_col = turned[:, r : r + 1]
        gate_col = turned[:, chunks + r : chunks + r + 1]
        log_weight = jnp.where(causal, within_col - within_row + gate_row, -jnp.inf)
        carried = within_col + level
        top = jnp.maximum(carried, jnp.max(log_weight, axis=1, keepdims=True))
        weight = jnp.exp(log_weight - top)
        carried_weight = jnp.exp(carried - top) * scale
        scores = dot(query, key, NT) * (scale * weight)
        older = dot(query, state.astype(BF16), NT)
        numer = dot(scores.astype(BF16), value, NN) + carried_weight * older
        denom = jnp.sum(scores, axis=1, keepdims=True) + carried_weight * older[:, width : width + 1]
        result = numer[:, :width] / jnp.maximum(jnp.abs(denom), 1.0)
        x, c = r // nc, r % nc
        sent = jnp.concatenate(
            [result.astype(BF16), conv_ref[x, c * length : (c + 1) * length]], axis=1
        )
        for y in range(ny):
            out_ref[x, c, y] = sent
        last = within_row[:, length - 1 :]
        end_row = last - within_row + gate_row
        new_level = jnp.maximum(last + level, jnp.max(end_row, axis=1, keepdims=True))
        keep = jnp.exp(last + level - new_level)
        fresh = jnp.exp(last - within_col + gate_col - new_level)
        scaled = (fresh * key.astype(F32)).astype(BF16)
        state = keep * state + dot(value, scaled, TN)
        level = new_level


def vmem(count):
    return [pl.BlockSpec(memory_space=pltpu.VMEM)] * count


def layer(
    tokens,
    conv_value_weight,
    conv_gate_weight,
    conv_kernel,
    conv_norm_gain,
    query_weight,
    key_weight,
    value_weight,
    input_gate_weight,
    forget_gate_weight,
    input_offset,
    forget_offset,
    memory_norm_gain,
    conv_out_weight,
    memory_out_weight,
):
    nzh, nzl, nx, nc, ny = (size(a) for a in AXES)
    xi, ci, yi = lax.axis_index("x"), lax.axis_index("c"), lax.axis_index("tp")
    members = nzh * nzl
    zi = lax.axis_index("zh") * nzl + lax.axis_index("zl")
    length, part = tokens.shape
    slab = length * nx * nc
    head = query_weight.shape[1] // nc
    width = head // nx
    chan = conv_value_weight.shape[1] // nc // nx
    rows = query_weight.shape[0]
    wide = 3 * width + 2 * chan

    def from_z(value, ahead):
        return lax.ppermute(value, Z, [(j, (j - ahead) % members) for j in range(members)])

    out_rows = jnp.concatenate([memory_out_weight, conv_out_weight], axis=0).T
    pieces = pl.pallas_call(
        piece_kernel,
        out_shape=jax.ShapeDtypeStruct((nx, nc, 4 * rows, wide), BF16),
        in_specs=vmem(6),
        out_specs=pl.BlockSpec(memory_space=pltpu.VMEM),
        interpret=INTERPRET,
        name="pieces",
    )(query_weight, key_weight, value_weight, conv_value_weight, conv_gate_weight, out_rows)
    pieces = exchange(pieces.reshape(nx * nc, 4 * rows, wide), ("x", "c"))
    mine = pieces[:, :rows].reshape(nx * nc * rows, wide)
    turned = lax.ppermute(
        pieces[:, rows:],
        ("zh", "tp"),
        [(a * ny + b, b * ny + a) for a in range(nzh) for b in range(ny)],
    )
    step = members // 4
    far = [from_z(mine, k * step) for k in (1, 2, 3)]

    offsets = jnp.concatenate([input_offset.T, forget_offset.T], axis=0)
    offsets, turned = lax.optimization_barrier((offsets, turned))
    tall = length + 8
    sent = pl.pallas_call(
        pack_kernel,
        out_shape=jax.ShapeDtypeStruct((nx * ny, tall, part), BF16),
        in_specs=vmem(4),
        out_specs=pl.BlockSpec(memory_space=pltpu.VMEM),
        interpret=INTERPRET,
        name="pack",
    )(tokens, offsets, conv_norm_gain[None], memory_norm_gain[None])
    own = exchange(sent, ("x", "tp")).reshape(nx, ny, tall, part)
    other = swapped(own, "c")
    near = jnp.stack([mine, *far], axis=0)
    sets = [near, from_z(near, 1), from_z(near, 2), from_z(near, -1)]
    out_weight = lax.all_gather(turned, Z, axis=0, tiled=False)
    out_weight = out_weight.reshape(members, nx * nc, 3 * rows, wide)

    gate_weight = jnp.pad(
        jnp.concatenate([input_gate_weight, forget_gate_weight], axis=1), ((0, 0), (0, 124))
    )
    place = jnp.stack([zi, ci, yi, xi])
    smem = pl.BlockSpec(memory_space=pltpu.SMEM)
    qk, value, packed, gates, conv_gain, memory_gain = pl.pallas_call(
        project_kernel,
        out_shape=(
            jax.ShapeDtypeStruct((nx, nx, nc, length, 2 * width), BF16),
            jax.ShapeDtypeStruct((nx, nc, length, 2 * width), BF16),
            jax.ShapeDtypeStruct((nc, length, nx * chan), BF16),
            jax.ShapeDtypeStruct((2, nx * nc, length), F32),
            jax.ShapeDtypeStruct((ny, conv_norm_gain.shape[0]), F32),
            jax.ShapeDtypeStruct((ny, memory_norm_gain.shape[0]), F32),
        ),
        in_specs=[smem] + vmem(7),
        out_specs=vmem(6),
        interpret=INTERPRET,
        name="project",
    )(place, own, other, *sets, gate_weight)
    value = value.reshape(slab, 2 * width)
    group = slab // nx
    hold = 32
    prior = lax.ppermute(
        packed[nc - 1, length - hold :, (nx - 1) * chan :],
        Z,
        [(j, j + 1) for j in range(members - 1)],
    )
    all_qk = exchange(qk.reshape(nx, slab, 2 * width), "x")

    state_rows = width + 8
    states, query, key, conv_sent = pl.pallas_call(
        slab_kernel,
        out_shape=(
            jax.ShapeDtypeStruct((members, state_rows, head), BF16),
            jax.ShapeDtypeStruct((slab, head), BF16),
            jax.ShapeDtypeStruct((slab, head), BF16),
            jax.ShapeDtypeStruct((nx, group, 2 * chan), BF16),
        ),
        in_specs=[smem] + vmem(6),
        out_specs=vmem(4),
        interpret=INTERPRET,
        name="slab_state",
    )(place, all_qk, value, gates, packed, prior, conv_kernel)
    states = exchange(states, Z)
    last = pl.pallas_call(
        cell_kernel,
        out_shape=jax.ShapeDtypeStruct((nx, nc, ny, length, 2 * width), BF16),
        in_specs=[smem] + vmem(6),
        out_specs=pl.BlockSpec(memory_space=pltpu.VMEM),
        interpret=INTERPRET,
        name="cell",
    )(place, states, query, key, value, gates, conv_sent)
    arrived = exchange(last.reshape(nx * nc * ny, length, -1), ("x", "c", "tp"))
    arrived = arrived.reshape(nx, nc, ny, length, -1)
    return pl.pallas_call(
        finish_kernel,
        out_shape=jax.ShapeDtypeStruct((length, part), BF16),
        in_specs=vmem(4),
        out_specs=pl.BlockSpec(memory_space=pltpu.VMEM),
        interpret=INTERPRET,
        name="finish",
    )(arrived, out_weight, conv_gain, memory_gain)


def solution(mesh):
    shape = mesh.shape
    depth = shape["sp"] // 32
    split = Mesh(mesh.devices.reshape(4, depth, 4, 2, shape["tp"]), AXES)
    in_specs = (
        P(SP, "tp"),
        P(SP, "tp"),
        P(SP, "tp"),
        P(None, "tp"),
        P("tp"),
        P(SP, "tp"),
        P(SP, "tp"),
        P(SP, "tp"),
        P(None, "tp"),
        P(None, "tp"),
        P(SP, "tp"),
        P(SP, "tp"),
        P("tp"),
        P("tp", SP),
        P("tp", SP),
    )
    return jax.shard_map(
        layer, mesh=split, in_specs=in_specs, out_specs=P(SP, "tp"), check_vma=False
    )
```

time: 278 us -> 276 us (level)
  blocking collectives: 42.9 us -> 125 us
  waiting for transfers between devices: 102 us -> 52.3 us
  local copies, waits for them, and re-layouts: 28.5 us -> 4.66 us
  Pallas kernels: 9.74 us -> 27.2 us
  other arithmetic: 13.5 us -> 3.3 us
  matrix products: 9.61 us -> 0 us
  starting transfers between devices: 56.2 us -> 49.3 us
    all_to_all x2 -> x3, blocking collectives: 42.9 us -> 125 us  [exchange(): return lax.all_to_all(pieces, axes, split_axis=0, concat_axis=0, tiled=True)]
    all_to_all x5 -> x2, waiting for transfers between devices: 69.6 us -> 24.8 us  [exchange(): return lax.all_to_all(pieces, axes, split_axis=0, concat_axis=0, tiled=True)]
    all_to_all x5 -> x2, starting transfers between devices: 46.4 us -> 12.9 us  [exchange(): return lax.all_to_all(pieces, axes, split_axis=0, concat_axis=0, tiled=True)]
    all_gather x1, waiting for transfers between devices: 28.1 us -> 0.02 us  [layer(): out_weight = lax.all_gather(turned, Z, axis=0, tiled=False)]
    ppermute x2 -> x8, starting transfers between devices: 3.9 us -> 32 us  [the longest x6 30 us: from_z(): lax.ppermute(value, Z, [(j, (j - ahead) % members) for j in range(members)])]
    ppermute x2 -> x8, waiting for transfers between devices: 4.1 us -> 27.5 us  [the longest x6 26.7 us: from_z(): lax.ppermute(value, Z, [(j, (j - ahead) % members) for j in range(members)])]
    pallas_call x2 -> x6, Pallas kernels: 9.74 us -> 27.2 us  [the longest x1 7.37 us: layer(): pl.pallas_call(cell_kernel, out_shape=jax.ShapeDtypeStruct((nx, nc, ny, l...]
    dot_general x10 -> x0, matrix products: 9.61 us -> none  [the longest x8 4.93 us: dot(): return lax.dot_general(a, b, (dims, ((), ())), preferred_element_type=F32)]
  transfers between devices with their start and end apart: 9 -> 12, of which waited for: 7 -> 7; matrix products, arithmetic and copies ran while one was open for 13% -> 1% of each run, Pallas kernels for 4% -> 7%
where the time goes in v2:
time: 276 us; the launch traced here: 275 us
  blocking collectives  125 us (45%)
  waiting for transfers between devices  52.3 us (19%)
  starting transfers between devices  49.3 us (18%)
  Pallas kernels  27.2 us (10%)
  between operations  13.6 us (5%)
  local copies, waits for them, and re-layouts  4.66 us (2%)
  other arithmetic  3.3 us (1%)
    all_to_all x3, blocking collectives, exchange(): return lax.all_to_all(pieces, axes, split_axis=0, concat_axis=0, tiled=True)  125 us
    ppermute x6, starting transfers between devices, from_z(): lax.ppermute(value, Z, [(j, (j - ahead) % members) for j in range(members)])  30 us
    ppermute x6, waiting for transfers between devices, from_z(): lax.ppermute(value, Z, [(j, (j - ahead) % members) for j in range(members)])  26.7 us
    all_to_all x2, waiting for transfers between devices, exchange(): return lax.all_to_all(pieces, axes, split_axis=0, concat_axis=0, tiled=True)  24.8 us
    all_to_all x2, starting transfers between devices, exchange(): return lax.all_to_all(pieces, axes, split_axis=0, concat_axis=0, tiled=True)  12.9 us
    pallas_call x1, Pallas kernels, layer(): pl.pallas_call(cell_kernel, out_shape=jax.ShapeDtypeStruct((nx, nc, ny, l...  7.37 us
    pallas_call x1, Pallas kernels, layer(): pl.pallas_call(project_kernel, out_shape=(jax.ShapeDtypeStruct((nx, nx, n...  6.25 us
  transfers between devices with their start and end apart: 12, of which 7 were waited for; matrix products, arithmetic and copies ran while one was open for 1% of the time, Pallas kernels for 7%

profile of v2, /device:TPU:1, one launch (start us, length us, event | category | flops | bytes accessed | tf_op | source)
XLA Modules:
  0.0 275.2 jit_solution(7687690144393879142)
XLA Ops:
  7.9 1.6 pieces.1
  9.5 16.6 %all_to_all.25 = bf16[8,64,256]{2,1,0:T(8,128)(2,1)S(1)} all-to-all(bf16[8,64,256]{2,1,0:T(8,128)(2,1)} %bitcast.30), channel_id=1, replica_groups=mesh['zh'=4,'zl'=4,'x'=4,'c'=2,'tp'=4] {'x','c'}, dimensions={0} | all-to-all | bytes 524288 | tf_op jit(solution)/shard_map/all_to_all | solution.py:24
  28.1 2.5 pack.1
  30.6 63.8 %all_to_all.26 = bf16[16,136,512]{2,1,0:T(8,128)(2,1)S(1)} all-to-all(bf16[16,136,512]{2,1,0:T(8,128)(2,1)} %pack.1), channel_id=1, replica_groups=mesh['zh'=4,'zl'=4,'x'=4,'c'=2,'tp'=4] {'x','tp'}, dimensions={0} | all-to-all | bytes 4456448 | tf_op jit(solution)/shard_map/all_to_all | solution.py:24
  94.5 4.5 %collective-permute-start.1 = (bf16[4,4,136,512]{3,2,1,0:T(8,128)(2,1)S(1)}, bf16[4,4,136,512]{3,2,1,0:T(8,128)(2,1)}, u32[]{:S(2)}, u32[]{:S(2)}) collective-permute-start(bf16[4,4,136,512]{3,2,1,0:T(8,128)(2,1)S(1)} %bitcast.24), channel_id=1, source_target_pairs={{0,4},{4,0},{1,5},{5,1},{2,6},{6,2},{3,7},{7,3},{8,12},{12,8},{9,1... | collective-permute-start | bytes 6684680 | tf_op jit(solution)/shard_map/ppermute | solution.py:28
  99.0 9.7 %collective-permute-start.2 = (bf16[128,256]{1,0:T(8,128)(2,1)S(1)}, bf16[128,256]{1,0:T(8,128)(2,1)S(1)}, u32[]{:S(2)}, u32[]{:S(2)}) collective-permute-start(bf16[128,256]{1,0:T(8,128)(2,1)S(1)} %bitcast.33), channel_id=1, source_target_pairs={{0,384},{32,416},{64,448},{96,480},{128,0},{160,32},{192,64},{224,... | collective-permute-start | bytes 196616 | tf_op jit(solution)/shard_map/ppermute | solution.py:380
  108.7 4.5 %collective-permute-start.3 = (bf16[128,256]{1,0:T(8,128)(2,1)S(1)}, bf16[128,256]{1,0:T(8,128)(2,1)S(1)}, u32[]{:S(2)}, u32[]{:S(2)}) collective-permute-start(bf16[128,256]{1,0:T(8,128)(2,1)S(1)} %bitcast.34), channel_id=1, source_target_pairs={{0,256},{32,288},{64,320},{96,352},{128,384},{160,416},{192,448},{... | collective-permute-start | bytes 196616 | tf_op jit(solution)/shard_map/ppermute | solution.py:380
  113.2 7.3 %collective-permute-start.4 = (bf16[128,256]{1,0:T(8,128)(2,1)S(1)}, bf16[128,256]{1,0:T(8,128)(2,1)S(1)}, u32[]{:S(2)}, u32[]{:S(2)}) collective-permute-start(bf16[128,256]{1,0:T(8,128)(2,1)S(1)} %bitcast.35), channel_id=1, source_target_pairs={{0,128},{32,160},{64,192},{96,224},{128,256},{160,288},{192,320},{... | collective-permute-start | bytes 196616 | tf_op jit(solution)/shard_map/ppermute | solution.py:380
  120.5 2.3 collective-permute-done.3
  122.8 5.4 %collective-permute-done.4 = bf16[128,256]{1,0:T(8,128)(2,1)S(1)} collective-permute-done((bf16[128,256]{1,0:T(8,128)(2,1)S(1)}, bf16[128,256]{1,0:T(8,128)(2,1)S(1)}, u32[]{:S(2)}, u32[]{:S(2)}) %collective-permute-start.4) | collective-permute-done | bytes 65568 | tf_op jit(solution)/shard_map/ppermute | solution.py:380
  128.3 3.6 %collective-permute-start.5 = (bf16[4,128,256]{2,1,0:T(8,128)(2,1)S(1)}, bf16[4,128,256]{2,1,0:T(8,128)(2,1)S(1)}, u32[]{:S(2)}, u32[]{:S(2)}) collective-permute-start(bf16[4,128,256]{2,1,0:T(8,128)(2,1)S(1)} %pad_maximum_fusion.w0_ref), channel_id=1, source_target_pairs={{0,480},{32,0},{64,32},{96,64},{128,96},{160,128},{192,160},{224,1... | collective-permute-start | bytes 786440 | tf_op jit(solution)/shard_map/ppermute | solution.py:380
  131.8 1.9 collective-permute-start.6
  133.7 3.1 %collective-permute-start.7 = (bf16[4,128,256]{2,1,0:T(8,128)(2,1)S(1)}, bf16[4,128,256]{2,1,0:T(8,128)(2,1)}, u32[]{:S(2)}, u32[]{:S(2)}) collective-permute-start(bf16[4,128,256]{2,1,0:T(8,128)(2,1)S(1)} %pad_maximum_fusion.w0_ref), channel_id=1, source_target_pairs={{0,32},{32,64},{64,96},{96,128},{128,160},{160,192},{192,224},{224... | collective-permute-start | bytes 786440 | tf_op jit(solution)/shard_map/ppermute | solution.py:380
  138.8 3.4 %collective-permute-done.5.w1_ref = bf16[4,128,256]{2,1,0:T(8,128)(2,1)S(1)} collective-permute-done((bf16[4,128,256]{2,1,0:T(8,128)(2,1)S(1)}, bf16[4,128,256]{2,1,0:T(8,128)(2,1)S(1)}, u32[]{:S(2)}, u32[]{:S(2)}) %collective-permute-start.5) | collective-permute-done | bytes 262176 | tf_op jit(solution)/shard_map/ppermute | solution.py:380
  142.2 15.6 %collective-permute-done.6.w2_ref = bf16[4,128,256]{2,1,0:T(8,128)(2,1)S(1)} collective-permute-done((bf16[4,128,256]{2,1,0:T(8,128)(2,1)S(1)}, bf16[4,128,256]{2,1,0:T(8,128)(2,1)S(1)}, u32[]{:S(2)}, u32[]{:S(2)}) %collective-permute-start.6) | collective-permute-done | bytes 262176 | tf_op jit(solution)/shard_map/ppermute | solution.py:380
  158.4 6.2 %project.1 = (bf16[4,4,2,128,128]{4,3,2,1,0:T(8,128)(2,1)}, bf16[4,2,128,128]{3,2,1,0:T(8,128)(2,1)}, bf16[2,128,128]{2,1,0:T(8,128)(2,1)}, f32[2,8,128]{2,1,0:T...) custom-call(s32[4]{0:T(128)} %pad_add_fusion.place_ref, bf16[4,4,136,512]{3,2,1,0:T(8,128)(2,1)} %bitcast.25, ...), custom_call_target="tpu_custom_call" | custom-call | tf_op jit(solution)/shard_map/project/pallas_call | solution.py:424
  164.7 3.5 %all-to-all-start.2 = ((bf16[4,1024,128]{2,1,0:T(8,128)(2,1)}), bf16[4,1024,128]{2,1,0:T(8,128)(2,1)S(1)}, u32[]{:S(2)}, u32[]{:S(2)}) async-start(bf16[4,1024,128]{2,1,0:T(8,128)(2,1)} %bitcast.29), calls=%async_computation.2 | async-start | bytes 2097152 | tf_op jit(solution)/shard_map/all_to_all | solution.py:24
  171.1 8.6 %all-to-all-done.2.qk_ref = bf16[4,1024,128]{2,1,0:T(8,128)(2,1)S(1)} async-done(((bf16[4,1024,128]{2,1,0:T(8,128)(2,1)}), bf16[4,1024,128]{2,1,0:T(8,128)(2,1)S(1)}, u32[]{:S(2)}, u32[]{:S(2)}) %all-to-all-start.2) | async-done | bytes 1048608 | tf_op jit(solution)/shard_map/all_to_all | solution.py:24
  180.6 4.4 %slab_state.1 = (bf16[16,72,256]{2,1,0:T(8,128)(2,1)}, bf16[1024,256]{1,0:T(8,128)(2,1)}, bf16[1024,256]{1,0:T(8,128)(2,1)}, bf16[4,256,64]{2,1,0:T(8,128)(2,1)}) custom-call(s32[4]{0:T(128)} %pad_add_fusion.place_ref, bf16[4,1024,128]{2,1,0:T(8,128)(2,1)} %copy-done.2, bf16[1024,128]{1,0:T(8,128)(2,1)} %bitcast.31, ...), custom_call_target="tpu_custom_call" | custom-call | tf_op jit(solution)/shard_map/slab_state/pallas_call | solution.py:450
  184.9 44.4 %all_to_all.27.in_ref = bf16[16,72,256]{2,1,0:T(8,128)(2,1)} all-to-all(bf16[16,72,256]{2,1,0:T(8,128)(2,1)} %get-tuple-element.22), channel_id=1, replica_groups=mesh['zh'=4,'zl'=4,'x'=4,'c'=2,'tp'=4] {'zh','zl'}, dimensions={0} | all-to-all | bytes 1179648 | tf_op jit(solution)/shard_map/all_to_all | solution.py:24
  229.3 7.4 %cell.1 = bf16[4,2,4,128,128]{4,3,2,1,0:T(8,128)(2,1)} custom-call(s32[4]{0:T(128)} %pad_add_fusion.place_ref, bf16[16,72,256]{2,1,0:T(8,128)(2,1)} %all_to_all.27.in_ref, bf16[1024,256]{1,0:T(8,128)(2,1)} %get-tuple-element.23.q_ref, bf16[1024,256]{1,0:T(8,128)(2,1)} %get-tuple-element.24.k_ref, bf16[1024,128]{1,0:T(8,128)(2,1)} %bitcast.32, ...), custom_call_target="tpu_custom_call" | custom-call | tf_op jit(solution)/shard_map/cell/pallas_call | solution.py:464
  236.7 9.4 %all-to-all-start.4 = ((bf16[32,128,128]{2,1,0:T(8,128)(2,1)}), bf16[32,128,128]{2,1,0:T(8,128)(2,1)S(1)}, u32[]{:S(2)}, u32[]{:S(2)}) async-start(bf16[32,128,128]{2,1,0:T(8,128)(2,1)} %bitcast.27), calls=%async_computation.4 | async-start | bytes 2097152 | tf_op jit(solution)/shard_map/all_to_all | solution.py:24
  246.1 16.2 %all-to-all-done.4 = bf16[32,128,128]{2,1,0:T(8,128)(2,1)S(1)} async-done(((bf16[32,128,128]{2,1,0:T(8,128)(2,1)}), bf16[32,128,128]{2,1,0:T(8,128)(2,1)S(1)}, u32[]{:S(2)}, u32[]{:S(2)}) %all-to-all-start.4) | async-done | bytes 1048608 | tf_op jit(solution)/shard_map/all_to_all | solution.py:24
  263.3 5.1 %finish.1 = bf16[128,512]{1,0:T(8,128)(2,1)} custom-call(bf16[4,2,4,128,128]{4,3,2,1,0:T(8,128)(2,1)} %bitcast.26, bf16[16,8,48,256]{3,2,1,0:T(8,128)(2,1)} %bitcast.28, f32[4,256]{1,0:T(4,128)} %get-tuple-element.27.conv_gain_ref, f32[4,512]{1,0:T(4,128)} %get-tuple-element.28.memory_gain_ref), custom_call_target="tpu_custom_call" | custom-call | tf_op jit(solution)/shard_map/finish/pallas_call | solution.py:474
  (40 shorter events, 10.7 us)
Async XLA Ops:
  6.5 239.6 %all-gather.3.cloned.1.call-start = ((), (), s32[]{:S(2)}) async-start(), calls=%async_computation.5 | async-start | bytes 3342336 | tf_op jit(solution)/shard_map/all_gather | solution.py:416
  26.1 2.0 collective-permute-start
  28.1 66.4 %copy-start.6 = (bf16[8,48,256]{2,1,0:T(8,128)(2,1)}, bf16[8,48,256]{2,1,0:T(8,128)(2,1)S(1)}, u32[]{:S(2)}) copy-start(bf16[8,48,256]{2,1,0:T(8,128)(2,1)S(1)} %collective-permute-done) | copy-start | bytes 589828
  30.6 106.2 %copy-start.8 = (bf16[2048,2]{0,1:T(2,128)(2,1)S(1)}, bf16[2048,2]{0,1:T(2,128)(2,1)}, u32[]{:S(2)}) copy-start(bf16[2048,2]{0,1:T(2,128)(2,1)} %param.24) | copy-start | bytes 24580
  30.6 106.2 %copy-start.9 = (bf16[2048,2]{0,1:T(2,128)(2,1)S(1)}, bf16[2048,2]{0,1:T(2,128)(2,1)}, u32[]{:S(2)}) copy-start(bf16[2048,2]{0,1:T(2,128)(2,1)} %param.23) | copy-start | bytes 24580
  94.5 63.3 %copy-start = (bf16[16,136,512]{2,1,0:T(8,128)(2,1)}, bf16[16,136,512]{2,1,0:T(8,128)(2,1)S(1)}, u32[]{:S(2)}) copy-start(bf16[16,136,512]{2,1,0:T(8,128)(2,1)S(1)} %all_to_all.26) | copy-start | bytes 6684676
  94.5 63.3 %collective-permute-start.1 = (bf16[4,4,136,512]{3,2,1,0:T(8,128)(2,1)S(1)}, bf16[4,4,136,512]{3,2,1,0:T(8,128)(2,1)}, u32[]{:S(2)}, u32[]{:S(2)}) collective-permute-start(bf16[4,4,136,512]{3,2,1,0:T(8,128)(2,1)S(1)} %bitcast.24), channel_id=1, source_target_pairs={{0,4},{4,0},{1,5},{5,1},{2,6},{6,2},{3,7},{7,3},{8,12},{12,8},{9,1... | collective-permute-start | bytes 6684680 | tf_op jit(solution)/shard_map/ppermute | solution.py:28
  99.0 21.5 %collective-permute-start.2 = (bf16[128,256]{1,0:T(8,128)(2,1)S(1)}, bf16[128,256]{1,0:T(8,128)(2,1)S(1)}, u32[]{:S(2)}, u32[]{:S(2)}) collective-permute-start(bf16[128,256]{1,0:T(8,128)(2,1)S(1)} %bitcast.33), channel_id=1, source_target_pairs={{0,384},{32,416},{64,448},{96,480},{128,0},{160,32},{192,64},{224,... | collective-permute-start | bytes 196616 | tf_op jit(solution)/shard_map/ppermute | solution.py:380
  108.7 14.1 %collective-permute-start.3 = (bf16[128,256]{1,0:T(8,128)(2,1)S(1)}, bf16[128,256]{1,0:T(8,128)(2,1)S(1)}, u32[]{:S(2)}, u32[]{:S(2)}) collective-permute-start(bf16[128,256]{1,0:T(8,128)(2,1)S(1)} %bitcast.34), channel_id=1, source_target_pairs={{0,256},{32,288},{64,320},{96,352},{128,384},{160,416},{192,448},{... | collective-permute-start | bytes 196616 | tf_op jit(solution)/shard_map/ppermute | solution.py:380
  113.2 15.0 %collective-permute-start.4 = (bf16[128,256]{1,0:T(8,128)(2,1)S(1)}, bf16[128,256]{1,0:T(8,128)(2,1)S(1)}, u32[]{:S(2)}, u32[]{:S(2)}) collective-permute-start(bf16[128,256]{1,0:T(8,128)(2,1)S(1)} %bitcast.35), channel_id=1, source_target_pairs={{0,128},{32,160},{64,192},{96,224},{128,256},{160,288},{192,320},{... | collective-permute-start | bytes 196616 | tf_op jit(solution)/shard_map/ppermute | solution.py:380
  128.2 29.5 %copy-start.3 = (bf16[4,128,256]{2,1,0:T(8,128)(2,1)}, bf16[4,128,256]{2,1,0:T(8,128)(2,1)S(1)}, u32[]{:S(2)}) copy-start(bf16[4,128,256]{2,1,0:T(8,128)(2,1)S(1)} %pad_maximum_fusion.w0_ref) | copy-start | bytes 786436
  128.3 13.9 %collective-permute-start.5 = (bf16[4,128,256]{2,1,0:T(8,128)(2,1)S(1)}, bf16[4,128,256]{2,1,0:T(8,128)(2,1)S(1)}, u32[]{:S(2)}, u32[]{:S(2)}) collective-permute-start(bf16[4,128,256]{2,1,0:T(8,128)(2,1)S(1)} %pad_maximum_fusion.w0_ref), channel_id=1, source_target_pairs={{0,480},{32,0},{64,32},{96,64},{128,96},{160,128},{192,160},{224,1... | collective-permute-start | bytes 786440 | tf_op jit(solution)/shard_map/ppermute | solution.py:380
  131.8 25.9 %collective-permute-start.6 = (bf16[4,128,256]{2,1,0:T(8,128)(2,1)S(1)}, bf16[4,128,256]{2,1,0:T(8,128)(2,1)S(1)}, u32[]{:S(2)}, u32[]{:S(2)}) collective-permute-start(bf16[4,128,256]{2,1,0:T(8,128)(2,1)S(1)} %pad_maximum_fusion.w0_ref), channel_id=1, source_target_pairs={{0,448},{32,480},{64,0},{96,32},{128,64},{160,96},{192,128},{224,1... | collective-permute-start | bytes 786440 | tf_op jit(solution)/shard_map/ppermute | solution.py:380
  133.7 24.0 %collective-permute-start.7 = (bf16[4,128,256]{2,1,0:T(8,128)(2,1)S(1)}, bf16[4,128,256]{2,1,0:T(8,128)(2,1)}, u32[]{:S(2)}, u32[]{:S(2)}) collective-permute-start(bf16[4,128,256]{2,1,0:T(8,128)(2,1)S(1)} %pad_maximum_fusion.w0_ref), channel_id=1, source_target_pairs={{0,32},{32,64},{64,96},{96,128},{128,160},{160,192},{192,224},{224... | collective-permute-start | bytes 786440 | tf_op jit(solution)/shard_map/ppermute | solution.py:380
  142.2 15.6 %copy-start.4 = (bf16[4,128,256]{2,1,0:T(8,128)(2,1)}, bf16[4,128,256]{2,1,0:T(8,128)(2,1)S(1)}, u32[]{:S(2)}) copy-start(bf16[4,128,256]{2,1,0:T(8,128)(2,1)S(1)} %collective-permute-done.5.w1_ref) | copy-start | bytes 786436
  157.7 0.7 copy-start.5
  164.7 14.9 %all-to-all-start.2 = ((bf16[4,1024,128]{2,1,0:T(8,128)(2,1)}), bf16[4,1024,128]{2,1,0:T(8,128)(2,1)S(1)}, u32[]{:S(2)}, u32[]{:S(2)}) async-start(bf16[4,1024,128]{2,1,0:T(8,128)(2,1)} %bitcast.29), calls=%async_computation.2 | async-start | bytes 2097152 | tf_op jit(solution)/shard_map/all_to_all | solution.py:24
  169.0 2.1 collective-permute-start.8
  171.0 8.6 %copy-start.7 = (bf16[32,32]{1,0:T(8,128)(2,1)}, bf16[32,32]{1,0:T(8,128)(2,1)S(1)}, u32[]{:S(2)}) copy-start(bf16[32,32]{1,0:T(8,128)(2,1)S(1)} %collective-permute-done.8.prior_ref) | copy-start | bytes 6148
  179.6 1.0 copy-start.2
  236.7 25.6 %all-to-all-start.4 = ((bf16[32,128,128]{2,1,0:T(8,128)(2,1)}), bf16[32,128,128]{2,1,0:T(8,128)(2,1)S(1)}, u32[]{:S(2)}, u32[]{:S(2)}) async-start(bf16[32,128,128]{2,1,0:T(8,128)(2,1)} %bitcast.27), calls=%async_computation.4 | async-start | bytes 2097152 | tf_op jit(solution)/shard_map/all_to_all | solution.py:24
  262.3 1.0 copy-start.1
Sparse Core Ops, SparseCore 0:
  99.1 82.0 all-gather.2

commit v3 on v2

--- a/solution.py
+++ b/solution.py
@@ -85,9 +85,7 @@
 
 def piece_kernel(query_ref, key_ref, value_ref, left_ref, right_ref, out_weight_ref, out_ref):
     rows = query_ref.shape[0]
-    nx, nc = out_ref.shape[0], out_ref.shape[1]
-    wide = out_ref.shape[3]
-    chunks = out_weight_ref.shape[1] // wide
+    copies, nx, nc, _, half = out_ref.shape
     for x in range(nx):
         for c in range(nc):
             at = c * nx + x
@@ -95,24 +93,24 @@
             for ref in (query_ref, key_ref, value_ref, left_ref, right_ref):
                 width = ref.shape[1] // (nx * nc)
                 parts.append(ref[:, at * width : (at + 1) * width])
-            out_ref[x, c, :rows] = jnp.concatenate(parts, axis=1)
-            for k in range(chunks):
-                out_ref[x, c, rows * (k + 1) : rows * (k + 2)] = out_weight_ref[
-                    :, k * wide : (k + 1) * wide
-                ]
+            whole = jnp.concatenate(parts, axis=1)
+            for j in range(copies):
+                out_ref[j, x, c, :rows] = whole[:, :half]
+                out_ref[j, x, c, rows : 2 * rows] = whole[:, half:]
+                out_ref[j, x, c, 2 * rows :] = out_weight_ref[x, c]
 
 
 def project_kernel(
-    place_ref, own_ref, other_ref, w0_ref, w1_ref, w2_ref, w3_ref, gate_ref,
-    qk_ref, v_ref, glu_ref, gates_ref, conv_gain_ref, memory_gain_ref,
+    place_ref, own_ref, other_ref, w0_ref, w1_ref, w3_ref, low_ref, high_ref, gate_ref,
+    qk_ref, v_ref, glu_ref, gates_ref, gain_ref, out_weight_ref,
 ):
     nx, ny, _, part = own_ref.shape
-    block = w0_ref.shape[1]
+    far, senders, tall_piece, side = w0_ref.shape
+    rows = tall_piece // 3
+    block = senders * rows
+    close = part // block
     length = glu_ref.shape[1]
-    blocks = part * ny // block
-    per_part = part // block
-    place, core, column = place_ref[0], place_ref[1], place_ref[2]
-    groups = ((w0_ref, 0, w1_ref, 1), (w2_ref, 2, w3_ref, blocks - 1))
+    at_close, core, column = place_ref[0], place_ref[1], place_ref[2]
     tokens_rows = nx * length
     width = qk_ref.shape[4] // 2
     chan = glu_ref.shape[2] // nx
@@ -121,21 +119,40 @@
     row = lax.broadcasted_iota(jnp.int32, (2 * nx, length), 0)
     gate_in = jnp.zeros((2 * nx, length), F32)
     forget = jnp.zeros((2 * nx, length), F32)
+
+    def piece(distance, k):
+        if distance == 2:
+            return low_ref[k] if k < far // 2 else high_ref[k - far // 2]
+        return (w0_ref, w1_ref, None, w3_ref)[distance][k]
+
+    homes = [lax.rem(at_close + distance, close) for distance in range(close)]
+    for distance in range(close):
+        for k in range(far):
+            out_weight_ref[k, pl.ds(homes[distance], 1)] = piece(distance, k)[:, 2 * rows :][None]
+
+    def weight_block(distance, k):
+        mine = piece(distance, k)
+        return jnp.concatenate(
+            [
+                mine[:, :rows].reshape(block, side),
+                mine[:, rows : 2 * rows].reshape(block, side),
+            ],
+            axis=1,
+        )
+
     for half, ref in enumerate((own_ref, other_ref)):
         home = core if half == 0 else 1 - core
-        acc = jnp.zeros((tokens_rows, w0_ref.shape[2]), F32)
+        acc = jnp.zeros((tokens_rows, 2 * side), F32)
         pre = jnp.zeros((tokens_rows, gate_ref.shape[1]), F32)
-        for first_ref, first_at, second_ref, second_at in groups:
-            for k in range(w0_ref.shape[0]):
+        for k in range(far):
+            for pair in ((0, 1), (2, 3)):
                 left, right, gate_rows = [], [], []
-                for w_ref, at in ((first_ref, first_at), (second_ref, second_at)):
-                    kb = lax.rem(place + at + k * (blocks // w0_ref.shape[0]), blocks)
-                    lanes = pl.ds(pl.multiple_of(lax.rem(kb, per_part) * block, block), block)
-                    left.append(
-                        ref[:, lax.div(kb, per_part), :length, lanes].reshape(tokens_rows, block)
-                    )
-                    right.append(w_ref[k])
-                    gate_rows.append(gate_ref[pl.ds(pl.multiple_of(kb * block, block), block)])
+                for distance in pair:
+                    start = pl.multiple_of(homes[distance] * block, block)
+                    lanes = pl.ds(start, block)
+                    left.append(ref[:, k, :length, lanes].reshape(tokens_rows, block))
+                    right.append(weight_block(distance, k))
+                    gate_rows.append(gate_ref[pl.ds(k * part + start, block)])
                 lhs = jnp.concatenate(left, axis=1)
                 acc = acc + dot(lhs, jnp.concatenate(right, axis=0), NN)
                 pre = pre + dot(lhs, jnp.concatenate(gate_rows, axis=0), NN)
@@ -167,46 +184,70 @@
         glu_ref[pl.ds(home, 1)] = jnp.concatenate(packed, axis=1).astype(BF16)[None]
     for b in range(ny):
         extra = own_ref[0, b, length : length + 8].astype(F32)
-        memory_gain_ref[b : b + 1] = extra[3:4] + extra[4:5] + extra[5:6]
+        memory_gain = extra[3:4] + extra[4:5] + extra[5:6]
         half = part // 2
-        conv_gain_ref[b : b + 1] = extra[6:7, :half] + extra[6:7, half:] + extra[7:8, :half]
+        conv_gain = extra[6:7, :half] + extra[6:7, half:] + extra[7:8, :half]
+        for at in range(2 * nx):
+            gain_ref[b, at : at + 1] = jnp.concatenate(
+                [
+                    memory_gain[:, at * width : (at + 1) * width],
+                    conv_gain[:, at * chan : (at + 1) * chan],
+                    jnp.zeros((1, width - chan), F32),
+                ],
+                axis=1,
+            )
     y = jnp.exp(-jnp.abs(forget))
     small = y * (1.0 - y * (1 / 2 - y * (1 / 3 - y * (1 / 4 - y * (1 / 5)))))
     gates_ref[0] = gate_in
     gates_ref[1] = jnp.minimum(forget, 0.0) - jnp.where(y < 0.03, small, jnp.log(1.0 + y))
 
 
-def finish_kernel(arrived_ref, weight_ref, conv_gain_ref, memory_gain_ref, out_ref):
+def finish_kernel(place_ref, arrived_ref, own_ref, other_ref, gain_ref, out_ref):
     nx, nc, ny, length, lanes = arrived_ref.shape
+    core, x_at = place_ref[1], place_ref[3]
     width = lanes // 2
     chan = width // 2
-    rows = weight_ref.shape[2] // 3
-    depth = weight_ref.shape[0] // ny
-    conv, memory = [], []
+    part = out_ref.shape[1]
+    lane = lax.broadcasted_iota(jnp.int32, (length, lanes), 1)
+    is_memory = lane < width
+    is_conv = (lane >= width) & (lane < width + chan)
+
+    def block(x, c, b):
+        got = arrived_ref[x, c, b].astype(F32)
+        both = got + pltpu.roll(got, lanes - chan, 1)
+        return jnp.where(is_memory, got, jnp.where(is_conv, both, 0.0))
+
+    first = jnp.zeros((length, lanes), F32)
+    second = jnp.zeros((length, lanes), F32)
+    for x in range(nx):
+        for c in range(nc):
+            for b in range(ny):
+                got = block(x, c, b)
+                first = first + got
+                second = second + got * got
+    senders = nx * nc * ny
+    memory_mean = jnp.sum(jnp.where(is_memory, second, 0.0), axis=1, keepdims=True)
+    scale = lax.rsqrt(memory_mean / (senders * width) + EPS)
+    mean = jnp.sum(jnp.where(is_conv, first, 0.0), axis=1, keepdims=True) / (senders * chan)
+    power = jnp.sum(jnp.where(is_conv, second, 0.0), axis=1, keepdims=True) / (senders * chan)
+    spread = lax.rsqrt(power - mean * mean + EPS)
+    shift = jnp.where(is_memory, 0.0, mean)
+    factor = jnp.where(is_memory, scale, spread)
+    total = jnp.zeros((length, part), F32)
     for b in range(ny):
-        pairs = [(x, c) for c in range(nc) for x in range(nx)]
-        blocks = [arrived_ref[x, c, b].astype(F32) for x, c in pairs]
-        memory.append(jnp.concatenate([t[:, :width] for t in blocks], axis=1))
-        conv.append(
-            jnp.concatenate(
-                [t[:, width : width + chan] + t[:, width + chan :] for t in blocks], axis=1
+        for ahead in range(nx):
+            x = lax.rem(x_at + ahead, nx)
+            left, right = [], []
+            for c, ref in ((core, own_ref), (1 - core, other_ref)):
+                gain = gain_ref[b, pl.ds(c * nx + x, 1)]
+                normed = (block(x, c, b) - shift) * factor * gain
+                branch = normed / (1.0 + jnp.exp(-normed))
+                used = jnp.where(is_memory, normed, jnp.where(is_conv, branch, 0.0))
+                left.append(used.astype(BF16))
+                right.append(ref[ahead, b].reshape(part, lanes))
+            total = total + dot(
+                jnp.concatenate(left, axis=1), jnp.concatenate(right, axis=1), NT
             )
-        )
-    squares = sum(jnp.sum(m * m, axis=1, keepdims=True) for m in memory)
-    scale = lax.rsqrt(squares / (ny * memory[0].shape[1]) + EPS)
-    channels = ny * conv[0].shape[1]
-    mean = sum(jnp.sum(t, axis=1, keepdims=True) for t in conv) / channels
-    second = sum(jnp.sum(t * t, axis=1, keepdims=True) for t in conv) / channels
-    spread = lax.rsqrt(second - mean * mean + EPS)
-    total = jnp.zeros((length, out_ref.shape[1]), F32)
-    for b in range(ny):
-        scaled = (memory[b] * scale * memory_gain_ref[b : b + 1]).astype(BF16)
-        normed = (conv[b] - mean) * spread * conv_gain_ref[b : b + 1]
-        branch = (normed / (1.0 + jnp.exp(-normed))).astype(BF16)
-        wide = branch.shape[1]
-        for k, lhs in enumerate((scaled[:, :wide], scaled[:, wide:], branch)):
-            rhs = weight_ref[b * depth : (b + 1) * depth, :, k * rows : (k + 1) * rows]
-            total = total + dot(lhs, rhs.reshape(out_ref.shape[1], wide), NT)
     out_ref[...] = total.astype(BF16)
 
 
@@ -287,7 +328,7 @@
     width = out_ref.shape[4] // 2
     nc, ny = out_ref.shape[1], out_ref.shape[2]
     scale = head ** (-0.5)
-    place = place_ref[0]
+    place = place_ref[4]
     acc = jnp.zeros((1, 1), F32)
     logs = [None] * members
     for j in range(members - 1, -1, -1):
@@ -379,27 +420,20 @@
     def from_z(value, ahead):
         return lax.ppermute(value, Z, [(j, (j - ahead) % members) for j in range(members)])
 
-    out_rows = jnp.concatenate([memory_out_weight, conv_out_weight], axis=0).T
-    pieces = pl.pallas_call(
-        piece_kernel,
-        out_shape=jax.ShapeDtypeStruct((nx, nc, 4 * rows, wide), BF16),
-        in_specs=vmem(6),
-        out_specs=pl.BlockSpec(memory_space=pltpu.VMEM),
-        interpret=INTERPRET,
-        name="pieces",
-    )(query_weight, key_weight, value_weight, conv_value_weight, conv_gate_weight, out_rows)
-    pieces = exchange(pieces.reshape(nx * nc, 4 * rows, wide), ("x", "c"))
-    mine = pieces[:, :rows].reshape(nx * nc * rows, wide)
+    out_rows = jnp.concatenate(
+        [
+            memory_out_weight.reshape(nc, nx, width, rows),
+            conv_out_weight.reshape(nc, nx, chan, rows),
+            jnp.zeros((nc, nx, width - chan, rows), BF16),
+        ],
+        axis=2,
+    ).transpose(1, 0, 3, 2)
     turned = lax.ppermute(
-        pieces[:, rows:],
+        out_rows,
         ("zh", "tp"),
         [(a * ny + b, b * ny + a) for a in range(nzh) for b in range(ny)],
     )
-    step = members // 4
-    far = [from_z(mine, k * step) for k in (1, 2, 3)]
-
     offsets = jnp.concatenate([input_offset.T, forget_offset.T], axis=0)
-    offsets, turned = lax.optimization_barrier((offsets, turned))
     tall = length + 8
     sent = pl.pallas_call(
         pack_kernel,
@@ -411,27 +445,36 @@
     )(tokens, offsets, conv_norm_gain[None], memory_norm_gain[None])
     own = exchange(sent, ("x", "tp")).reshape(nx, ny, tall, part)
     other = swapped(own, "c")
-    near = jnp.stack([mine, *far], axis=0)
-    sets = [near, from_z(near, 1), from_z(near, 2), from_z(near, -1)]
-    out_weight = lax.all_gather(turned, Z, axis=0, tiled=False)
-    out_weight = out_weight.reshape(members, nx * nc, 3 * rows, wide)
+    own, turned = lax.optimization_barrier((own, turned))
+    pieces = pl.pallas_call(
+        piece_kernel,
+        out_shape=jax.ShapeDtypeStruct((nzh, nx, nc, 3 * rows, wide // 2), BF16),
+        in_specs=vmem(6),
+        out_specs=pl.BlockSpec(memory_space=pltpu.VMEM),
+        interpret=INTERPRET,
+        name="pieces",
+    )(query_weight, key_weight, value_weight, conv_value_weight, conv_gate_weight, turned)
+    near = exchange(pieces.reshape(nzh * nx * nc, 3 * rows, wide // 2), ("zh", "x", "c"))
+    near = near.reshape(nzh, nx * nc, 3 * rows, wide // 2)
+    sets = [near, from_z(near, 1), from_z(near, -1)]
+    sets += [from_z(near[: nzh // 2], 2), from_z(near[nzh // 2 :], -2)]
 
     gate_weight = jnp.pad(
         jnp.concatenate([input_gate_weight, forget_gate_weight], axis=1), ((0, 0), (0, 124))
     )
-    place = jnp.stack([zi, ci, yi, xi])
+    place = jnp.stack([lax.axis_index("zl"), ci, yi, xi, zi])
     smem = pl.BlockSpec(memory_space=pltpu.SMEM)
-    qk, value, packed, gates, conv_gain, memory_gain = pl.pallas_call(
+    qk, value, packed, gates, gain, out_part = pl.pallas_call(
         project_kernel,
         out_shape=(
             jax.ShapeDtypeStruct((nx, nx, nc, length, 2 * width), BF16),
             jax.ShapeDtypeStruct((nx, nc, length, 2 * width), BF16),
             jax.ShapeDtypeStruct((nc, length, nx * chan), BF16),
             jax.ShapeDtypeStruct((2, nx * nc, length), F32),
-            jax.ShapeDtypeStruct((ny, conv_norm_gain.shape[0]), F32),
-            jax.ShapeDtypeStruct((ny, memory_norm_gain.shape[0]), F32),
+            jax.ShapeDtypeStruct((ny, nc * nx, 2 * width), F32),
+            jax.ShapeDtypeStruct((nzh, nzl, nx * nc, rows, wide // 2), BF16),
         ),
-        in_specs=[smem] + vmem(7),
+        in_specs=[smem] + vmem(8),
         out_specs=vmem(6),
         interpret=INTERPRET,
         name="project",
@@ -445,6 +488,13 @@
         [(j, j + 1) for j in range(members - 1)],
     )
     all_qk = exchange(qk.reshape(nx, slab, 2 * width), "x")
+    out_part, all_qk = lax.optimization_barrier((out_part, all_qk))
+    out_parts = [out_part] + [
+        lax.ppermute(out_part, "x", [(j, (j - ahead) % nx) for j in range(nx)])
+        for ahead in range(1, nx)
+    ]
+    own_out = jnp.stack(out_parts, axis=0)
+    other_out = swapped(own_out, "c")
 
     state_rows = width + 8
     states, query, key, conv_sent = pl.pallas_call(
@@ -474,11 +524,11 @@
     return pl.pallas_call(
         finish_kernel,
         out_shape=jax.ShapeDtypeStruct((length, part), BF16),
-        in_specs=vmem(4),
+        in_specs=[smem] + vmem(4),
         out_specs=pl.BlockSpec(memory_space=pltpu.VMEM),
         interpret=INTERPRET,
         name="finish",
-    )(arrived, out_weight, conv_gain, memory_gain)
+    )(place, arrived, own_out, other_out, gain)
 
 
 def solution(mesh):

time: 276 us -> 241 us (0.87)
  blocking collectives: 125 us -> 0 us
  waiting for transfers between devices: 52.3 us -> 110 us
  starting transfers between devices: 49.3 us -> 92.1 us
  between operations: 13.6 us -> 0.33 us
  local copies, waits for them, and re-layouts: 4.66 us -> 7.91 us
    all_to_all x3 -> x0, blocking collectives: 125 us -> none  [exchange(): return lax.all_to_all(pieces, axes, split_axis=0, concat_axis=0, tiled=True)]
    all_to_all x2 -> x5, waiting for transfers between devices: 24.8 us -> 77.8 us  [exchange(): return lax.all_to_all(pieces, axes, split_axis=0, concat_axis=0, tiled=True)]
    all_to_all x2 -> x5, starting transfers between devices: 12.9 us -> 53.7 us  [exchange(): return lax.all_to_all(pieces, axes, split_axis=0, concat_axis=0, tiled=True)]
    ppermute x1 -> x4, waiting for transfers between devices: 0.01 us -> 21.2 us  [the longest x3 21.2 us: layer(): lax.ppermute(out_part, 'x', [(j, (j - ahead) % nx) for j in range(nx)])]
    ppermute x6 -> x4, waiting for transfers between devices: 26.7 us -> 10.8 us  [from_z(): lax.ppermute(value, Z, [(j, (j - ahead) % members) for j in range(members)])]
    ppermute x6 -> x4, starting transfers between devices: 30 us -> 16 us  [from_z(): lax.ppermute(value, Z, [(j, (j - ahead) % members) for j in range(members)])]
    ppermute x1 -> x4, starting transfers between devices: 0.67 us -> 9.08 us  [the longest x3 8.42 us: layer(): lax.ppermute(out_part, 'x', [(j, (j - ahead) % nx) for j in range(nx)])]
    ppermute x1 -> x2, starting transfers between devices: 4.48 us -> 10.9 us  [swapped(): return lax.ppermute(value, axis, [(0, 1), (1, 0)])]
  transfers between devices with their start and end apart: 12 -> 16, of which waited for: 7 -> 8; matrix products, arithmetic and copies ran while one was open for 1% -> 2% of each run, Pallas kernels for 7% -> 4%
where the time goes in v3:
time: 241 us; the launch traced here: 240 us
  waiting for transfers between devices  110 us (46%)
  starting transfers between devices  92.1 us (38%)
  Pallas kernels  28 us (12%)
  local copies, waits for them, and re-layouts  7.91 us (3%)
    all_to_all x5, waiting for transfers between devices, exchange(): return lax.all_to_all(pieces, axes, split_axis=0, concat_axis=0, tiled=True)  77.8 us
    all_to_all x5, starting transfers between devices, exchange(): return lax.all_to_all(pieces, axes, split_axis=0, concat_axis=0, tiled=True)  53.7 us
    ppermute x3, waiting for transfers between devices, layer(): lax.ppermute(out_part, 'x', [(j, (j - ahead) % nx) for j in range(nx)])  21.2 us
    ppermute x4, starting transfers between devices, from_z(): lax.ppermute(value, Z, [(j, (j - ahead) % members) for j in range(members)])  16 us
    ppermute x2, starting transfers between devices, swapped(): return lax.ppermute(value, axis, [(0, 1), (1, 0)])  10.9 us
    ppermute x4, waiting for transfers between devices, from_z(): lax.ppermute(value, Z, [(j, (j - ahead) % members) for j in range(members)])  10.8 us
    ppermute x3, starting transfers between devices, layer(): lax.ppermute(out_part, 'x', [(j, (j - ahead) % nx) for j in range(nx)])  8.42 us
    pallas_call x1, Pallas kernels, layer(): pl.pallas_call(cell_kernel, out_shape=jax.ShapeDtypeStruct((nx, nc, ny, l...  7.44 us
  transfers between devices with their start and end apart: 16, of which 8 were waited for; matrix products, arithmetic and copies ran while one was open for 2% of the time, Pallas kernels for 4%

profile of v3, /device:TPU:1, one launch (start us, length us, event | category | flops | bytes accessed | tf_op | source)
XLA Modules:
  0.0 239.8 jit_solution(15421995074407061885)
XLA Ops:
  3.8 7.7 %all-to-all-start = ((bf16[16,136,512]{2,1,0:T(8,128)(2,1)}), bf16[16,136,512]{2,1,0:T(8,128)(2,1)S(1)}, u32[]{:S(2)}, u32[]{:S(2)}) async-start(bf16[16,136,512]{2,1,0:T(8,128)(2,1)} %pack.1), calls=%async_computation | async-start | bytes 4456448 | tf_op jit(solution)/shard_map/all_to_all | solution.py:24
  11.8 26.3 %all-to-all-done = bf16[16,136,512]{2,1,0:T(8,128)(2,1)S(1)} async-done(((bf16[16,136,512]{2,1,0:T(8,128)(2,1)}), bf16[16,136,512]{2,1,0:T(8,128)(2,1)S(1)}, u32[]{:S(2)}, u32[]{:S(2)}) %all-to-all-start) | async-done | bytes 2228256 | tf_op jit(solution)/shard_map/all_to_all | solution.py:24
  38.1 7.5 %collective-permute-start.1 = (bf16[4,4,136,512]{3,2,1,0:T(8,128)(2,1)S(1)}, bf16[4,4,136,512]{3,2,1,0:T(8,128)(2,1)}, u32[]{:S(2)}, u32[]{:S(2)}) collective-permute-start(bf16[4,4,136,512]{3,2,1,0:T(8,128)(2,1)S(1)} %bitcast.30), channel_id=1, source_target_pairs={{0,4},{4,0},{1,5},{5,1},{2,6},{6,2},{3,7},{7,3},{8,12},{12,8},{9,1... | collective-permute-start | bytes 6684680 | tf_op jit(solution)/shard_map/ppermute | solution.py:28
  48.7 32.6 %all-to-all-start.1 = ((bf16[32,48,128]{2,1,0:T(8,128)(2,1)}), bf16[32,48,128]{2,1,0:T(8,128)(2,1)S(1)}, u32[]{:S(2)}, u32[]{:S(2)}) async-start(bf16[32,48,128]{2,1,0:T(8,128)(2,1)} %bitcast.37), calls=%async_computation.1 | async-start | bytes 786432 | tf_op jit(solution)/shard_map/all_to_all | solution.py:24
  81.3 23.6 %all-to-all-done.1 = bf16[32,48,128]{2,1,0:T(8,128)(2,1)S(1)} async-done(((bf16[32,48,128]{2,1,0:T(8,128)(2,1)}), bf16[32,48,128]{2,1,0:T(8,128)(2,1)S(1)}, u32[]{:S(2)}, u32[]{:S(2)}) %all-to-all-start.1) | async-done | bytes 393248 | tf_op jit(solution)/shard_map/all_to_all | solution.py:24
  104.9 7.9 %collective-permute-start.3 = (bf16[4,8,48,128]{3,2,1,0:T(8,128)(2,1)S(1)}, bf16[4,8,48,128]{3,2,1,0:T(8,128)(2,1)S(1)}, u32[]{:S(2)}, u32[]{:S(2)}) collective-permute-start(bf16[4,8,48,128]{3,2,1,0:T(8,128)(2,1)S(1)} %bitcast.34), channel_id=1, source_target_pairs={{0,32},{32,64},{64,96},{96,128},{128,160},{160,192},{192,224},{224... | collective-permute-start | bytes 1179656 | tf_op jit(solution)/shard_map/ppermute | solution.py:421
  115.5 2.7 %collective-permute-start.4 = (bf16[2,8,48,128]{3,2,1,0:T(8,128)(2,1)}, bf16[2,8,48,128]{3,2,1,0:T(8,128)(2,1)}, u32[]{:S(2)}, u32[]{:S(2)}) collective-permute-start(bf16[2,8,48,128]{3,2,1,0:T(8,128)(2,1)} %bitcast.13), channel_id=1, source_target_pairs={{0,448},{32,480},{64,0},{96,32},{128,64},{160,96},{192,128},{224,1... | collective-permute-start | bytes 589832 | tf_op jit(solution)/shard_map/ppermute | solution.py:421
  118.2 3.4 %collective-permute-start.5 = (bf16[2,8,48,128]{3,2,1,0:T(8,128)(2,1)}, bf16[2,8,48,128]{3,2,1,0:T(8,128)(2,1)}, u32[]{:S(2)}, u32[]{:S(2)}) collective-permute-start(bf16[2,8,48,128]{3,2,1,0:T(8,128)(2,1)} %bitcast.14), channel_id=1, source_target_pairs={{0,64},{32,96},{64,128},{96,160},{128,192},{160,224},{192,256},{22... | collective-permute-start | bytes 589832 | tf_op jit(solution)/shard_map/ppermute | solution.py:421
  123.6 10.8 %collective-permute-done.4.low_ref = bf16[2,8,48,128]{3,2,1,0:T(8,128)(2,1)} collective-permute-done((bf16[2,8,48,128]{3,2,1,0:T(8,128)(2,1)}, bf16[2,8,48,128]{3,2,1,0:T(8,128)(2,1)}, u32[]{:S(2)}, u32[]{:S(2)}) %collective-permute-start.4) | collective-permute-done | bytes 196640 | tf_op jit(solution)/shard_map/ppermute | solution.py:421
  135.2 6.5 %project.1 = (bf16[4,4,2,128,128]{4,3,2,1,0:T(8,128)(2,1)}, bf16[4,2,128,128]{3,2,1,0:T(8,128)(2,1)}, bf16[2,128,128]{2,1,0:T(8,128)(2,1)}, f32[2,8,128]{2,1,0:T...) custom-call(s32[5]{0:T(128)} %stack.38.place_ref, bf16[4,4,136,512]{3,2,1,0:T(8,128)(2,1)} %bitcast.31, ...), custom_call_target="tpu_custom_call" | custom-call | tf_op jit(solution)/shard_map/project/pallas_call | solution.py:467
  141.7 3.6 %all-to-all-start.2 = ((bf16[4,1024,128]{2,1,0:T(8,128)(2,1)}), bf16[4,1024,128]{2,1,0:T(8,128)(2,1)S(1)}, u32[]{:S(2)}, u32[]{:S(2)}) async-start(bf16[4,1024,128]{2,1,0:T(8,128)(2,1)} %bitcast.38), calls=%async_computation.2 | async-start | bytes 2097152 | tf_op jit(solution)/shard_map/all_to_all | solution.py:24
  148.5 11.7 %all-to-all-done.2.qk_ref = bf16[4,1024,128]{2,1,0:T(8,128)(2,1)S(1)} async-done(((bf16[4,1024,128]{2,1,0:T(8,128)(2,1)}), bf16[4,1024,128]{2,1,0:T(8,128)(2,1)S(1)}, u32[]{:S(2)}, u32[]{:S(2)}) %all-to-all-start.2) | async-done | bytes 1048608 | tf_op jit(solution)/shard_map/all_to_all | solution.py:24
  161.2 4.4 %slab_state.1 = (bf16[16,72,256]{2,1,0:T(8,128)(2,1)}, bf16[1024,256]{1,0:T(8,128)(2,1)}, bf16[1024,256]{1,0:T(8,128)(2,1)}, bf16[4,256,64]{2,1,0:T(8,128)(2,1)}) custom-call(s32[5]{0:T(128)} %stack.38.place_ref, bf16[4,1024,128]{2,1,0:T(8,128)(2,1)} %copy-done.2, bf16[1024,128]{1,0:T(8,128)(2,1)} %bitcast.39, f32[2,8,128]{2,1,0:T(8,128)} %get-tuple-element.25.gate_ref, ...), custom_call_target="tpu_custom_call" | custom-call | tf_op jit(solution)/shard_map/slab_state/pallas_call | solution.py:500
  165.5 5.6 %all-to-all-start.3 = ((bf16[16,72,256]{2,1,0:T(8,128)(2,1)}), bf16[16,72,256]{2,1,0:T(8,128)(2,1)S(1)}, u32[]{:S(2)}, u32[]{:S(2)}) async-start(bf16[16,72,256]{2,1,0:T(8,128)(2,1)} %get-tuple-element.27), calls=%async_computation.3 | async-start | bytes 1179648 | tf_op jit(solution)/shard_map/all_to_all | solution.py:24
  173.4 3.7 %collective-permute-start.8 = (bf16[4,4,8,16,128]{4,3,2,1,0:T(8,128)(2,1)S(1)}, bf16[4,4,8,16,128]{4,3,2,1,0:T(8,128)(2,1)S(1)}, u32[]{:S(2)}, u32[]{:S(2)}) collective-permute-start(bf16[4,4,8,16,128]{4,3,2,1,0:T(8,128)(2,1)S(1)} %copy-done.6), channel_id=1, source_target_pairs={{0,16},{8,24},{16,0},{24,8},{1,17},{9,25},{17,1},{25,9},{2,18},{10... | collective-permute-start | bytes 1572872 | tf_op jit(solution)/shard_map/ppermute | solution.py:493
  177.0 2.5 %collective-permute-start.7 = (bf16[4,4,8,16,128]{4,3,2,1,0:T(8,128)(2,1)S(1)}, bf16[4,4,8,16,128]{4,3,2,1,0:T(8,128)(2,1)S(1)}, u32[]{:S(2)}, u32[]{:S(2)}) collective-permute-start(bf16[4,4,8,16,128]{4,3,2,1,0:T(8,128)(2,1)S(1)} %copy-done.6), channel_id=1, source_target_pairs={{0,24},{8,0},{16,8},{24,16},{1,25},{9,1},{17,9},{25,17},{2,26},{10... | collective-permute-start | bytes 1572872 | tf_op jit(solution)/shard_map/ppermute | solution.py:493
  179.6 7.3 %collective-permute-done.9 = bf16[4,4,8,16,128]{4,3,2,1,0:T(8,128)(2,1)S(1)} collective-permute-done((bf16[4,4,8,16,128]{4,3,2,1,0:T(8,128)(2,1)S(1)}, bf16[4,4,8,16,128]{4,3,2,1,0:T(8,128)(2,1)S(1)}, u32[]{:S(2)}, u32[]{:S(2)}) %collective-permute-start.9) | collective-permute-done | bytes 524320 | tf_op jit(solution)/shard_map/ppermute | solution.py:493
  186.9 10.0 %collective-permute-done.8 = bf16[4,4,8,16,128]{4,3,2,1,0:T(8,128)(2,1)S(1)} collective-permute-done((bf16[4,4,8,16,128]{4,3,2,1,0:T(8,128)(2,1)S(1)}, bf16[4,4,8,16,128]{4,3,2,1,0:T(8,128)(2,1)S(1)}, u32[]{:S(2)}, u32[]{:S(2)}) %collective-permute-start.8) | collective-permute-done | bytes 524320 | tf_op jit(solution)/shard_map/ppermute | solution.py:493
  196.9 4.0 %collective-permute-done.7 = bf16[4,4,8,16,128]{4,3,2,1,0:T(8,128)(2,1)S(1)} collective-permute-done((bf16[4,4,8,16,128]{4,3,2,1,0:T(8,128)(2,1)S(1)}, bf16[4,4,8,16,128]{4,3,2,1,0:T(8,128)(2,1)S(1)}, u32[]{:S(2)}, u32[]{:S(2)}) %collective-permute-start.7) | collective-permute-done | bytes 524320 | tf_op jit(solution)/shard_map/ppermute | solution.py:493
  201.1 3.5 %collective-permute-start.10 = (bf16[4,4,4,8,16,128]{5,4,3,2,1,0:T(8,128)(2,1)S(1)}, bf16[4,4,4,8,16,128]{5,4,3,2,1,0:T(8,128)(2,1)}, u32[]{:S(2)}, u32[]{:S(2)}) collective-permute-start(bf16[4,4,4,8,16,128]{5,4,3,2,1,0:T(8,128)(2,1)S(1)} %pad_maximum_fusion.own_ref), channel_id=1, source_target_pairs={{0,4},{4,0},{1,5},{5,1},{2,6},{6,2},{3,7},{7,3},{8,12},{12,8},{9,1... | collective-permute-start | bytes 6291464 | tf_op jit(solution)/shard_map/ppermute | solution.py:28
  205.4 7.4 %cell.1 = bf16[4,2,4,128,128]{4,3,2,1,0:T(8,128)(2,1)} custom-call(s32[5]{0:T(128)} %stack.38.place_ref, bf16[16,72,256]{2,1,0:T(8,128)(2,1)} %copy-done.5, bf16[1024,256]{1,0:T(8,128)(2,1)} %get-tuple-element.28.q_ref, bf16[1024,256]{1,0:T(8,128)(2,1)} %get-tuple-element.29.k_ref, bf16[1024,128]{1,0:T(8,128)(2,1)} %bitcast.40, ...), custom_call_target="tpu_custom_call" | custom-call | tf_op jit(solution)/shard_map/cell/pallas_call | solution.py:514
  212.8 4.2 %all-to-all-start.4 = ((bf16[32,128,128]{2,1,0:T(8,128)(2,1)}), bf16[32,128,128]{2,1,0:T(8,128)(2,1)S(1)}, u32[]{:S(2)}, u32[]{:S(2)}) async-start(bf16[32,128,128]{2,1,0:T(8,128)(2,1)} %bitcast.32), calls=%async_computation.4 | async-start | bytes 2097152 | tf_op jit(solution)/shard_map/all_to_all | solution.py:24
  217.0 16.2 %all-to-all-done.4 = bf16[32,128,128]{2,1,0:T(8,128)(2,1)S(1)} async-done(((bf16[32,128,128]{2,1,0:T(8,128)(2,1)}), bf16[32,128,128]{2,1,0:T(8,128)(2,1)S(1)}, u32[]{:S(2)}, u32[]{:S(2)}) %all-to-all-start.4) | async-done | bytes 1048608 | tf_op jit(solution)/shard_map/all_to_all | solution.py:24
  234.3 5.5 %finish.1 = bf16[128,512]{1,0:T(8,128)(2,1)} custom-call(s32[5]{0:T(128)} %stack.38.place_ref, bf16[4,2,4,128,128]{4,3,2,1,0:T(8,128)(2,1)} %bitcast.33, bf16[4,4,4,8,16,128]{5,4,3,2,1,0:T(8,128)(2,1)} %copy-done.1, bf16[4,4,4,8,16,128]{5,4,3,2,1,0:T(8,128)(2,1)} %collective-permute-done.10.other_ref, f32[4,8,128]{2,1,0:T(8,128)} %get-tuple-element.32.gain_ref), custom_call_target="tpu_custom_call" | custom-call | tf_op jit(solution)/shard_map/finish/pallas_call | solution.py:524
  (57 shorter events, 20.9 us)
Async XLA Ops:
  3.7 7.7 %copy-start.11 = (bf16[256,16]{0,1:T(8,128)(2,1)S(1)}, bf16[256,16]{0,1:T(8,128)(2,1)}, u32[]{:S(2)}) copy-start(bf16[256,16]{0,1:T(8,128)(2,1)} %param.28) | copy-start | bytes 24580
  3.8 7.9 %copy-start.9 = (bf16[512,16]{0,1:T(8,128)(2,1)S(1)}, bf16[512,16]{0,1:T(8,128)(2,1)}, u32[]{:S(2)}) copy-start(bf16[512,16]{0,1:T(8,128)(2,1)} %param.29) | copy-start | bytes 49156
  3.8 34.3 %all-to-all-start = ((bf16[16,136,512]{2,1,0:T(8,128)(2,1)}), bf16[16,136,512]{2,1,0:T(8,128)(2,1)S(1)}, u32[]{:S(2)}, u32[]{:S(2)}) async-start(bf16[16,136,512]{2,1,0:T(8,128)(2,1)} %pack.1), calls=%async_computation | async-start | bytes 4456448 | tf_op jit(solution)/shard_map/all_to_all | solution.py:24
  11.5 110.2 %copy-start.12 = (bf16[2048,2]{0,1:T(2,128)(2,1)S(1)}, bf16[2048,2]{0,1:T(2,128)(2,1)}, u32[]{:S(2)}) copy-start(bf16[2048,2]{0,1:T(2,128)(2,1)} %param.24) | copy-start | bytes 24580
  11.5 110.2 %copy-start.13 = (bf16[2048,2]{0,1:T(2,128)(2,1)S(1)}, bf16[2048,2]{0,1:T(2,128)(2,1)}, u32[]{:S(2)}) copy-start(bf16[2048,2]{0,1:T(2,128)(2,1)} %param.23) | copy-start | bytes 24580
  38.1 96.3 %copy-start = (bf16[16,136,512]{2,1,0:T(8,128)(2,1)}, bf16[16,136,512]{2,1,0:T(8,128)(2,1)S(1)}, u32[]{:S(2)}) copy-start(bf16[16,136,512]{2,1,0:T(8,128)(2,1)S(1)} %all-to-all-done) | copy-start | bytes 6684676
  38.1 96.3 %collective-permute-start.1 = (bf16[4,4,136,512]{3,2,1,0:T(8,128)(2,1)S(1)}, bf16[4,4,136,512]{3,2,1,0:T(8,128)(2,1)}, u32[]{:S(2)}, u32[]{:S(2)}) collective-permute-start(bf16[4,4,136,512]{3,2,1,0:T(8,128)(2,1)S(1)} %bitcast.30), channel_id=1, source_target_pairs={{0,4},{4,0},{1,5},{5,1},{2,6},{6,2},{3,7},{7,3},{8,12},{12,8},{9,1... | collective-permute-start | bytes 6684680 | tf_op jit(solution)/shard_map/ppermute | solution.py:28
  45.7 0.7 collective-permute-start
  48.7 56.3 %all-to-all-start.1 = ((bf16[32,48,128]{2,1,0:T(8,128)(2,1)}), bf16[32,48,128]{2,1,0:T(8,128)(2,1)S(1)}, u32[]{:S(2)}, u32[]{:S(2)}) async-start(bf16[32,48,128]{2,1,0:T(8,128)(2,1)} %bitcast.37), calls=%async_computation.1 | async-start | bytes 786432 | tf_op jit(solution)/shard_map/all_to_all | solution.py:24
  104.9 29.5 %copy-start.4 = (bf16[32,48,128]{2,1,0:T(8,128)(2,1)}, bf16[32,48,128]{2,1,0:T(8,128)(2,1)S(1)}, u32[]{:S(2)}) copy-start(bf16[32,48,128]{2,1,0:T(8,128)(2,1)S(1)} %all-to-all-done.1) | copy-start | bytes 1179652
  104.9 29.5 %collective-permute-start.3 = (bf16[4,8,48,128]{3,2,1,0:T(8,128)(2,1)S(1)}, bf16[4,8,48,128]{3,2,1,0:T(8,128)(2,1)S(1)}, u32[]{:S(2)}, u32[]{:S(2)}) collective-permute-start(bf16[4,8,48,128]{3,2,1,0:T(8,128)(2,1)S(1)} %bitcast.34), channel_id=1, source_target_pairs={{0,32},{32,64},{64,96},{96,128},{128,160},{160,192},{192,224},{224... | collective-permute-start | bytes 1179656 | tf_op jit(solution)/shard_map/ppermute | solution.py:421
  112.8 21.6 %collective-permute-start.2 = (bf16[4,8,48,128]{3,2,1,0:T(8,128)(2,1)S(1)}, bf16[4,8,48,128]{3,2,1,0:T(8,128)(2,1)}, u32[]{:S(2)}, u32[]{:S(2)}) collective-permute-start(bf16[4,8,48,128]{3,2,1,0:T(8,128)(2,1)S(1)} %bitcast.35), channel_id=1, source_target_pairs={{0,480},{32,0},{64,32},{96,64},{128,96},{160,128},{192,160},{224,1... | collective-permute-start | bytes 1179656 | tf_op jit(solution)/shard_map/ppermute | solution.py:421
  115.5 18.9 %collective-permute-start.4 = (bf16[2,8,48,128]{3,2,1,0:T(8,128)(2,1)}, bf16[2,8,48,128]{3,2,1,0:T(8,128)(2,1)}, u32[]{:S(2)}, u32[]{:S(2)}) collective-permute-start(bf16[2,8,48,128]{3,2,1,0:T(8,128)(2,1)} %bitcast.13), channel_id=1, source_target_pairs={{0,448},{32,480},{64,0},{96,32},{128,64},{160,96},{192,128},{224,1... | collective-permute-start | bytes 589832 | tf_op jit(solution)/shard_map/ppermute | solution.py:421
  118.2 16.2 %collective-permute-start.5 = (bf16[2,8,48,128]{3,2,1,0:T(8,128)(2,1)}, bf16[2,8,48,128]{3,2,1,0:T(8,128)(2,1)}, u32[]{:S(2)}, u32[]{:S(2)}) collective-permute-start(bf16[2,8,48,128]{3,2,1,0:T(8,128)(2,1)} %bitcast.14), channel_id=1, source_target_pairs={{0,64},{32,96},{64,128},{96,160},{128,192},{160,224},{192,256},{22... | collective-permute-start | bytes 589832 | tf_op jit(solution)/shard_map/ppermute | solution.py:421
  141.7 29.5 %copy-start.6 = (bf16[4,4,8,16,128]{4,3,2,1,0:T(8,128)(2,1)S(1)}, bf16[4,4,8,16,128]{4,3,2,1,0:T(8,128)(2,1)}, u32[]{:S(2)}) copy-start(bf16[4,4,8,16,128]{4,3,2,1,0:T(8,128)(2,1)} %get-tuple-element.31) | copy-start | bytes 1572868
  141.7 18.5 %all-to-all-start.2 = ((bf16[4,1024,128]{2,1,0:T(8,128)(2,1)}), bf16[4,1024,128]{2,1,0:T(8,128)(2,1)S(1)}, u32[]{:S(2)}, u32[]{:S(2)}) async-start(bf16[4,1024,128]{2,1,0:T(8,128)(2,1)} %bitcast.38), calls=%async_computation.2 | async-start | bytes 2097152 | tf_op jit(solution)/shard_map/all_to_all | solution.py:24
  146.1 14.1 %collective-permute-start.6 = (bf16[32,32]{1,0:T(8,128)(2,1)S(1)}, bf16[32,32]{1,0:T(8,128)(2,1)S(1)}, u32[]{:S(2)}, u32[]{:S(2)}) collective-permute-start(bf16[32,32]{1,0:T(8,128)(2,1)S(1)} %slice_bitcast_fusion), channel_id=1, source_target_pairs={{0,32},{32,64},{64,96},{96,128},{128,160},{160,192},{192,224},{224... | collective-permute-start | bytes 6152 | tf_op jit(solution)/shard_map/ppermute | solution.py:485
  165.5 39.0 %all-to-all-start.3 = ((bf16[16,72,256]{2,1,0:T(8,128)(2,1)}), bf16[16,72,256]{2,1,0:T(8,128)(2,1)S(1)}, u32[]{:S(2)}, u32[]{:S(2)}) async-start(bf16[16,72,256]{2,1,0:T(8,128)(2,1)} %get-tuple-element.27), calls=%async_computation.3 | async-start | bytes 1179648 | tf_op jit(solution)/shard_map/all_to_all | solution.py:24
  171.2 15.7 %collective-permute-start.9 = (bf16[4,4,8,16,128]{4,3,2,1,0:T(8,128)(2,1)S(1)}, bf16[4,4,8,16,128]{4,3,2,1,0:T(8,128)(2,1)S(1)}, u32[]{:S(2)}, u32[]{:S(2)}) collective-permute-start(bf16[4,4,8,16,128]{4,3,2,1,0:T(8,128)(2,1)S(1)} %copy-done.6), channel_id=1, source_target_pairs={{0,8},{8,16},{16,24},{24,0},{1,9},{9,17},{17,25},{25,1},{2,10},{10... | collective-permute-start | bytes 1572872 | tf_op jit(solution)/shard_map/ppermute | solution.py:493
  173.4 23.5 %collective-permute-start.8 = (bf16[4,4,8,16,128]{4,3,2,1,0:T(8,128)(2,1)S(1)}, bf16[4,4,8,16,128]{4,3,2,1,0:T(8,128)(2,1)S(1)}, u32[]{:S(2)}, u32[]{:S(2)}) collective-permute-start(bf16[4,4,8,16,128]{4,3,2,1,0:T(8,128)(2,1)S(1)} %copy-done.6), channel_id=1, source_target_pairs={{0,16},{8,24},{16,0},{24,8},{1,17},{9,25},{17,1},{25,9},{2,18},{10... | collective-permute-start | bytes 1572872 | tf_op jit(solution)/shard_map/ppermute | solution.py:493
  177.0 23.8 %collective-permute-start.7 = (bf16[4,4,8,16,128]{4,3,2,1,0:T(8,128)(2,1)S(1)}, bf16[4,4,8,16,128]{4,3,2,1,0:T(8,128)(2,1)S(1)}, u32[]{:S(2)}, u32[]{:S(2)}) collective-permute-start(bf16[4,4,8,16,128]{4,3,2,1,0:T(8,128)(2,1)S(1)} %copy-done.6), channel_id=1, source_target_pairs={{0,24},{8,0},{16,8},{24,16},{1,25},{9,1},{17,9},{25,17},{2,26},{10... | collective-permute-start | bytes 1572872 | tf_op jit(solution)/shard_map/ppermute | solution.py:493
  201.1 11.8 %copy-start.1 = (bf16[4,4,4,8,16,128]{5,4,3,2,1,0:T(8,128)(2,1)}, bf16[4,4,4,8,16,128]{5,4,3,2,1,0:T(8,128)(2,1)S(1)}, u32[]{:S(2)}) copy-start(bf16[4,4,4,8,16,128]{5,4,3,2,1,0:T(8,128)(2,1)S(1)} %pad_maximum_fusion.own_ref) | copy-start | bytes 6291460
  201.1 15.9 %collective-permute-start.10 = (bf16[4,4,4,8,16,128]{5,4,3,2,1,0:T(8,128)(2,1)S(1)}, bf16[4,4,4,8,16,128]{5,4,3,2,1,0:T(8,128)(2,1)}, u32[]{:S(2)}, u32[]{:S(2)}) collective-permute-start(bf16[4,4,4,8,16,128]{5,4,3,2,1,0:T(8,128)(2,1)S(1)} %pad_maximum_fusion.own_ref), channel_id=1, source_target_pairs={{0,4},{4,0},{1,5},{5,1},{2,6},{6,2},{3,7},{7,3},{8,12},{12,8},{9,1... | collective-permute-start | bytes 6291464 | tf_op jit(solution)/shard_map/ppermute | solution.py:28
  212.8 20.4 %all-to-all-start.4 = ((bf16[32,128,128]{2,1,0:T(8,128)(2,1)}), bf16[32,128,128]{2,1,0:T(8,128)(2,1)S(1)}, u32[]{:S(2)}, u32[]{:S(2)}) async-start(bf16[32,128,128]{2,1,0:T(8,128)(2,1)} %bitcast.32), calls=%async_computation.4 | async-start | bytes 2097152 | tf_op jit(solution)/shard_map/all_to_all | solution.py:24
  (6 other events, 5.2 us)

commit v4 on v3

--- a/solution.py
+++ b/solution.py
@@ -67,8 +67,8 @@
     return high, mid, value - high - mid
 
 
-def pack_kernel(tokens_ref, offsets_ref, conv_gain_ref, memory_gain_ref, out_ref):
-    length = tokens_ref.shape[0]
+def pack_kernel(tokens_ref, offsets_ref, conv_gain_ref, memory_gain_ref, upper_ref, lower_ref):
+    length = tokens_ref.shape[0] // 2
     offsets = three_parts(offsets_ref[...])
     conv_gain = three_parts(conv_gain_ref[...])
     memory_gain = three_parts(memory_gain_ref[...])
@@ -77,15 +77,29 @@
     rows.append(jnp.concatenate(conv_gain[:2], axis=1))
     rows.append(jnp.concatenate([conv_gain[2], jnp.zeros_like(conv_gain[2])], axis=1))
     extra = jnp.concatenate(rows, axis=0).astype(BF16)
-    tokens = tokens_ref[...]
-    for j in range(out_ref.shape[0]):
-        out_ref[j, :length] = tokens
-        out_ref[j, length:] = extra
-
-
-def piece_kernel(query_ref, key_ref, value_ref, left_ref, right_ref, out_weight_ref, out_ref):
-    rows = query_ref.shape[0]
-    copies, nx, nc, _, half = out_ref.shape
+    upper, lower = tokens_ref[:length], tokens_ref[length:]
+    for j in range(upper_ref.shape[0]):
+        upper_ref[j, :length] = upper
+        upper_ref[j, length:] = extra
+        lower_ref[j] = lower
+
+
+def piece_kernel(
+    query_ref, key_ref, value_ref, left_ref, right_ref, memory_ref, conv_ref, out_ref, turn_ref
+):
+    nx, nc = out_ref.shape[0], out_ref.shape[1]
+    rows = turn_ref.shape[0]
+    width, chan = memory_ref.shape[0] // (nx * nc), conv_ref.shape[0] // (nx * nc)
+    parts = []
+    for at in range(nx * nc):
+        parts.append(memory_ref[at * width : (at + 1) * width].astype(F32))
+        parts.append(conv_ref[at * chan : (at + 1) * chan].astype(F32))
+    whole = jnp.concatenate(parts, axis=0)
+    lanes = 128
+    for j in range(whole.shape[0] // lanes):
+        tile = whole[j * lanes : (j + 1) * lanes]
+        tile = jnp.concatenate([tile, jnp.zeros((lanes, lanes - rows), F32)], axis=1)
+        turn_ref[:, j * lanes : (j + 1) * lanes] = tile.T[:rows].astype(BF16)
     for x in range(nx):
         for c in range(nc):
             at = c * nx + x
@@ -93,84 +107,81 @@
             for ref in (query_ref, key_ref, value_ref, left_ref, right_ref):
                 width = ref.shape[1] // (nx * nc)
                 parts.append(ref[:, at * width : (at + 1) * width])
-            whole = jnp.concatenate(parts, axis=1)
-            for j in range(copies):
-                out_ref[j, x, c, :rows] = whole[:, :half]
-                out_ref[j, x, c, rows : 2 * rows] = whole[:, half:]
-                out_ref[j, x, c, 2 * rows :] = out_weight_ref[x, c]
+            out_ref[x, c] = jnp.concatenate(parts, axis=1)
 
 
 def project_kernel(
-    place_ref, own_ref, other_ref, w0_ref, w1_ref, w3_ref, low_ref, high_ref, gate_ref,
+    place_ref, own_a_ref, own_b_ref, other_a_ref, other_b_ref,
+    w0_ref, w1_ref, w3_ref, low_ref, high_ref, gate_ref,
     qk_ref, v_ref, glu_ref, gates_ref, gain_ref, out_weight_ref,
 ):
-    nx, ny, _, part = own_ref.shape
-    far, senders, tall_piece, side = w0_ref.shape
-    rows = tall_piece // 3
-    block = senders * rows
-    close = part // block
+    nx, ny, _, part = own_a_ref.shape
+    far, tall, wide = w0_ref.shape
+    depth, chunks = out_weight_ref.shape[2], out_weight_ref.shape[3] // wide
+    rows = tall - depth * chunks
+    close = part // rows
+    members = far * close
     length = glu_ref.shape[1]
-    at_close, core, column = place_ref[0], place_ref[1], place_ref[2]
-    tokens_rows = nx * length
+    half_length = length // 2
+    place, core, column = place_ref[0], place_ref[1], place_ref[2]
+    tokens_rows = nx * half_length
     width = qk_ref.shape[4] // 2
     chan = glu_ref.shape[2] // nx
-    lane = lax.broadcasted_iota(jnp.int32, (length, width), 1)
+    lane = lax.broadcasted_iota(jnp.int32, (half_length, width), 1)
     ones = jnp.where(lane == 0, 1.0, 0.0).astype(BF16)
     row = lax.broadcasted_iota(jnp.int32, (2 * nx, length), 0)
     gate_in = jnp.zeros((2 * nx, length), F32)
     forget = jnp.zeros((2 * nx, length), F32)
 
-    def piece(distance, k):
-        if distance == 2:
-            return low_ref[k] if k < far // 2 else high_ref[k - far // 2]
-        return (w0_ref, w1_ref, None, w3_ref)[distance][k]
-
-    homes = [lax.rem(at_close + distance, close) for distance in range(close)]
-    for distance in range(close):
-        for k in range(far):
-            out_weight_ref[k, pl.ds(homes[distance], 1)] = piece(distance, k)[:, 2 * rows :][None]
-
-    def weight_block(distance, k):
-        mine = piece(distance, k)
-        return jnp.concatenate(
-            [
-                mine[:, :rows].reshape(block, side),
-                mine[:, rows : 2 * rows].reshape(block, side),
-            ],
-            axis=1,
-        )
-
-    for half, ref in enumerate((own_ref, other_ref)):
+    blocks = [(ref, i, ahead + close * (i - 1)) for ref, ahead in ((w0_ref, 0), (w1_ref, 1), (w3_ref, -1)) for i in range(far)]
+    blocks += [(low_ref, i, 2 + close * i) for i in range(far // 2)]
+    blocks += [(high_ref, i, -2 + close * (i - 1)) for i in range(far // 2)]
+    homes = []
+    for ref, i, ahead in blocks:
+        home = lax.rem(place + (ahead + members), members)
+        homes.append((lax.div(home, close), lax.rem(home, close)))
+        out_weight_ref[pl.ds(homes[-1][0], 1), pl.ds(homes[-1][1], 1)] = jnp.concatenate(
+            [ref[i, rows + j * depth : rows + (j + 1) * depth] for j in range(chunks)], axis=1
+        )[None, None]
+    packed = [[None, None], [None, None]]
+    for half, refs in enumerate(((own_a_ref, own_b_ref), (other_a_ref, other_b_ref))):
         home = core if half == 0 else 1 - core
-        acc = jnp.zeros((tokens_rows, 2 * side), F32)
-        pre = jnp.zeros((tokens_rows, gate_ref.shape[1]), F32)
-        for k in range(far):
-            for pair in ((0, 1), (2, 3)):
+        for side, ref in enumerate(refs):
+            acc = jnp.zeros((tokens_rows, wide), F32)
+            pre = jnp.zeros((tokens_rows, gate_ref.shape[1]), F32)
+            for pair in range(0, len(blocks), 2):
                 left, right, gate_rows = [], [], []
-                for distance in pair:
-                    start = pl.multiple_of(homes[distance] * block, block)
-                    lanes = pl.ds(start, block)
-                    left.append(ref[:, k, :length, lanes].reshape(tokens_rows, block))
-                    right.append(weight_block(distance, k))
-                    gate_rows.append(gate_ref[pl.ds(k * part + start, block)])
+                for at in (pair, pair + 1):
+                    w_ref, i, _ = blocks[at]
+                    y, z = homes[at]
+                    start = pl.multiple_of(z * rows, rows)
+                    lanes = pl.ds(start, rows)
+                    left.append(ref[:, pl.ds(y, 1), :half_length, lanes].reshape(tokens_rows, rows))
+                    right.append(w_ref[i, :rows])
+                    gate_rows.append(gate_ref[pl.ds(y * part + start, rows)])
                 lhs = jnp.concatenate(left, axis=1)
                 acc = acc + dot(lhs, jnp.concatenate(right, axis=0), NN)
                 pre = pre + dot(lhs, jnp.concatenate(gate_rows, axis=0), NN)
-        packed = []
+            glu = []
+            span = slice(side * half_length, (side + 1) * half_length)
+            for x in range(nx):
+                here = slice(x * half_length, (x + 1) * half_length)
+                mine = acc[here]
+                qk = mine[:, : 2 * width].astype(BF16)[None]
+                for j in range(qk_ref.shape[0]):
+                    qk_ref[j, x, pl.ds(home, 1), span] = qk
+                v_ref[x, pl.ds(home, 1), span] = jnp.concatenate(
+                    [mine[:, 2 * width : 3 * width].astype(BF16), ones], axis=1
+                )[None]
+                left = mine[:, 3 * width : 3 * width + chan]
+                right = mine[:, 3 * width + chan :]
+                glu.append(left / (1.0 + jnp.exp(-right)))
+            glu_ref[pl.ds(home, 1), span] = jnp.concatenate(glu, axis=1).astype(BF16)[None]
+            packed[half][side] = pre
         for x in range(nx):
-            here = slice(x * length, (x + 1) * length)
-            mine = acc[here]
-            qk = mine[:, : 2 * width].astype(BF16)[None]
-            for j in range(qk_ref.shape[0]):
-                qk_ref[j, x, pl.ds(home, 1)] = qk
-            v_ref[x, pl.ds(home, 1)] = jnp.concatenate(
-                [mine[:, 2 * width : 3 * width].astype(BF16), ones], axis=1
-            )[None]
-            left = mine[:, 3 * width : 3 * width + chan]
-            right = mine[:, 3 * width + chan :]
-            packed.append(left / (1.0 + jnp.exp(-right)))
-            turned = pre[here].T
-            extra = ref[x, column, length : length + 8].astype(F32)
+            here = slice(x * half_length, (x + 1) * half_length)
+            turned = jnp.concatenate([packed[half][0][here], packed[half][1][here]], axis=0).T
+            extra = refs[0][x, column, half_length : half_length + 8].astype(F32)
             values = extra[0:1] + extra[1:2] + extra[2:3]
             offsets = jnp.where(core == 0, values[:, :length], values[:, length : 2 * length])
             offsets_f = jnp.where(
@@ -181,9 +192,8 @@
             forget_pre = jnp.where(core == 0, turned[2:3], turned[3:4])
             gate_in = jnp.where(at, gate_pre + offsets, gate_in)
             forget = jnp.where(at, forget_pre + offsets_f, forget)
-        glu_ref[pl.ds(home, 1)] = jnp.concatenate(packed, axis=1).astype(BF16)[None]
     for b in range(ny):
-        extra = own_ref[0, b, length : length + 8].astype(F32)
+        extra = own_a_ref[0, b, half_length : half_length + 8].astype(F32)
         memory_gain = extra[3:4] + extra[4:5] + extra[5:6]
         half = part // 2
         conv_gain = extra[6:7, :half] + extra[6:7, half:] + extra[7:8, :half]
@@ -202,7 +212,7 @@
     gates_ref[1] = jnp.minimum(forget, 0.0) - jnp.where(y < 0.03, small, jnp.log(1.0 + y))
 
 
-def finish_kernel(place_ref, arrived_ref, own_ref, other_ref, gain_ref, out_ref):
+def finish_kernel(place_ref, arrived_ref, own_ref, other_ref, gain_ref, out_ref, weight_ref):
     nx, nc, ny, length, lanes = arrived_ref.shape
     core, x_at = place_ref[1], place_ref[3]
     width = lanes // 2
@@ -233,34 +243,39 @@
     spread = lax.rsqrt(power - mean * mean + EPS)
     shift = jnp.where(is_memory, 0.0, mean)
     factor = jnp.where(is_memory, scale, spread)
+    deep = weight_ref.shape[5]
+    for ahead in range(nx):
+        x = lax.rem(x_at + ahead, nx)
+        for c, ref in ((core, own_ref), (1 - core, other_ref)):
+            for b in range(ny):
+                for near in range(ref.shape[2]):
+                    weight_ref[b, near, pl.ds(x, 1), pl.ds(c, 1)] = ref[ahead, b, near][None, None]
     total = jnp.zeros((length, part), F32)
     for b in range(ny):
-        for ahead in range(nx):
-            x = lax.rem(x_at + ahead, nx)
-            left, right = [], []
-            for c, ref in ((core, own_ref), (1 - core, other_ref)):
-                gain = gain_ref[b, pl.ds(c * nx + x, 1)]
+        left = []
+        for c in range(nc):
+            for x in range(nx):
+                gain = gain_ref[b, c * nx + x : c * nx + x + 1]
                 normed = (block(x, c, b) - shift) * factor * gain
                 branch = normed / (1.0 + jnp.exp(-normed))
-                used = jnp.where(is_memory, normed, jnp.where(is_conv, branch, 0.0))
-                left.append(used.astype(BF16))
-                right.append(ref[ahead, b].reshape(part, lanes))
-            total = total + dot(
-                jnp.concatenate(left, axis=1), jnp.concatenate(right, axis=1), NT
-            )
+                used = jnp.where(is_memory, normed, branch).astype(BF16)
+                left.append(used[:, : width + chan])
+        total = total + dot(
+            jnp.concatenate(left, axis=1), weight_ref[b].reshape(part, deep), NT
+        )
     out_ref[...] = total.astype(BF16)
 
 
-def convolve(glu_ref, prior_ref, taps_ref, out_ref, core, x_at):
+def convolve(glu_ref, prior, taps_ref, nx, core, x_at):
     nc, length, lanes = glu_ref.shape
-    nx, chan = out_ref.shape[0], out_ref.shape[2] // 2
+    chan = lanes // nx
     group = nc * length
     glu = glu_ref[...].reshape(group, lanes).astype(F32)
     taps = taps_ref.shape[0]
     hold = 32
     lane = lax.broadcasted_iota(jnp.int32, (hold, lanes), 1)
     before = pltpu.roll(glu[group - hold :], chan, 1)
-    prior = jnp.concatenate([prior_ref[...].astype(F32), jnp.zeros((hold, lanes - chan), F32)], axis=1)
+    prior = jnp.concatenate([prior, jnp.zeros((hold, lanes - chan), F32)], axis=1)
     extended = jnp.concatenate([jnp.where(lane < chan, prior, before), glu], axis=0)
     weights = taps_ref[...].astype(F32)
     weights = jnp.where(core == 0, weights[:, :lanes], weights[:, lanes:])
@@ -277,16 +292,13 @@
                 total = total + moved[at - shift : at - shift + group] * weights[j : j + 1]
     high = total.astype(BF16)
     low = (total - high.astype(F32)).astype(BF16)
-    for x in range(nx):
-        mine = slice(x * chan, (x + 1) * chan)
-        out_ref[x] = jnp.concatenate([high[:, mine], low[:, mine]], axis=1)
+    sides = [slice(x * chan, (x + 1) * chan) for x in range(nx)]
+    return [jnp.concatenate([high[:, mine], low[:, mine]], axis=1) for mine in sides]
 
 
 def slab_kernel(
-    place_ref, qk_ref, v_ref, gate_ref, glu_ref, prior_ref, taps_ref,
-    out_ref, q_ref, k_ref, conv_ref,
+    qk_ref, v_ref, gate_ref, glu_ref, out_ref, q_ref, k_ref,
 ):
-    convolve(glu_ref, prior_ref, taps_ref, conv_ref, place_ref[1], place_ref[3])
     chunks, length = gate_ref.shape[1], gate_ref.shape[2]
     width = qk_ref.shape[2] // 2
     gate, forget = gate_ref[0], gate_ref[1]
@@ -307,7 +319,7 @@
         k_ref[r * length : (r + 1) * length] = key
         scaled = (fresh[:, r : r + 1] * key.astype(F32)).astype(BF16)
         state = state + dot(v_ref[r * length : (r + 1) * length], scaled, TN)
-    rows = out_ref.shape[1]
+    rows, head_lanes = out_ref.shape[1], out_ref.shape[2]
     kept = state[:rows]
     row = lax.broadcasted_iota(jnp.int32, kept.shape, 0)
     lane = lax.broadcasted_iota(jnp.int32, kept.shape, 1)
@@ -317,18 +329,32 @@
         low = value - high - mid
         for k, part in enumerate((high, mid, low)):
             kept = jnp.where((row == width + 1) & (lane == at + k), part, kept)
+    chan = glu_ref.shape[2] // qk_ref.shape[0]
+    hold = 32
+    tail = glu_ref[glu_ref.shape[0] - 1, length - hold :].astype(F32)[:, glu_ref.shape[2] - chan :]
+    group = head_lanes // chan
+    each = hold // group
+    tail = jnp.concatenate([tail[g * each : (g + 1) * each] for g in range(group)], axis=1)
+    kept = jnp.concatenate([kept[: width + 2], tail, kept[width + 2 + each :]], axis=0)
     kept = kept.astype(BF16)
     for j in range(out_ref.shape[0]):
         out_ref[j] = kept
 
 
-def cell_kernel(place_ref, in_ref, q_ref, k_ref, v_ref, gate_ref, conv_ref, out_ref):
+def cell_kernel(place_ref, in_ref, q_ref, k_ref, v_ref, gate_ref, glu_ref, taps_ref, out_ref):
     chunks, length = gate_ref.shape[1], gate_ref.shape[2]
     members, rows, head = in_ref.shape
     width = out_ref.shape[4] // 2
     nc, ny = out_ref.shape[1], out_ref.shape[2]
     scale = head ** (-0.5)
-    place = place_ref[4]
+    place = place_ref[0]
+    chan = glu_ref.shape[2] // out_ref.shape[0]
+    hold, group = 32, head // chan
+    each = hold // group
+    last_rows = in_ref[jnp.maximum(place - 1, 0), width : width + 8].astype(F32)
+    last_rows = jnp.where(place > 0, last_rows[2 : 2 + each], 0.0)
+    prior = jnp.concatenate([last_rows[:, g * chan : (g + 1) * chan] for g in range(group)], axis=0)
+    conv = convolve(glu_ref, prior, taps_ref, out_ref.shape[0], place_ref[1], place_ref[3])
     acc = jnp.zeros((1, 1), F32)
     logs = [None] * members
     for j in range(members - 1, -1, -1):
@@ -370,7 +396,7 @@
         result = numer[:, :width] / jnp.maximum(jnp.abs(denom), 1.0)
         x, c = r // nc, r % nc
         sent = jnp.concatenate(
-            [result.astype(BF16), conv_ref[x, c * length : (c + 1) * length]], axis=1
+            [result.astype(BF16), conv[x][c * length : (c + 1) * length]], axis=1
         )
         for y in range(ny):
             out_ref[x, c, y] = sent
@@ -420,49 +446,71 @@
     def from_z(value, ahead):
         return lax.ppermute(value, Z, [(j, (j - ahead) % members) for j in range(members)])
 
-    out_rows = jnp.concatenate(
-        [
-            memory_out_weight.reshape(nc, nx, width, rows),
-            conv_out_weight.reshape(nc, nx, chan, rows),
-            jnp.zeros((nc, nx, width - chan, rows), BF16),
-        ],
-        axis=2,
-    ).transpose(1, 0, 3, 2)
+    deep = memory_out_weight.shape[0] + conv_out_weight.shape[0]
+    pieces, out_rows = pl.pallas_call(
+        piece_kernel,
+        out_shape=(
+            jax.ShapeDtypeStruct((nx, nc, rows, wide), BF16),
+            jax.ShapeDtypeStruct((rows, deep), BF16),
+        ),
+        in_specs=vmem(7),
+        out_specs=vmem(2),
+        interpret=INTERPRET,
+        name="pieces",
+    )(
+        query_weight,
+        key_weight,
+        value_weight,
+        conv_value_weight,
+        conv_gate_weight,
+        memory_out_weight,
+        conv_out_weight,
+    )
     turned = lax.ppermute(
         out_rows,
         ("zh", "tp"),
         [(a * ny + b, b * ny + a) for a in range(nzh) for b in range(ny)],
     )
     offsets = jnp.concatenate([input_offset.T, forget_offset.T], axis=0)
-    tall = length + 8
-    sent = pl.pallas_call(
+    half = length // 2
+    upper, lower = pl.pallas_call(
         pack_kernel,
-        out_shape=jax.ShapeDtypeStruct((nx * ny, tall, part), BF16),
+        out_shape=(
+            jax.ShapeDtypeStruct((nx * ny, half + 8, part), BF16),
+            jax.ShapeDtypeStruct((nx * ny, half, part), BF16),
+        ),
         in_specs=vmem(4),
-        out_specs=pl.BlockSpec(memory_space=pltpu.VMEM),
+        out_specs=vmem(2),
         interpret=INTERPRET,
         name="pack",
     )(tokens, offsets, conv_norm_gain[None], memory_norm_gain[None])
-    own = exchange(sent, ("x", "tp")).reshape(nx, ny, tall, part)
-    other = swapped(own, "c")
-    own, turned = lax.optimization_barrier((own, turned))
-    pieces = pl.pallas_call(
-        piece_kernel,
-        out_shape=jax.ShapeDtypeStruct((nzh, nx, nc, 3 * rows, wide // 2), BF16),
-        in_specs=vmem(6),
-        out_specs=pl.BlockSpec(memory_space=pltpu.VMEM),
-        interpret=INTERPRET,
-        name="pieces",
-    )(query_weight, key_weight, value_weight, conv_value_weight, conv_gate_weight, turned)
-    near = exchange(pieces.reshape(nzh * nx * nc, 3 * rows, wide // 2), ("zh", "x", "c"))
-    near = near.reshape(nzh, nx * nc, 3 * rows, wide // 2)
+    mine = exchange(pieces.reshape(nx * nc, rows, wide), ("x", "c"))
+    mine = mine.reshape(nx * nc * rows, wide)
+    upper, lower, mine = lax.optimization_barrier((upper, lower, mine))
+    own_a = exchange(upper, ("x", "tp"))
+    turned = jnp.concatenate([turned[:, j * wide : (j + 1) * wide] for j in range(deep // wide)], 0)
+    mine = jnp.concatenate([mine, turned], axis=0)
+    step, cut = members // 4, mine.shape[0] // 2
+    far = [
+        from_z(mine, -step),
+        from_z(mine, step),
+        from_z(mine[:cut], 2 * step),
+        from_z(mine[cut:], -2 * step),
+    ]
+    near = jnp.stack([far[0], mine, far[1], jnp.concatenate(far[2:], axis=0)], axis=0)
+    near, lower, own_a = lax.optimization_barrier((near, lower, own_a))
+    own_b = exchange(lower, ("x", "tp"))
     sets = [near, from_z(near, 1), from_z(near, -1)]
-    sets += [from_z(near[: nzh // 2], 2), from_z(near[nzh // 2 :], -2)]
+    sets += [from_z(near[1:3], 2), from_z(near[:2], -2)]
+    own_a = own_a.reshape(nx, ny, half + 8, part)
+    own_b = own_b.reshape(nx, ny, half, part)
+    others = [swapped(own_a, "c")]
+    others.append(swapped(own_b, "c"))
 
     gate_weight = jnp.pad(
         jnp.concatenate([input_gate_weight, forget_gate_weight], axis=1), ((0, 0), (0, 124))
     )
-    place = jnp.stack([lax.axis_index("zl"), ci, yi, xi, zi])
+    place = jnp.stack([zi, ci, yi, xi])
     smem = pl.BlockSpec(memory_space=pltpu.SMEM)
     qk, value, packed, gates, gain, out_part = pl.pallas_call(
         project_kernel,
@@ -472,21 +520,14 @@
             jax.ShapeDtypeStruct((nc, length, nx * chan), BF16),
             jax.ShapeDtypeStruct((2, nx * nc, length), F32),
             jax.ShapeDtypeStruct((ny, nc * nx, 2 * width), F32),
-            jax.ShapeDtypeStruct((nzh, nzl, nx * nc, rows, wide // 2), BF16),
+            jax.ShapeDtypeStruct((nzh, nzl, rows, deep), BF16),
         ),
-        in_specs=[smem] + vmem(8),
+        in_specs=[smem] + vmem(10),
         out_specs=vmem(6),
         interpret=INTERPRET,
         name="project",
-    )(place, own, other, *sets, gate_weight)
+    )(place, own_a, own_b, *others, *sets, gate_weight)
     value = value.reshape(slab, 2 * width)
-    group = slab // nx
-    hold = 32
-    prior = lax.ppermute(
-        packed[nc - 1, length - hold :, (nx - 1) * chan :],
-        Z,
-        [(j, j + 1) for j in range(members - 1)],
-    )
     all_qk = exchange(qk.reshape(nx, slab, 2 * width), "x")
     out_part, all_qk = lax.optimization_barrier((out_part, all_qk))
     out_parts = [out_part] + [
@@ -497,28 +538,27 @@
     other_out = swapped(own_out, "c")
 
     state_rows = width + 8
-    states, query, key, conv_sent = pl.pallas_call(
+    states, query, key = pl.pallas_call(
         slab_kernel,
         out_shape=(
             jax.ShapeDtypeStruct((members, state_rows, head), BF16),
             jax.ShapeDtypeStruct((slab, head), BF16),
             jax.ShapeDtypeStruct((slab, head), BF16),
-            jax.ShapeDtypeStruct((nx, group, 2 * chan), BF16),
         ),
-        in_specs=[smem] + vmem(6),
-        out_specs=vmem(4),
+        in_specs=vmem(4),
+        out_specs=vmem(3),
         interpret=INTERPRET,
         name="slab_state",
-    )(place, all_qk, value, gates, packed, prior, conv_kernel)
+    )(all_qk, value, gates, packed)
     states = exchange(states, Z)
     last = pl.pallas_call(
         cell_kernel,
         out_shape=jax.ShapeDtypeStruct((nx, nc, ny, length, 2 * width), BF16),
-        in_specs=[smem] + vmem(6),
+        in_specs=[smem] + vmem(7),
         out_specs=pl.BlockSpec(memory_space=pltpu.VMEM),
         interpret=INTERPRET,
         name="cell",
-    )(place, states, query, key, value, gates, conv_sent)
+    )(place, states, query, key, value, gates, packed, conv_kernel)
     arrived = exchange(last.reshape(nx * nc * ny, length, -1), ("x", "c", "tp"))
     arrived = arrived.reshape(nx, nc, ny, length, -1)
     return pl.pallas_call(
@@ -526,6 +566,7 @@
         out_shape=jax.ShapeDtypeStruct((length, part), BF16),
         in_specs=[smem] + vmem(4),
         out_specs=pl.BlockSpec(memory_space=pltpu.VMEM),
+        scratch_shapes=[pltpu.VMEM((ny, nzl, nx, nc, rows, deep), BF16)],
         interpret=INTERPRET,
         name="finish",
     )(place, arrived, own_out, other_out, gain)

time: 241 us -> 233 us (0.967)
  waiting for transfers between devices: 110 us -> 58.2 us
  starting transfers between devices: 92.1 us -> 117 us
  blocking collectives: 0 us -> 18.3 us
    all_to_all x5, waiting for transfers between devices: 77.8 us -> 21.2 us  [exchange(): return lax.all_to_all(pieces, axes, split_axis=0, concat_axis=0, tiled=True)]
    ppermute x4 -> x8, starting transfers between devices: 16 us -> 54.9 us  [from_z(): lax.ppermute(value, Z, [(j, (j - ahead) % members) for j in range(members)])]
    all_to_all x5, starting transfers between devices: 53.7 us -> 32.3 us  [exchange(): return lax.all_to_all(pieces, axes, split_axis=0, concat_axis=0, tiled=True)]
    all_to_all x0 -> x1, blocking collectives: none -> 18.3 us  [exchange(): return lax.all_to_all(pieces, axes, split_axis=0, concat_axis=0, tiled=True)]
    ppermute x4 -> x8, waiting for transfers between devices: 10.8 us -> 21.4 us  [from_z(): lax.ppermute(value, Z, [(j, (j - ahead) % members) for j in range(members)])]
    ppermute x2 -> x3, starting transfers between devices: 10.9 us -> 20.7 us  [swapped(): return lax.ppermute(value, axis, [(0, 1), (1, 0)])]
    ppermute x3, waiting for transfers between devices: 21.2 us -> 15.6 us  [layer(): lax.ppermute(out_part, 'x', [(j, (j - ahead) % nx) for j in range(nx)])]
    unnamed x28 -> x26, local copies, waits for them, and re-layouts: 4.17 us -> 5.44 us
  transfers between devices with their start and end apart: 16 -> 20, of which waited for: 8 -> 9; matrix products, arithmetic and copies ran while one was open for 2% -> 2% of each run, Pallas kernels for 4% -> 4%
where the time goes in v4:
time: 233 us; the launch traced here: 231 us
  starting transfers between devices  117 us (50%)
  waiting for transfers between devices  58.2 us (25%)
  Pallas kernels  27.8 us (12%)
  blocking collectives  18.3 us (8%)
  local copies, waits for them, and re-layouts  7.37 us (3%)
    ppermute x8, starting transfers between devices, from_z(): lax.ppermute(value, Z, [(j, (j - ahead) % members) for j in range(members)])  54.9 us
    all_to_all x5, starting transfers between devices, exchange(): return lax.all_to_all(pieces, axes, split_axis=0, concat_axis=0, tiled=True)  32.3 us
    ppermute x8, waiting for transfers between devices, from_z(): lax.ppermute(value, Z, [(j, (j - ahead) % members) for j in range(members)])  21.4 us
    all_to_all x5, waiting for transfers between devices, exchange(): return lax.all_to_all(pieces, axes, split_axis=0, concat_axis=0, tiled=True)  21.2 us
    ppermute x3, starting transfers between devices, swapped(): return lax.ppermute(value, axis, [(0, 1), (1, 0)])  20.7 us
    all_to_all x1, blocking collectives, exchange(): return lax.all_to_all(pieces, axes, split_axis=0, concat_axis=0, tiled=True)  18.3 us
    ppermute x3, waiting for transfers between devices, layer(): lax.ppermute(out_part, 'x', [(j, (j - ahead) % nx) for j in range(nx)])  15.6 us
    ppermute x3, starting transfers between devices, layer(): lax.ppermute(out_part, 'x', [(j, (j - ahead) % nx) for j in range(nx)])  8.42 us
  transfers between devices with their start and end apart: 20, of which 9 were waited for; matrix products, arithmetic and copies ran while one was open for 2% of the time, Pallas kernels for 4%

profile of v4, /device:TPU:1, one launch (start us, length us, event | category | flops | bytes accessed | tf_op | source)
XLA Modules:
  0.0 231.2 jit_solution(15098880154913270649)
XLA Ops:
  4.7 10.2 %all-to-all-start = ((bf16[8,16,256]{2,1,0:T(8,128)(2,1)}), bf16[8,16,256]{2,1,0:T(8,128)(2,1)S(1)}, u32[]{:S(2)}, u32[]{:S(2)}) async-start(bf16[8,16,256]{2,1,0:T(8,128)(2,1)} %bitcast.43), calls=%async_computation | async-start | bytes 131072 | tf_op jit(solution)/shard_map/all_to_all | solution.py:24
  19.8 3.7 %all-to-all-start.1 = ((bf16[16,72,512]{2,1,0:T(8,128)(2,1)}), bf16[16,72,512]{2,1,0:T(8,128)(2,1)S(1)}, u32[]{:S(2)}, u32[]{:S(2)}) async-start(bf16[16,72,512]{2,1,0:T(8,128)(2,1)} %get-tuple-element.32), calls=%async_computation.1 | async-start | bytes 2359296 | tf_op jit(solution)/shard_map/all_to_all | solution.py:24
  24.2 28.9 %collective-permute-start.3 = (bf16[88,256]{1,0:T(8,128)(2,1)S(1)}, bf16[88,256]{1,0:T(8,128)(2,1)S(1)}, u32[]{:S(2)}, u32[]{:S(2)}) collective-permute-start(bf16[88,256]{1,0:T(8,128)(2,1)S(1)} %slice.24), channel_id=1, source_target_pairs={{0,256},{32,288},{64,320},{96,352},{128,384},{160,416},{192,448},{... | collective-permute-start | bytes 135176 | tf_op jit(solution)/shard_map/ppermute | solution.py:447
  55.1 3.6 %collective-permute-start.2 = (bf16[176,256]{1,0:T(8,128)(2,1)S(1)}, bf16[176,256]{1,0:T(8,128)(2,1)S(1)}, u32[]{:S(2)}, u32[]{:S(2)}) collective-permute-start(bf16[176,256]{1,0:T(8,128)(2,1)S(1)} %get-tuple-element.50), channel_id=1, source_target_pairs={{0,384},{32,416},{64,448},{96,480},{128,0},{160,32},{192,64},{224,... | collective-permute-start | bytes 270344 | tf_op jit(solution)/shard_map/ppermute | solution.py:447
  58.7 5.6 %collective-permute-start.1 = (bf16[176,256]{1,0:T(8,128)(2,1)S(1)}, bf16[176,256]{1,0:T(8,128)(2,1)S(1)}, u32[]{:S(2)}, u32[]{:S(2)}) collective-permute-start(bf16[176,256]{1,0:T(8,128)(2,1)S(1)} %get-tuple-element.50), channel_id=1, source_target_pairs={{0,128},{32,160},{64,192},{96,224},{128,256},{160,288},{192,320},{... | collective-permute-start | bytes 270344 | tf_op jit(solution)/shard_map/ppermute | solution.py:447
  66.6 5.7 %collective-permute-done.2 = bf16[176,256]{1,0:T(8,128)(2,1)S(1)} collective-permute-done((bf16[176,256]{1,0:T(8,128)(2,1)S(1)}, bf16[176,256]{1,0:T(8,128)(2,1)S(1)}, u32[]{:S(2)}, u32[]{:S(2)}) %collective-permute-start.2) | collective-permute-done | bytes 90144 | tf_op jit(solution)/shard_map/ppermute | solution.py:447
  72.5 7.0 %all-to-all-start.2 = ((bf16[16,64,512]{2,1,0:T(8,128)(2,1)}), bf16[16,64,512]{2,1,0:T(8,128)(2,1)S(1)}, u32[]{:S(2)}, u32[]{:S(2)}) async-start(bf16[16,64,512]{2,1,0:T(8,128)(2,1)} %get-tuple-element.34), calls=%async_computation.2 | async-start | bytes 2097152 | tf_op jit(solution)/shard_map/all_to_all | solution.py:24
  79.5 8.1 %collective-permute-start.5 = (bf16[4,4,72,512]{3,2,1,0:T(8,128)(2,1)S(1)}, bf16[4,4,72,512]{3,2,1,0:T(8,128)(2,1)}, u32[]{:S(2)}, u32[]{:S(2)}) collective-permute-start(bf16[4,4,72,512]{3,2,1,0:T(8,128)(2,1)S(1)} %bitcast.26), channel_id=1, source_target_pairs={{0,4},{4,0},{1,5},{5,1},{2,6},{6,2},{3,7},{7,3},{8,12},{12,8},{9,1... | collective-permute-start | bytes 3538952 | tf_op jit(solution)/shard_map/ppermute | solution.py:28
  87.6 3.7 %all-to-all-done.2 = bf16[16,64,512]{2,1,0:T(8,128)(2,1)S(1)} async-done(((bf16[16,64,512]{2,1,0:T(8,128)(2,1)}), bf16[16,64,512]{2,1,0:T(8,128)(2,1)S(1)}, u32[]{:S(2)}, u32[]{:S(2)}) %all-to-all-start.2) | async-done | bytes 1048608 | tf_op jit(solution)/shard_map/all_to_all | solution.py:24
  91.4 9.1 %collective-permute-start.6 = (bf16[4,4,64,512]{3,2,1,0:T(8,128)(2,1)S(1)}, bf16[4,4,64,512]{3,2,1,0:T(8,128)(2,1)}, u32[]{:S(2)}, u32[]{:S(2)}) collective-permute-start(bf16[4,4,64,512]{3,2,1,0:T(8,128)(2,1)S(1)} %bitcast.28), channel_id=1, source_target_pairs={{0,4},{4,0},{1,5},{5,1},{2,6},{6,2},{3,7},{7,3},{8,12},{12,8},{9,1... | collective-permute-start | bytes 3145736 | tf_op jit(solution)/shard_map/ppermute | solution.py:28
  101.2 4.1 %collective-permute-start.10 = (bf16[2,176,256]{2,1,0:T(8,128)(2,1)S(1)}, bf16[2,176,256]{2,1,0:T(8,128)(2,1)S(1)}, u32[]{:S(2)}, u32[]{:S(2)}) collective-permute-start(bf16[2,176,256]{2,1,0:T(8,128)(2,1)S(1)} %get-tuple-element.47), channel_id=1, source_target_pairs={{0,64},{32,96},{64,128},{96,160},{128,192},{160,224},{192,256},{22... | collective-permute-start | bytes 540680 | tf_op jit(solution)/shard_map/ppermute | solution.py:447
  105.3 7.0 %collective-permute-start.8 = (bf16[4,176,256]{2,1,0:T(8,128)(2,1)S(1)}, bf16[4,176,256]{2,1,0:T(8,128)(2,1)S(1)}, u32[]{:S(2)}, u32[]{:S(2)}) collective-permute-start(bf16[4,176,256]{2,1,0:T(8,128)(2,1)S(1)} %pad_maximum_fusion.1.w0_ref), channel_id=1, source_target_pairs={{0,32},{32,64},{64,96},{96,128},{128,160},{160,192},{192,224},{224... | collective-permute-start | bytes 1081352 | tf_op jit(solution)/shard_map/ppermute | solution.py:447
  118.1 13.3 %collective-permute-done.9.low_ref = bf16[2,176,256]{2,1,0:T(8,128)(2,1)} collective-permute-done((bf16[2,176,256]{2,1,0:T(8,128)(2,1)}, bf16[2,176,256]{2,1,0:T(8,128)(2,1)}, u32[]{:S(2)}, u32[]{:S(2)}) %collective-permute-start.9) | collective-permute-done | bytes 180256 | tf_op jit(solution)/shard_map/ppermute | solution.py:447
  132.2 6.7 %project.1 = (bf16[4,4,2,128,128]{4,3,2,1,0:T(8,128)(2,1)}, bf16[4,2,128,128]{3,2,1,0:T(8,128)(2,1)}, bf16[2,128,128]{2,1,0:T(8,128)(2,1)}, f32[2,8,128]{2,1,0:T...) custom-call(s32[4]{0:T(128)} %pad_add_fusion.place_ref, bf16[4,4,72,512]{3,2,1,0:T(8,128)(2,1)} %bitcast.27, ...), custom_call_target="tpu_custom_call" | custom-call | tf_op jit(solution)/shard_map/project/pallas_call | solution.py:515
  138.9 18.3 %all_to_all.30.qk_ref = bf16[4,1024,128]{2,1,0:T(8,128)(2,1)} all-to-all(bf16[4,1024,128]{2,1,0:T(8,128)(2,1)} %bitcast.32), channel_id=1, replica_groups=mesh['zh'=4,'zl'=4,'x'=4,'c'=2,'tp'=4] {'x'}, dimensions={0} | all-to-all | bytes 2097152 | tf_op jit(solution)/shard_map/all_to_all | solution.py:24
  157.2 3.8 %slab_state.1 = (bf16[16,72,256]{2,1,0:T(8,128)(2,1)}, bf16[1024,256]{1,0:T(8,128)(2,1)}, bf16[1024,256]{1,0:T(8,128)(2,1)}) custom-call(bf16[4,1024,128]{2,1,0:T(8,128)(2,1)} %all_to_all.30.qk_ref, bf16[1024,128]{1,0:T(8,128)(2,1)} %bitcast.33, f32[2,8,128]{2,1,0:T(8,128)} %get-tuple-element.40.gate_ref, bf16[2,128,128]{2,1,0:T(8,128)(2,1)} %get-tuple-element.41.glu_ref), custom_call_target="tpu_custom_call" | custom-call | tf_op jit(solution)/shard_map/slab_state/pallas_call | solution.py:541
  160.9 4.0 %all-to-all-start.4 = ((bf16[16,72,256]{2,1,0:T(8,128)(2,1)}), bf16[16,72,256]{2,1,0:T(8,128)(2,1)S(1)}, u32[]{:S(2)}, u32[]{:S(2)}) async-start(bf16[16,72,256]{2,1,0:T(8,128)(2,1)} %get-tuple-element.42), calls=%async_computation.4 | async-start | bytes 1179648 | tf_op jit(solution)/shard_map/all_to_all | solution.py:24
  167.2 3.7 %collective-permute-start.12 = (bf16[4,4,16,768]{3,2,1,0:T(8,128)(2,1)S(1)}, bf16[4,4,16,768]{3,2,1,0:T(8,128)(2,1)S(1)}, u32[]{:S(2)}, u32[]{:S(2)}) collective-permute-start(bf16[4,4,16,768]{3,2,1,0:T(8,128)(2,1)S(1)} %copy-done.6), channel_id=1, source_target_pairs={{0,16},{8,24},{16,0},{24,8},{1,17},{9,25},{17,1},{25,9},{2,18},{10... | collective-permute-start | bytes 1179656 | tf_op jit(solution)/shard_map/ppermute | solution.py:534
  177.0 7.3 %collective-permute-done.12 = bf16[4,4,16,768]{3,2,1,0:T(8,128)(2,1)S(1)} collective-permute-done((bf16[4,4,16,768]{3,2,1,0:T(8,128)(2,1)S(1)}, bf16[4,4,16,768]{3,2,1,0:T(8,128)(2,1)S(1)}, u32[]{:S(2)}, u32[]{:S(2)}) %collective-permute-start.12) | collective-permute-done | bytes 393248 | tf_op jit(solution)/shard_map/ppermute | solution.py:534
  184.3 4.7 %collective-permute-done.11 = bf16[4,4,16,768]{3,2,1,0:T(8,128)(2,1)S(1)} collective-permute-done((bf16[4,4,16,768]{3,2,1,0:T(8,128)(2,1)S(1)}, bf16[4,4,16,768]{3,2,1,0:T(8,128)(2,1)S(1)}, u32[]{:S(2)}, u32[]{:S(2)}) %collective-permute-start.11) | collective-permute-done | bytes 393248 | tf_op jit(solution)/shard_map/ppermute | solution.py:534
  193.6 7.6 %cell.1 = bf16[4,2,4,128,128]{4,3,2,1,0:T(8,128)(2,1)} custom-call(s32[4]{0:T(128)} %pad_add_fusion.place_ref, bf16[16,72,256]{2,1,0:T(8,128)(2,1)} %copy-done.5, bf16[1024,256]{1,0:T(8,128)(2,1)} %get-tuple-element.43.q_ref, bf16[1024,256]{1,0:T(8,128)(2,1)} %get-tuple-element.44.k_ref, bf16[1024,128]{1,0:T(8,128)(2,1)} %bitcast.34, ...), custom_call_target="tpu_custom_call" | custom-call | tf_op jit(solution)/shard_map/cell/pallas_call | solution.py:554
  201.1 7.3 %all-to-all-start.5 = ((bf16[32,128,128]{2,1,0:T(8,128)(2,1)}), bf16[32,128,128]{2,1,0:T(8,128)(2,1)S(1)}, u32[]{:S(2)}, u32[]{:S(2)}) async-start(bf16[32,128,128]{2,1,0:T(8,128)(2,1)} %bitcast.31), calls=%async_computation.5 | async-start | bytes 2097152 | tf_op jit(solution)/shard_map/all_to_all | solution.py:24
  208.5 16.3 %all-to-all-done.5 = bf16[32,128,128]{2,1,0:T(8,128)(2,1)S(1)} async-done(((bf16[32,128,128]{2,1,0:T(8,128)(2,1)}), bf16[32,128,128]{2,1,0:T(8,128)(2,1)S(1)}, u32[]{:S(2)}, u32[]{:S(2)}) %all-to-all-start.5) | async-done | bytes 1048608 | tf_op jit(solution)/shard_map/all_to_all | solution.py:24
  225.8 5.5 %finish.1 = bf16[128,512]{1,0:T(8,128)(2,1)} custom-call(s32[4]{0:T(128)} %pad_add_fusion.place_ref, bf16[4,2,4,128,128]{4,3,2,1,0:T(8,128)(2,1)} %bitcast.30, bf16[4,4,4,16,768]{4,3,2,1,0:T(8,128)(2,1)} %copy-done, bf16[4,4,4,16,768]{4,3,2,1,0:T(8,128)(2,1)} %collective-permute-done.14.other_ref, f32[4,8,128]{2,1,0:T(8,128)} %get-tuple-element.46.gain_ref), custom_call_target="tpu_custom_call" | custom-call | tf_op jit(solution)/shard_map/finish/pallas_call | solution.py:564
  (62 shorter events, 35.5 us)
Async XLA Ops:
  4.7 15.1 %all-to-all-start = ((bf16[8,16,256]{2,1,0:T(8,128)(2,1)}), bf16[8,16,256]{2,1,0:T(8,128)(2,1)S(1)}, u32[]{:S(2)}, u32[]{:S(2)}) async-start(bf16[8,16,256]{2,1,0:T(8,128)(2,1)} %bitcast.43), calls=%async_computation | async-start | bytes 131072 | tf_op jit(solution)/shard_map/all_to_all | solution.py:24
  19.8 52.7 %all-to-all-start.1 = ((bf16[16,72,512]{2,1,0:T(8,128)(2,1)}), bf16[16,72,512]{2,1,0:T(8,128)(2,1)S(1)}, u32[]{:S(2)}, u32[]{:S(2)}) async-start(bf16[16,72,512]{2,1,0:T(8,128)(2,1)} %get-tuple-element.32), calls=%async_computation.1 | async-start | bytes 2359296 | tf_op jit(solution)/shard_map/all_to_all | solution.py:24
  23.5 0.7 collective-permute-start
  24.2 40.1 %collective-permute-start.3 = (bf16[88,256]{1,0:T(8,128)(2,1)S(1)}, bf16[88,256]{1,0:T(8,128)(2,1)S(1)}, u32[]{:S(2)}, u32[]{:S(2)}) collective-permute-start(bf16[88,256]{1,0:T(8,128)(2,1)S(1)} %slice.24), channel_id=1, source_target_pairs={{0,256},{32,288},{64,320},{96,352},{128,384},{160,416},{192,448},{... | collective-permute-start | bytes 135176 | tf_op jit(solution)/shard_map/ppermute | solution.py:447
  53.1 13.5 %collective-permute-start.4 = (bf16[88,256]{1,0:T(8,128)(2,1)S(1)}, bf16[88,256]{1,0:T(8,128)(2,1)S(1)}, u32[]{:S(2)}, u32[]{:S(2)}) collective-permute-start(bf16[88,256]{1,0:T(8,128)(2,1)S(1)} %slice.31), channel_id=1, source_target_pairs={{0,256},{32,288},{64,320},{96,352},{128,384},{160,416},{192,448},{... | collective-permute-start | bytes 135176 | tf_op jit(solution)/shard_map/ppermute | solution.py:447
  55.1 17.3 %collective-permute-start.2 = (bf16[176,256]{1,0:T(8,128)(2,1)S(1)}, bf16[176,256]{1,0:T(8,128)(2,1)S(1)}, u32[]{:S(2)}, u32[]{:S(2)}) collective-permute-start(bf16[176,256]{1,0:T(8,128)(2,1)S(1)} %get-tuple-element.50), channel_id=1, source_target_pairs={{0,384},{32,416},{64,448},{96,480},{128,0},{160,32},{192,64},{224,... | collective-permute-start | bytes 270344 | tf_op jit(solution)/shard_map/ppermute | solution.py:447
  58.7 13.7 %collective-permute-start.1 = (bf16[176,256]{1,0:T(8,128)(2,1)S(1)}, bf16[176,256]{1,0:T(8,128)(2,1)S(1)}, u32[]{:S(2)}, u32[]{:S(2)}) collective-permute-start(bf16[176,256]{1,0:T(8,128)(2,1)S(1)} %get-tuple-element.50), channel_id=1, source_target_pairs={{0,128},{32,160},{64,192},{96,224},{128,256},{160,288},{192,320},{... | collective-permute-start | bytes 270344 | tf_op jit(solution)/shard_map/ppermute | solution.py:447
  72.4 44.1 %copy-start.4 = (bf16[4,176,256]{2,1,0:T(8,128)(2,1)}, bf16[4,176,256]{2,1,0:T(8,128)(2,1)S(1)}, u32[]{:S(2)}) copy-start(bf16[4,176,256]{2,1,0:T(8,128)(2,1)S(1)} %pad_maximum_fusion.1.w0_ref) | copy-start | bytes 1081348
  72.4 43.7 %copy-start.9 = (bf16[2048,2]{0,1:T(2,128)(2,1)S(1)}, bf16[2048,2]{0,1:T(2,128)(2,1)}, u32[]{:S(2)}) copy-start(bf16[2048,2]{0,1:T(2,128)(2,1)} %param.24) | copy-start | bytes 24580
  72.4 43.7 %copy-start.10 = (bf16[2048,2]{0,1:T(2,128)(2,1)S(1)}, bf16[2048,2]{0,1:T(2,128)(2,1)}, u32[]{:S(2)}) copy-start(bf16[2048,2]{0,1:T(2,128)(2,1)} %param.23) | copy-start | bytes 24580
  72.5 44.1 %copy-start.1 = (bf16[16,72,512]{2,1,0:T(8,128)(2,1)}, bf16[16,72,512]{2,1,0:T(8,128)(2,1)S(1)}, u32[]{:S(2)}) copy-start(bf16[16,72,512]{2,1,0:T(8,128)(2,1)S(1)} %all-to-all-done.1) | copy-start | bytes 3538948
  72.5 18.9 %all-to-all-start.2 = ((bf16[16,64,512]{2,1,0:T(8,128)(2,1)}), bf16[16,64,512]{2,1,0:T(8,128)(2,1)S(1)}, u32[]{:S(2)}, u32[]{:S(2)}) async-start(bf16[16,64,512]{2,1,0:T(8,128)(2,1)} %get-tuple-element.34), calls=%async_computation.2 | async-start | bytes 2097152 | tf_op jit(solution)/shard_map/all_to_all | solution.py:24
  79.5 51.9 %collective-permute-start.5 = (bf16[4,4,72,512]{3,2,1,0:T(8,128)(2,1)S(1)}, bf16[4,4,72,512]{3,2,1,0:T(8,128)(2,1)}, u32[]{:S(2)}, u32[]{:S(2)}) collective-permute-start(bf16[4,4,72,512]{3,2,1,0:T(8,128)(2,1)S(1)} %bitcast.26), channel_id=1, source_target_pairs={{0,4},{4,0},{1,5},{5,1},{2,6},{6,2},{3,7},{7,3},{8,12},{12,8},{9,1... | collective-permute-start | bytes 3538952 | tf_op jit(solution)/shard_map/ppermute | solution.py:28
  91.4 40.1 %collective-permute-start.6 = (bf16[4,4,64,512]{3,2,1,0:T(8,128)(2,1)S(1)}, bf16[4,4,64,512]{3,2,1,0:T(8,128)(2,1)}, u32[]{:S(2)}, u32[]{:S(2)}) collective-permute-start(bf16[4,4,64,512]{3,2,1,0:T(8,128)(2,1)S(1)} %bitcast.28), channel_id=1, source_target_pairs={{0,4},{4,0},{1,5},{5,1},{2,6},{6,2},{3,7},{7,3},{8,12},{12,8},{9,1... | collective-permute-start | bytes 3145736 | tf_op jit(solution)/shard_map/ppermute | solution.py:28
  101.2 13.0 %collective-permute-start.10 = (bf16[2,176,256]{2,1,0:T(8,128)(2,1)S(1)}, bf16[2,176,256]{2,1,0:T(8,128)(2,1)S(1)}, u32[]{:S(2)}, u32[]{:S(2)}) collective-permute-start(bf16[2,176,256]{2,1,0:T(8,128)(2,1)S(1)} %get-tuple-element.47), channel_id=1, source_target_pairs={{0,64},{32,96},{64,128},{96,160},{128,192},{160,224},{192,256},{22... | collective-permute-start | bytes 540680 | tf_op jit(solution)/shard_map/ppermute | solution.py:447
  105.3 26.1 %collective-permute-start.8 = (bf16[4,176,256]{2,1,0:T(8,128)(2,1)S(1)}, bf16[4,176,256]{2,1,0:T(8,128)(2,1)S(1)}, u32[]{:S(2)}, u32[]{:S(2)}) collective-permute-start(bf16[4,176,256]{2,1,0:T(8,128)(2,1)S(1)} %pad_maximum_fusion.1.w0_ref), channel_id=1, source_target_pairs={{0,32},{32,64},{64,96},{96,128},{128,160},{160,192},{192,224},{224... | collective-permute-start | bytes 1081352 | tf_op jit(solution)/shard_map/ppermute | solution.py:447
  112.3 19.2 %collective-permute-start.7 = (bf16[4,176,256]{2,1,0:T(8,128)(2,1)S(1)}, bf16[4,176,256]{2,1,0:T(8,128)(2,1)}, u32[]{:S(2)}, u32[]{:S(2)}) collective-permute-start(bf16[4,176,256]{2,1,0:T(8,128)(2,1)S(1)} %pad_maximum_fusion.1.w0_ref), channel_id=1, source_target_pairs={{0,480},{32,0},{64,32},{96,64},{128,96},{160,128},{192,160},{224,1... | collective-permute-start | bytes 1081352 | tf_op jit(solution)/shard_map/ppermute | solution.py:447
  114.2 17.2 %collective-permute-start.9 = (bf16[2,176,256]{2,1,0:T(8,128)(2,1)}, bf16[2,176,256]{2,1,0:T(8,128)(2,1)}, u32[]{:S(2)}, u32[]{:S(2)}) collective-permute-start(bf16[2,176,256]{2,1,0:T(8,128)(2,1)} %get-tuple-element.48), channel_id=1, source_target_pairs={{0,448},{32,480},{64,0},{96,32},{128,64},{160,96},{192,128},{224,1... | collective-permute-start | bytes 540680 | tf_op jit(solution)/shard_map/ppermute | solution.py:447
  160.9 31.8 %all-to-all-start.4 = ((bf16[16,72,256]{2,1,0:T(8,128)(2,1)}), bf16[16,72,256]{2,1,0:T(8,128)(2,1)S(1)}, u32[]{:S(2)}, u32[]{:S(2)}) async-start(bf16[16,72,256]{2,1,0:T(8,128)(2,1)} %get-tuple-element.42), calls=%async_computation.4 | async-start | bytes 1179648 | tf_op jit(solution)/shard_map/all_to_all | solution.py:24
  165.0 12.0 %collective-permute-start.13 = (bf16[4,4,16,768]{3,2,1,0:T(8,128)(2,1)S(1)}, bf16[4,4,16,768]{3,2,1,0:T(8,128)(2,1)S(1)}, u32[]{:S(2)}, u32[]{:S(2)}) collective-permute-start(bf16[4,4,16,768]{3,2,1,0:T(8,128)(2,1)S(1)} %copy-done.6), channel_id=1, source_target_pairs={{0,8},{8,16},{16,24},{24,0},{1,9},{9,17},{17,25},{25,1},{2,10},{10... | collective-permute-start | bytes 1179656 | tf_op jit(solution)/shard_map/ppermute | solution.py:534
  167.2 17.1 %collective-permute-start.12 = (bf16[4,4,16,768]{3,2,1,0:T(8,128)(2,1)S(1)}, bf16[4,4,16,768]{3,2,1,0:T(8,128)(2,1)S(1)}, u32[]{:S(2)}, u32[]{:S(2)}) collective-permute-start(bf16[4,4,16,768]{3,2,1,0:T(8,128)(2,1)S(1)} %copy-done.6), channel_id=1, source_target_pairs={{0,16},{8,24},{16,0},{24,8},{1,17},{9,25},{17,1},{25,9},{2,18},{10... | collective-permute-start | bytes 1179656 | tf_op jit(solution)/shard_map/ppermute | solution.py:534
  170.9 18.1 %collective-permute-start.11 = (bf16[4,4,16,768]{3,2,1,0:T(8,128)(2,1)S(1)}, bf16[4,4,16,768]{3,2,1,0:T(8,128)(2,1)S(1)}, u32[]{:S(2)}, u32[]{:S(2)}) collective-permute-start(bf16[4,4,16,768]{3,2,1,0:T(8,128)(2,1)S(1)} %copy-done.6), channel_id=1, source_target_pairs={{0,24},{8,0},{16,8},{24,16},{1,25},{9,1},{17,9},{25,17},{2,26},{10... | collective-permute-start | bytes 1179656 | tf_op jit(solution)/shard_map/ppermute | solution.py:534
  189.2 19.2 %collective-permute-start.14 = (bf16[4,4,4,16,768]{4,3,2,1,0:T(8,128)(2,1)S(1)}, bf16[4,4,4,16,768]{4,3,2,1,0:T(8,128)(2,1)}, u32[]{:S(2)}, u32[]{:S(2)}) collective-permute-start(bf16[4,4,4,16,768]{4,3,2,1,0:T(8,128)(2,1)S(1)} %pad_maximum_fusion.own_ref), channel_id=1, source_target_pairs={{0,4},{4,0},{1,5},{5,1},{2,6},{6,2},{3,7},{7,3},{8,12},{12,8},{9,1... | collective-permute-start | bytes 4718600 | tf_op jit(solution)/shard_map/ppermute | solution.py:28
  201.1 23.6 %all-to-all-start.5 = ((bf16[32,128,128]{2,1,0:T(8,128)(2,1)}), bf16[32,128,128]{2,1,0:T(8,128)(2,1)S(1)}, u32[]{:S(2)}, u32[]{:S(2)}) async-start(bf16[32,128,128]{2,1,0:T(8,128)(2,1)} %bitcast.31), calls=%async_computation.5 | async-start | bytes 2097152 | tf_op jit(solution)/shard_map/all_to_all | solution.py:24
  (8 other events, 83.2 us)

commit v5 on v4

--- a/solution.py
+++ b/solution.py
@@ -67,8 +67,8 @@
     return high, mid, value - high - mid
 
 
-def pack_kernel(tokens_ref, offsets_ref, conv_gain_ref, memory_gain_ref, upper_ref, lower_ref):
-    length = tokens_ref.shape[0] // 2
+def pack_kernel(tokens_ref, offsets_ref, conv_gain_ref, memory_gain_ref, out_ref):
+    length = tokens_ref.shape[0]
     offsets = three_parts(offsets_ref[...])
     conv_gain = three_parts(conv_gain_ref[...])
     memory_gain = three_parts(memory_gain_ref[...])
@@ -77,29 +77,26 @@
     rows.append(jnp.concatenate(conv_gain[:2], axis=1))
     rows.append(jnp.concatenate([conv_gain[2], jnp.zeros_like(conv_gain[2])], axis=1))
     extra = jnp.concatenate(rows, axis=0).astype(BF16)
-    upper, lower = tokens_ref[:length], tokens_ref[length:]
-    for j in range(upper_ref.shape[0]):
-        upper_ref[j, :length] = upper
-        upper_ref[j, length:] = extra
-        lower_ref[j] = lower
+    tokens = tokens_ref[...]
+    for j in range(out_ref.shape[0]):
+        out_ref[j, :length] = tokens
+        out_ref[j, length:] = extra
 
 
 def piece_kernel(
     query_ref, key_ref, value_ref, left_ref, right_ref, memory_ref, conv_ref, out_ref, turn_ref
 ):
     nx, nc = out_ref.shape[0], out_ref.shape[1]
-    rows = turn_ref.shape[0]
-    width, chan = memory_ref.shape[0] // (nx * nc), conv_ref.shape[0] // (nx * nc)
+    rows = memory_ref.shape[0]
+    width, chan = memory_ref.shape[1] // (nx * nc), conv_ref.shape[1] // (nx * nc)
     parts = []
     for at in range(nx * nc):
-        parts.append(memory_ref[at * width : (at + 1) * width].astype(F32))
-        parts.append(conv_ref[at * chan : (at + 1) * chan].astype(F32))
-    whole = jnp.concatenate(parts, axis=0)
-    lanes = 128
-    for j in range(whole.shape[0] // lanes):
-        tile = whole[j * lanes : (j + 1) * lanes]
-        tile = jnp.concatenate([tile, jnp.zeros((lanes, lanes - rows), F32)], axis=1)
-        turn_ref[:, j * lanes : (j + 1) * lanes] = tile.T[:rows].astype(BF16)
+        parts.append(memory_ref[:, at * width : (at + 1) * width])
+        parts.append(conv_ref[:, at * chan : (at + 1) * chan])
+    whole = jnp.concatenate(parts, axis=1)
+    wide = out_ref.shape[3]
+    for j in range(whole.shape[1] // wide):
+        turn_ref[j * rows : (j + 1) * rows] = whole[:, j * wide : (j + 1) * wide]
     for x in range(nx):
         for c in range(nc):
             at = c * nx + x
@@ -111,77 +108,71 @@
 
 
 def project_kernel(
-    place_ref, own_a_ref, own_b_ref, other_a_ref, other_b_ref,
+    place_ref, own_ref, other_ref,
     w0_ref, w1_ref, w3_ref, low_ref, high_ref, gate_ref,
     qk_ref, v_ref, glu_ref, gates_ref, gain_ref, out_weight_ref,
 ):
-    nx, ny, _, part = own_a_ref.shape
+    nx, ny, _, part = own_ref.shape
     far, tall, wide = w0_ref.shape
     depth, chunks = out_weight_ref.shape[2], out_weight_ref.shape[3] // wide
     rows = tall - depth * chunks
     close = part // rows
-    members = far * close
     length = glu_ref.shape[1]
-    half_length = length // 2
     place, core, column = place_ref[0], place_ref[1], place_ref[2]
-    tokens_rows = nx * half_length
+    tokens_rows = nx * length
     width = qk_ref.shape[4] // 2
     chan = glu_ref.shape[2] // nx
-    lane = lax.broadcasted_iota(jnp.int32, (half_length, width), 1)
+    lane = lax.broadcasted_iota(jnp.int32, (length, width), 1)
     ones = jnp.where(lane == 0, 1.0, 0.0).astype(BF16)
     row = lax.broadcasted_iota(jnp.int32, (2 * nx, length), 0)
     gate_in = jnp.zeros((2 * nx, length), F32)
     forget = jnp.zeros((2 * nx, length), F32)
 
-    blocks = [(ref, i, ahead + close * (i - 1)) for ref, ahead in ((w0_ref, 0), (w1_ref, 1), (w3_ref, -1)) for i in range(far)]
-    blocks += [(low_ref, i, 2 + close * i) for i in range(far // 2)]
-    blocks += [(high_ref, i, -2 + close * (i - 1)) for i in range(far // 2)]
+    blocks = [
+        (ref, i, ahead, i)
+        for ref, ahead in ((w0_ref, 0), (w1_ref, 1), (w3_ref, close - 1))
+        for i in range(far)
+    ]
+    blocks += [(low_ref, i, 2, i) for i in range(far // 2)]
+    blocks += [(high_ref, i, 2, i + far // 2) for i in range(far // 2)]
     homes = []
-    for ref, i, ahead in blocks:
-        home = lax.rem(place + (ahead + members), members)
-        homes.append((lax.div(home, close), lax.rem(home, close)))
-        out_weight_ref[pl.ds(homes[-1][0], 1), pl.ds(homes[-1][1], 1)] = jnp.concatenate(
+    for ref, i, ahead, y in blocks:
+        homes.append((y, lax.rem(place + ahead, close)))
+        out_weight_ref[y, pl.ds(homes[-1][1], 1)] = jnp.concatenate(
             [ref[i, rows + j * depth : rows + (j + 1) * depth] for j in range(chunks)], axis=1
-        )[None, None]
-    packed = [[None, None], [None, None]]
-    for half, refs in enumerate(((own_a_ref, own_b_ref), (other_a_ref, other_b_ref))):
+        )[None]
+    for half, ref in enumerate((own_ref, other_ref)):
         home = core if half == 0 else 1 - core
-        for side, ref in enumerate(refs):
-            acc = jnp.zeros((tokens_rows, wide), F32)
-            pre = jnp.zeros((tokens_rows, gate_ref.shape[1]), F32)
-            for pair in range(0, len(blocks), 2):
-                left, right, gate_rows = [], [], []
-                for at in (pair, pair + 1):
-                    w_ref, i, _ = blocks[at]
-                    y, z = homes[at]
-                    start = pl.multiple_of(z * rows, rows)
-                    lanes = pl.ds(start, rows)
-                    left.append(ref[:, pl.ds(y, 1), :half_length, lanes].reshape(tokens_rows, rows))
-                    right.append(w_ref[i, :rows])
-                    gate_rows.append(gate_ref[pl.ds(y * part + start, rows)])
-                lhs = jnp.concatenate(left, axis=1)
-                acc = acc + dot(lhs, jnp.concatenate(right, axis=0), NN)
-                pre = pre + dot(lhs, jnp.concatenate(gate_rows, axis=0), NN)
-            glu = []
-            span = slice(side * half_length, (side + 1) * half_length)
-            for x in range(nx):
-                here = slice(x * half_length, (x + 1) * half_length)
-                mine = acc[here]
-                qk = mine[:, : 2 * width].astype(BF16)[None]
-                for j in range(qk_ref.shape[0]):
-                    qk_ref[j, x, pl.ds(home, 1), span] = qk
-                v_ref[x, pl.ds(home, 1), span] = jnp.concatenate(
-                    [mine[:, 2 * width : 3 * width].astype(BF16), ones], axis=1
-                )[None]
-                left = mine[:, 3 * width : 3 * width + chan]
-                right = mine[:, 3 * width + chan :]
-                glu.append(left / (1.0 + jnp.exp(-right)))
-            glu_ref[pl.ds(home, 1), span] = jnp.concatenate(glu, axis=1).astype(BF16)[None]
-            packed[half][side] = pre
+        acc = jnp.zeros((tokens_rows, wide), F32)
+        pre = jnp.zeros((tokens_rows, gate_ref.shape[1]), F32)
+        for pair in range(0, len(blocks), 2):
+            left, right, gate_rows = [], [], []
+            for at in (pair, pair + 1):
+                w_ref, i, _, _ = blocks[at]
+                y, z = homes[at]
+                start = pl.multiple_of(z * rows, rows)
+                left.append(ref[:, y, :length, pl.ds(start, rows)].reshape(tokens_rows, rows))
+                right.append(w_ref[i, :rows])
+                gate_rows.append(gate_ref[pl.ds(y * part + start, rows)])
+            lhs = jnp.concatenate(left, axis=1)
+            acc = acc + dot(lhs, jnp.concatenate(right, axis=0), NN)
+            pre = pre + dot(lhs, jnp.concatenate(gate_rows, axis=0), NN)
+        glu = []
         for x in range(nx):
-            here = slice(x * half_length, (x + 1) * half_length)
-            turned = jnp.concatenate([packed[half][0][here], packed[half][1][here]], axis=0).T
-            extra = refs[0][x, column, half_length : half_length + 8].astype(F32)
+            mine = acc[x * length : (x + 1) * length]
+            qk = mine[:, : 2 * width].astype(BF16)[None]
+            for j in range(qk_ref.shape[0]):
+                qk_ref[j, x, pl.ds(home, 1)] = qk
+            v_ref[x, pl.ds(home, 1)] = jnp.concatenate(
+                [mine[:, 2 * width : 3 * width].astype(BF16), ones], axis=1
+            )[None]
+            left = mine[:, 3 * width : 3 * width + chan]
+            right = mine[:, 3 * width + chan :]
+            glu.append(left / (1.0 + jnp.exp(-right)))
+        glu_ref[pl.ds(home, 1)] = jnp.concatenate(glu, axis=1).astype(BF16)[None]
+        for x in range(nx):
+            turned = pre[x * length : (x + 1) * length].T
+            extra = ref[x, column, length : length + 8].astype(F32)
             values = extra[0:1] + extra[1:2] + extra[2:3]
             offsets = jnp.where(core == 0, values[:, :length], values[:, length : 2 * length])
             offsets_f = jnp.where(
@@ -193,7 +184,7 @@
             gate_in = jnp.where(at, gate_pre + offsets, gate_in)
             forget = jnp.where(at, forget_pre + offsets_f, forget)
     for b in range(ny):
-        extra = own_a_ref[0, b, half_length : half_length + 8].astype(F32)
+        extra = own_ref[0, b, length : length + 8].astype(F32)
         memory_gain = extra[3:4] + extra[4:5] + extra[5:6]
         half = part // 2
         conv_gain = extra[6:7, :half] + extra[6:7, half:] + extra[7:8, :half]
@@ -451,7 +442,7 @@
         piece_kernel,
         out_shape=(
             jax.ShapeDtypeStruct((nx, nc, rows, wide), BF16),
-            jax.ShapeDtypeStruct((rows, deep), BF16),
+            jax.ShapeDtypeStruct((deep // wide * rows, wide), BF16),
         ),
         in_specs=vmem(7),
         out_specs=vmem(2),
@@ -463,8 +454,8 @@
         value_weight,
         conv_value_weight,
         conv_gate_weight,
-        memory_out_weight,
-        conv_out_weight,
+        memory_out_weight.T,
+        conv_out_weight.T,
     )
     turned = lax.ppermute(
         out_rows,
@@ -472,40 +463,22 @@
         [(a * ny + b, b * ny + a) for a in range(nzh) for b in range(ny)],
     )
     offsets = jnp.concatenate([input_offset.T, forget_offset.T], axis=0)
-    half = length // 2
-    upper, lower = pl.pallas_call(
+    sent = pl.pallas_call(
         pack_kernel,
-        out_shape=(
-            jax.ShapeDtypeStruct((nx * ny, half + 8, part), BF16),
-            jax.ShapeDtypeStruct((nx * ny, half, part), BF16),
-        ),
+        out_shape=jax.ShapeDtypeStruct((nx * ny, length + 8, part), BF16),
         in_specs=vmem(4),
-        out_specs=vmem(2),
+        out_specs=pl.BlockSpec(memory_space=pltpu.VMEM),
         interpret=INTERPRET,
         name="pack",
     )(tokens, offsets, conv_norm_gain[None], memory_norm_gain[None])
     mine = exchange(pieces.reshape(nx * nc, rows, wide), ("x", "c"))
     mine = mine.reshape(nx * nc * rows, wide)
-    upper, lower, mine = lax.optimization_barrier((upper, lower, mine))
-    own_a = exchange(upper, ("x", "tp"))
-    turned = jnp.concatenate([turned[:, j * wide : (j + 1) * wide] for j in range(deep // wide)], 0)
     mine = jnp.concatenate([mine, turned], axis=0)
-    step, cut = members // 4, mine.shape[0] // 2
-    far = [
-        from_z(mine, -step),
-        from_z(mine, step),
-        from_z(mine[:cut], 2 * step),
-        from_z(mine[cut:], -2 * step),
-    ]
-    near = jnp.stack([far[0], mine, far[1], jnp.concatenate(far[2:], axis=0)], axis=0)
-    near, lower, own_a = lax.optimization_barrier((near, lower, own_a))
-    own_b = exchange(lower, ("x", "tp"))
+    near = exchange(jnp.broadcast_to(mine, (nzh, *mine.shape)), "zh")
+    own = exchange(sent, ("x", "tp")).reshape(nx, ny, length + 8, part)
     sets = [near, from_z(near, 1), from_z(near, -1)]
-    sets += [from_z(near[1:3], 2), from_z(near[:2], -2)]
-    own_a = own_a.reshape(nx, ny, half + 8, part)
-    own_b = own_b.reshape(nx, ny, half, part)
-    others = [swapped(own_a, "c")]
-    others.append(swapped(own_b, "c"))
+    sets += [from_z(near[: nzh // 2], 2), from_z(near[nzh // 2 :], -2)]
+    other = swapped(own, "c")
 
     gate_weight = jnp.pad(
         jnp.concatenate([input_gate_weight, forget_gate_weight], axis=1), ((0, 0), (0, 124))
@@ -522,11 +495,11 @@
             jax.ShapeDtypeStruct((ny, nc * nx, 2 * width), F32),
             jax.ShapeDtypeStruct((nzh, nzl, rows, deep), BF16),
         ),
-        in_specs=[smem] + vmem(10),
+        in_specs=[smem] + vmem(8),
         out_specs=vmem(6),
         interpret=INTERPRET,
         name="project",
-    )(place, own_a, own_b, *others, *sets, gate_weight)
+    )(place, own, other, *sets, gate_weight)
     value = value.reshape(slab, 2 * width)
     all_qk = exchange(qk.reshape(nx, slab, 2 * width), "x")
     out_part, all_qk = lax.optimization_barrier((out_part, all_qk))

time: 233 us -> 227 us (0.974)
  blocking collectives: 18.3 us -> 95.3 us
  starting transfers between devices: 117 us -> 53.1 us
  waiting for transfers between devices: 58.2 us -> 42.9 us
  local copies, waits for them, and re-layouts: 7.37 us -> 4.53 us
    all_to_all x1 -> x3, blocking collectives: 18.3 us -> 95.3 us  [exchange(): return lax.all_to_all(pieces, axes, split_axis=0, concat_axis=0, tiled=True)]
    ppermute x8 -> x4, starting transfers between devices: 54.9 us -> 19.8 us  [from_z(): lax.ppermute(value, Z, [(j, (j - ahead) % members) for j in range(members)])]
    all_to_all x5 -> x3, starting transfers between devices: 32.3 us -> 14 us  [exchange(): return lax.all_to_all(pieces, axes, split_axis=0, concat_axis=0, tiled=True)]
    ppermute x8 -> x4, waiting for transfers between devices: 21.4 us -> 7.57 us  [from_z(): lax.ppermute(value, Z, [(j, (j - ahead) % members) for j in range(members)])]
    ppermute x3 -> x2, starting transfers between devices: 20.7 us -> 9.49 us  [swapped(): return lax.ppermute(value, axis, [(0, 1), (1, 0)])]
    unnamed x26 -> x18, local copies, waits for them, and re-layouts: 5.44 us -> 2.52 us
    all_to_all x5 -> x3, waiting for transfers between devices: 21.2 us -> 19.8 us  [exchange(): return lax.all_to_all(pieces, axes, split_axis=0, concat_axis=0, tiled=True)]
  transfers between devices with their start and end apart: 20 -> 13, of which waited for: 9 -> 7; matrix products, arithmetic and copies ran while one was open for 2% -> 1% of each run, Pallas kernels for 4% -> 4%
where the time goes in v5:
time: 227 us; the launch traced here: 225 us
  blocking collectives  95.3 us (42%)
  starting transfers between devices  53.1 us (23%)
  waiting for transfers between devices  42.9 us (19%)
  Pallas kernels  27.2 us (12%)
  local copies, waits for them, and re-layouts  4.53 us (2%)
    all_to_all x3, blocking collectives, exchange(): return lax.all_to_all(pieces, axes, split_axis=0, concat_axis=0, tiled=True)  95.3 us
    ppermute x4, starting transfers between devices, from_z(): lax.ppermute(value, Z, [(j, (j - ahead) % members) for j in range(members)])  19.8 us
    all_to_all x3, waiting for transfers between devices, exchange(): return lax.all_to_all(pieces, axes, split_axis=0, concat_axis=0, tiled=True)  19.8 us
    ppermute x3, waiting for transfers between devices, layer(): lax.ppermute(out_part, 'x', [(j, (j - ahead) % nx) for j in range(nx)])  15.6 us
    all_to_all x3, starting transfers between devices, exchange(): return lax.all_to_all(pieces, axes, split_axis=0, concat_axis=0, tiled=True)  14 us
    ppermute x2, starting transfers between devices, swapped(): return lax.ppermute(value, axis, [(0, 1), (1, 0)])  9.49 us
    ppermute x3, starting transfers between devices, layer(): lax.ppermute(out_part, 'x', [(j, (j - ahead) % nx) for j in range(nx)])  8.46 us
    ppermute x4, waiting for transfers between devices, from_z(): lax.ppermute(value, Z, [(j, (j - ahead) % members) for j in range(members)])  7.57 us
  transfers between devices with their start and end apart: 13, of which 7 were waited for; matrix products, arithmetic and copies ran while one was open for 1% of the time, Pallas kernels for 4%

profile of v5, /device:TPU:1, one launch (start us, length us, event | category | flops | bytes accessed | tf_op | source)
XLA Modules:
  0.0 225.4 jit_solution(11031146621524273345)
XLA Ops:
  1.3 2.5 %pack.1 = bf16[16,136,512]{2,1,0:T(8,128)(2,1)} custom-call(bf16[128,512]{1,0:T(8,128)(2,1)} %tokens_ref.1, f32[4,128]{1,0:T(4,128)} %pad_maximum_fusion.3.offsets_ref, f32[1,256]{1,0:T(1,128)} %bitcast.37, f32[1,512]{1,0:T(1,128)} %bitcast.36), custom_call_target="tpu_custom_call" | custom-call | tf_op jit(solution)/shard_map/pack/pallas_call | solution.py:466
  3.7 34.1 %all_to_all.30 = bf16[16,136,512]{2,1,0:T(8,128)(2,1)S(1)} all-to-all(bf16[16,136,512]{2,1,0:T(8,128)(2,1)} %pack.1), channel_id=1, replica_groups=mesh['zh'=4,'zl'=4,'x'=4,'c'=2,'tp'=4] {'x','tp'}, dimensions={0} | all-to-all | bytes 4456448 | tf_op jit(solution)/shard_map/all_to_all | solution.py:24
  37.9 6.0 %collective-permute-start = (bf16[4,4,136,512]{3,2,1,0:T(8,128)(2,1)S(1)}, bf16[4,4,136,512]{3,2,1,0:T(8,128)(2,1)}, u32[]{:S(2)}, u32[]{:S(2)}) collective-permute-start(bf16[4,4,136,512]{3,2,1,0:T(8,128)(2,1)S(1)} %bitcast.21), channel_id=1, source_target_pairs={{0,4},{4,0},{1,5},{5,1},{2,6},{6,2},{3,7},{7,3},{8,12},{12,8},{9,1... | collective-permute-start | bytes 6684680 | tf_op jit(solution)/shard_map/ppermute | solution.py:28
  45.4 3.3 %all-to-all-start.1 = ((bf16[8,16,256]{2,1,0:T(8,128)(2,1)}), bf16[8,16,256]{2,1,0:T(8,128)(2,1)S(1)}, u32[]{:S(2)}, u32[]{:S(2)}) async-start(bf16[8,16,256]{2,1,0:T(8,128)(2,1)} %bitcast.33), calls=%async_computation.1 | async-start | bytes 131072 | tf_op jit(solution)/shard_map/all_to_all | solution.py:24
  50.2 3.4 %all-to-all-done.1 = bf16[8,16,256]{2,1,0:T(8,128)(2,1)S(1)} async-done(((bf16[8,16,256]{2,1,0:T(8,128)(2,1)}), bf16[8,16,256]{2,1,0:T(8,128)(2,1)S(1)}, u32[]{:S(2)}, u32[]{:S(2)}) %all-to-all-start.1) | async-done | bytes 65568 | tf_op jit(solution)/shard_map/all_to_all | solution.py:24
  53.6 43.2 %all_to_all.31.w0_ref = bf16[4,176,256]{2,1,0:T(8,128)(2,1)S(1)} all-to-all(bf16[4,176,256]{2,1,0:T(8,128)(2,1)S(1)} %broadcast_in_dim.11), channel_id=1, replica_groups=mesh['zh'=4,'zl'=4,'x'=4,'c'=2,'tp'=4] {'zh'}, dimensions={0} | all-to-all | bytes 720896 | tf_op jit(solution)/shard_map/all_to_all | solution.py:24
  96.8 10.5 %collective-permute-start.3 = (bf16[4,176,256]{2,1,0:T(8,128)(2,1)S(1)}, bf16[4,176,256]{2,1,0:T(8,128)(2,1)S(1)}, u32[]{:S(2)}, u32[]{:S(2)}) collective-permute-start(bf16[4,176,256]{2,1,0:T(8,128)(2,1)S(1)} %all_to_all.31.w0_ref), channel_id=1, source_target_pairs={{0,32},{32,64},{64,96},{96,128},{128,160},{160,192},{192,224},{224... | collective-permute-start | bytes 1081352 | tf_op jit(solution)/shard_map/ppermute | solution.py:438
  110.0 3.8 %collective-permute-start.5 = (bf16[2,176,256]{2,1,0:T(8,128)(2,1)}, bf16[2,176,256]{2,1,0:T(8,128)(2,1)}, u32[]{:S(2)}, u32[]{:S(2)}) collective-permute-start(bf16[2,176,256]{2,1,0:T(8,128)(2,1)} %get-tuple-element.31), channel_id=1, source_target_pairs={{0,64},{32,96},{64,128},{96,160},{128,192},{160,224},{192,256},{22... | collective-permute-start | bytes 540680 | tf_op jit(solution)/shard_map/ppermute | solution.py:438
  113.8 3.5 %collective-permute-start.4 = (bf16[2,176,256]{2,1,0:T(8,128)(2,1)}, bf16[2,176,256]{2,1,0:T(8,128)(2,1)}, u32[]{:S(2)}, u32[]{:S(2)}) collective-permute-start(bf16[2,176,256]{2,1,0:T(8,128)(2,1)} %get-tuple-element.32), channel_id=1, source_target_pairs={{0,448},{32,480},{64,0},{96,32},{128,64},{160,96},{192,128},{224,1... | collective-permute-start | bytes 540680 | tf_op jit(solution)/shard_map/ppermute | solution.py:438
  119.4 7.4 %collective-permute-done.4.low_ref = bf16[2,176,256]{2,1,0:T(8,128)(2,1)} collective-permute-done((bf16[2,176,256]{2,1,0:T(8,128)(2,1)}, bf16[2,176,256]{2,1,0:T(8,128)(2,1)}, u32[]{:S(2)}, u32[]{:S(2)}) %collective-permute-start.4) | collective-permute-done | bytes 180256 | tf_op jit(solution)/shard_map/ppermute | solution.py:438
  127.6 6.4 %project.1 = (bf16[4,4,2,128,128]{4,3,2,1,0:T(8,128)(2,1)}, bf16[4,2,128,128]{3,2,1,0:T(8,128)(2,1)}, bf16[2,128,128]{2,1,0:T(8,128)(2,1)}, f32[2,8,128]{2,1,0:T...) custom-call(s32[4]{0:T(128)} %pad_add_fusion.place_ref, bf16[4,4,136,512]{3,2,1,0:T(8,128)(2,1)} %bitcast.22, ...), custom_call_target="tpu_custom_call" | custom-call | tf_op jit(solution)/shard_map/project/pallas_call | solution.py:488
  134.0 18.0 %all_to_all.32.qk_ref = bf16[4,1024,128]{2,1,0:T(8,128)(2,1)} all-to-all(bf16[4,1024,128]{2,1,0:T(8,128)(2,1)} %bitcast.25), channel_id=1, replica_groups=mesh['zh'=4,'zl'=4,'x'=4,'c'=2,'tp'=4] {'x'}, dimensions={0} | all-to-all | bytes 2097152 | tf_op jit(solution)/shard_map/all_to_all | solution.py:24
  152.0 3.8 %slab_state.1 = (bf16[16,72,256]{2,1,0:T(8,128)(2,1)}, bf16[1024,256]{1,0:T(8,128)(2,1)}, bf16[1024,256]{1,0:T(8,128)(2,1)}) custom-call(bf16[4,1024,128]{2,1,0:T(8,128)(2,1)} %all_to_all.32.qk_ref, bf16[1024,128]{1,0:T(8,128)(2,1)} %bitcast.26, f32[2,8,128]{2,1,0:T(8,128)} %get-tuple-element.24.gate_ref, bf16[2,128,128]{2,1,0:T(8,128)(2,1)} %get-tuple-element.25.glu_ref), custom_call_target="tpu_custom_call" | custom-call | tf_op jit(solution)/shard_map/slab_state/pallas_call | solution.py:514
  155.8 3.6 %all-to-all-start.4 = ((bf16[16,72,256]{2,1,0:T(8,128)(2,1)}), bf16[16,72,256]{2,1,0:T(8,128)(2,1)S(1)}, u32[]{:S(2)}, u32[]{:S(2)}) async-start(bf16[16,72,256]{2,1,0:T(8,128)(2,1)} %get-tuple-element.26), calls=%async_computation.4 | async-start | bytes 1179648 | tf_op jit(solution)/shard_map/all_to_all | solution.py:24
  161.6 3.6 %collective-permute-start.7 = (bf16[4,4,16,768]{3,2,1,0:T(8,128)(2,1)S(1)}, bf16[4,4,16,768]{3,2,1,0:T(8,128)(2,1)S(1)}, u32[]{:S(2)}, u32[]{:S(2)}) collective-permute-start(bf16[4,4,16,768]{3,2,1,0:T(8,128)(2,1)S(1)} %copy-done.5), channel_id=1, source_target_pairs={{0,16},{8,24},{16,0},{24,8},{1,17},{9,25},{17,1},{25,9},{2,18},{10... | collective-permute-start | bytes 1179656 | tf_op jit(solution)/shard_map/ppermute | solution.py:507
  165.3 2.6 %collective-permute-start.6 = (bf16[4,4,16,768]{3,2,1,0:T(8,128)(2,1)S(1)}, bf16[4,4,16,768]{3,2,1,0:T(8,128)(2,1)S(1)}, u32[]{:S(2)}, u32[]{:S(2)}) collective-permute-start(bf16[4,4,16,768]{3,2,1,0:T(8,128)(2,1)S(1)} %copy-done.5), channel_id=1, source_target_pairs={{0,24},{8,0},{16,8},{24,16},{1,25},{9,1},{17,9},{25,17},{2,26},{10... | collective-permute-start | bytes 1179656 | tf_op jit(solution)/shard_map/ppermute | solution.py:507
  167.9 3.3 %collective-permute-done.8 = bf16[4,4,16,768]{3,2,1,0:T(8,128)(2,1)S(1)} collective-permute-done((bf16[4,4,16,768]{3,2,1,0:T(8,128)(2,1)S(1)}, bf16[4,4,16,768]{3,2,1,0:T(8,128)(2,1)S(1)}, u32[]{:S(2)}, u32[]{:S(2)}) %collective-permute-start.8) | collective-permute-done | bytes 393248 | tf_op jit(solution)/shard_map/ppermute | solution.py:507
  171.1 7.3 %collective-permute-done.7 = bf16[4,4,16,768]{3,2,1,0:T(8,128)(2,1)S(1)} collective-permute-done((bf16[4,4,16,768]{3,2,1,0:T(8,128)(2,1)S(1)}, bf16[4,4,16,768]{3,2,1,0:T(8,128)(2,1)S(1)}, u32[]{:S(2)}, u32[]{:S(2)}) %collective-permute-start.7) | collective-permute-done | bytes 393248 | tf_op jit(solution)/shard_map/ppermute | solution.py:507
  178.4 5.0 %collective-permute-done.6 = bf16[4,4,16,768]{3,2,1,0:T(8,128)(2,1)S(1)} collective-permute-done((bf16[4,4,16,768]{3,2,1,0:T(8,128)(2,1)S(1)}, bf16[4,4,16,768]{3,2,1,0:T(8,128)(2,1)S(1)}, u32[]{:S(2)}, u32[]{:S(2)}) %collective-permute-start.6) | collective-permute-done | bytes 393248 | tf_op jit(solution)/shard_map/ppermute | solution.py:507
  183.6 3.5 %collective-permute-start.9 = (bf16[4,4,4,16,768]{4,3,2,1,0:T(8,128)(2,1)S(1)}, bf16[4,4,4,16,768]{4,3,2,1,0:T(8,128)(2,1)}, u32[]{:S(2)}, u32[]{:S(2)}) collective-permute-start(bf16[4,4,4,16,768]{4,3,2,1,0:T(8,128)(2,1)S(1)} %pad_maximum_fusion.own_ref), channel_id=1, source_target_pairs={{0,4},{4,0},{1,5},{5,1},{2,6},{6,2},{3,7},{7,3},{8,12},{12,8},{9,1... | collective-permute-start | bytes 4718600 | tf_op jit(solution)/shard_map/ppermute | solution.py:28
  188.0 7.5 %cell.1 = bf16[4,2,4,128,128]{4,3,2,1,0:T(8,128)(2,1)} custom-call(s32[4]{0:T(128)} %pad_add_fusion.place_ref, bf16[16,72,256]{2,1,0:T(8,128)(2,1)} %copy-done.4, bf16[1024,256]{1,0:T(8,128)(2,1)} %get-tuple-element.27.q_ref, bf16[1024,256]{1,0:T(8,128)(2,1)} %get-tuple-element.28.k_ref, bf16[1024,128]{1,0:T(8,128)(2,1)} %bitcast.27, ...), custom_call_target="tpu_custom_call" | custom-call | tf_op jit(solution)/shard_map/cell/pallas_call | solution.py:527
  195.5 7.1 %all-to-all-start.5 = ((bf16[32,128,128]{2,1,0:T(8,128)(2,1)}), bf16[32,128,128]{2,1,0:T(8,128)(2,1)S(1)}, u32[]{:S(2)}, u32[]{:S(2)}) async-start(bf16[32,128,128]{2,1,0:T(8,128)(2,1)} %bitcast.24), calls=%async_computation.5 | async-start | bytes 2097152 | tf_op jit(solution)/shard_map/all_to_all | solution.py:24
  202.6 16.3 %all-to-all-done.5 = bf16[32,128,128]{2,1,0:T(8,128)(2,1)S(1)} async-done(((bf16[32,128,128]{2,1,0:T(8,128)(2,1)}), bf16[32,128,128]{2,1,0:T(8,128)(2,1)S(1)}, u32[]{:S(2)}, u32[]{:S(2)}) %all-to-all-start.5) | async-done | bytes 1048608 | tf_op jit(solution)/shard_map/all_to_all | solution.py:24
  219.9 5.5 %finish.1 = bf16[128,512]{1,0:T(8,128)(2,1)} custom-call(s32[4]{0:T(128)} %pad_add_fusion.place_ref, bf16[4,2,4,128,128]{4,3,2,1,0:T(8,128)(2,1)} %bitcast.23, bf16[4,4,4,16,768]{4,3,2,1,0:T(8,128)(2,1)} %copy-done.1, bf16[4,4,4,16,768]{4,3,2,1,0:T(8,128)(2,1)} %collective-permute-done.9.other_ref, f32[4,8,128]{2,1,0:T(8,128)} %get-tuple-element.30.gain_ref), custom_call_target="tpu_custom_call" | custom-call | tf_op jit(solution)/shard_map/finish/pallas_call | solution.py:537
  (38 shorter events, 13.9 us)
Async XLA Ops:
  37.9 80.8 %copy-start = (bf16[16,136,512]{2,1,0:T(8,128)(2,1)}, bf16[16,136,512]{2,1,0:T(8,128)(2,1)S(1)}, u32[]{:S(2)}) copy-start(bf16[16,136,512]{2,1,0:T(8,128)(2,1)S(1)} %all_to_all.30) | copy-start | bytes 6684676
  37.9 79.5 %copy-start.7 = (bf16[2048,2]{0,1:T(2,128)(2,1)S(1)}, bf16[2048,2]{0,1:T(2,128)(2,1)}, u32[]{:S(2)}) copy-start(bf16[2048,2]{0,1:T(2,128)(2,1)} %param.24) | copy-start | bytes 24580
  37.9 79.5 %copy-start.8 = (bf16[2048,2]{0,1:T(2,128)(2,1)S(1)}, bf16[2048,2]{0,1:T(2,128)(2,1)}, u32[]{:S(2)}) copy-start(bf16[2048,2]{0,1:T(2,128)(2,1)} %param.23) | copy-start | bytes 24580
  37.9 88.9 %collective-permute-start = (bf16[4,4,136,512]{3,2,1,0:T(8,128)(2,1)S(1)}, bf16[4,4,136,512]{3,2,1,0:T(8,128)(2,1)}, u32[]{:S(2)}, u32[]{:S(2)}) collective-permute-start(bf16[4,4,136,512]{3,2,1,0:T(8,128)(2,1)S(1)} %bitcast.21), channel_id=1, source_target_pairs={{0,4},{4,0},{1,5},{5,1},{2,6},{6,2},{3,7},{7,3},{8,12},{12,8},{9,1... | collective-permute-start | bytes 6684680 | tf_op jit(solution)/shard_map/ppermute | solution.py:28
  45.4 8.1 %all-to-all-start.1 = ((bf16[8,16,256]{2,1,0:T(8,128)(2,1)}), bf16[8,16,256]{2,1,0:T(8,128)(2,1)S(1)}, u32[]{:S(2)}, u32[]{:S(2)}) async-start(bf16[8,16,256]{2,1,0:T(8,128)(2,1)} %bitcast.33), calls=%async_computation.1 | async-start | bytes 131072 | tf_op jit(solution)/shard_map/all_to_all | solution.py:24
  48.8 1.4 collective-permute-start.1
  96.8 30.1 %copy-start.3 = (bf16[4,176,256]{2,1,0:T(8,128)(2,1)}, bf16[4,176,256]{2,1,0:T(8,128)(2,1)S(1)}, u32[]{:S(2)}) copy-start(bf16[4,176,256]{2,1,0:T(8,128)(2,1)S(1)} %all_to_all.31.w0_ref) | copy-start | bytes 1081348
  96.8 30.0 %collective-permute-start.3 = (bf16[4,176,256]{2,1,0:T(8,128)(2,1)S(1)}, bf16[4,176,256]{2,1,0:T(8,128)(2,1)S(1)}, u32[]{:S(2)}, u32[]{:S(2)}) collective-permute-start(bf16[4,176,256]{2,1,0:T(8,128)(2,1)S(1)} %all_to_all.31.w0_ref), channel_id=1, source_target_pairs={{0,32},{32,64},{64,96},{96,128},{128,160},{160,192},{192,224},{224... | collective-permute-start | bytes 1081352 | tf_op jit(solution)/shard_map/ppermute | solution.py:438
  107.3 19.5 %collective-permute-start.2 = (bf16[4,176,256]{2,1,0:T(8,128)(2,1)S(1)}, bf16[4,176,256]{2,1,0:T(8,128)(2,1)}, u32[]{:S(2)}, u32[]{:S(2)}) collective-permute-start(bf16[4,176,256]{2,1,0:T(8,128)(2,1)S(1)} %all_to_all.31.w0_ref), channel_id=1, source_target_pairs={{0,480},{32,0},{64,32},{96,64},{128,96},{160,128},{192,160},{224,1... | collective-permute-start | bytes 1081352 | tf_op jit(solution)/shard_map/ppermute | solution.py:438
  110.0 9.4 %collective-permute-start.5 = (bf16[2,176,256]{2,1,0:T(8,128)(2,1)}, bf16[2,176,256]{2,1,0:T(8,128)(2,1)}, u32[]{:S(2)}, u32[]{:S(2)}) collective-permute-start(bf16[2,176,256]{2,1,0:T(8,128)(2,1)} %get-tuple-element.31), channel_id=1, source_target_pairs={{0,64},{32,96},{64,128},{96,160},{128,192},{160,224},{192,256},{22... | collective-permute-start | bytes 540680 | tf_op jit(solution)/shard_map/ppermute | solution.py:438
  113.8 13.0 %collective-permute-start.4 = (bf16[2,176,256]{2,1,0:T(8,128)(2,1)}, bf16[2,176,256]{2,1,0:T(8,128)(2,1)}, u32[]{:S(2)}, u32[]{:S(2)}) collective-permute-start(bf16[2,176,256]{2,1,0:T(8,128)(2,1)} %get-tuple-element.32), channel_id=1, source_target_pairs={{0,448},{32,480},{64,0},{96,32},{128,64},{160,96},{192,128},{224,1... | collective-permute-start | bytes 540680 | tf_op jit(solution)/shard_map/ppermute | solution.py:438
  126.8 0.7 copy-start.6
  152.0 7.4 %copy-start.5 = (bf16[4,4,16,768]{3,2,1,0:T(8,128)(2,1)S(1)}, bf16[4,4,16,768]{3,2,1,0:T(8,128)(2,1)}, u32[]{:S(2)}) copy-start(bf16[4,4,16,768]{3,2,1,0:T(8,128)(2,1)} %get-tuple-element.29) | copy-start | bytes 1179652
  155.8 31.3 %all-to-all-start.4 = ((bf16[16,72,256]{2,1,0:T(8,128)(2,1)}), bf16[16,72,256]{2,1,0:T(8,128)(2,1)S(1)}, u32[]{:S(2)}, u32[]{:S(2)}) async-start(bf16[16,72,256]{2,1,0:T(8,128)(2,1)} %get-tuple-element.26), calls=%async_computation.4 | async-start | bytes 1179648 | tf_op jit(solution)/shard_map/all_to_all | solution.py:24
  159.4 11.7 %collective-permute-start.8 = (bf16[4,4,16,768]{3,2,1,0:T(8,128)(2,1)S(1)}, bf16[4,4,16,768]{3,2,1,0:T(8,128)(2,1)S(1)}, u32[]{:S(2)}, u32[]{:S(2)}) collective-permute-start(bf16[4,4,16,768]{3,2,1,0:T(8,128)(2,1)S(1)} %copy-done.5), channel_id=1, source_target_pairs={{0,8},{8,16},{16,24},{24,0},{1,9},{9,17},{17,25},{25,1},{2,10},{10... | collective-permute-start | bytes 1179656 | tf_op jit(solution)/shard_map/ppermute | solution.py:507
  161.6 16.8 %collective-permute-start.7 = (bf16[4,4,16,768]{3,2,1,0:T(8,128)(2,1)S(1)}, bf16[4,4,16,768]{3,2,1,0:T(8,128)(2,1)S(1)}, u32[]{:S(2)}, u32[]{:S(2)}) collective-permute-start(bf16[4,4,16,768]{3,2,1,0:T(8,128)(2,1)S(1)} %copy-done.5), channel_id=1, source_target_pairs={{0,16},{8,24},{16,0},{24,8},{1,17},{9,25},{17,1},{25,9},{2,18},{10... | collective-permute-start | bytes 1179656 | tf_op jit(solution)/shard_map/ppermute | solution.py:507
  165.3 18.1 %collective-permute-start.6 = (bf16[4,4,16,768]{3,2,1,0:T(8,128)(2,1)S(1)}, bf16[4,4,16,768]{3,2,1,0:T(8,128)(2,1)S(1)}, u32[]{:S(2)}, u32[]{:S(2)}) collective-permute-start(bf16[4,4,16,768]{3,2,1,0:T(8,128)(2,1)S(1)} %copy-done.5), channel_id=1, source_target_pairs={{0,24},{8,0},{16,8},{24,16},{1,25},{9,1},{17,9},{25,17},{2,26},{10... | collective-permute-start | bytes 1179656 | tf_op jit(solution)/shard_map/ppermute | solution.py:507
  183.6 11.9 %copy-start.1 = (bf16[4,4,4,16,768]{4,3,2,1,0:T(8,128)(2,1)}, bf16[4,4,4,16,768]{4,3,2,1,0:T(8,128)(2,1)S(1)}, u32[]{:S(2)}) copy-start(bf16[4,4,4,16,768]{4,3,2,1,0:T(8,128)(2,1)S(1)} %pad_maximum_fusion.own_ref) | copy-start | bytes 4718596
  183.6 19.0 %collective-permute-start.9 = (bf16[4,4,4,16,768]{4,3,2,1,0:T(8,128)(2,1)S(1)}, bf16[4,4,4,16,768]{4,3,2,1,0:T(8,128)(2,1)}, u32[]{:S(2)}, u32[]{:S(2)}) collective-permute-start(bf16[4,4,4,16,768]{4,3,2,1,0:T(8,128)(2,1)S(1)} %pad_maximum_fusion.own_ref), channel_id=1, source_target_pairs={{0,4},{4,0},{1,5},{5,1},{2,6},{6,2},{3,7},{7,3},{8,12},{12,8},{9,1... | collective-permute-start | bytes 4718600 | tf_op jit(solution)/shard_map/ppermute | solution.py:28
  187.1 0.8 copy-start.4
  195.5 23.4 %all-to-all-start.5 = ((bf16[32,128,128]{2,1,0:T(8,128)(2,1)}), bf16[32,128,128]{2,1,0:T(8,128)(2,1)S(1)}, u32[]{:S(2)}, u32[]{:S(2)}) async-start(bf16[32,128,128]{2,1,0:T(8,128)(2,1)} %bitcast.24), calls=%async_computation.5 | async-start | bytes 2097152 | tf_op jit(solution)/shard_map/all_to_all | solution.py:24
  219.0 1.0 copy-start.2

commit v6 on v5

--- a/solution.py
+++ b/solution.py
@@ -107,6 +107,13 @@
             out_ref[x, c] = jnp.concatenate(parts, axis=1)
 
 
+def arrange_kernel(in_ref, near_ref, low_ref, high_ref):
+    half = low_ref.shape[0]
+    near_ref[...] = in_ref[...]
+    low_ref[...] = in_ref[:half]
+    high_ref[...] = in_ref[half:]
+
+
 def project_kernel(
     place_ref, own_ref, other_ref,
     w0_ref, w1_ref, w3_ref, low_ref, high_ref, gate_ref,
@@ -138,9 +145,10 @@
     homes = []
     for ref, i, ahead, y in blocks:
         homes.append((y, lax.rem(place + ahead, close)))
-        out_weight_ref[y, pl.ds(homes[-1][1], 1)] = jnp.concatenate(
+        behind = lax.rem(y + ny - column, ny)
+        out_weight_ref[pl.ds(behind, 1), pl.ds(homes[-1][1], 1)] = jnp.concatenate(
             [ref[i, rows + j * depth : rows + (j + 1) * depth] for j in range(chunks)], axis=1
-        )[None]
+        )[None, None]
     for half, ref in enumerate((own_ref, other_ref)):
         home = core if half == 0 else 1 - core
         acc = jnp.zeros((tokens_rows, wide), F32)
@@ -204,33 +212,31 @@
 
 
 def finish_kernel(place_ref, arrived_ref, own_ref, other_ref, gain_ref, out_ref, weight_ref):
-    nx, nc, ny, length, lanes = arrived_ref.shape
+    nx, nc, ny, _, lanes = arrived_ref.shape
     core, x_at = place_ref[1], place_ref[3]
     width = lanes // 2
     chan = width // 2
-    part = out_ref.shape[1]
-    lane = lax.broadcasted_iota(jnp.int32, (length, lanes), 1)
+    length, part = out_ref.shape
+    lane = lax.broadcasted_iota(jnp.int32, (length, width + chan), 1)
     is_memory = lane < width
-    is_conv = (lane >= width) & (lane < width + chan)
+    half = length // 2
 
     def block(x, c, b):
         got = arrived_ref[x, c, b].astype(F32)
-        both = got + pltpu.roll(got, lanes - chan, 1)
-        return jnp.where(is_memory, got, jnp.where(is_conv, both, 0.0))
-
-    first = jnp.zeros((length, lanes), F32)
-    second = jnp.zeros((length, lanes), F32)
-    for x in range(nx):
-        for c in range(nc):
-            for b in range(ny):
-                got = block(x, c, b)
-                first = first + got
-                second = second + got * got
+        memory = jnp.concatenate([got[:half, :width], got[:half, width:]], axis=0)
+        conv = [got[half:, k * chan : (k + 1) * chan] for k in range(4)]
+        return jnp.concatenate([memory, jnp.concatenate(conv, axis=0)], axis=1)
+
+    blocks = {
+        (x, c, b): block(x, c, b) for x in range(nx) for c in range(nc) for b in range(ny)
+    }
+    first = sum(blocks.values())
+    second = sum(got * got for got in blocks.values())
     senders = nx * nc * ny
     memory_mean = jnp.sum(jnp.where(is_memory, second, 0.0), axis=1, keepdims=True)
     scale = lax.rsqrt(memory_mean / (senders * width) + EPS)
-    mean = jnp.sum(jnp.where(is_conv, first, 0.0), axis=1, keepdims=True) / (senders * chan)
-    power = jnp.sum(jnp.where(is_conv, second, 0.0), axis=1, keepdims=True) / (senders * chan)
+    mean = jnp.sum(jnp.where(is_memory, 0.0, first), axis=1, keepdims=True) / (senders * chan)
+    power = jnp.sum(jnp.where(is_memory, 0.0, second), axis=1, keepdims=True) / (senders * chan)
     spread = lax.rsqrt(power - mean * mean + EPS)
     shift = jnp.where(is_memory, 0.0, mean)
     factor = jnp.where(is_memory, scale, spread)
@@ -240,17 +246,19 @@
         for c, ref in ((core, own_ref), (1 - core, other_ref)):
             for b in range(ny):
                 for near in range(ref.shape[2]):
-                    weight_ref[b, near, pl.ds(x, 1), pl.ds(c, 1)] = ref[ahead, b, near][None, None]
+                    at = lax.rem(place_ref[2] + ny - b, ny)
+                    weight_ref[pl.ds(at, 1), near, pl.ds(x, 1), pl.ds(c, 1)] = ref[ahead, b, near][
+                        None, None, None
+                    ]
     total = jnp.zeros((length, part), F32)
     for b in range(ny):
         left = []
         for c in range(nc):
             for x in range(nx):
-                gain = gain_ref[b, c * nx + x : c * nx + x + 1]
-                normed = (block(x, c, b) - shift) * factor * gain
+                gain = gain_ref[b, c * nx + x : c * nx + x + 1, : width + chan]
+                normed = (blocks[x, c, b] - shift) * factor * gain
                 branch = normed / (1.0 + jnp.exp(-normed))
-                used = jnp.where(is_memory, normed, branch).astype(BF16)
-                left.append(used[:, : width + chan])
+                left.append(jnp.where(is_memory, normed, branch).astype(BF16))
         total = total + dot(
             jnp.concatenate(left, axis=1), weight_ref[b].reshape(part, deep), NT
         )
@@ -281,10 +289,7 @@
             at = first + j
             if at % 8 == shift:
                 total = total + moved[at - shift : at - shift + group] * weights[j : j + 1]
-    high = total.astype(BF16)
-    low = (total - high.astype(F32)).astype(BF16)
-    sides = [slice(x * chan, (x + 1) * chan) for x in range(nx)]
-    return [jnp.concatenate([high[:, mine], low[:, mine]], axis=1) for mine in sides]
+    return [total[:, x * chan : (x + 1) * chan].astype(BF16) for x in range(nx)]
 
 
 def slab_kernel(
@@ -335,7 +340,7 @@
 def cell_kernel(place_ref, in_ref, q_ref, k_ref, v_ref, gate_ref, glu_ref, taps_ref, out_ref):
     chunks, length = gate_ref.shape[1], gate_ref.shape[2]
     members, rows, head = in_ref.shape
-    width = out_ref.shape[4] // 2
+    width = v_ref.shape[1] // 2
     nc, ny = out_ref.shape[1], out_ref.shape[2]
     scale = head ** (-0.5)
     place = place_ref[0]
@@ -386,9 +391,10 @@
         denom = jnp.sum(scores, axis=1, keepdims=True) + carried_weight * older[:, width : width + 1]
         result = numer[:, :width] / jnp.maximum(jnp.abs(denom), 1.0)
         x, c = r // nc, r % nc
-        sent = jnp.concatenate(
-            [result.astype(BF16), conv[x][c * length : (c + 1) * length]], axis=1
-        )
+        half, quarter = length // 2, length // 4
+        memory = jnp.concatenate([result[:half], result[half:]], axis=1).astype(BF16)
+        branch = [conv[x][c * length + g * quarter : c * length + (g + 1) * quarter] for g in range(4)]
+        sent = jnp.concatenate([memory, jnp.concatenate(branch, axis=1)], axis=0)
         for y in range(ny):
             out_ref[x, c, y] = sent
         last = within_row[:, length - 1 :]
@@ -457,27 +463,36 @@
         memory_out_weight.T,
         conv_out_weight.T,
     )
-    turned = lax.ppermute(
-        out_rows,
-        ("zh", "tp"),
-        [(a * ny + b, b * ny + a) for a in range(nzh) for b in range(ny)],
-    )
     offsets = jnp.concatenate([input_offset.T, forget_offset.T], axis=0)
-    sent = pl.pallas_call(
+    call_pack = pl.pallas_call(
         pack_kernel,
         out_shape=jax.ShapeDtypeStruct((nx * ny, length + 8, part), BF16),
         in_specs=vmem(4),
         out_specs=pl.BlockSpec(memory_space=pltpu.VMEM),
         interpret=INTERPRET,
         name="pack",
-    )(tokens, offsets, conv_norm_gain[None], memory_norm_gain[None])
+    )
+    sent = call_pack(tokens, offsets, conv_norm_gain[None], memory_norm_gain[None])
     mine = exchange(pieces.reshape(nx * nc, rows, wide), ("x", "c"))
     mine = mine.reshape(nx * nc * rows, wide)
-    mine = jnp.concatenate([mine, turned], axis=0)
+    mine = jnp.concatenate([mine, out_rows], axis=0)
     near = exchange(jnp.broadcast_to(mine, (nzh, *mine.shape)), "zh")
     own = exchange(sent, ("x", "tp")).reshape(nx, ny, length + 8, part)
+    half_shape = (nzh // 2, *mine.shape)
+    near, *halves = pl.pallas_call(
+        arrange_kernel,
+        out_shape=(
+            jax.ShapeDtypeStruct(near.shape, BF16),
+            jax.ShapeDtypeStruct(half_shape, BF16),
+            jax.ShapeDtypeStruct(half_shape, BF16),
+        ),
+        in_specs=vmem(1),
+        out_specs=vmem(3),
+        interpret=INTERPRET,
+        name="arrange",
+    )(near)
     sets = [near, from_z(near, 1), from_z(near, -1)]
-    sets += [from_z(near[: nzh // 2], 2), from_z(near[nzh // 2 :], -2)]
+    sets += [from_z(halves[0], 2), from_z(halves[1], -2)]
     other = swapped(own, "c")
 
     gate_weight = jnp.pad(
@@ -502,7 +517,11 @@
     )(place, own, other, *sets, gate_weight)
     value = value.reshape(slab, 2 * width)
     all_qk = exchange(qk.reshape(nx, slab, 2 * width), "x")
-    out_part, all_qk = lax.optimization_barrier((out_part, all_qk))
+    out_part = [out_part[0]] + [
+        lax.ppermute(out_part[ahead], "tp", [(j, (j + ahead) % ny) for j in range(ny)])
+        for ahead in range(1, ny)
+    ]
+    out_part = jnp.stack(out_part, axis=0)
     out_parts = [out_part] + [
         lax.ppermute(out_part, "x", [(j, (j - ahead) % nx) for j in range(nx)])
         for ahead in range(1, nx)
@@ -511,7 +530,7 @@
     other_out = swapped(own_out, "c")
 
     state_rows = width + 8
-    states, query, key = pl.pallas_call(
+    call_slab = pl.pallas_call(
         slab_kernel,
         out_shape=(
             jax.ShapeDtypeStruct((members, state_rows, head), BF16),
@@ -522,18 +541,20 @@
         out_specs=vmem(3),
         interpret=INTERPRET,
         name="slab_state",
-    )(all_qk, value, gates, packed)
+    )
+    states, query, key = call_slab(all_qk, value, gates, packed)
     states = exchange(states, Z)
-    last = pl.pallas_call(
+    call_cell = pl.pallas_call(
         cell_kernel,
-        out_shape=jax.ShapeDtypeStruct((nx, nc, ny, length, 2 * width), BF16),
+        out_shape=jax.ShapeDtypeStruct((nx, nc, ny, length // 4 * 3, 2 * width), BF16),
         in_specs=[smem] + vmem(7),
         out_specs=pl.BlockSpec(memory_space=pltpu.VMEM),
         interpret=INTERPRET,
         name="cell",
-    )(place, states, query, key, value, gates, packed, conv_kernel)
-    arrived = exchange(last.reshape(nx * nc * ny, length, -1), ("x", "c", "tp"))
-    arrived = arrived.reshape(nx, nc, ny, length, -1)
+    )
+    last = call_cell(place, states, query, key, value, gates, packed, conv_kernel)
+    arrived = exchange(last.reshape(nx * nc * ny, length // 4 * 3, -1), ("x", "c", "tp"))
+    arrived = arrived.reshape(nx, nc, ny, length // 4 * 3, -1)
     return pl.pallas_call(
         finish_kernel,
         out_shape=jax.ShapeDtypeStruct((length, part), BF16),

time: 227 us -> 225 us (level)
  starting transfers between devices: 53.1 us -> 59 us
  blocking collectives: 95.3 us -> 90 us
  waiting for transfers between devices: 42.9 us -> 39 us
    ppermute x1 -> x3, starting transfers between devices: 1.4 us -> 7.83 us  [layer(): lax.ppermute(out_part[ahead], 'tp', [(j, (j + ahead) % ny) for j in range...]
    all_to_all x3 -> x2, waiting for transfers between devices: 19.8 us -> 13.5 us  [exchange(): return lax.all_to_all(pieces, axes, split_axis=0, concat_axis=0, tiled=True)]
    ppermute x1 -> x3, waiting for transfers between devices: 0.01 us -> 5.38 us  [layer(): lax.ppermute(out_part[ahead], 'tp', [(j, (j + ahead) % ny) for j in range...]
    all_to_all x3 -> x4, blocking collectives: 95.3 us -> 90 us  [exchange(): return lax.all_to_all(pieces, axes, split_axis=0, concat_axis=0, tiled=True)]
    ppermute x3, waiting for transfers between devices: 15.6 us -> 12.9 us  [layer(): lax.ppermute(out_part, 'x', [(j, (j - ahead) % nx) for j in range(nx)])]
    pallas_call x3 -> x4, Pallas kernels: 13.8 us -> 15.3 us  [the longest x1 7.1 us: layer(): call_cell(place, states, query, key, value, gates, packed, conv_kernel)]
    all_to_all x3 -> x2, starting transfers between devices: 14 us -> 13.7 us  [exchange(): return lax.all_to_all(pieces, axes, split_axis=0, concat_axis=0, tiled=True)]
  transfers between devices with their start and end apart: 13 -> 14, of which waited for: 7 -> 8; matrix products, arithmetic and copies ran while one was open for 1% -> 1% of each run, Pallas kernels for 4% -> 5%
where the time goes in v6:
time: 225 us; the launch traced here: 224 us
  blocking collectives  90 us (40%)
  starting transfers between devices  59 us (26%)
  waiting for transfers between devices  39 us (17%)
  Pallas kernels  28.8 us (13%)
  local copies, waits for them, and re-layouts  3.83 us (2%)
  other arithmetic  2.89 us (1%)
    all_to_all x4, blocking collectives, exchange(): return lax.all_to_all(pieces, axes, split_axis=0, concat_axis=0, tiled=True)  90 us
    ppermute x4, starting transfers between devices, from_z(): lax.ppermute(value, Z, [(j, (j - ahead) % members) for j in range(members)])  18.6 us
    all_to_all x2, starting transfers between devices, exchange(): return lax.all_to_all(pieces, axes, split_axis=0, concat_axis=0, tiled=True)  13.7 us
    all_to_all x2, waiting for transfers between devices, exchange(): return lax.all_to_all(pieces, axes, split_axis=0, concat_axis=0, tiled=True)  13.5 us
    ppermute x3, waiting for transfers between devices, layer(): lax.ppermute(out_part, 'x', [(j, (j - ahead) % nx) for j in range(nx)])  12.9 us
    ppermute x2, starting transfers between devices, swapped(): return lax.ppermute(value, axis, [(0, 1), (1, 0)])  10.4 us
    ppermute x3, starting transfers between devices, layer(): lax.ppermute(out_part, 'x', [(j, (j - ahead) % nx) for j in range(nx)])  8.42 us
    ppermute x3, starting transfers between devices, layer(): lax.ppermute(out_part[ahead], 'tp', [(j, (j + ahead) % ny) for j in range...  7.83 us
  transfers between devices with their start and end apart: 14, of which 8 were waited for; matrix products, arithmetic and copies ran while one was open for 1% of the time, Pallas kernels for 5%

profile of v6, /device:TPU:1, one launch (start us, length us, event | category | flops | bytes accessed | tf_op | source)
XLA Modules:
  0.0 223.8 jit_solution(14787038987033096461)
XLA Ops:
  1.3 2.5 %pack.1 = bf16[16,136,512]{2,1,0:T(8,128)(2,1)} custom-call(bf16[128,512]{1,0:T(8,128)(2,1)} %tokens_ref.1, f32[4,128]{1,0:T(4,128)} %pad_maximum_fusion.4.offsets_ref, f32[1,256]{1,0:T(1,128)} %bitcast.49, f32[1,512]{1,0:T(1,128)} %bitcast.48), custom_call_target="tpu_custom_call" | custom-call | tf_op jit(solution)/shard_map/pack/pallas_call | solution.py:475
  3.8 34.1 %all_to_all.30 = bf16[16,136,512]{2,1,0:T(8,128)(2,1)S(1)} all-to-all(bf16[16,136,512]{2,1,0:T(8,128)(2,1)} %pack.1), channel_id=1, replica_groups=mesh['zh'=4,'zl'=4,'x'=4,'c'=2,'tp'=4] {'x','tp'}, dimensions={0} | all-to-all | bytes 4456448 | tf_op jit(solution)/shard_map/all_to_all | solution.py:24
  37.9 6.0 %collective-permute-start = (bf16[4,4,136,512]{3,2,1,0:T(8,128)(2,1)S(1)}, bf16[4,4,136,512]{3,2,1,0:T(8,128)(2,1)}, u32[]{:S(2)}, u32[]{:S(2)}) collective-permute-start(bf16[4,4,136,512]{3,2,1,0:T(8,128)(2,1)S(1)} %bitcast.31), channel_id=1, source_target_pairs={{0,4},{4,0},{1,5},{5,1},{2,6},{6,2},{3,7},{7,3},{8,12},{12,8},{9,1... | collective-permute-start | bytes 6684680 | tf_op jit(solution)/shard_map/ppermute | solution.py:28
  45.5 8.1 %all_to_all.31 = bf16[8,16,256]{2,1,0:T(8,128)(2,1)S(1)} all-to-all(bf16[8,16,256]{2,1,0:T(8,128)(2,1)} %bitcast.45), channel_id=1, replica_groups=mesh['zh'=4,'zl'=4,'x'=4,'c'=2,'tp'=4] {'x','c'}, dimensions={0} | all-to-all | bytes 131072 | tf_op jit(solution)/shard_map/all_to_all | solution.py:24
  54.4 32.2 %all_to_all.32.in_ref = bf16[4,176,256]{2,1,0:T(8,128)(2,1)} all-to-all(bf16[4,176,256]{2,1,0:T(8,128)(2,1)S(1)} %broadcast_in_dim.11), channel_id=1, replica_groups=mesh['zh'=4,'zl'=4,'x'=4,'c'=2,'tp'=4] {'zh'}, dimensions={0} | all-to-all | bytes 720896 | tf_op jit(solution)/shard_map/all_to_all | solution.py:24
  88.4 10.5 %collective-permute-start.2 = (bf16[4,176,256]{2,1,0:T(8,128)(2,1)}, bf16[4,176,256]{2,1,0:T(8,128)(2,1)S(1)}, u32[]{:S(2)}, u32[]{:S(2)}) collective-permute-start(bf16[4,176,256]{2,1,0:T(8,128)(2,1)} %get-tuple-element.21.w0_ref), channel_id=1, source_target_pairs={{0,32},{32,64},{64,96},{96,128},{128,160},{160,192},{192,224},{224... | collective-permute-start | bytes 1081352 | tf_op jit(solution)/shard_map/ppermute | solution.py:444
  100.9 3.0 %collective-permute-start.3 = (bf16[2,176,256]{2,1,0:T(8,128)(2,1)}, bf16[2,176,256]{2,1,0:T(8,128)(2,1)}, u32[]{:S(2)}, u32[]{:S(2)}) collective-permute-start(bf16[2,176,256]{2,1,0:T(8,128)(2,1)} %get-tuple-element.22), channel_id=1, source_target_pairs={{0,448},{32,480},{64,0},{96,32},{128,64},{160,96},{192,128},{224,1... | collective-permute-start | bytes 540680 | tf_op jit(solution)/shard_map/ppermute | solution.py:444
  103.8 3.2 %collective-permute-start.4 = (bf16[2,176,256]{2,1,0:T(8,128)(2,1)}, bf16[2,176,256]{2,1,0:T(8,128)(2,1)}, u32[]{:S(2)}, u32[]{:S(2)}) collective-permute-start(bf16[2,176,256]{2,1,0:T(8,128)(2,1)} %get-tuple-element.23), channel_id=1, source_target_pairs={{0,64},{32,96},{64,128},{96,160},{128,192},{160,224},{192,256},{22... | collective-permute-start | bytes 540680 | tf_op jit(solution)/shard_map/ppermute | solution.py:444
  108.9 6.5 %collective-permute-done.3.low_ref = bf16[2,176,256]{2,1,0:T(8,128)(2,1)} collective-permute-done((bf16[2,176,256]{2,1,0:T(8,128)(2,1)}, bf16[2,176,256]{2,1,0:T(8,128)(2,1)}, u32[]{:S(2)}, u32[]{:S(2)}) %collective-permute-start.3) | collective-permute-done | bytes 180256 | tf_op jit(solution)/shard_map/ppermute | solution.py:444
  117.1 6.5 %project.1 = (bf16[4,4,2,128,128]{4,3,2,1,0:T(8,128)(2,1)}, bf16[4,2,128,128]{3,2,1,0:T(8,128)(2,1)}, bf16[2,128,128]{2,1,0:T(8,128)(2,1)}, f32[2,8,128]{2,1,0:T...) custom-call(s32[4]{0:T(128)} %pad_add_fusion.place_ref, bf16[4,4,136,512]{3,2,1,0:T(8,128)(2,1)} %bitcast.32, ...), custom_call_target="tpu_custom_call" | custom-call | tf_op jit(solution)/shard_map/project/pallas_call | solution.py:503
  123.6 15.6 %all_to_all.33.qk_ref = bf16[4,1024,128]{2,1,0:T(8,128)(2,1)} all-to-all(bf16[4,1024,128]{2,1,0:T(8,128)(2,1)} %bitcast.35), channel_id=1, replica_groups=mesh['zh'=4,'zl'=4,'x'=4,'c'=2,'tp'=4] {'x'}, dimensions={0} | all-to-all | bytes 2097152 | tf_op jit(solution)/shard_map/all_to_all | solution.py:24
  139.2 3.8 %slab_state.1 = (bf16[16,72,256]{2,1,0:T(8,128)(2,1)}, bf16[1024,256]{1,0:T(8,128)(2,1)}, bf16[1024,256]{1,0:T(8,128)(2,1)}) custom-call(bf16[4,1024,128]{2,1,0:T(8,128)(2,1)} %all_to_all.33.qk_ref, bf16[1024,128]{1,0:T(8,128)(2,1)} %bitcast.36, f32[2,8,128]{2,1,0:T(8,128)} %get-tuple-element.26.gate_ref, bf16[2,128,128]{2,1,0:T(8,128)(2,1)} %get-tuple-element.27.glu_ref), custom_call_target="tpu_custom_call" | custom-call | tf_op jit(solution)/shard_map/slab_state/pallas_call | solution.py:545
  143.0 10.0 %all-to-all-start.4 = ((bf16[16,72,256]{2,1,0:T(8,128)(2,1)}), bf16[16,72,256]{2,1,0:T(8,128)(2,1)S(1)}, u32[]{:S(2)}, u32[]{:S(2)}) async-start(bf16[16,72,256]{2,1,0:T(8,128)(2,1)} %get-tuple-element.28), calls=%async_computation.4 | async-start | bytes 1179648 | tf_op jit(solution)/shard_map/all_to_all | solution.py:24
  153.1 2.9 %collective-permute-start.7 = (bf16[4,16,768]{2,1,0:T(8,128)(2,1)S(1)}, bf16[4,16,768]{2,1,0:T(8,128)(2,1)S(1)}, u32[]{:S(2)}, u32[]{:S(2)}) collective-permute-start(bf16[4,16,768]{2,1,0:T(8,128)(2,1)S(1)} %get-tuple-element.36), channel_id=1, source_target_pairs={{0,3},{1,0},{2,1},{3,2},{4,7},{5,4},{6,5},{7,6},{8,11},{9,8},{10,9... | collective-permute-start | bytes 294920 | tf_op jit(solution)/shard_map/ppermute | solution.py:521
  156.0 2.9 %collective-permute-start.6 = (bf16[4,16,768]{2,1,0:T(8,128)(2,1)S(1)}, bf16[4,16,768]{2,1,0:T(8,128)(2,1)S(1)}, u32[]{:S(2)}, u32[]{:S(2)}) collective-permute-start(bf16[4,16,768]{2,1,0:T(8,128)(2,1)S(1)} %get-tuple-element.37), channel_id=1, source_target_pairs={{0,2},{1,3},{2,0},{3,1},{4,6},{5,7},{6,4},{7,5},{8,10},{9,11},{10,... | collective-permute-start | bytes 294920 | tf_op jit(solution)/shard_map/ppermute | solution.py:521
  163.2 3.1 %collective-permute-done.5 = bf16[4,16,768]{2,1,0:T(8,128)(2,1)S(1)} collective-permute-done((bf16[4,16,768]{2,1,0:T(8,128)(2,1)S(1)}, bf16[4,16,768]{2,1,0:T(8,128)(2,1)S(1)}, u32[]{:S(2)}, u32[]{:S(2)}) %collective-permute-start.5) | collective-permute-done | bytes 98336 | tf_op jit(solution)/shard_map/ppermute | solution.py:521
  168.3 4.6 %collective-permute-start.8 = (bf16[4,4,16,768]{3,2,1,0:T(8,128)(2,1)S(1)}, bf16[4,4,16,768]{3,2,1,0:T(8,128)(2,1)S(1)}, u32[]{:S(2)}, u32[]{:S(2)}) collective-permute-start(bf16[4,4,16,768]{3,2,1,0:T(8,128)(2,1)S(1)} %get-tuple-element.34), channel_id=1, source_target_pairs={{0,24},{8,0},{16,8},{24,16},{1,25},{9,1},{17,9},{25,17},{2,26},{10... | collective-permute-start | bytes 1179656 | tf_op jit(solution)/shard_map/ppermute | solution.py:526
  174.9 2.4 %collective-permute-done.9 = bf16[4,4,16,768]{3,2,1,0:T(8,128)(2,1)S(1)} collective-permute-done((bf16[4,4,16,768]{3,2,1,0:T(8,128)(2,1)S(1)}, bf16[4,4,16,768]{3,2,1,0:T(8,128)(2,1)S(1)}, u32[]{:S(2)}, u32[]{:S(2)}) %collective-permute-start.9) | collective-permute-done | bytes 393248 | tf_op jit(solution)/shard_map/ppermute | solution.py:526
  177.3 8.3 %collective-permute-done.8 = bf16[4,4,16,768]{3,2,1,0:T(8,128)(2,1)S(1)} collective-permute-done((bf16[4,4,16,768]{3,2,1,0:T(8,128)(2,1)S(1)}, bf16[4,4,16,768]{3,2,1,0:T(8,128)(2,1)S(1)}, u32[]{:S(2)}, u32[]{:S(2)}) %collective-permute-start.8) | collective-permute-done | bytes 393248 | tf_op jit(solution)/shard_map/ppermute | solution.py:526
  187.9 4.4 %collective-permute-start.11 = (bf16[4,4,4,16,768]{4,3,2,1,0:T(8,128)(2,1)S(1)}, bf16[4,4,4,16,768]{4,3,2,1,0:T(8,128)(2,1)}, u32[]{:S(2)}, u32[]{:S(2)}) collective-permute-start(bf16[4,4,4,16,768]{4,3,2,1,0:T(8,128)(2,1)S(1)} %pad_maximum_fusion.own_ref), channel_id=1, source_target_pairs={{0,4},{4,0},{1,5},{5,1},{2,6},{6,2},{3,7},{7,3},{8,12},{12,8},{9,1... | collective-permute-start | bytes 4718600 | tf_op jit(solution)/shard_map/ppermute | solution.py:28
  193.2 7.1 %cell.1 = bf16[4,2,4,96,128]{4,3,2,1,0:T(8,128)(2,1)} custom-call(s32[4]{0:T(128)} %pad_add_fusion.place_ref, bf16[16,72,256]{2,1,0:T(8,128)(2,1)} %copy-done.3, bf16[1024,256]{1,0:T(8,128)(2,1)} %get-tuple-element.29.q_ref, bf16[1024,256]{1,0:T(8,128)(2,1)} %get-tuple-element.30.k_ref, bf16[1024,128]{1,0:T(8,128)(2,1)} %bitcast.37, ...), custom_call_target="tpu_custom_call" | custom-call | tf_op jit(solution)/shard_map/cell/pallas_call | solution.py:555
  200.3 3.7 %all-to-all-start.5 = ((bf16[32,96,128]{2,1,0:T(8,128)(2,1)}), bf16[32,96,128]{2,1,0:T(8,128)(2,1)S(1)}, u32[]{:S(2)}, u32[]{:S(2)}) async-start(bf16[32,96,128]{2,1,0:T(8,128)(2,1)} %bitcast.34), calls=%async_computation.5 | async-start | bytes 1572864 | tf_op jit(solution)/shard_map/all_to_all | solution.py:24
  204.0 13.5 %all-to-all-done.5 = bf16[32,96,128]{2,1,0:T(8,128)(2,1)S(1)} async-done(((bf16[32,96,128]{2,1,0:T(8,128)(2,1)}), bf16[32,96,128]{2,1,0:T(8,128)(2,1)S(1)}, u32[]{:S(2)}, u32[]{:S(2)}) %all-to-all-start.5) | async-done | bytes 786464 | tf_op jit(solution)/shard_map/all_to_all | solution.py:24
  218.4 5.5 %finish.1 = bf16[128,512]{1,0:T(8,128)(2,1)} custom-call(s32[4]{0:T(128)} %pad_add_fusion.place_ref, bf16[4,2,4,96,128]{4,3,2,1,0:T(8,128)(2,1)} %bitcast.33, bf16[4,4,4,16,768]{4,3,2,1,0:T(8,128)(2,1)} %copy-done.1, bf16[4,4,4,16,768]{4,3,2,1,0:T(8,128)(2,1)} %collective-permute-done.11.other_ref, f32[4,8,128]{2,1,0:T(8,128)} %get-tuple-element.32.gain_ref), custom_call_target="tpu_custom_call" | custom-call | tf_op jit(solution)/shard_map/finish/pallas_call | solution.py:558
  (43 shorter events, 23.1 us)
Async XLA Ops:
  37.9 70.5 %copy-start = (bf16[16,136,512]{2,1,0:T(8,128)(2,1)}, bf16[16,136,512]{2,1,0:T(8,128)(2,1)S(1)}, u32[]{:S(2)}) copy-start(bf16[16,136,512]{2,1,0:T(8,128)(2,1)S(1)} %all_to_all.30) | copy-start | bytes 6684676
  37.9 69.2 %copy-start.7 = (bf16[2048,2]{0,1:T(2,128)(2,1)S(1)}, bf16[2048,2]{0,1:T(2,128)(2,1)}, u32[]{:S(2)}) copy-start(bf16[2048,2]{0,1:T(2,128)(2,1)} %param.24) | copy-start | bytes 24580
  37.9 69.2 %copy-start.8 = (bf16[2048,2]{0,1:T(2,128)(2,1)S(1)}, bf16[2048,2]{0,1:T(2,128)(2,1)}, u32[]{:S(2)}) copy-start(bf16[2048,2]{0,1:T(2,128)(2,1)} %param.23) | copy-start | bytes 24580
  37.9 78.4 %collective-permute-start = (bf16[4,4,136,512]{3,2,1,0:T(8,128)(2,1)S(1)}, bf16[4,4,136,512]{3,2,1,0:T(8,128)(2,1)}, u32[]{:S(2)}, u32[]{:S(2)}) collective-permute-start(bf16[4,4,136,512]{3,2,1,0:T(8,128)(2,1)S(1)} %bitcast.31), channel_id=1, source_target_pairs={{0,4},{4,0},{1,5},{5,1},{2,6},{6,2},{3,7},{7,3},{8,12},{12,8},{9,1... | collective-permute-start | bytes 6684680 | tf_op jit(solution)/shard_map/ppermute | solution.py:28
  88.4 27.8 %collective-permute-start.2 = (bf16[4,176,256]{2,1,0:T(8,128)(2,1)}, bf16[4,176,256]{2,1,0:T(8,128)(2,1)S(1)}, u32[]{:S(2)}, u32[]{:S(2)}) collective-permute-start(bf16[4,176,256]{2,1,0:T(8,128)(2,1)} %get-tuple-element.21.w0_ref), channel_id=1, source_target_pairs={{0,32},{32,64},{64,96},{96,128},{128,160},{160,192},{192,224},{224... | collective-permute-start | bytes 1081352 | tf_op jit(solution)/shard_map/ppermute | solution.py:444
  98.9 17.3 %collective-permute-start.1 = (bf16[4,176,256]{2,1,0:T(8,128)(2,1)}, bf16[4,176,256]{2,1,0:T(8,128)(2,1)S(1)}, u32[]{:S(2)}, u32[]{:S(2)}) collective-permute-start(bf16[4,176,256]{2,1,0:T(8,128)(2,1)} %get-tuple-element.21.w0_ref), channel_id=1, source_target_pairs={{0,480},{32,0},{64,32},{96,64},{128,96},{160,128},{192,160},{224,1... | collective-permute-start | bytes 1081352 | tf_op jit(solution)/shard_map/ppermute | solution.py:444
  100.9 14.6 %collective-permute-start.3 = (bf16[2,176,256]{2,1,0:T(8,128)(2,1)}, bf16[2,176,256]{2,1,0:T(8,128)(2,1)}, u32[]{:S(2)}, u32[]{:S(2)}) collective-permute-start(bf16[2,176,256]{2,1,0:T(8,128)(2,1)} %get-tuple-element.22), channel_id=1, source_target_pairs={{0,448},{32,480},{64,0},{96,32},{128,64},{160,96},{192,128},{224,1... | collective-permute-start | bytes 540680 | tf_op jit(solution)/shard_map/ppermute | solution.py:444
  103.8 12.4 %collective-permute-start.4 = (bf16[2,176,256]{2,1,0:T(8,128)(2,1)}, bf16[2,176,256]{2,1,0:T(8,128)(2,1)}, u32[]{:S(2)}, u32[]{:S(2)}) collective-permute-start(bf16[2,176,256]{2,1,0:T(8,128)(2,1)} %get-tuple-element.23), channel_id=1, source_target_pairs={{0,64},{32,96},{64,128},{96,160},{128,192},{160,224},{192,256},{22... | collective-permute-start | bytes 540680 | tf_op jit(solution)/shard_map/ppermute | solution.py:444
  116.3 0.7 copy-start.5
  116.3 0.8 copy-start.6
  139.2 13.9 %copy-start.4 = (bf16[4,4,16,768]{3,2,1,0:T(8,128)(2,1)S(1)}, bf16[4,4,16,768]{3,2,1,0:T(8,128)(2,1)}, u32[]{:S(2)}) copy-start(bf16[4,4,16,768]{3,2,1,0:T(8,128)(2,1)} %get-tuple-element.31) | copy-start | bytes 1179652
  143.0 49.3 %all-to-all-start.4 = ((bf16[16,72,256]{2,1,0:T(8,128)(2,1)}), bf16[16,72,256]{2,1,0:T(8,128)(2,1)S(1)}, u32[]{:S(2)}, u32[]{:S(2)}) async-start(bf16[16,72,256]{2,1,0:T(8,128)(2,1)} %get-tuple-element.28), calls=%async_computation.4 | async-start | bytes 1179648 | tf_op jit(solution)/shard_map/all_to_all | solution.py:24
  153.1 7.9 %collective-permute-start.7 = (bf16[4,16,768]{2,1,0:T(8,128)(2,1)S(1)}, bf16[4,16,768]{2,1,0:T(8,128)(2,1)S(1)}, u32[]{:S(2)}, u32[]{:S(2)}) collective-permute-start(bf16[4,16,768]{2,1,0:T(8,128)(2,1)S(1)} %get-tuple-element.36), channel_id=1, source_target_pairs={{0,3},{1,0},{2,1},{3,2},{4,7},{5,4},{6,5},{7,6},{8,11},{9,8},{10,9... | collective-permute-start | bytes 294920 | tf_op jit(solution)/shard_map/ppermute | solution.py:521
  156.0 7.2 %collective-permute-start.6 = (bf16[4,16,768]{2,1,0:T(8,128)(2,1)S(1)}, bf16[4,16,768]{2,1,0:T(8,128)(2,1)S(1)}, u32[]{:S(2)}, u32[]{:S(2)}) collective-permute-start(bf16[4,16,768]{2,1,0:T(8,128)(2,1)S(1)} %get-tuple-element.37), channel_id=1, source_target_pairs={{0,2},{1,3},{2,0},{3,1},{4,6},{5,7},{6,4},{7,5},{8,10},{9,11},{10,... | collective-permute-start | bytes 294920 | tf_op jit(solution)/shard_map/ppermute | solution.py:521
  158.9 7.4 %collective-permute-start.5 = (bf16[4,16,768]{2,1,0:T(8,128)(2,1)S(1)}, bf16[4,16,768]{2,1,0:T(8,128)(2,1)S(1)}, u32[]{:S(2)}, u32[]{:S(2)}) collective-permute-start(bf16[4,16,768]{2,1,0:T(8,128)(2,1)S(1)} %get-tuple-element.38), channel_id=1, source_target_pairs={{0,1},{1,2},{2,3},{3,0},{4,5},{5,6},{6,7},{7,4},{8,9},{9,10},{10,1... | collective-permute-start | bytes 294920 | tf_op jit(solution)/shard_map/ppermute | solution.py:521
  166.4 10.9 %collective-permute-start.9 = (bf16[4,4,16,768]{3,2,1,0:T(8,128)(2,1)S(1)}, bf16[4,4,16,768]{3,2,1,0:T(8,128)(2,1)S(1)}, u32[]{:S(2)}, u32[]{:S(2)}) collective-permute-start(bf16[4,4,16,768]{3,2,1,0:T(8,128)(2,1)S(1)} %get-tuple-element.34), channel_id=1, source_target_pairs={{0,16},{8,24},{16,0},{24,8},{1,17},{9,25},{17,1},{25,9},{2,18},{10... | collective-permute-start | bytes 1179656 | tf_op jit(solution)/shard_map/ppermute | solution.py:526
  168.3 17.2 %collective-permute-start.8 = (bf16[4,4,16,768]{3,2,1,0:T(8,128)(2,1)S(1)}, bf16[4,4,16,768]{3,2,1,0:T(8,128)(2,1)S(1)}, u32[]{:S(2)}, u32[]{:S(2)}) collective-permute-start(bf16[4,4,16,768]{3,2,1,0:T(8,128)(2,1)S(1)} %get-tuple-element.34), channel_id=1, source_target_pairs={{0,24},{8,0},{16,8},{24,16},{1,25},{9,1},{17,9},{25,17},{2,26},{10... | collective-permute-start | bytes 1179656 | tf_op jit(solution)/shard_map/ppermute | solution.py:526
  172.9 14.8 %collective-permute-start.10 = (bf16[4,4,16,768]{3,2,1,0:T(8,128)(2,1)S(1)}, bf16[4,4,16,768]{3,2,1,0:T(8,128)(2,1)S(1)}, u32[]{:S(2)}, u32[]{:S(2)}) collective-permute-start(bf16[4,4,16,768]{3,2,1,0:T(8,128)(2,1)S(1)} %get-tuple-element.34), channel_id=1, source_target_pairs={{0,8},{8,16},{16,24},{24,0},{1,9},{9,17},{17,25},{25,1},{2,10},{10... | collective-permute-start | bytes 1179656 | tf_op jit(solution)/shard_map/ppermute | solution.py:526
  187.9 12.4 %copy-start.1 = (bf16[4,4,4,16,768]{4,3,2,1,0:T(8,128)(2,1)}, bf16[4,4,4,16,768]{4,3,2,1,0:T(8,128)(2,1)S(1)}, u32[]{:S(2)}) copy-start(bf16[4,4,4,16,768]{4,3,2,1,0:T(8,128)(2,1)S(1)} %pad_maximum_fusion.own_ref) | copy-start | bytes 4718596
  187.9 16.1 %collective-permute-start.11 = (bf16[4,4,4,16,768]{4,3,2,1,0:T(8,128)(2,1)S(1)}, bf16[4,4,4,16,768]{4,3,2,1,0:T(8,128)(2,1)}, u32[]{:S(2)}, u32[]{:S(2)}) collective-permute-start(bf16[4,4,4,16,768]{4,3,2,1,0:T(8,128)(2,1)S(1)} %pad_maximum_fusion.own_ref), channel_id=1, source_target_pairs={{0,4},{4,0},{1,5},{5,1},{2,6},{6,2},{3,7},{7,3},{8,12},{12,8},{9,1... | collective-permute-start | bytes 4718600 | tf_op jit(solution)/shard_map/ppermute | solution.py:28
  192.4 0.8 copy-start.3
  200.3 17.2 %all-to-all-start.5 = ((bf16[32,96,128]{2,1,0:T(8,128)(2,1)}), bf16[32,96,128]{2,1,0:T(8,128)(2,1)S(1)}, u32[]{:S(2)}, u32[]{:S(2)}) async-start(bf16[32,96,128]{2,1,0:T(8,128)(2,1)} %bitcast.34), calls=%async_computation.5 | async-start | bytes 1572864 | tf_op jit(solution)/shard_map/all_to_all | solution.py:24
  217.5 0.9 copy-start.2

commit v7 on v6

--- a/solution.py
+++ b/solution.py
@@ -107,11 +107,33 @@
             out_ref[x, c] = jnp.concatenate(parts, axis=1)
 
 
-def arrange_kernel(in_ref, near_ref, low_ref, high_ref):
-    half = low_ref.shape[0]
-    near_ref[...] = in_ref[...]
-    low_ref[...] = in_ref[:half]
-    high_ref[...] = in_ref[half:]
+def arrange_kernel(
+    before_ref, mine_ref, after_ref, main_ref, rest_ref, near_ref, low_ref, high_ref
+):
+    rows = main_ref.shape[0]
+    for refs in ((near_ref, 0), (high_ref, 0)):
+        refs[0][refs[1]] = before_ref[...]
+    for refs in ((near_ref, 1), (high_ref, 1), (low_ref, 0)):
+        refs[0][refs[1]] = mine_ref[...]
+    for refs in ((near_ref, 2), (low_ref, 1)):
+        refs[0][refs[1]] = after_ref[...]
+    near_ref[3, :rows] = main_ref[...]
+    near_ref[3, rows:] = rest_ref[...]
+
+
+def assemble_kernel(place_ref, *refs):
+    out_ref = refs[-1]
+    nx, ny = out_ref.shape[2], out_ref.shape[0]
+    core, column, x_at = place_ref[1], place_ref[2], place_ref[3]
+    for ahead in range(nx):
+        x = lax.rem(x_at + ahead, nx)
+        for c, ref in ((core, refs[ahead]), (1 - core, refs[nx + ahead])):
+            for b in range(ny):
+                at = lax.rem(column + ny - b, ny)
+                for near in range(ref.shape[1]):
+                    out_ref[pl.ds(at, 1), near, pl.ds(x, 1), pl.ds(c, 1)] = ref[b, near][
+                        None, None, None
+                    ]
 
 
 def project_kernel(
@@ -135,16 +157,19 @@
     gate_in = jnp.zeros((2 * nx, length), F32)
     forget = jnp.zeros((2 * nx, length), F32)
 
+    members = far * close
     blocks = [
-        (ref, i, ahead, i)
-        for ref, ahead in ((w0_ref, 0), (w1_ref, 1), (w3_ref, close - 1))
+        (ref, i, ahead + close * (i - 1))
+        for ref, ahead in ((w0_ref, 0), (w1_ref, 1), (w3_ref, -1))
         for i in range(far)
     ]
-    blocks += [(low_ref, i, 2, i) for i in range(far // 2)]
-    blocks += [(high_ref, i, 2, i + far // 2) for i in range(far // 2)]
+    blocks += [(low_ref, i, 2 + close * i) for i in range(far // 2)]
+    blocks += [(high_ref, i, -2 + close * (i - 1)) for i in range(far // 2)]
     homes = []
-    for ref, i, ahead, y in blocks:
-        homes.append((y, lax.rem(place + ahead, close)))
+    for ref, i, ahead in blocks:
+        home = lax.rem(place + (ahead + members), members)
+        y = lax.div(home, close)
+        homes.append((y, lax.rem(home, close)))
         behind = lax.rem(y + ny - column, ny)
         out_weight_ref[pl.ds(behind, 1), pl.ds(homes[-1][1], 1)] = jnp.concatenate(
             [ref[i, rows + j * depth : rows + (j + 1) * depth] for j in range(chunks)], axis=1
@@ -156,10 +181,12 @@
         for pair in range(0, len(blocks), 2):
             left, right, gate_rows = [], [], []
             for at in (pair, pair + 1):
-                w_ref, i, _, _ = blocks[at]
+                w_ref, i, _ = blocks[at]
                 y, z = homes[at]
                 start = pl.multiple_of(z * rows, rows)
-                left.append(ref[:, y, :length, pl.ds(start, rows)].reshape(tokens_rows, rows))
+                left.append(
+                    ref[:, pl.ds(y, 1), :length, pl.ds(start, rows)].reshape(tokens_rows, rows)
+                )
                 right.append(w_ref[i, :rows])
                 gate_rows.append(gate_ref[pl.ds(y * part + start, rows)])
             lhs = jnp.concatenate(left, axis=1)
@@ -211,9 +238,8 @@
     gates_ref[1] = jnp.minimum(forget, 0.0) - jnp.where(y < 0.03, small, jnp.log(1.0 + y))
 
 
-def finish_kernel(place_ref, arrived_ref, own_ref, other_ref, gain_ref, out_ref, weight_ref):
+def finish_kernel(arrived_ref, weight_ref, gain_ref, out_ref):
     nx, nc, ny, _, lanes = arrived_ref.shape
-    core, x_at = place_ref[1], place_ref[3]
     width = lanes // 2
     chan = width // 2
     length, part = out_ref.shape
@@ -241,15 +267,6 @@
     shift = jnp.where(is_memory, 0.0, mean)
     factor = jnp.where(is_memory, scale, spread)
     deep = weight_ref.shape[5]
-    for ahead in range(nx):
-        x = lax.rem(x_at + ahead, nx)
-        for c, ref in ((core, own_ref), (1 - core, other_ref)):
-            for b in range(ny):
-                for near in range(ref.shape[2]):
-                    at = lax.rem(place_ref[2] + ny - b, ny)
-                    weight_ref[pl.ds(at, 1), near, pl.ds(x, 1), pl.ds(c, 1)] = ref[ahead, b, near][
-                        None, None, None
-                    ]
     total = jnp.zeros((length, part), F32)
     for b in range(ny):
         left = []
@@ -265,31 +282,30 @@
     out_ref[...] = total.astype(BF16)
 
 
-def convolve(glu_ref, prior, taps_ref, nx, core, x_at):
-    nc, length, lanes = glu_ref.shape
+HOLD = 32
+
+
+def tap_rows(taps_ref, core, x_at, nx, lanes):
     chan = lanes // nx
-    group = nc * length
-    glu = glu_ref[...].reshape(group, lanes).astype(F32)
-    taps = taps_ref.shape[0]
-    hold = 32
-    lane = lax.broadcasted_iota(jnp.int32, (hold, lanes), 1)
-    before = pltpu.roll(glu[group - hold :], chan, 1)
-    prior = jnp.concatenate([prior, jnp.zeros((hold, lanes - chan), F32)], axis=1)
-    extended = jnp.concatenate([jnp.where(lane < chan, prior, before), glu], axis=0)
     weights = taps_ref[...].astype(F32)
     weights = jnp.where(core == 0, weights[:, :lanes], weights[:, lanes:])
     weights = pltpu.roll(weights, lax.rem(lanes - chan * x_at, lanes), 1)
     weights = jnp.where(lax.broadcasted_iota(jnp.int32, weights.shape, 1) < chan, weights, 0.0)
-    weights = sum(pltpu.roll(weights, chan * k, 1) for k in range(1, nx)) + weights
-    total = jnp.zeros((group, lanes), F32)
-    first = hold - (taps - 1)
+    return sum(pltpu.roll(weights, chan * k, 1) for k in range(1, nx)) + weights
+
+
+def convolve(extended, weights):
+    taps = weights.shape[0]
+    length = extended.shape[0] - HOLD
+    total = jnp.zeros((length, extended.shape[1]), F32)
+    first = HOLD - (taps - 1)
     for shift in range(8):
-        moved = extended[shift : shift + group + hold - 8] if shift else extended
+        moved = extended[shift : shift + length + HOLD - 8] if shift else extended
         for j in range(taps):
             at = first + j
             if at % 8 == shift:
-                total = total + moved[at - shift : at - shift + group] * weights[j : j + 1]
-    return [total[:, x * chan : (x + 1) * chan].astype(BF16) for x in range(nx)]
+                total = total + moved[at - shift : at - shift + length] * weights[j : j + 1]
+    return total
 
 
 def slab_kernel(
@@ -326,7 +342,7 @@
         for k, part in enumerate((high, mid, low)):
             kept = jnp.where((row == width + 1) & (lane == at + k), part, kept)
     chan = glu_ref.shape[2] // qk_ref.shape[0]
-    hold = 32
+    hold = HOLD
     tail = glu_ref[glu_ref.shape[0] - 1, length - hold :].astype(F32)[:, glu_ref.shape[2] - chan :]
     group = head_lanes // chan
     each = hold // group
@@ -337,20 +353,70 @@
         out_ref[j] = kept
 
 
-def cell_kernel(place_ref, in_ref, q_ref, k_ref, v_ref, gate_ref, glu_ref, taps_ref, out_ref):
+def local_kernel(place_ref, q_ref, k_ref, v_ref, gate_ref, glu_ref, taps_ref, out_ref, conv_ref):
     chunks, length = gate_ref.shape[1], gate_ref.shape[2]
+    head = q_ref.shape[1]
+    lanes = v_ref.shape[1]
+    width = lanes // 2
+    nx = chunks // glu_ref.shape[0]
+    group = glu_ref.shape[0] * glu_ref.shape[1]
+    glu = glu_ref[...].reshape(group, lanes).astype(F32)
+    lane = lax.broadcasted_iota(jnp.int32, (HOLD, lanes), 1)
+    before = pltpu.roll(glu[group - HOLD :], lanes // nx, 1)
+    before = jnp.where(lane < lanes // nx, 0.0, before)
+    weights = tap_rows(taps_ref, place_ref[1], place_ref[3], nx, lanes)
+    conv_ref[...] = convolve(jnp.concatenate([before, glu], axis=0), weights)
+
+    scale = head ** (-0.5)
+    gate, forget = gate_ref[0], gate_ref[1]
+    within = lane_cumsum(forget)
+    turned = columns_of(jnp.concatenate([within, gate], axis=0))
+    causal = lax.broadcasted_iota(jnp.int32, (length, length), 0) >= lax.broadcasted_iota(
+        jnp.int32, (length, length), 1
+    )
+    lane = lax.broadcasted_iota(jnp.int32, (length, lanes), 1)
+    state = jnp.zeros((lanes, head), F32)
+    level = jnp.full((1, 1), LOW, F32)
+    passed = jnp.zeros((1, 1), F32)
+    for r in range(chunks):
+        here = slice(r * length, (r + 1) * length)
+        query, key, value = q_ref[here], k_ref[here], v_ref[here]
+        within_row, gate_row = within[r : r + 1], gate[r : r + 1]
+        within_col = turned[:, r : r + 1]
+        gate_col = turned[:, chunks + r : chunks + r + 1]
+        log_weight = jnp.where(causal, within_col - within_row + gate_row, -jnp.inf)
+        carried = within_col + level
+        top = jnp.maximum(carried, jnp.max(log_weight, axis=1, keepdims=True))
+        weight = jnp.exp(log_weight - top)
+        carried_weight = jnp.exp(carried - top) * scale
+        scores = dot(query, key, NT) * (scale * weight)
+        numer = dot(scores.astype(BF16), value, NN)
+        denom = jnp.sum(scores, axis=1, keepdims=True)
+        if r:
+            older = dot(query, state.astype(BF16), NT)
+            numer = numer + carried_weight * older
+            denom = denom + carried_weight * older[:, width : width + 1]
+        sent = jnp.where(lane == width, denom, numer)
+        sent = jnp.where(lane == width + 1, top, sent)
+        out_ref[here] = jnp.where(lane == width + 2, within_col + passed, sent)
+        last = within_row[:, length - 1 :]
+        passed = passed + last
+        end_row = last - within_row + gate_row
+        new_level = jnp.maximum(last + level, jnp.max(end_row, axis=1, keepdims=True))
+        keep = jnp.exp(last + level - new_level)
+        fresh = jnp.exp(last - within_col + gate_col - new_level)
+        scaled = (fresh * key.astype(F32)).astype(BF16)
+        state = keep * state + dot(value, scaled, TN)
+        level = new_level
+
+
+def cell_kernel(place_ref, in_ref, q_ref, local_ref, conv_ref, taps_ref, out_ref):
     members, rows, head = in_ref.shape
-    width = v_ref.shape[1] // 2
-    nc, ny = out_ref.shape[1], out_ref.shape[2]
+    nx, nc, ny, _, lanes = out_ref.shape
+    width, chan = lanes // 2, lanes // nx
+    length = q_ref.shape[0] // (nx * nc)
     scale = head ** (-0.5)
     place = place_ref[0]
-    chan = glu_ref.shape[2] // out_ref.shape[0]
-    hold, group = 32, head // chan
-    each = hold // group
-    last_rows = in_ref[jnp.maximum(place - 1, 0), width : width + 8].astype(F32)
-    last_rows = jnp.where(place > 0, last_rows[2 : 2 + each], 0.0)
-    prior = jnp.concatenate([last_rows[:, g * chan : (g + 1) * chan] for g in range(group)], axis=0)
-    conv = convolve(glu_ref, prior, taps_ref, out_ref.shape[0], place_ref[1], place_ref[3])
     acc = jnp.zeros((1, 1), F32)
     logs = [None] * members
     for j in range(members - 1, -1, -1):
@@ -367,44 +433,40 @@
     for j in range(members):
         weight = jnp.where(j < place, jnp.exp(logs[j] - level), 0.0)
         state = state + weight * in_ref[j].astype(F32)
-    state = jnp.concatenate([state, jnp.zeros((2 * width - rows, head), F32)], axis=0)
-    gate, forget = gate_ref[0], gate_ref[1]
-    within = lane_cumsum(forget)
-    turned = columns_of(jnp.concatenate([within, gate], axis=0))
-    causal = lax.broadcasted_iota(jnp.int32, (length, length), 0) >= lax.broadcasted_iota(
-        jnp.int32, (length, length), 1
-    )
-    for r in range(chunks):
+    state = jnp.concatenate([state, jnp.zeros((lanes - rows, head), F32)], axis=0).astype(BF16)
+
+    group = head // chan
+    each = HOLD // group
+    last_rows = in_ref[jnp.maximum(place - 1, 0), width : width + 8].astype(F32)
+    last_rows = jnp.where(place > 0, last_rows[2 : 2 + each], 0.0)
+    prior = jnp.concatenate([last_rows[:, g * chan : (g + 1) * chan] for g in range(group)], axis=0)
+    prior = jnp.concatenate([prior, jnp.zeros((HOLD, lanes - chan), F32)], axis=1)
+    weights = tap_rows(taps_ref, place_ref[1], place_ref[3], nx, lanes)
+    edge = convolve(jnp.concatenate([prior, jnp.zeros((HOLD, lanes), F32)], axis=0), weights)
+    half, quarter = length // 2, length // 4
+    for r in range(nx * nc):
         here = slice(r * length, (r + 1) * length)
-        query, key, value = q_ref[here], k_ref[here], v_ref[here]
-        within_row, gate_row = within[r : r + 1], gate[r : r + 1]
-        within_col = turned[:, r : r + 1]
-        gate_col = turned[:, chunks + r : chunks + r + 1]
-        log_weight = jnp.where(causal, within_col - within_row + gate_row, -jnp.inf)
-        carried = within_col + level
-        top = jnp.maximum(carried, jnp.max(log_weight, axis=1, keepdims=True))
-        weight = jnp.exp(log_weight - top)
+        local = local_ref[here]
+        top_here, passed = local[:, width + 1 : width + 2], local[:, width + 2 : width + 3]
+        carried = passed + level
+        top = jnp.maximum(carried, top_here)
+        local_weight = jnp.exp(top_here - top)
         carried_weight = jnp.exp(carried - top) * scale
-        scores = dot(query, key, NT) * (scale * weight)
-        older = dot(query, state.astype(BF16), NT)
-        numer = dot(scores.astype(BF16), value, NN) + carried_weight * older
-        denom = jnp.sum(scores, axis=1, keepdims=True) + carried_weight * older[:, width : width + 1]
-        result = numer[:, :width] / jnp.maximum(jnp.abs(denom), 1.0)
+        mixed = local_weight * local + carried_weight * dot(q_ref[here], state, NT)
+        denom = mixed[:, width : width + 1]
+        result = mixed[:, :width] / jnp.maximum(jnp.abs(denom), 1.0)
         x, c = r // nc, r % nc
-        half, quarter = length // 2, length // 4
-        memory = jnp.concatenate([result[:half], result[half:]], axis=1).astype(BF16)
-        branch = [conv[x][c * length + g * quarter : c * length + (g + 1) * quarter] for g in range(4)]
-        sent = jnp.concatenate([memory, jnp.concatenate(branch, axis=1)], axis=0)
+        memory = jnp.concatenate([result[:half], result[half:]], axis=1)
+        branch = []
+        for g in range(4):
+            at = c * length + g * quarter
+            part = conv_ref[at : at + quarter]
+            if at == 0:
+                part = part + edge
+            branch.append(part[:, x * chan : (x + 1) * chan])
+        sent = jnp.concatenate([memory, jnp.concatenate(branch, axis=1)], axis=0).astype(BF16)
         for y in range(ny):
             out_ref[x, c, y] = sent
-        last = within_row[:, length - 1 :]
-        end_row = last - within_row + gate_row
-        new_level = jnp.maximum(last + level, jnp.max(end_row, axis=1, keepdims=True))
-        keep = jnp.exp(last + level - new_level)
-        fresh = jnp.exp(last - within_col + gate_col - new_level)
-        scaled = (fresh * key.astype(F32)).astype(BF16)
-        state = keep * state + dot(value, scaled, TN)
-        level = new_level
 
 
 def vmem(count):
@@ -474,23 +536,31 @@
     )
     sent = call_pack(tokens, offsets, conv_norm_gain[None], memory_norm_gain[None])
     mine = exchange(pieces.reshape(nx * nc, rows, wide), ("x", "c"))
-    mine = mine.reshape(nx * nc * rows, wide)
-    mine = jnp.concatenate([mine, out_rows], axis=0)
-    near = exchange(jnp.broadcast_to(mine, (nzh, *mine.shape)), "zh")
+    main = mine.reshape(nx * nc * rows, wide)
+    mine = jnp.concatenate([main, out_rows], axis=0)
+    step = members // 4
+    far = [
+        from_z(mine, -step),
+        mine,
+        from_z(mine, step),
+        from_z(main, 2 * step),
+        from_z(out_rows, -2 * step),
+    ]
     own = exchange(sent, ("x", "tp")).reshape(nx, ny, length + 8, part)
     half_shape = (nzh // 2, *mine.shape)
-    near, *halves = pl.pallas_call(
+    call_arrange = pl.pallas_call(
         arrange_kernel,
         out_shape=(
-            jax.ShapeDtypeStruct(near.shape, BF16),
+            jax.ShapeDtypeStruct((nzh, *mine.shape), BF16),
             jax.ShapeDtypeStruct(half_shape, BF16),
             jax.ShapeDtypeStruct(half_shape, BF16),
         ),
-        in_specs=vmem(1),
+        in_specs=vmem(5),
         out_specs=vmem(3),
         interpret=INTERPRET,
         name="arrange",
-    )(near)
+    )
+    near, *halves = call_arrange(*far)
     sets = [near, from_z(near, 1), from_z(near, -1)]
     sets += [from_z(halves[0], 2), from_z(halves[1], -2)]
     other = swapped(own, "c")
@@ -526,8 +596,7 @@
         lax.ppermute(out_part, "x", [(j, (j - ahead) % nx) for j in range(nx)])
         for ahead in range(1, nx)
     ]
-    own_out = jnp.stack(out_parts, axis=0)
-    other_out = swapped(own_out, "c")
+    other_parts = [swapped(out, "c") for out in out_parts]
 
     state_rows = width + 8
     call_slab = pl.pallas_call(
@@ -544,26 +613,46 @@
     )
     states, query, key = call_slab(all_qk, value, gates, packed)
     states = exchange(states, Z)
+    call_local = pl.pallas_call(
+        local_kernel,
+        out_shape=(
+            jax.ShapeDtypeStruct((slab, 2 * width), F32),
+            jax.ShapeDtypeStruct((nc * length, nx * chan), F32),
+        ),
+        in_specs=[smem] + vmem(6),
+        out_specs=vmem(2),
+        interpret=INTERPRET,
+        name="local",
+    )
+    local, conv = call_local(place, query, key, value, gates, packed, conv_kernel)
     call_cell = pl.pallas_call(
         cell_kernel,
         out_shape=jax.ShapeDtypeStruct((nx, nc, ny, length // 4 * 3, 2 * width), BF16),
-        in_specs=[smem] + vmem(7),
+        in_specs=[smem] + vmem(5),
         out_specs=pl.BlockSpec(memory_space=pltpu.VMEM),
         interpret=INTERPRET,
         name="cell",
     )
-    last = call_cell(place, states, query, key, value, gates, packed, conv_kernel)
+    last = call_cell(place, states, query, local, conv, conv_kernel)
     arrived = exchange(last.reshape(nx * nc * ny, length // 4 * 3, -1), ("x", "c", "tp"))
     arrived = arrived.reshape(nx, nc, ny, length // 4 * 3, -1)
+    call_assemble = pl.pallas_call(
+        assemble_kernel,
+        out_shape=jax.ShapeDtypeStruct((ny, nzl, nx, nc, rows, deep), BF16),
+        in_specs=[smem] + vmem(2 * nx),
+        out_specs=pl.BlockSpec(memory_space=pltpu.VMEM),
+        interpret=INTERPRET,
+        name="assemble",
+    )
+    out_weight = call_assemble(place, *out_parts, *other_parts)
     return pl.pallas_call(
         finish_kernel,
         out_shape=jax.ShapeDtypeStruct((length, part), BF16),
-        in_specs=[smem] + vmem(4),
+        in_specs=vmem(3),
         out_specs=pl.BlockSpec(memory_space=pltpu.VMEM),
-        scratch_shapes=[pltpu.VMEM((ny, nzl, nx, nc, rows, deep), BF16)],
         interpret=INTERPRET,
         name="finish",
-    )(place, arrived, own_out, other_out, gain)
+    )(arrived, out_weight, gain)
 
 
 def solution(mesh):

time: 225 us -> 219 us (0.973)
  starting transfers between devices: 59 us -> 95.4 us
  blocking collectives: 90 us -> 56.6 us
  waiting for transfers between devices: 39 us -> 19.6 us
  Pallas kernels: 28.8 us -> 36.7 us
    all_to_all x4 -> x3, blocking collectives: 90 us -> 56.6 us  [exchange(): return lax.all_to_all(pieces, axes, split_axis=0, concat_axis=0, tiled=True)]
    ppermute x4 -> x8, starting transfers between devices: 18.6 us -> 41.3 us  [from_z(): lax.ppermute(value, Z, [(j, (j - ahead) % members) for j in range(members)])]
    all_to_all x2, waiting for transfers between devices: 13.5 us -> 0.01 us  [exchange(): return lax.all_to_all(pieces, axes, split_axis=0, concat_axis=0, tiled=True)]
    ppermute x3, waiting for transfers between devices: 12.9 us -> 0.01 us  [layer(): lax.ppermute(out_part, 'x', [(j, (j - ahead) % nx) for j in range(nx)])]
    all_to_all x2, starting transfers between devices: 13.7 us -> 23.3 us  [exchange(): return lax.all_to_all(pieces, axes, split_axis=0, concat_axis=0, tiled=True)]
    pallas_call x2 -> x4, Pallas kernels: 9 us -> 17.2 us  [the longest x1 7.21 us: layer(): call_local(place, query, key, value, gates, packed, conv_kernel)]
    ppermute x4 -> x8, waiting for transfers between devices: 7.32 us -> 14 us  [from_z(): lax.ppermute(value, Z, [(j, (j - ahead) % members) for j in range(members)])]
    ppermute x2 -> x5, starting transfers between devices: 10.4 us -> 14.5 us  [swapped(): return lax.ppermute(value, axis, [(0, 1), (1, 0)])]
  transfers between devices with their start and end apart: 14 -> 21, of which waited for: 8 -> 6; matrix products, arithmetic and copies ran while one was open for 1% -> 1% of each run, Pallas kernels for 5% -> 9%
where the time goes in v7:
time: 219 us; the launch traced here: 217 us
  starting transfers between devices  95.4 us (44%)
  blocking collectives  56.6 us (26%)
  Pallas kernels  36.7 us (17%)
  waiting for transfers between devices  19.6 us (9%)
  local copies, waits for them, and re-layouts  5.9 us (3%)
  other arithmetic  2.71 us (1%)
    all_to_all x3, blocking collectives, exchange(): return lax.all_to_all(pieces, axes, split_axis=0, concat_axis=0, tiled=True)  56.6 us
    ppermute x8, starting transfers between devices, from_z(): lax.ppermute(value, Z, [(j, (j - ahead) % members) for j in range(members)])  41.3 us
    all_to_all x2, starting transfers between devices, exchange(): return lax.all_to_all(pieces, axes, split_axis=0, concat_axis=0, tiled=True)  23.3 us
    ppermute x5, starting transfers between devices, swapped(): return lax.ppermute(value, axis, [(0, 1), (1, 0)])  14.5 us
    ppermute x8, waiting for transfers between devices, from_z(): lax.ppermute(value, Z, [(j, (j - ahead) % members) for j in range(members)])  14 us
    ppermute x3, starting transfers between devices, layer(): lax.ppermute(out_part, 'x', [(j, (j - ahead) % nx) for j in range(nx)])  8.41 us
    ppermute x3, starting transfers between devices, layer(): lax.ppermute(out_part[ahead], 'tp', [(j, (j + ahead) % ny) for j in range...  7.83 us
    pallas_call x1, Pallas kernels, layer(): call_local(place, query, key, value, gates, packed, conv_kernel)  7.21 us
  transfers between devices with their start and end apart: 21, of which 6 were waited for; matrix products, arithmetic and copies ran while one was open for 1% of the time, Pallas kernels for 9%

profile of v7, /device:TPU:1, one launch (start us, length us, event | category | flops | bytes accessed | tf_op | source)
XLA Modules:
  0.0 217.4 jit_solution(5573465571001342323)
XLA Ops:
  3.8 34.3 %all_to_all.25 = bf16[16,136,512]{2,1,0:T(8,128)(2,1)S(1)} all-to-all(bf16[16,136,512]{2,1,0:T(8,128)(2,1)} %pack.1), channel_id=1, replica_groups=mesh['zh'=4,'zl'=4,'x'=4,'c'=2,'tp'=4] {'x','tp'}, dimensions={0} | all-to-all | bytes 4456448 | tf_op jit(solution)/shard_map/all_to_all | solution.py:24
  38.0 5.9 %collective-permute-start = (bf16[4,4,136,512]{3,2,1,0:T(8,128)(2,1)S(1)}, bf16[4,4,136,512]{3,2,1,0:T(8,128)(2,1)}, u32[]{:S(2)}, u32[]{:S(2)}) collective-permute-start(bf16[4,4,136,512]{3,2,1,0:T(8,128)(2,1)S(1)} %bitcast.26), channel_id=1, source_target_pairs={{0,4},{4,0},{1,5},{5,1},{2,6},{6,2},{3,7},{7,3},{8,12},{12,8},{9,1... | collective-permute-start | bytes 6684680 | tf_op jit(solution)/shard_map/ppermute | solution.py:28
  45.5 8.1 %all_to_all.26 = bf16[8,16,256]{2,1,0:T(8,128)(2,1)S(1)} all-to-all(bf16[8,16,256]{2,1,0:T(8,128)(2,1)} %bitcast.38), channel_id=1, replica_groups=mesh['zh'=4,'zl'=4,'x'=4,'c'=2,'tp'=4] {'x','c'}, dimensions={0} | all-to-all | bytes 131072 | tf_op jit(solution)/shard_map/all_to_all | solution.py:24
  54.3 12.7 %collective-permute-start.2 = (bf16[176,256]{1,0:T(8,128)(2,1)S(1)}, bf16[176,256]{1,0:T(8,128)(2,1)S(1)}, u32[]{:S(2)}, u32[]{:S(2)}) collective-permute-start(bf16[176,256]{1,0:T(8,128)(2,1)S(1)} %pad_maximum_fusion.1.mine_ref), channel_id=1, source_target_pairs={{0,384},{32,416},{64,448},{96,480},{128,0},{160,32},{192,64},{224,... | collective-permute-start | bytes 270344 | tf_op jit(solution)/shard_map/ppermute | solution.py:506
  69.0 10.3 %collective-permute-start.3 = (bf16[128,256]{1,0:T(8,128)(2,1)S(1)}, bf16[128,256]{1,0:T(8,128)(2,1)S(1)}, u32[]{:S(2)}, u32[]{:S(2)}) collective-permute-start(bf16[128,256]{1,0:T(8,128)(2,1)S(1)} %bitcast.34), channel_id=1, source_target_pairs={{0,256},{32,288},{64,320},{96,352},{128,384},{160,416},{192,448},{... | collective-permute-start | bytes 196616 | tf_op jit(solution)/shard_map/ppermute | solution.py:506
  79.2 3.7 %collective-permute-start.4 = (bf16[48,256]{1,0:T(8,128)(2,1)}, bf16[48,256]{1,0:T(8,128)(2,1)S(1)}, u32[]{:S(2)}, u32[]{:S(2)}) collective-permute-start(bf16[48,256]{1,0:T(8,128)(2,1)} %get-tuple-element.22), channel_id=1, source_target_pairs={{0,256},{32,288},{64,320},{96,352},{128,384},{160,416},{192,448},{... | collective-permute-start | bytes 73736 | tf_op jit(solution)/shard_map/ppermute | solution.py:506
  83.0 9.8 %collective-permute-done.4.rest_ref = bf16[48,256]{1,0:T(8,128)(2,1)S(1)} collective-permute-done((bf16[48,256]{1,0:T(8,128)(2,1)}, bf16[48,256]{1,0:T(8,128)(2,1)S(1)}, u32[]{:S(2)}, u32[]{:S(2)}) %collective-permute-start.4) | collective-permute-done | bytes 24608 | tf_op jit(solution)/shard_map/ppermute | solution.py:506
  96.1 2.6 %collective-permute-start.6 = (bf16[4,176,256]{2,1,0:T(8,128)(2,1)}, bf16[4,176,256]{2,1,0:T(8,128)(2,1)S(1)}, u32[]{:S(2)}, u32[]{:S(2)}) collective-permute-start(bf16[4,176,256]{2,1,0:T(8,128)(2,1)} %get-tuple-element.23.w0_ref), channel_id=1, source_target_pairs={{0,32},{32,64},{64,96},{96,128},{128,160},{160,192},{192,224},{224... | collective-permute-start | bytes 1081352 | tf_op jit(solution)/shard_map/ppermute | solution.py:506
  98.6 3.9 %collective-permute-start.5 = (bf16[4,176,256]{2,1,0:T(8,128)(2,1)}, bf16[4,176,256]{2,1,0:T(8,128)(2,1)S(1)}, u32[]{:S(2)}, u32[]{:S(2)}) collective-permute-start(bf16[4,176,256]{2,1,0:T(8,128)(2,1)} %get-tuple-element.23.w0_ref), channel_id=1, source_target_pairs={{0,480},{32,0},{64,32},{96,64},{128,96},{160,128},{192,160},{224,1... | collective-permute-start | bytes 1081352 | tf_op jit(solution)/shard_map/ppermute | solution.py:506
  104.5 4.3 %collective-permute-start.8 = (bf16[2,176,256]{2,1,0:T(8,128)(2,1)}, bf16[2,176,256]{2,1,0:T(8,128)(2,1)}, u32[]{:S(2)}, u32[]{:S(2)}) collective-permute-start(bf16[2,176,256]{2,1,0:T(8,128)(2,1)} %get-tuple-element.25), channel_id=1, source_target_pairs={{0,64},{32,96},{64,128},{96,160},{128,192},{160,224},{192,256},{22... | collective-permute-start | bytes 540680 | tf_op jit(solution)/shard_map/ppermute | solution.py:506
  110.6 3.4 %collective-permute-done.7.low_ref = bf16[2,176,256]{2,1,0:T(8,128)(2,1)} collective-permute-done((bf16[2,176,256]{2,1,0:T(8,128)(2,1)}, bf16[2,176,256]{2,1,0:T(8,128)(2,1)}, u32[]{:S(2)}, u32[]{:S(2)}) %collective-permute-start.7) | collective-permute-done | bytes 180256 | tf_op jit(solution)/shard_map/ppermute | solution.py:506
  115.7 6.4 %project.1 = (bf16[4,4,2,128,128]{4,3,2,1,0:T(8,128)(2,1)}, bf16[4,2,128,128]{3,2,1,0:T(8,128)(2,1)}, bf16[2,128,128]{2,1,0:T(8,128)(2,1)}, f32[2,8,128]{2,1,0:T...) custom-call(s32[4]{0:T(128)} %pad_add_fusion.place_ref, bf16[4,4,136,512]{3,2,1,0:T(8,128)(2,1)} %bitcast.27, ...), custom_call_target="tpu_custom_call" | custom-call | tf_op jit(solution)/shard_map/project/pallas_call | solution.py:573
  122.1 14.2 %all_to_all.27.qk_ref = bf16[4,1024,128]{2,1,0:T(8,128)(2,1)} all-to-all(bf16[4,1024,128]{2,1,0:T(8,128)(2,1)} %bitcast.30), channel_id=1, replica_groups=mesh['zh'=4,'zl'=4,'x'=4,'c'=2,'tp'=4] {'x'}, dimensions={0} | all-to-all | bytes 2097152 | tf_op jit(solution)/shard_map/all_to_all | solution.py:24
  136.3 3.7 %slab_state.1 = (bf16[16,72,256]{2,1,0:T(8,128)(2,1)}, bf16[1024,256]{1,0:T(8,128)(2,1)}, bf16[1024,256]{1,0:T(8,128)(2,1)}) custom-call(bf16[4,1024,128]{2,1,0:T(8,128)(2,1)} %all_to_all.27.qk_ref, bf16[1024,128]{1,0:T(8,128)(2,1)} %bitcast.31, f32[2,8,128]{2,1,0:T(8,128)} %get-tuple-element.28.gate_ref, bf16[2,128,128]{2,1,0:T(8,128)(2,1)} %get-tuple-element.29.glu_ref), custom_call_target="tpu_custom_call" | custom-call | tf_op jit(solution)/shard_map/slab_state/pallas_call | solution.py:614
  140.0 13.8 %all-to-all-start.3 = ((bf16[16,72,256]{2,1,0:T(8,128)(2,1)}), bf16[16,72,256]{2,1,0:T(8,128)(2,1)S(1)}, u32[]{:S(2)}, u32[]{:S(2)}) async-start(bf16[16,72,256]{2,1,0:T(8,128)(2,1)} %get-tuple-element.30), calls=%async_computation.3 | async-start | bytes 1179648 | tf_op jit(solution)/shard_map/all_to_all | solution.py:24
  153.9 2.9 %collective-permute-start.11 = (bf16[4,16,768]{2,1,0:T(8,128)(2,1)S(1)}, bf16[4,16,768]{2,1,0:T(8,128)(2,1)S(1)}, u32[]{:S(2)}, u32[]{:S(2)}) collective-permute-start(bf16[4,16,768]{2,1,0:T(8,128)(2,1)S(1)} %get-tuple-element.38), channel_id=1, source_target_pairs={{0,3},{1,0},{2,1},{3,2},{4,7},{5,4},{6,5},{7,6},{8,11},{9,8},{10,9... | collective-permute-start | bytes 294920 | tf_op jit(solution)/shard_map/ppermute | solution.py:591
  156.8 2.9 %collective-permute-start.10 = (bf16[4,16,768]{2,1,0:T(8,128)(2,1)S(1)}, bf16[4,16,768]{2,1,0:T(8,128)(2,1)S(1)}, u32[]{:S(2)}, u32[]{:S(2)}) collective-permute-start(bf16[4,16,768]{2,1,0:T(8,128)(2,1)S(1)} %get-tuple-element.39), channel_id=1, source_target_pairs={{0,2},{1,3},{2,0},{3,1},{4,6},{5,7},{6,4},{7,5},{8,10},{9,11},{10,... | collective-permute-start | bytes 294920 | tf_op jit(solution)/shard_map/ppermute | solution.py:591
  163.7 3.0 %collective-permute-done.9 = bf16[4,16,768]{2,1,0:T(8,128)(2,1)S(1)} collective-permute-done((bf16[4,16,768]{2,1,0:T(8,128)(2,1)S(1)}, bf16[4,16,768]{2,1,0:T(8,128)(2,1)S(1)}, u32[]{:S(2)}, u32[]{:S(2)}) %collective-permute-start.9) | collective-permute-done | bytes 98336 | tf_op jit(solution)/shard_map/ppermute | solution.py:591
  168.9 3.7 %collective-permute-start.13 = (bf16[4,4,16,768]{3,2,1,0:T(8,128)(2,1)S(1)}, bf16[4,4,16,768]{3,2,1,0:T(8,128)(2,1)S(1)}, u32[]{:S(2)}, u32[]{:S(2)}) collective-permute-start(bf16[4,4,16,768]{3,2,1,0:T(8,128)(2,1)S(1)} %pad_maximum_fusion.refs_0_), channel_id=1, source_target_pairs={{0,16},{8,24},{16,0},{24,8},{1,17},{9,25},{17,1},{25,9},{2,18},{10... | collective-permute-start | bytes 1179656 | tf_op jit(solution)/shard_map/ppermute | solution.py:596
  175.2 7.2 %local.1 = (f32[1024,128]{1,0:T(8,128)}, f32[256,128]{1,0:T(8,128)}) custom-call(s32[4]{0:T(128)} %pad_add_fusion.place_ref, bf16[1024,256]{1,0:T(8,128)(2,1)} %get-tuple-element.31.q_ref, bf16[1024,256]{1,0:T(8,128)(2,1)} %get-tuple-element.32.k_ref, bf16[1024,128]{1,0:T(8,128)(2,1)} %bitcast.32, f32[2,8,128]{2,1,0:T(8,128)} %get-tuple-element.28.gate_ref, ...), custom_call_target="tpu_custom_call" | custom-call | tf_op jit(solution)/shard_map/local/pallas_call | solution.py:627
  183.2 4.4 %cell.1 = bf16[4,2,4,96,128]{4,3,2,1,0:T(8,128)(2,1)} custom-call(s32[4]{0:T(128)} %pad_add_fusion.place_ref, bf16[16,72,256]{2,1,0:T(8,128)(2,1)} %copy-done.2, bf16[1024,256]{1,0:T(8,128)(2,1)} %get-tuple-element.31.q_ref, f32[1024,128]{1,0:T(8,128)} %get-tuple-element.33.local_ref, f32[256,128]{1,0:T(8,128)} %get-tuple-element.34.conv_ref, ...), custom_call_target="tpu_custom_call" | custom-call | tf_op jit(solution)/shard_map/cell/pallas_call | solution.py:636
  187.6 9.6 %all-to-all-start.4 = ((bf16[32,96,128]{2,1,0:T(8,128)(2,1)}), bf16[32,96,128]{2,1,0:T(8,128)(2,1)S(1)}, u32[]{:S(2)}, u32[]{:S(2)}) async-start(bf16[32,96,128]{2,1,0:T(8,128)(2,1)} %bitcast.28), calls=%async_computation.4 | async-start | bytes 1572864 | tf_op jit(solution)/shard_map/all_to_all | solution.py:24
  207.5 3.7 %assemble.1.weight_ref = bf16[4,4,4,2,16,768]{5,4,3,2,1,0:T(8,128)(2,1)} custom-call(s32[4]{0:T(128)} %pad_add_fusion.place_ref, bf16[4,4,16,768]{3,2,1,0:T(8,128)(2,1)} %copy-done.3, bf16[4,4,16,768]{3,2,1,0:T(8,128)(2,1)} %copy-done.6, bf16[4,4,16,768]{3,2,1,0:T(8,128)(2,1)} %copy-done.5, bf16[4,4,16,768]{3,2,1,0:T(8,128)(2,1)} %copy-done.4, ...), custom_call_target="tpu_custom_call" | custom-call | tf_op jit(solution)/shard_map/assemble/pallas_call | solution.py:647
  212.1 5.3 %finish.1 = bf16[128,512]{1,0:T(8,128)(2,1)} custom-call(bf16[4,2,4,96,128]{4,3,2,1,0:T(8,128)(2,1)} %bitcast.29, bf16[4,4,4,2,16,768]{5,4,3,2,1,0:T(8,128)(2,1)} %assemble.1.weight_ref, f32[4,8,128]{2,1,0:T(8,128)} %get-tuple-element.36.gain_ref), custom_call_target="tpu_custom_call" | custom-call | tf_op jit(solution)/shard_map/finish/pallas_call | solution.py:648
  (78 shorter events, 37.2 us)
Async XLA Ops:
  3.7 105.0 %copy-start.18 = (bf16[2048,2]{0,1:T(2,128)(2,1)S(1)}, bf16[2048,2]{0,1:T(2,128)(2,1)}, u32[]{:S(2)}) copy-start(bf16[2048,2]{0,1:T(2,128)(2,1)} %param.24) | copy-start | bytes 24580
  3.8 105.0 %copy-start.19 = (bf16[2048,2]{0,1:T(2,128)(2,1)S(1)}, bf16[2048,2]{0,1:T(2,128)(2,1)}, u32[]{:S(2)}) copy-start(bf16[2048,2]{0,1:T(2,128)(2,1)} %param.23) | copy-start | bytes 24580
  38.0 76.8 %copy-start = (bf16[16,136,512]{2,1,0:T(8,128)(2,1)}, bf16[16,136,512]{2,1,0:T(8,128)(2,1)S(1)}, u32[]{:S(2)}) copy-start(bf16[16,136,512]{2,1,0:T(8,128)(2,1)S(1)} %all_to_all.25) | copy-start | bytes 6684676
  38.0 76.8 %collective-permute-start = (bf16[4,4,136,512]{3,2,1,0:T(8,128)(2,1)S(1)}, bf16[4,4,136,512]{3,2,1,0:T(8,128)(2,1)}, u32[]{:S(2)}, u32[]{:S(2)}) collective-permute-start(bf16[4,4,136,512]{3,2,1,0:T(8,128)(2,1)S(1)} %bitcast.26), channel_id=1, source_target_pairs={{0,4},{4,0},{1,5},{5,1},{2,6},{6,2},{3,7},{7,3},{8,12},{12,8},{9,1... | collective-permute-start | bytes 6684680 | tf_op jit(solution)/shard_map/ppermute | solution.py:28
  54.3 38.5 %collective-permute-start.2 = (bf16[176,256]{1,0:T(8,128)(2,1)S(1)}, bf16[176,256]{1,0:T(8,128)(2,1)S(1)}, u32[]{:S(2)}, u32[]{:S(2)}) collective-permute-start(bf16[176,256]{1,0:T(8,128)(2,1)S(1)} %pad_maximum_fusion.1.mine_ref), channel_id=1, source_target_pairs={{0,384},{32,416},{64,448},{96,480},{128,0},{160,32},{192,64},{224,... | collective-permute-start | bytes 270344 | tf_op jit(solution)/shard_map/ppermute | solution.py:506
  67.0 25.8 %collective-permute-start.1 = (bf16[176,256]{1,0:T(8,128)(2,1)S(1)}, bf16[176,256]{1,0:T(8,128)(2,1)S(1)}, u32[]{:S(2)}, u32[]{:S(2)}) collective-permute-start(bf16[176,256]{1,0:T(8,128)(2,1)S(1)} %pad_maximum_fusion.1.mine_ref), channel_id=1, source_target_pairs={{0,128},{32,160},{64,192},{96,224},{128,256},{160,288},{192,320},{... | collective-permute-start | bytes 270344 | tf_op jit(solution)/shard_map/ppermute | solution.py:506
  69.0 23.8 %collective-permute-start.3 = (bf16[128,256]{1,0:T(8,128)(2,1)S(1)}, bf16[128,256]{1,0:T(8,128)(2,1)S(1)}, u32[]{:S(2)}, u32[]{:S(2)}) collective-permute-start(bf16[128,256]{1,0:T(8,128)(2,1)S(1)} %bitcast.34), channel_id=1, source_target_pairs={{0,256},{32,288},{64,320},{96,352},{128,384},{160,416},{192,448},{... | collective-permute-start | bytes 196616 | tf_op jit(solution)/shard_map/ppermute | solution.py:506
  79.2 13.6 %collective-permute-start.4 = (bf16[48,256]{1,0:T(8,128)(2,1)}, bf16[48,256]{1,0:T(8,128)(2,1)S(1)}, u32[]{:S(2)}, u32[]{:S(2)}) collective-permute-start(bf16[48,256]{1,0:T(8,128)(2,1)} %get-tuple-element.22), channel_id=1, source_target_pairs={{0,256},{32,288},{64,320},{96,352},{128,384},{160,416},{192,448},{... | collective-permute-start | bytes 73736 | tf_op jit(solution)/shard_map/ppermute | solution.py:506
  96.1 18.8 %collective-permute-start.6 = (bf16[4,176,256]{2,1,0:T(8,128)(2,1)}, bf16[4,176,256]{2,1,0:T(8,128)(2,1)S(1)}, u32[]{:S(2)}, u32[]{:S(2)}) collective-permute-start(bf16[4,176,256]{2,1,0:T(8,128)(2,1)} %get-tuple-element.23.w0_ref), channel_id=1, source_target_pairs={{0,32},{32,64},{64,96},{96,128},{128,160},{160,192},{192,224},{224... | collective-permute-start | bytes 1081352 | tf_op jit(solution)/shard_map/ppermute | solution.py:506
  98.6 16.2 %collective-permute-start.5 = (bf16[4,176,256]{2,1,0:T(8,128)(2,1)}, bf16[4,176,256]{2,1,0:T(8,128)(2,1)S(1)}, u32[]{:S(2)}, u32[]{:S(2)}) collective-permute-start(bf16[4,176,256]{2,1,0:T(8,128)(2,1)} %get-tuple-element.23.w0_ref), channel_id=1, source_target_pairs={{0,480},{32,0},{64,32},{96,64},{128,96},{160,128},{192,160},{224,1... | collective-permute-start | bytes 1081352 | tf_op jit(solution)/shard_map/ppermute | solution.py:506
  102.6 11.5 %collective-permute-start.7 = (bf16[2,176,256]{2,1,0:T(8,128)(2,1)}, bf16[2,176,256]{2,1,0:T(8,128)(2,1)}, u32[]{:S(2)}, u32[]{:S(2)}) collective-permute-start(bf16[2,176,256]{2,1,0:T(8,128)(2,1)} %get-tuple-element.24), channel_id=1, source_target_pairs={{0,448},{32,480},{64,0},{96,32},{128,64},{160,96},{192,128},{224,1... | collective-permute-start | bytes 540680 | tf_op jit(solution)/shard_map/ppermute | solution.py:506
  104.5 10.3 %collective-permute-start.8 = (bf16[2,176,256]{2,1,0:T(8,128)(2,1)}, bf16[2,176,256]{2,1,0:T(8,128)(2,1)}, u32[]{:S(2)}, u32[]{:S(2)}) collective-permute-start(bf16[2,176,256]{2,1,0:T(8,128)(2,1)} %get-tuple-element.25), channel_id=1, source_target_pairs={{0,64},{32,96},{64,128},{96,160},{128,192},{160,224},{192,256},{22... | collective-permute-start | bytes 540680 | tf_op jit(solution)/shard_map/ppermute | solution.py:506
  140.0 42.3 %all-to-all-start.3 = ((bf16[16,72,256]{2,1,0:T(8,128)(2,1)}), bf16[16,72,256]{2,1,0:T(8,128)(2,1)S(1)}, u32[]{:S(2)}, u32[]{:S(2)}) async-start(bf16[16,72,256]{2,1,0:T(8,128)(2,1)} %get-tuple-element.30), calls=%async_computation.3 | async-start | bytes 1179648 | tf_op jit(solution)/shard_map/all_to_all | solution.py:24
  153.9 7.9 %collective-permute-start.11 = (bf16[4,16,768]{2,1,0:T(8,128)(2,1)S(1)}, bf16[4,16,768]{2,1,0:T(8,128)(2,1)S(1)}, u32[]{:S(2)}, u32[]{:S(2)}) collective-permute-start(bf16[4,16,768]{2,1,0:T(8,128)(2,1)S(1)} %get-tuple-element.38), channel_id=1, source_target_pairs={{0,3},{1,0},{2,1},{3,2},{4,7},{5,4},{6,5},{7,6},{8,11},{9,8},{10,9... | collective-permute-start | bytes 294920 | tf_op jit(solution)/shard_map/ppermute | solution.py:591
  156.8 6.9 %collective-permute-start.10 = (bf16[4,16,768]{2,1,0:T(8,128)(2,1)S(1)}, bf16[4,16,768]{2,1,0:T(8,128)(2,1)S(1)}, u32[]{:S(2)}, u32[]{:S(2)}) collective-permute-start(bf16[4,16,768]{2,1,0:T(8,128)(2,1)S(1)} %get-tuple-element.39), channel_id=1, source_target_pairs={{0,2},{1,3},{2,0},{3,1},{4,6},{5,7},{6,4},{7,5},{8,10},{9,11},{10,... | collective-permute-start | bytes 294920 | tf_op jit(solution)/shard_map/ppermute | solution.py:591
  159.7 7.0 %collective-permute-start.9 = (bf16[4,16,768]{2,1,0:T(8,128)(2,1)S(1)}, bf16[4,16,768]{2,1,0:T(8,128)(2,1)S(1)}, u32[]{:S(2)}, u32[]{:S(2)}) collective-permute-start(bf16[4,16,768]{2,1,0:T(8,128)(2,1)S(1)} %get-tuple-element.40), channel_id=1, source_target_pairs={{0,1},{1,2},{2,3},{3,0},{4,5},{5,6},{6,7},{7,4},{8,9},{9,10},{10,1... | collective-permute-start | bytes 294920 | tf_op jit(solution)/shard_map/ppermute | solution.py:591
  166.7 32.6 %collective-permute-start.14 = (bf16[4,4,16,768]{3,2,1,0:T(8,128)(2,1)S(1)}, bf16[4,4,16,768]{3,2,1,0:T(8,128)(2,1)S(1)}, u32[]{:S(2)}, u32[]{:S(2)}) collective-permute-start(bf16[4,4,16,768]{3,2,1,0:T(8,128)(2,1)S(1)} %pad_maximum_fusion.refs_0_), channel_id=1, source_target_pairs={{0,8},{8,16},{16,24},{24,0},{1,9},{9,17},{17,25},{25,1},{2,10},{10... | collective-permute-start | bytes 1179656 | tf_op jit(solution)/shard_map/ppermute | solution.py:596
  168.9 32.7 %collective-permute-start.13 = (bf16[4,4,16,768]{3,2,1,0:T(8,128)(2,1)S(1)}, bf16[4,4,16,768]{3,2,1,0:T(8,128)(2,1)S(1)}, u32[]{:S(2)}, u32[]{:S(2)}) collective-permute-start(bf16[4,4,16,768]{3,2,1,0:T(8,128)(2,1)S(1)} %pad_maximum_fusion.refs_0_), channel_id=1, source_target_pairs={{0,16},{8,24},{16,0},{24,8},{1,17},{9,25},{17,1},{25,9},{2,18},{10... | collective-permute-start | bytes 1179656 | tf_op jit(solution)/shard_map/ppermute | solution.py:596
  172.6 31.1 %collective-permute-start.12 = (bf16[4,4,16,768]{3,2,1,0:T(8,128)(2,1)S(1)}, bf16[4,4,16,768]{3,2,1,0:T(8,128)(2,1)S(1)}, u32[]{:S(2)}, u32[]{:S(2)}) collective-permute-start(bf16[4,4,16,768]{3,2,1,0:T(8,128)(2,1)S(1)} %pad_maximum_fusion.refs_0_), channel_id=1, source_target_pairs={{0,24},{8,0},{16,8},{24,16},{1,25},{9,1},{17,9},{25,17},{2,26},{10... | collective-permute-start | bytes 1179656 | tf_op jit(solution)/shard_map/ppermute | solution.py:596
  187.6 23.6 %all-to-all-start.4 = ((bf16[32,96,128]{2,1,0:T(8,128)(2,1)}), bf16[32,96,128]{2,1,0:T(8,128)(2,1)S(1)}, u32[]{:S(2)}, u32[]{:S(2)}) async-start(bf16[32,96,128]{2,1,0:T(8,128)(2,1)} %bitcast.28), calls=%async_computation.4 | async-start | bytes 1572864 | tf_op jit(solution)/shard_map/all_to_all | solution.py:24
  197.2 8.8 %collective-permute-start.15 = (bf16[4,4,16,768]{3,2,1,0:T(8,128)(2,1)S(1)}, bf16[4,4,16,768]{3,2,1,0:T(8,128)(2,1)S(1)}, u32[]{:S(2)}, u32[]{:S(2)}) collective-permute-start(bf16[4,4,16,768]{3,2,1,0:T(8,128)(2,1)S(1)} %pad_maximum_fusion.refs_0_), channel_id=1, source_target_pairs={{0,4},{4,0},{1,5},{5,1},{2,6},{6,2},{3,7},{7,3},{8,12},{12,8},{9,1... | collective-permute-start | bytes 1179656 | tf_op jit(solution)/shard_map/ppermute | solution.py:28
  199.4 6.6 %collective-permute-start.18 = (bf16[4,4,16,768]{3,2,1,0:T(8,128)(2,1)S(1)}, bf16[4,4,16,768]{3,2,1,0:T(8,128)(2,1)S(1)}, u32[]{:S(2)}, u32[]{:S(2)}) collective-permute-start(bf16[4,4,16,768]{3,2,1,0:T(8,128)(2,1)S(1)} %collective-permute-done.14.refs_3_), channel_id=1, source_target_pairs={{0,4},{4,0},{1,5},{5,1},{2,6},{6,2},{3,7},{7,3},{8,12},{12,8},{9,1... | collective-permute-start | bytes 1179656 | tf_op jit(solution)/shard_map/ppermute | solution.py:28
  201.6 4.4 %collective-permute-start.17 = (bf16[4,4,16,768]{3,2,1,0:T(8,128)(2,1)S(1)}, bf16[4,4,16,768]{3,2,1,0:T(8,128)(2,1)S(1)}, u32[]{:S(2)}, u32[]{:S(2)}) collective-permute-start(bf16[4,4,16,768]{3,2,1,0:T(8,128)(2,1)S(1)} %collective-permute-done.13.refs_2_), channel_id=1, source_target_pairs={{0,4},{4,0},{1,5},{5,1},{2,6},{6,2},{3,7},{7,3},{8,12},{12,8},{9,1... | collective-permute-start | bytes 1179656 | tf_op jit(solution)/shard_map/ppermute | solution.py:28
  203.7 3.7 %collective-permute-start.16 = (bf16[4,4,16,768]{3,2,1,0:T(8,128)(2,1)S(1)}, bf16[4,4,16,768]{3,2,1,0:T(8,128)(2,1)}, u32[]{:S(2)}, u32[]{:S(2)}) collective-permute-start(bf16[4,4,16,768]{3,2,1,0:T(8,128)(2,1)S(1)} %collective-permute-done.12.refs_1_), channel_id=1, source_target_pairs={{0,4},{4,0},{1,5},{5,1},{2,6},{6,2},{3,7},{7,3},{8,12},{12,8},{9,1... | collective-permute-start | bytes 1179656 | tf_op jit(solution)/shard_map/ppermute | solution.py:28
  (17 other events, 128.4 us)

commit v8 on v7

--- a/solution.py
+++ b/solution.py
@@ -308,6 +308,49 @@
     return total
 
 
+def with_logs(kept, width, level, total):
+    row = lax.broadcasted_iota(jnp.int32, kept.shape, 0)
+    lane = lax.broadcasted_iota(jnp.int32, kept.shape, 1)
+    for at, value in ((0, level), (3, total)):
+        for k, part in enumerate(three_parts(value)):
+            kept = jnp.where((row == width + 1) & (lane == at + k), part, kept)
+    return kept
+
+
+def read_logs(block, width):
+    line = block[width + 1 : width + 2, :128].astype(F32)
+    level = line[:, 0:1] + line[:, 1:2] + line[:, 2:3]
+    return level, line[:, 3:4] + line[:, 4:5] + line[:, 5:6]
+
+
+def merged(blocks, passed, width):
+    acc = jnp.zeros((1, 1), F32)
+    logs = []
+    for block, use in zip(blocks[::-1], passed[::-1]):
+        level, total = read_logs(block, width)
+        logs.insert(0, jnp.where(use, level + acc, LOW))
+        acc = acc + jnp.where(use, total, 0.0)
+    level = logs[0]
+    for log in logs[1:]:
+        level = jnp.maximum(level, log)
+    state = jnp.zeros(blocks[0].shape, F32)
+    for block, use, log in zip(blocks, passed, logs):
+        state = state + jnp.where(use, jnp.exp(log - level), 0.0) * block.astype(F32)
+    return state, level, acc
+
+
+def group_kernel(in_ref, out_ref):
+    members, rows, _ = in_ref.shape
+    width = rows - 8
+    blocks = [in_ref[j] for j in range(members)]
+    state, level, total = merged(blocks, [True] * members, width)
+    last = blocks[-1].astype(F32)
+    kept = jnp.concatenate([state[: width + 2], last[width + 2 :]], axis=0)
+    kept = with_logs(kept, width, level, total).astype(BF16)
+    for j in range(out_ref.shape[0]):
+        out_ref[j] = kept
+
+
 def slab_kernel(
     qk_ref, v_ref, gate_ref, glu_ref, out_ref, q_ref, k_ref,
 ):
@@ -333,14 +376,7 @@
         state = state + dot(v_ref[r * length : (r + 1) * length], scaled, TN)
     rows, head_lanes = out_ref.shape[1], out_ref.shape[2]
     kept = state[:rows]
-    row = lax.broadcasted_iota(jnp.int32, kept.shape, 0)
-    lane = lax.broadcasted_iota(jnp.int32, kept.shape, 1)
-    for at, value in ((0, level), (3, total)):
-        high = value.astype(BF16).astype(F32)
-        mid = (value - high).astype(BF16).astype(F32)
-        low = value - high - mid
-        for k, part in enumerate((high, mid, low)):
-            kept = jnp.where((row == width + 1) & (lane == at + k), part, kept)
+    kept = with_logs(kept, width, level, total)
     chan = glu_ref.shape[2] // qk_ref.shape[0]
     hold = HOLD
     tail = glu_ref[glu_ref.shape[0] - 1, length - hold :].astype(F32)[:, glu_ref.shape[2] - chan :]
@@ -410,35 +446,26 @@
         level = new_level
 
 
-def cell_kernel(place_ref, in_ref, q_ref, local_ref, conv_ref, taps_ref, out_ref):
+def cell_kernel(place_ref, far_ref, in_ref, q_ref, local_ref, conv_ref, taps_ref, out_ref):
     members, rows, head = in_ref.shape
+    groups = far_ref.shape[0]
     nx, nc, ny, _, lanes = out_ref.shape
     width, chan = lanes // 2, lanes // nx
     length = q_ref.shape[0] // (nx * nc)
     scale = head ** (-0.5)
     place = place_ref[0]
-    acc = jnp.zeros((1, 1), F32)
-    logs = [None] * members
-    for j in range(members - 1, -1, -1):
-        line = in_ref[j, width + 1 : width + 2, :128].astype(F32)
-        level_j = line[:, 0:1] + line[:, 1:2] + line[:, 2:3]
-        total_j = line[:, 3:4] + line[:, 4:5] + line[:, 5:6]
-        before = j < place
-        logs[j] = jnp.where(before, level_j + acc, LOW)
-        acc = acc + jnp.where(before, total_j, 0.0)
-    level = logs[0]
-    for j in range(1, members):
-        level = jnp.maximum(level, logs[j])
-    state = jnp.zeros((rows, head), F32)
-    for j in range(members):
-        weight = jnp.where(j < place, jnp.exp(logs[j] - level), 0.0)
-        state = state + weight * in_ref[j].astype(F32)
+    at_far, at_close = lax.div(place, members), lax.rem(place, members)
+    blocks = [far_ref[j] for j in range(groups)] + [in_ref[j] for j in range(members)]
+    passed = [j < at_far for j in range(groups)] + [j < at_close for j in range(members)]
+    state, level, _ = merged(blocks, passed, width)
     state = jnp.concatenate([state, jnp.zeros((lanes - rows, head), F32)], axis=0).astype(BF16)
 
     group = head // chan
     each = HOLD // group
-    last_rows = in_ref[jnp.maximum(place - 1, 0), width : width + 8].astype(F32)
-    last_rows = jnp.where(place > 0, last_rows[2 : 2 + each], 0.0)
+    near_rows = in_ref[jnp.maximum(at_close - 1, 0), width : width + 8].astype(F32)
+    far_rows = far_ref[jnp.maximum(at_far - 1, 0), width : width + 8].astype(F32)
+    last_rows = jnp.where(at_close > 0, near_rows, jnp.where(at_far > 0, far_rows, 0.0))
+    last_rows = last_rows[2 : 2 + each]
     prior = jnp.concatenate([last_rows[:, g * chan : (g + 1) * chan] for g in range(group)], axis=0)
     prior = jnp.concatenate([prior, jnp.zeros((HOLD, lanes - chan), F32)], axis=1)
     weights = tap_rows(taps_ref, place_ref[1], place_ref[3], nx, lanes)
@@ -447,8 +474,8 @@
     for r in range(nx * nc):
         here = slice(r * length, (r + 1) * length)
         local = local_ref[here]
-        top_here, passed = local[:, width + 1 : width + 2], local[:, width + 2 : width + 3]
-        carried = passed + level
+        top_here, since = local[:, width + 1 : width + 2], local[:, width + 2 : width + 3]
+        carried = since + level
         top = jnp.maximum(carried, top_here)
         local_weight = jnp.exp(top_here - top)
         carried_weight = jnp.exp(carried - top) * scale
@@ -602,7 +629,7 @@
     call_slab = pl.pallas_call(
         slab_kernel,
         out_shape=(
-            jax.ShapeDtypeStruct((members, state_rows, head), BF16),
+            jax.ShapeDtypeStruct((nzl, state_rows, head), BF16),
             jax.ShapeDtypeStruct((slab, head), BF16),
             jax.ShapeDtypeStruct((slab, head), BF16),
         ),
@@ -612,7 +639,17 @@
         name="slab_state",
     )
     states, query, key = call_slab(all_qk, value, gates, packed)
-    states = exchange(states, Z)
+    states = exchange(states, "zl")
+    call_group = pl.pallas_call(
+        group_kernel,
+        out_shape=jax.ShapeDtypeStruct((nzh, state_rows, head), BF16),
+        in_specs=vmem(1),
+        out_specs=pl.BlockSpec(memory_space=pltpu.VMEM),
+        interpret=INTERPRET,
+        name="group",
+    )
+    groups = call_group(states)
+    groups = exchange(groups, "zh")
     call_local = pl.pallas_call(
         local_kernel,
         out_shape=(
@@ -628,12 +665,12 @@
     call_cell = pl.pallas_call(
         cell_kernel,
         out_shape=jax.ShapeDtypeStruct((nx, nc, ny, length // 4 * 3, 2 * width), BF16),
-        in_specs=[smem] + vmem(5),
+        in_specs=[smem] + vmem(6),
         out_specs=pl.BlockSpec(memory_space=pltpu.VMEM),
         interpret=INTERPRET,
         name="cell",
     )
-    last = call_cell(place, states, query, local, conv, conv_kernel)
+    last = call_cell(place, groups, states, query, local, conv, conv_kernel)
     arrived = exchange(last.reshape(nx * nc * ny, length // 4 * 3, -1), ("x", "c", "tp"))
     arrived = arrived.reshape(nx, nc, ny, length // 4 * 3, -1)
     call_assemble = pl.pallas_call(

time: 219 us -> 231 us (1.055)
  blocking collectives: 56.6 us -> 66.7 us
    all_to_all x3 -> x4, blocking collectives: 56.6 us -> 66.7 us  [exchange(): return lax.all_to_all(pieces, axes, split_axis=0, concat_axis=0, tiled=True)]
    pallas_call x1 -> x2, Pallas kernels: 4.43 us -> 6.06 us  [the longest x1 4.27 us: layer(): last = call_cell(place, groups, states, query, local, conv, conv_kernel)]
  transfers between devices with their start and end apart: 21 -> 21, of which waited for: 6 -> 6; matrix products, arithmetic and copies ran while one was open for 1% -> 1% of each run, Pallas kernels for 9% -> 8%
where the time goes in v8:
time: 231 us; the launch traced here: 229 us
  starting transfers between devices  95.9 us (42%)
  blocking collectives  66.7 us (29%)
  Pallas kernels  38.1 us (16%)
  waiting for transfers between devices  19.5 us (8%)
  local copies, waits for them, and re-layouts  5.75 us (2%)
  other arithmetic  2.71 us (1%)
    all_to_all x4, blocking collectives, exchange(): return lax.all_to_all(pieces, axes, split_axis=0, concat_axis=0, tiled=True)  66.7 us
    ppermute x8, starting transfers between devices, from_z(): lax.ppermute(value, Z, [(j, (j - ahead) % members) for j in range(members)])  41.3 us
    all_to_all x2, starting transfers between devices, exchange(): return lax.all_to_all(pieces, axes, split_axis=0, concat_axis=0, tiled=True)  23.8 us
    ppermute x5, starting transfers between devices, swapped(): return lax.ppermute(value, axis, [(0, 1), (1, 0)])  14.5 us
    ppermute x8, waiting for transfers between devices, from_z(): lax.ppermute(value, Z, [(j, (j - ahead) % members) for j in range(members)])  14 us
    ppermute x3, starting transfers between devices, layer(): lax.ppermute(out_part, 'x', [(j, (j - ahead) % nx) for j in range(nx)])  8.41 us
    ppermute x3, starting transfers between devices, layer(): lax.ppermute(out_part[ahead], 'tp', [(j, (j + ahead) % ny) for j in range...  7.83 us
    pallas_call x1, Pallas kernels, layer(): call_local(place, query, key, value, gates, packed, conv_kernel)  7.19 us
  transfers between devices with their start and end apart: 21, of which 6 were waited for; matrix products, arithmetic and copies ran while one was open for 1% of the time, Pallas kernels for 8%

profile of v8, /device:TPU:1, one launch (start us, length us, event | category | flops | bytes accessed | tf_op | source)
XLA Modules:
  0.0 229.2 jit_solution(7854912237638574018)
XLA Ops:
  3.8 34.3 %all_to_all.30 = bf16[16,136,512]{2,1,0:T(8,128)(2,1)S(1)} all-to-all(bf16[16,136,512]{2,1,0:T(8,128)(2,1)} %pack.1), channel_id=1, replica_groups=mesh['zh'=4,'zl'=4,'x'=4,'c'=2,'tp'=4] {'x','tp'}, dimensions={0} | all-to-all | bytes 4456448 | tf_op jit(solution)/shard_map/all_to_all | solution.py:24
  38.0 5.9 %collective-permute-start = (bf16[4,4,136,512]{3,2,1,0:T(8,128)(2,1)S(1)}, bf16[4,4,136,512]{3,2,1,0:T(8,128)(2,1)}, u32[]{:S(2)}, u32[]{:S(2)}) collective-permute-start(bf16[4,4,136,512]{3,2,1,0:T(8,128)(2,1)S(1)} %bitcast.26), channel_id=1, source_target_pairs={{0,4},{4,0},{1,5},{5,1},{2,6},{6,2},{3,7},{7,3},{8,12},{12,8},{9,1... | collective-permute-start | bytes 6684680 | tf_op jit(solution)/shard_map/ppermute | solution.py:28
  45.5 8.1 %all_to_all.31 = bf16[8,16,256]{2,1,0:T(8,128)(2,1)S(1)} all-to-all(bf16[8,16,256]{2,1,0:T(8,128)(2,1)} %bitcast.38), channel_id=1, replica_groups=mesh['zh'=4,'zl'=4,'x'=4,'c'=2,'tp'=4] {'x','c'}, dimensions={0} | all-to-all | bytes 131072 | tf_op jit(solution)/shard_map/all_to_all | solution.py:24
  54.3 12.7 %collective-permute-start.2 = (bf16[176,256]{1,0:T(8,128)(2,1)S(1)}, bf16[176,256]{1,0:T(8,128)(2,1)S(1)}, u32[]{:S(2)}, u32[]{:S(2)}) collective-permute-start(bf16[176,256]{1,0:T(8,128)(2,1)S(1)} %pad_maximum_fusion.1.mine_ref), channel_id=1, source_target_pairs={{0,384},{32,416},{64,448},{96,480},{128,0},{160,32},{192,64},{224,... | collective-permute-start | bytes 270344 | tf_op jit(solution)/shard_map/ppermute | solution.py:533
  69.0 10.3 %collective-permute-start.3 = (bf16[128,256]{1,0:T(8,128)(2,1)S(1)}, bf16[128,256]{1,0:T(8,128)(2,1)S(1)}, u32[]{:S(2)}, u32[]{:S(2)}) collective-permute-start(bf16[128,256]{1,0:T(8,128)(2,1)S(1)} %bitcast.34), channel_id=1, source_target_pairs={{0,256},{32,288},{64,320},{96,352},{128,384},{160,416},{192,448},{... | collective-permute-start | bytes 196616 | tf_op jit(solution)/shard_map/ppermute | solution.py:533
  79.2 3.7 %collective-permute-start.4 = (bf16[48,256]{1,0:T(8,128)(2,1)}, bf16[48,256]{1,0:T(8,128)(2,1)S(1)}, u32[]{:S(2)}, u32[]{:S(2)}) collective-permute-start(bf16[48,256]{1,0:T(8,128)(2,1)} %get-tuple-element.22), channel_id=1, source_target_pairs={{0,256},{32,288},{64,320},{96,352},{128,384},{160,416},{192,448},{... | collective-permute-start | bytes 73736 | tf_op jit(solution)/shard_map/ppermute | solution.py:533
  83.0 9.8 %collective-permute-done.4.rest_ref = bf16[48,256]{1,0:T(8,128)(2,1)S(1)} collective-permute-done((bf16[48,256]{1,0:T(8,128)(2,1)}, bf16[48,256]{1,0:T(8,128)(2,1)S(1)}, u32[]{:S(2)}, u32[]{:S(2)}) %collective-permute-start.4) | collective-permute-done | bytes 24608 | tf_op jit(solution)/shard_map/ppermute | solution.py:533
  98.6 3.9 %collective-permute-start.5 = (bf16[4,176,256]{2,1,0:T(8,128)(2,1)}, bf16[4,176,256]{2,1,0:T(8,128)(2,1)S(1)}, u32[]{:S(2)}, u32[]{:S(2)}) collective-permute-start(bf16[4,176,256]{2,1,0:T(8,128)(2,1)} %get-tuple-element.23.w0_ref), channel_id=1, source_target_pairs={{0,480},{32,0},{64,32},{96,64},{128,96},{160,128},{192,160},{224,1... | collective-permute-start | bytes 1081352 | tf_op jit(solution)/shard_map/ppermute | solution.py:533
  104.5 4.3 %collective-permute-start.8 = (bf16[2,176,256]{2,1,0:T(8,128)(2,1)}, bf16[2,176,256]{2,1,0:T(8,128)(2,1)}, u32[]{:S(2)}, u32[]{:S(2)}) collective-permute-start(bf16[2,176,256]{2,1,0:T(8,128)(2,1)} %get-tuple-element.25), channel_id=1, source_target_pairs={{0,64},{32,96},{64,128},{96,160},{128,192},{160,224},{192,256},{22... | collective-permute-start | bytes 540680 | tf_op jit(solution)/shard_map/ppermute | solution.py:533
  110.6 3.4 %collective-permute-done.7.low_ref = bf16[2,176,256]{2,1,0:T(8,128)(2,1)} collective-permute-done((bf16[2,176,256]{2,1,0:T(8,128)(2,1)}, bf16[2,176,256]{2,1,0:T(8,128)(2,1)}, u32[]{:S(2)}, u32[]{:S(2)}) %collective-permute-start.7) | collective-permute-done | bytes 180256 | tf_op jit(solution)/shard_map/ppermute | solution.py:533
  115.7 6.4 %project.1 = (bf16[4,4,2,128,128]{4,3,2,1,0:T(8,128)(2,1)}, bf16[4,2,128,128]{3,2,1,0:T(8,128)(2,1)}, bf16[2,128,128]{2,1,0:T(8,128)(2,1)}, f32[2,8,128]{2,1,0:T...) custom-call(s32[4]{0:T(128)} %pad_add_fusion.place_ref, bf16[4,4,136,512]{3,2,1,0:T(8,128)(2,1)} %bitcast.27, ...), custom_call_target="tpu_custom_call" | custom-call | tf_op jit(solution)/shard_map/project/pallas_call | solution.py:600
  122.1 14.2 %all_to_all.32.qk_ref = bf16[4,1024,128]{2,1,0:T(8,128)(2,1)} all-to-all(bf16[4,1024,128]{2,1,0:T(8,128)(2,1)} %bitcast.30), channel_id=1, replica_groups=mesh['zh'=4,'zl'=4,'x'=4,'c'=2,'tp'=4] {'x'}, dimensions={0} | all-to-all | bytes 2097152 | tf_op jit(solution)/shard_map/all_to_all | solution.py:24
  136.3 3.6 %slab_state.1 = (bf16[4,72,256]{2,1,0:T(8,128)(2,1)}, bf16[1024,256]{1,0:T(8,128)(2,1)}, bf16[1024,256]{1,0:T(8,128)(2,1)}) custom-call(bf16[4,1024,128]{2,1,0:T(8,128)(2,1)} %all_to_all.32.qk_ref, bf16[1024,128]{1,0:T(8,128)(2,1)} %bitcast.31, f32[2,8,128]{2,1,0:T(8,128)} %get-tuple-element.28.gate_ref, bf16[2,128,128]{2,1,0:T(8,128)(2,1)} %get-tuple-element.29.glu_ref), custom_call_target="tpu_custom_call" | custom-call | tf_op jit(solution)/shard_map/slab_state/pallas_call | solution.py:641
  139.9 10.2 %all_to_all.33.in_ref = bf16[4,72,256]{2,1,0:T(8,128)(2,1)} all-to-all(bf16[4,72,256]{2,1,0:T(8,128)(2,1)} %get-tuple-element.30), channel_id=1, replica_groups=mesh['zh'=4,'zl'=4,'x'=4,'c'=2,'tp'=4] {'zl'}, dimensions={0} | all-to-all | bytes 294912 | tf_op jit(solution)/shard_map/all_to_all | solution.py:24
  151.8 13.1 %all-to-all-start.4 = ((bf16[4,72,256]{2,1,0:T(8,128)(2,1)}), bf16[4,72,256]{2,1,0:T(8,128)(2,1)S(1)}, u32[]{:S(2)}, u32[]{:S(2)}) async-start(bf16[4,72,256]{2,1,0:T(8,128)(2,1)} %group.1), calls=%async_computation.4 | async-start | bytes 294912 | tf_op jit(solution)/shard_map/all_to_all | solution.py:24
  164.9 2.9 %collective-permute-start.11 = (bf16[4,16,768]{2,1,0:T(8,128)(2,1)S(1)}, bf16[4,16,768]{2,1,0:T(8,128)(2,1)S(1)}, u32[]{:S(2)}, u32[]{:S(2)}) collective-permute-start(bf16[4,16,768]{2,1,0:T(8,128)(2,1)S(1)} %get-tuple-element.38), channel_id=1, source_target_pairs={{0,3},{1,0},{2,1},{3,2},{4,7},{5,4},{6,5},{7,6},{8,11},{9,8},{10,9... | collective-permute-start | bytes 294920 | tf_op jit(solution)/shard_map/ppermute | solution.py:618
  167.8 2.9 %collective-permute-start.10 = (bf16[4,16,768]{2,1,0:T(8,128)(2,1)S(1)}, bf16[4,16,768]{2,1,0:T(8,128)(2,1)S(1)}, u32[]{:S(2)}, u32[]{:S(2)}) collective-permute-start(bf16[4,16,768]{2,1,0:T(8,128)(2,1)S(1)} %get-tuple-element.39), channel_id=1, source_target_pairs={{0,2},{1,3},{2,0},{3,1},{4,6},{5,7},{6,4},{7,5},{8,10},{9,11},{10,... | collective-permute-start | bytes 294920 | tf_op jit(solution)/shard_map/ppermute | solution.py:618
  174.7 2.9 %collective-permute-done.9 = bf16[4,16,768]{2,1,0:T(8,128)(2,1)S(1)} collective-permute-done((bf16[4,16,768]{2,1,0:T(8,128)(2,1)S(1)}, bf16[4,16,768]{2,1,0:T(8,128)(2,1)S(1)}, u32[]{:S(2)}, u32[]{:S(2)}) %collective-permute-start.9) | collective-permute-done | bytes 98336 | tf_op jit(solution)/shard_map/ppermute | solution.py:618
  179.9 3.7 %collective-permute-start.13 = (bf16[4,4,16,768]{3,2,1,0:T(8,128)(2,1)S(1)}, bf16[4,4,16,768]{3,2,1,0:T(8,128)(2,1)S(1)}, u32[]{:S(2)}, u32[]{:S(2)}) collective-permute-start(bf16[4,4,16,768]{3,2,1,0:T(8,128)(2,1)S(1)} %pad_maximum_fusion.refs_0_), channel_id=1, source_target_pairs={{0,16},{8,24},{16,0},{24,8},{1,17},{9,25},{17,1},{25,9},{2,18},{10... | collective-permute-start | bytes 1179656 | tf_op jit(solution)/shard_map/ppermute | solution.py:623
  186.1 7.2 %local.1 = (f32[1024,128]{1,0:T(8,128)}, f32[256,128]{1,0:T(8,128)}) custom-call(s32[4]{0:T(128)} %pad_add_fusion.place_ref, bf16[1024,256]{1,0:T(8,128)(2,1)} %get-tuple-element.31.q_ref, bf16[1024,256]{1,0:T(8,128)(2,1)} %get-tuple-element.32.k_ref, bf16[1024,128]{1,0:T(8,128)(2,1)} %bitcast.32, f32[2,8,128]{2,1,0:T(8,128)} %get-tuple-element.28.gate_ref, ...), custom_call_target="tpu_custom_call" | custom-call | tf_op jit(solution)/shard_map/local/pallas_call | solution.py:664
  194.0 4.3 %cell.1 = bf16[4,2,4,96,128]{4,3,2,1,0:T(8,128)(2,1)} custom-call(s32[4]{0:T(128)} %pad_add_fusion.place_ref, bf16[4,72,256]{2,1,0:T(8,128)(2,1)} %copy-done.3, bf16[4,72,256]{2,1,0:T(8,128)(2,1)} %all_to_all.33.in_ref, bf16[1024,256]{1,0:T(8,128)(2,1)} %get-tuple-element.31.q_ref, f32[1024,128]{1,0:T(8,128)} %get-tuple-element.33.local_ref, ...), custom_call_target="tpu_custom_call" | custom-call | tf_op jit(solution)/shard_map/cell/pallas_call | solution.py:673
  198.2 10.8 %all-to-all-start.5 = ((bf16[32,96,128]{2,1,0:T(8,128)(2,1)}), bf16[32,96,128]{2,1,0:T(8,128)(2,1)S(1)}, u32[]{:S(2)}, u32[]{:S(2)}) async-start(bf16[32,96,128]{2,1,0:T(8,128)(2,1)} %bitcast.28), calls=%async_computation.5 | async-start | bytes 1572864 | tf_op jit(solution)/shard_map/all_to_all | solution.py:24
  219.4 3.7 %assemble.1.weight_ref = bf16[4,4,4,2,16,768]{5,4,3,2,1,0:T(8,128)(2,1)} custom-call(s32[4]{0:T(128)} %pad_add_fusion.place_ref, bf16[4,4,16,768]{3,2,1,0:T(8,128)(2,1)} %copy-done.2, bf16[4,4,16,768]{3,2,1,0:T(8,128)(2,1)} %copy-done.6, bf16[4,4,16,768]{3,2,1,0:T(8,128)(2,1)} %copy-done.5, bf16[4,4,16,768]{3,2,1,0:T(8,128)(2,1)} %copy-done.4, ...), custom_call_target="tpu_custom_call" | custom-call | tf_op jit(solution)/shard_map/assemble/pallas_call | solution.py:684
  223.9 5.3 %finish.1 = bf16[128,512]{1,0:T(8,128)(2,1)} custom-call(bf16[4,2,4,96,128]{4,3,2,1,0:T(8,128)(2,1)} %bitcast.29, bf16[4,4,4,2,16,768]{5,4,3,2,1,0:T(8,128)(2,1)} %assemble.1.weight_ref, f32[4,8,128]{2,1,0:T(8,128)} %get-tuple-element.36.gain_ref), custom_call_target="tpu_custom_call" | custom-call | tf_op jit(solution)/shard_map/finish/pallas_call | solution.py:685
  (80 shorter events, 41.4 us)
Async XLA Ops:
  3.7 105.0 %copy-start.18 = (bf16[2048,2]{0,1:T(2,128)(2,1)S(1)}, bf16[2048,2]{0,1:T(2,128)(2,1)}, u32[]{:S(2)}) copy-start(bf16[2048,2]{0,1:T(2,128)(2,1)} %param.24) | copy-start | bytes 24580
  3.8 105.0 %copy-start.19 = (bf16[2048,2]{0,1:T(2,128)(2,1)S(1)}, bf16[2048,2]{0,1:T(2,128)(2,1)}, u32[]{:S(2)}) copy-start(bf16[2048,2]{0,1:T(2,128)(2,1)} %param.23) | copy-start | bytes 24580
  38.0 76.8 %copy-start = (bf16[16,136,512]{2,1,0:T(8,128)(2,1)}, bf16[16,136,512]{2,1,0:T(8,128)(2,1)S(1)}, u32[]{:S(2)}) copy-start(bf16[16,136,512]{2,1,0:T(8,128)(2,1)S(1)} %all_to_all.30) | copy-start | bytes 6684676
  38.0 76.8 %collective-permute-start = (bf16[4,4,136,512]{3,2,1,0:T(8,128)(2,1)S(1)}, bf16[4,4,136,512]{3,2,1,0:T(8,128)(2,1)}, u32[]{:S(2)}, u32[]{:S(2)}) collective-permute-start(bf16[4,4,136,512]{3,2,1,0:T(8,128)(2,1)S(1)} %bitcast.26), channel_id=1, source_target_pairs={{0,4},{4,0},{1,5},{5,1},{2,6},{6,2},{3,7},{7,3},{8,12},{12,8},{9,1... | collective-permute-start | bytes 6684680 | tf_op jit(solution)/shard_map/ppermute | solution.py:28
  54.3 38.5 %collective-permute-start.2 = (bf16[176,256]{1,0:T(8,128)(2,1)S(1)}, bf16[176,256]{1,0:T(8,128)(2,1)S(1)}, u32[]{:S(2)}, u32[]{:S(2)}) collective-permute-start(bf16[176,256]{1,0:T(8,128)(2,1)S(1)} %pad_maximum_fusion.1.mine_ref), channel_id=1, source_target_pairs={{0,384},{32,416},{64,448},{96,480},{128,0},{160,32},{192,64},{224,... | collective-permute-start | bytes 270344 | tf_op jit(solution)/shard_map/ppermute | solution.py:533
  67.0 25.8 %collective-permute-start.1 = (bf16[176,256]{1,0:T(8,128)(2,1)S(1)}, bf16[176,256]{1,0:T(8,128)(2,1)S(1)}, u32[]{:S(2)}, u32[]{:S(2)}) collective-permute-start(bf16[176,256]{1,0:T(8,128)(2,1)S(1)} %pad_maximum_fusion.1.mine_ref), channel_id=1, source_target_pairs={{0,128},{32,160},{64,192},{96,224},{128,256},{160,288},{192,320},{... | collective-permute-start | bytes 270344 | tf_op jit(solution)/shard_map/ppermute | solution.py:533
  69.0 23.8 %collective-permute-start.3 = (bf16[128,256]{1,0:T(8,128)(2,1)S(1)}, bf16[128,256]{1,0:T(8,128)(2,1)S(1)}, u32[]{:S(2)}, u32[]{:S(2)}) collective-permute-start(bf16[128,256]{1,0:T(8,128)(2,1)S(1)} %bitcast.34), channel_id=1, source_target_pairs={{0,256},{32,288},{64,320},{96,352},{128,384},{160,416},{192,448},{... | collective-permute-start | bytes 196616 | tf_op jit(solution)/shard_map/ppermute | solution.py:533
  79.2 13.6 %collective-permute-start.4 = (bf16[48,256]{1,0:T(8,128)(2,1)}, bf16[48,256]{1,0:T(8,128)(2,1)S(1)}, u32[]{:S(2)}, u32[]{:S(2)}) collective-permute-start(bf16[48,256]{1,0:T(8,128)(2,1)} %get-tuple-element.22), channel_id=1, source_target_pairs={{0,256},{32,288},{64,320},{96,352},{128,384},{160,416},{192,448},{... | collective-permute-start | bytes 73736 | tf_op jit(solution)/shard_map/ppermute | solution.py:533
  96.1 18.8 %collective-permute-start.6 = (bf16[4,176,256]{2,1,0:T(8,128)(2,1)}, bf16[4,176,256]{2,1,0:T(8,128)(2,1)S(1)}, u32[]{:S(2)}, u32[]{:S(2)}) collective-permute-start(bf16[4,176,256]{2,1,0:T(8,128)(2,1)} %get-tuple-element.23.w0_ref), channel_id=1, source_target_pairs={{0,32},{32,64},{64,96},{96,128},{128,160},{160,192},{192,224},{224... | collective-permute-start | bytes 1081352 | tf_op jit(solution)/shard_map/ppermute | solution.py:533
  98.6 16.2 %collective-permute-start.5 = (bf16[4,176,256]{2,1,0:T(8,128)(2,1)}, bf16[4,176,256]{2,1,0:T(8,128)(2,1)S(1)}, u32[]{:S(2)}, u32[]{:S(2)}) collective-permute-start(bf16[4,176,256]{2,1,0:T(8,128)(2,1)} %get-tuple-element.23.w0_ref), channel_id=1, source_target_pairs={{0,480},{32,0},{64,32},{96,64},{128,96},{160,128},{192,160},{224,1... | collective-permute-start | bytes 1081352 | tf_op jit(solution)/shard_map/ppermute | solution.py:533
  102.6 11.5 %collective-permute-start.7 = (bf16[2,176,256]{2,1,0:T(8,128)(2,1)}, bf16[2,176,256]{2,1,0:T(8,128)(2,1)}, u32[]{:S(2)}, u32[]{:S(2)}) collective-permute-start(bf16[2,176,256]{2,1,0:T(8,128)(2,1)} %get-tuple-element.24), channel_id=1, source_target_pairs={{0,448},{32,480},{64,0},{96,32},{128,64},{160,96},{192,128},{224,1... | collective-permute-start | bytes 540680 | tf_op jit(solution)/shard_map/ppermute | solution.py:533
  104.5 10.3 %collective-permute-start.8 = (bf16[2,176,256]{2,1,0:T(8,128)(2,1)}, bf16[2,176,256]{2,1,0:T(8,128)(2,1)}, u32[]{:S(2)}, u32[]{:S(2)}) collective-permute-start(bf16[2,176,256]{2,1,0:T(8,128)(2,1)} %get-tuple-element.25), channel_id=1, source_target_pairs={{0,64},{32,96},{64,128},{96,160},{128,192},{160,224},{192,256},{22... | collective-permute-start | bytes 540680 | tf_op jit(solution)/shard_map/ppermute | solution.py:533
  151.8 41.5 %all-to-all-start.4 = ((bf16[4,72,256]{2,1,0:T(8,128)(2,1)}), bf16[4,72,256]{2,1,0:T(8,128)(2,1)S(1)}, u32[]{:S(2)}, u32[]{:S(2)}) async-start(bf16[4,72,256]{2,1,0:T(8,128)(2,1)} %group.1), calls=%async_computation.4 | async-start | bytes 294912 | tf_op jit(solution)/shard_map/all_to_all | solution.py:24
  164.9 7.9 %collective-permute-start.11 = (bf16[4,16,768]{2,1,0:T(8,128)(2,1)S(1)}, bf16[4,16,768]{2,1,0:T(8,128)(2,1)S(1)}, u32[]{:S(2)}, u32[]{:S(2)}) collective-permute-start(bf16[4,16,768]{2,1,0:T(8,128)(2,1)S(1)} %get-tuple-element.38), channel_id=1, source_target_pairs={{0,3},{1,0},{2,1},{3,2},{4,7},{5,4},{6,5},{7,6},{8,11},{9,8},{10,9... | collective-permute-start | bytes 294920 | tf_op jit(solution)/shard_map/ppermute | solution.py:618
  167.8 6.9 %collective-permute-start.10 = (bf16[4,16,768]{2,1,0:T(8,128)(2,1)S(1)}, bf16[4,16,768]{2,1,0:T(8,128)(2,1)S(1)}, u32[]{:S(2)}, u32[]{:S(2)}) collective-permute-start(bf16[4,16,768]{2,1,0:T(8,128)(2,1)S(1)} %get-tuple-element.39), channel_id=1, source_target_pairs={{0,2},{1,3},{2,0},{3,1},{4,6},{5,7},{6,4},{7,5},{8,10},{9,11},{10,... | collective-permute-start | bytes 294920 | tf_op jit(solution)/shard_map/ppermute | solution.py:618
  170.7 6.9 %collective-permute-start.9 = (bf16[4,16,768]{2,1,0:T(8,128)(2,1)S(1)}, bf16[4,16,768]{2,1,0:T(8,128)(2,1)S(1)}, u32[]{:S(2)}, u32[]{:S(2)}) collective-permute-start(bf16[4,16,768]{2,1,0:T(8,128)(2,1)S(1)} %get-tuple-element.40), channel_id=1, source_target_pairs={{0,1},{1,2},{2,3},{3,0},{4,5},{5,6},{6,7},{7,4},{8,9},{9,10},{10,1... | collective-permute-start | bytes 294920 | tf_op jit(solution)/shard_map/ppermute | solution.py:618
  177.7 33.5 %collective-permute-start.14 = (bf16[4,4,16,768]{3,2,1,0:T(8,128)(2,1)S(1)}, bf16[4,4,16,768]{3,2,1,0:T(8,128)(2,1)S(1)}, u32[]{:S(2)}, u32[]{:S(2)}) collective-permute-start(bf16[4,4,16,768]{3,2,1,0:T(8,128)(2,1)S(1)} %pad_maximum_fusion.refs_0_), channel_id=1, source_target_pairs={{0,8},{8,16},{16,24},{24,0},{1,9},{9,17},{17,25},{25,1},{2,10},{10... | collective-permute-start | bytes 1179656 | tf_op jit(solution)/shard_map/ppermute | solution.py:623
  179.9 33.5 %collective-permute-start.13 = (bf16[4,4,16,768]{3,2,1,0:T(8,128)(2,1)S(1)}, bf16[4,4,16,768]{3,2,1,0:T(8,128)(2,1)S(1)}, u32[]{:S(2)}, u32[]{:S(2)}) collective-permute-start(bf16[4,4,16,768]{3,2,1,0:T(8,128)(2,1)S(1)} %pad_maximum_fusion.refs_0_), channel_id=1, source_target_pairs={{0,16},{8,24},{16,0},{24,8},{1,17},{9,25},{17,1},{25,9},{2,18},{10... | collective-permute-start | bytes 1179656 | tf_op jit(solution)/shard_map/ppermute | solution.py:623
  183.6 32.0 %collective-permute-start.12 = (bf16[4,4,16,768]{3,2,1,0:T(8,128)(2,1)S(1)}, bf16[4,4,16,768]{3,2,1,0:T(8,128)(2,1)S(1)}, u32[]{:S(2)}, u32[]{:S(2)}) collective-permute-start(bf16[4,4,16,768]{3,2,1,0:T(8,128)(2,1)S(1)} %pad_maximum_fusion.refs_0_), channel_id=1, source_target_pairs={{0,24},{8,0},{16,8},{24,16},{1,25},{9,1},{17,9},{25,17},{2,26},{10... | collective-permute-start | bytes 1179656 | tf_op jit(solution)/shard_map/ppermute | solution.py:623
  198.2 24.8 %all-to-all-start.5 = ((bf16[32,96,128]{2,1,0:T(8,128)(2,1)}), bf16[32,96,128]{2,1,0:T(8,128)(2,1)S(1)}, u32[]{:S(2)}, u32[]{:S(2)}) async-start(bf16[32,96,128]{2,1,0:T(8,128)(2,1)} %bitcast.28), calls=%async_computation.5 | async-start | bytes 1572864 | tf_op jit(solution)/shard_map/all_to_all | solution.py:24
  209.0 8.8 %collective-permute-start.15 = (bf16[4,4,16,768]{3,2,1,0:T(8,128)(2,1)S(1)}, bf16[4,4,16,768]{3,2,1,0:T(8,128)(2,1)S(1)}, u32[]{:S(2)}, u32[]{:S(2)}) collective-permute-start(bf16[4,4,16,768]{3,2,1,0:T(8,128)(2,1)S(1)} %pad_maximum_fusion.refs_0_), channel_id=1, source_target_pairs={{0,4},{4,0},{1,5},{5,1},{2,6},{6,2},{3,7},{7,3},{8,12},{12,8},{9,1... | collective-permute-start | bytes 1179656 | tf_op jit(solution)/shard_map/ppermute | solution.py:28
  211.2 6.6 %collective-permute-start.18 = (bf16[4,4,16,768]{3,2,1,0:T(8,128)(2,1)S(1)}, bf16[4,4,16,768]{3,2,1,0:T(8,128)(2,1)S(1)}, u32[]{:S(2)}, u32[]{:S(2)}) collective-permute-start(bf16[4,4,16,768]{3,2,1,0:T(8,128)(2,1)S(1)} %collective-permute-done.14.refs_3_), channel_id=1, source_target_pairs={{0,4},{4,0},{1,5},{5,1},{2,6},{6,2},{3,7},{7,3},{8,12},{12,8},{9,1... | collective-permute-start | bytes 1179656 | tf_op jit(solution)/shard_map/ppermute | solution.py:28
  213.4 4.4 %collective-permute-start.17 = (bf16[4,4,16,768]{3,2,1,0:T(8,128)(2,1)S(1)}, bf16[4,4,16,768]{3,2,1,0:T(8,128)(2,1)S(1)}, u32[]{:S(2)}, u32[]{:S(2)}) collective-permute-start(bf16[4,4,16,768]{3,2,1,0:T(8,128)(2,1)S(1)} %collective-permute-done.13.refs_2_), channel_id=1, source_target_pairs={{0,4},{4,0},{1,5},{5,1},{2,6},{6,2},{3,7},{7,3},{8,12},{12,8},{9,1... | collective-permute-start | bytes 1179656 | tf_op jit(solution)/shard_map/ppermute | solution.py:28
  215.6 3.7 %collective-permute-start.16 = (bf16[4,4,16,768]{3,2,1,0:T(8,128)(2,1)S(1)}, bf16[4,4,16,768]{3,2,1,0:T(8,128)(2,1)}, u32[]{:S(2)}, u32[]{:S(2)}) collective-permute-start(bf16[4,4,16,768]{3,2,1,0:T(8,128)(2,1)S(1)} %collective-permute-done.12.refs_1_), channel_id=1, source_target_pairs={{0,4},{4,0},{1,5},{5,1},{2,6},{6,2},{3,7},{7,3},{8,12},{12,8},{9,1... | collective-permute-start | bytes 1179656 | tf_op jit(solution)/shard_map/ppermute | solution.py:28
  (17 other events, 140.2 us)

commit v9 on v8

--- a/solution.py
+++ b/solution.py
@@ -107,18 +107,14 @@
             out_ref[x, c] = jnp.concatenate(parts, axis=1)
 
 
-def arrange_kernel(
-    before_ref, mine_ref, after_ref, main_ref, rest_ref, near_ref, low_ref, high_ref
-):
-    rows = main_ref.shape[0]
-    for refs in ((near_ref, 0), (high_ref, 0)):
-        refs[0][refs[1]] = before_ref[...]
-    for refs in ((near_ref, 1), (high_ref, 1), (low_ref, 0)):
-        refs[0][refs[1]] = mine_ref[...]
-    for refs in ((near_ref, 2), (low_ref, 1)):
-        refs[0][refs[1]] = after_ref[...]
-    near_ref[3, :rows] = main_ref[...]
-    near_ref[3, rows:] = rest_ref[...]
+def arrange_kernel(before_ref, mine_ref, after_ref, opposite_ref, near_ref, low_ref, high_ref):
+    for ref, at in ((near_ref, 0), (high_ref, 0)):
+        ref[at] = before_ref[...]
+    for ref, at in ((near_ref, 1), (high_ref, 1), (low_ref, 0)):
+        ref[at] = mine_ref[...]
+    for ref, at in ((near_ref, 2), (low_ref, 1)):
+        ref[at] = after_ref[...]
+    near_ref[3] = opposite_ref[...]
 
 
 def assemble_kernel(place_ref, *refs):
@@ -563,16 +559,10 @@
     )
     sent = call_pack(tokens, offsets, conv_norm_gain[None], memory_norm_gain[None])
     mine = exchange(pieces.reshape(nx * nc, rows, wide), ("x", "c"))
-    main = mine.reshape(nx * nc * rows, wide)
-    mine = jnp.concatenate([main, out_rows], axis=0)
+    mine = jnp.concatenate([mine.reshape(nx * nc * rows, wide), out_rows], axis=0)
     step = members // 4
-    far = [
-        from_z(mine, -step),
-        mine,
-        from_z(mine, step),
-        from_z(main, 2 * step),
-        from_z(out_rows, -2 * step),
-    ]
+    opposite = from_z(mine, 2 * step)
+    far = [from_z(mine, -step), mine, from_z(mine, step), opposite]
     own = exchange(sent, ("x", "tp")).reshape(nx, ny, length + 8, part)
     half_shape = (nzh // 2, *mine.shape)
     call_arrange = pl.pallas_call(
@@ -582,7 +572,7 @@
             jax.ShapeDtypeStruct(half_shape, BF16),
             jax.ShapeDtypeStruct(half_shape, BF16),
         ),
-        in_specs=vmem(5),
+        in_specs=vmem(4),
         out_specs=vmem(3),
         interpret=INTERPRET,
         name="arrange",

time: 231 us -> 228 us (0.987)
  starting transfers between devices: 95.9 us -> 84.9 us
  blocking collectives: 66.7 us -> 71.1 us
  waiting for transfers between devices: 19.5 us -> 23.5 us
    all_to_all x2, starting transfers between devices: 23.8 us -> 16.6 us  [exchange(): return lax.all_to_all(pieces, axes, split_axis=0, concat_axis=0, tiled=True)]
    all_to_all x4, blocking collectives: 66.7 us -> 71.1 us  [exchange(): return lax.all_to_all(pieces, axes, split_axis=0, concat_axis=0, tiled=True)]
    ppermute x8 -> x7, waiting for transfers between devices: 14 us -> 17.9 us  [from_z(): lax.ppermute(value, Z, [(j, (j - ahead) % members) for j in range(members)])]
    ppermute x8 -> x7, starting transfers between devices: 41.3 us -> 37.6 us  [from_z(): lax.ppermute(value, Z, [(j, (j - ahead) % members) for j in range(members)])]
  transfers between devices with their start and end apart: 21 -> 20, of which waited for: 6 -> 6; matrix products, arithmetic and copies ran while one was open for 1% -> 1% of each run, Pallas kernels for 8% -> 8%
where the time goes in v9:
time: 228 us; the launch traced here: 226 us
  starting transfers between devices  84.9 us (37%)
  blocking collectives  71.1 us (31%)
  Pallas kernels  38.2 us (17%)
  waiting for transfers between devices  23.5 us (10%)
  local copies, waits for them, and re-layouts  5.75 us (3%)
  other arithmetic  2.66 us (1%)
    all_to_all x4, blocking collectives, exchange(): return lax.all_to_all(pieces, axes, split_axis=0, concat_axis=0, tiled=True)  71.1 us
    ppermute x7, starting transfers between devices, from_z(): lax.ppermute(value, Z, [(j, (j - ahead) % members) for j in range(members)])  37.6 us
    ppermute x7, waiting for transfers between devices, from_z(): lax.ppermute(value, Z, [(j, (j - ahead) % members) for j in range(members)])  17.9 us
    all_to_all x2, starting transfers between devices, exchange(): return lax.all_to_all(pieces, axes, split_axis=0, concat_axis=0, tiled=True)  16.6 us
    ppermute x5, starting transfers between devices, swapped(): return lax.ppermute(value, axis, [(0, 1), (1, 0)])  14.5 us
    ppermute x3, starting transfers between devices, layer(): lax.ppermute(out_part, 'x', [(j, (j - ahead) % nx) for j in range(nx)])  8.41 us
    ppermute x3, starting transfers between devices, layer(): lax.ppermute(out_part[ahead], 'tp', [(j, (j + ahead) % ny) for j in range...  7.83 us
    pallas_call x1, Pallas kernels, layer(): call_local(place, query, key, value, gates, packed, conv_kernel)  7.2 us
  transfers between devices with their start and end apart: 20, of which 6 were waited for; matrix products, arithmetic and copies ran while one was open for 1% of the time, Pallas kernels for 8%

profile of v9, /device:TPU:1, one launch (start us, length us, event | category | flops | bytes accessed | tf_op | source)
XLA Modules:
  0.0 226.5 jit_solution(4972378792944815592)
XLA Ops:
  3.7 34.3 %all_to_all.30 = bf16[16,136,512]{2,1,0:T(8,128)(2,1)S(1)} all-to-all(bf16[16,136,512]{2,1,0:T(8,128)(2,1)} %pack.1), channel_id=1, replica_groups=mesh['zh'=4,'zl'=4,'x'=4,'c'=2,'tp'=4] {'x','tp'}, dimensions={0} | all-to-all | bytes 4456448 | tf_op jit(solution)/shard_map/all_to_all | solution.py:24
  38.0 5.9 %collective-permute-start = (bf16[4,4,136,512]{3,2,1,0:T(8,128)(2,1)S(1)}, bf16[4,4,136,512]{3,2,1,0:T(8,128)(2,1)}, u32[]{:S(2)}, u32[]{:S(2)}) collective-permute-start(bf16[4,4,136,512]{3,2,1,0:T(8,128)(2,1)S(1)} %bitcast.26), channel_id=1, source_target_pairs={{0,4},{4,0},{1,5},{5,1},{2,6},{6,2},{3,7},{7,3},{8,12},{12,8},{9,1... | collective-permute-start | bytes 6684680 | tf_op jit(solution)/shard_map/ppermute | solution.py:28
  45.4 8.1 %all_to_all.31 = bf16[8,16,256]{2,1,0:T(8,128)(2,1)S(1)} all-to-all(bf16[8,16,256]{2,1,0:T(8,128)(2,1)} %bitcast.37), channel_id=1, replica_groups=mesh['zh'=4,'zl'=4,'x'=4,'c'=2,'tp'=4] {'x','c'}, dimensions={0} | all-to-all | bytes 131072 | tf_op jit(solution)/shard_map/all_to_all | solution.py:24
  54.3 15.7 %collective-permute-start.3 = (bf16[176,256]{1,0:T(8,128)(2,1)S(1)}, bf16[176,256]{1,0:T(8,128)(2,1)S(1)}, u32[]{:S(2)}, u32[]{:S(2)}) collective-permute-start(bf16[176,256]{1,0:T(8,128)(2,1)S(1)} %pad_maximum_fusion.1.mine_ref), channel_id=1, source_target_pairs={{0,256},{32,288},{64,320},{96,352},{128,384},{160,416},{192,448},{... | collective-permute-start | bytes 270344 | tf_op jit(solution)/shard_map/ppermute | solution.py:529
  71.9 7.3 %collective-permute-start.1 = (bf16[176,256]{1,0:T(8,128)(2,1)S(1)}, bf16[176,256]{1,0:T(8,128)(2,1)S(1)}, u32[]{:S(2)}, u32[]{:S(2)}) collective-permute-start(bf16[176,256]{1,0:T(8,128)(2,1)S(1)} %pad_maximum_fusion.1.mine_ref), channel_id=1, source_target_pairs={{0,128},{32,160},{64,192},{96,224},{128,256},{160,288},{192,320},{... | collective-permute-start | bytes 270344 | tf_op jit(solution)/shard_map/ppermute | solution.py:529
  79.2 7.9 %collective-permute-done.2.after_ref = bf16[176,256]{1,0:T(8,128)(2,1)S(1)} collective-permute-done((bf16[176,256]{1,0:T(8,128)(2,1)S(1)}, bf16[176,256]{1,0:T(8,128)(2,1)S(1)}, u32[]{:S(2)}, u32[]{:S(2)}) %collective-permute-start.2) | collective-permute-done | bytes 90144 | tf_op jit(solution)/shard_map/ppermute | solution.py:529
  92.9 4.0 %collective-permute-start.4 = (bf16[4,176,256]{2,1,0:T(8,128)(2,1)}, bf16[4,176,256]{2,1,0:T(8,128)(2,1)S(1)}, u32[]{:S(2)}, u32[]{:S(2)}) collective-permute-start(bf16[4,176,256]{2,1,0:T(8,128)(2,1)} %get-tuple-element.23.w0_ref), channel_id=1, source_target_pairs={{0,480},{32,0},{64,32},{96,64},{128,96},{160,128},{192,160},{224,1... | collective-permute-start | bytes 1081352 | tf_op jit(solution)/shard_map/ppermute | solution.py:529
  98.8 4.3 %collective-permute-start.7 = (bf16[2,176,256]{2,1,0:T(8,128)(2,1)}, bf16[2,176,256]{2,1,0:T(8,128)(2,1)}, u32[]{:S(2)}, u32[]{:S(2)}) collective-permute-start(bf16[2,176,256]{2,1,0:T(8,128)(2,1)} %get-tuple-element.25), channel_id=1, source_target_pairs={{0,64},{32,96},{64,128},{96,160},{128,192},{160,224},{192,256},{22... | collective-permute-start | bytes 540680 | tf_op jit(solution)/shard_map/ppermute | solution.py:529
  104.9 5.8 %collective-permute-done.6.low_ref = bf16[2,176,256]{2,1,0:T(8,128)(2,1)} collective-permute-done((bf16[2,176,256]{2,1,0:T(8,128)(2,1)}, bf16[2,176,256]{2,1,0:T(8,128)(2,1)}, u32[]{:S(2)}, u32[]{:S(2)}) %collective-permute-start.6) | collective-permute-done | bytes 180256 | tf_op jit(solution)/shard_map/ppermute | solution.py:529
  110.8 4.1 %collective-permute-done.7.high_ref = bf16[2,176,256]{2,1,0:T(8,128)(2,1)} collective-permute-done((bf16[2,176,256]{2,1,0:T(8,128)(2,1)}, bf16[2,176,256]{2,1,0:T(8,128)(2,1)}, u32[]{:S(2)}, u32[]{:S(2)}) %collective-permute-start.7) | collective-permute-done | bytes 180256 | tf_op jit(solution)/shard_map/ppermute | solution.py:529
  115.8 6.4 %project.1 = (bf16[4,4,2,128,128]{4,3,2,1,0:T(8,128)(2,1)}, bf16[4,2,128,128]{3,2,1,0:T(8,128)(2,1)}, bf16[2,128,128]{2,1,0:T(8,128)(2,1)}, f32[2,8,128]{2,1,0:T...) custom-call(s32[4]{0:T(128)} %pad_add_fusion.place_ref, bf16[4,4,136,512]{3,2,1,0:T(8,128)(2,1)} %bitcast.27, ...), custom_call_target="tpu_custom_call" | custom-call | tf_op jit(solution)/shard_map/project/pallas_call | solution.py:590
  122.2 19.2 %all_to_all.32.qk_ref = bf16[4,1024,128]{2,1,0:T(8,128)(2,1)} all-to-all(bf16[4,1024,128]{2,1,0:T(8,128)(2,1)} %bitcast.30), channel_id=1, replica_groups=mesh['zh'=4,'zl'=4,'x'=4,'c'=2,'tp'=4] {'x'}, dimensions={0} | all-to-all | bytes 2097152 | tf_op jit(solution)/shard_map/all_to_all | solution.py:24
  141.4 3.6 %slab_state.1 = (bf16[4,72,256]{2,1,0:T(8,128)(2,1)}, bf16[1024,256]{1,0:T(8,128)(2,1)}, bf16[1024,256]{1,0:T(8,128)(2,1)}) custom-call(bf16[4,1024,128]{2,1,0:T(8,128)(2,1)} %all_to_all.32.qk_ref, bf16[1024,128]{1,0:T(8,128)(2,1)} %bitcast.31, f32[2,8,128]{2,1,0:T(8,128)} %get-tuple-element.28.gate_ref, bf16[2,128,128]{2,1,0:T(8,128)(2,1)} %get-tuple-element.29.glu_ref), custom_call_target="tpu_custom_call" | custom-call | tf_op jit(solution)/shard_map/slab_state/pallas_call | solution.py:631
  145.0 9.5 %all_to_all.33.in_ref = bf16[4,72,256]{2,1,0:T(8,128)(2,1)} all-to-all(bf16[4,72,256]{2,1,0:T(8,128)(2,1)} %get-tuple-element.30), channel_id=1, replica_groups=mesh['zh'=4,'zl'=4,'x'=4,'c'=2,'tp'=4] {'zl'}, dimensions={0} | all-to-all | bytes 294912 | tf_op jit(solution)/shard_map/all_to_all | solution.py:24
  156.3 5.5 %all-to-all-start.4 = ((bf16[4,72,256]{2,1,0:T(8,128)(2,1)}), bf16[4,72,256]{2,1,0:T(8,128)(2,1)S(1)}, u32[]{:S(2)}, u32[]{:S(2)}) async-start(bf16[4,72,256]{2,1,0:T(8,128)(2,1)} %group.1), calls=%async_computation.4 | async-start | bytes 294912 | tf_op jit(solution)/shard_map/all_to_all | solution.py:24
  161.9 2.9 %collective-permute-start.10 = (bf16[4,16,768]{2,1,0:T(8,128)(2,1)S(1)}, bf16[4,16,768]{2,1,0:T(8,128)(2,1)S(1)}, u32[]{:S(2)}, u32[]{:S(2)}) collective-permute-start(bf16[4,16,768]{2,1,0:T(8,128)(2,1)S(1)} %get-tuple-element.38), channel_id=1, source_target_pairs={{0,3},{1,0},{2,1},{3,2},{4,7},{5,4},{6,5},{7,6},{8,11},{9,8},{10,9... | collective-permute-start | bytes 294920 | tf_op jit(solution)/shard_map/ppermute | solution.py:608
  164.8 2.9 %collective-permute-start.9 = (bf16[4,16,768]{2,1,0:T(8,128)(2,1)S(1)}, bf16[4,16,768]{2,1,0:T(8,128)(2,1)S(1)}, u32[]{:S(2)}, u32[]{:S(2)}) collective-permute-start(bf16[4,16,768]{2,1,0:T(8,128)(2,1)S(1)} %get-tuple-element.39), channel_id=1, source_target_pairs={{0,2},{1,3},{2,0},{3,1},{4,6},{5,7},{6,4},{7,5},{8,10},{9,11},{10,... | collective-permute-start | bytes 294920 | tf_op jit(solution)/shard_map/ppermute | solution.py:608
  171.7 2.9 %collective-permute-done.8 = bf16[4,16,768]{2,1,0:T(8,128)(2,1)S(1)} collective-permute-done((bf16[4,16,768]{2,1,0:T(8,128)(2,1)S(1)}, bf16[4,16,768]{2,1,0:T(8,128)(2,1)S(1)}, u32[]{:S(2)}, u32[]{:S(2)}) %collective-permute-start.8) | collective-permute-done | bytes 98336 | tf_op jit(solution)/shard_map/ppermute | solution.py:608
  176.8 3.7 %collective-permute-start.12 = (bf16[4,4,16,768]{3,2,1,0:T(8,128)(2,1)S(1)}, bf16[4,4,16,768]{3,2,1,0:T(8,128)(2,1)S(1)}, u32[]{:S(2)}, u32[]{:S(2)}) collective-permute-start(bf16[4,4,16,768]{3,2,1,0:T(8,128)(2,1)S(1)} %pad_maximum_fusion.refs_0_), channel_id=1, source_target_pairs={{0,16},{8,24},{16,0},{24,8},{1,17},{9,25},{17,1},{25,9},{2,18},{10... | collective-permute-start | bytes 1179656 | tf_op jit(solution)/shard_map/ppermute | solution.py:613
  183.1 7.2 %local.1 = (f32[1024,128]{1,0:T(8,128)}, f32[256,128]{1,0:T(8,128)}) custom-call(s32[4]{0:T(128)} %pad_add_fusion.place_ref, bf16[1024,256]{1,0:T(8,128)(2,1)} %get-tuple-element.31.q_ref, bf16[1024,256]{1,0:T(8,128)(2,1)} %get-tuple-element.32.k_ref, bf16[1024,128]{1,0:T(8,128)(2,1)} %bitcast.32, f32[2,8,128]{2,1,0:T(8,128)} %get-tuple-element.28.gate_ref, ...), custom_call_target="tpu_custom_call" | custom-call | tf_op jit(solution)/shard_map/local/pallas_call | solution.py:654
  190.9 4.3 %cell.1 = bf16[4,2,4,96,128]{4,3,2,1,0:T(8,128)(2,1)} custom-call(s32[4]{0:T(128)} %pad_add_fusion.place_ref, bf16[4,72,256]{2,1,0:T(8,128)(2,1)} %copy-done.3, bf16[4,72,256]{2,1,0:T(8,128)(2,1)} %all_to_all.33.in_ref, bf16[1024,256]{1,0:T(8,128)(2,1)} %get-tuple-element.31.q_ref, f32[1024,128]{1,0:T(8,128)} %get-tuple-element.33.local_ref, ...), custom_call_target="tpu_custom_call" | custom-call | tf_op jit(solution)/shard_map/cell/pallas_call | solution.py:663
  195.2 11.1 %all-to-all-start.5 = ((bf16[32,96,128]{2,1,0:T(8,128)(2,1)}), bf16[32,96,128]{2,1,0:T(8,128)(2,1)S(1)}, u32[]{:S(2)}, u32[]{:S(2)}) async-start(bf16[32,96,128]{2,1,0:T(8,128)(2,1)} %bitcast.28), calls=%async_computation.5 | async-start | bytes 1572864 | tf_op jit(solution)/shard_map/all_to_all | solution.py:24
  216.6 3.7 %assemble.1.weight_ref = bf16[4,4,4,2,16,768]{5,4,3,2,1,0:T(8,128)(2,1)} custom-call(s32[4]{0:T(128)} %pad_add_fusion.place_ref, bf16[4,4,16,768]{3,2,1,0:T(8,128)(2,1)} %copy-done.2, bf16[4,4,16,768]{3,2,1,0:T(8,128)(2,1)} %copy-done.6, bf16[4,4,16,768]{3,2,1,0:T(8,128)(2,1)} %copy-done.5, bf16[4,4,16,768]{3,2,1,0:T(8,128)(2,1)} %copy-done.4, ...), custom_call_target="tpu_custom_call" | custom-call | tf_op jit(solution)/shard_map/assemble/pallas_call | solution.py:674
  221.2 5.3 %finish.1 = bf16[128,512]{1,0:T(8,128)(2,1)} custom-call(bf16[4,2,4,96,128]{4,3,2,1,0:T(8,128)(2,1)} %bitcast.29, bf16[4,4,4,2,16,768]{5,4,3,2,1,0:T(8,128)(2,1)} %assemble.1.weight_ref, f32[4,8,128]{2,1,0:T(8,128)} %get-tuple-element.36.gain_ref), custom_call_target="tpu_custom_call" | custom-call | tf_op jit(solution)/shard_map/finish/pallas_call | solution.py:675
  (76 shorter events, 40.5 us)
Async XLA Ops:
  3.7 99.4 %copy-start.17 = (bf16[2048,2]{0,1:T(2,128)(2,1)S(1)}, bf16[2048,2]{0,1:T(2,128)(2,1)}, u32[]{:S(2)}) copy-start(bf16[2048,2]{0,1:T(2,128)(2,1)} %param.24) | copy-start | bytes 24580
  3.7 99.4 %copy-start.18 = (bf16[2048,2]{0,1:T(2,128)(2,1)S(1)}, bf16[2048,2]{0,1:T(2,128)(2,1)}, u32[]{:S(2)}) copy-start(bf16[2048,2]{0,1:T(2,128)(2,1)} %param.23) | copy-start | bytes 24580
  38.0 76.9 %copy-start = (bf16[16,136,512]{2,1,0:T(8,128)(2,1)}, bf16[16,136,512]{2,1,0:T(8,128)(2,1)S(1)}, u32[]{:S(2)}) copy-start(bf16[16,136,512]{2,1,0:T(8,128)(2,1)S(1)} %all_to_all.30) | copy-start | bytes 6684676
  38.0 76.9 %collective-permute-start = (bf16[4,4,136,512]{3,2,1,0:T(8,128)(2,1)S(1)}, bf16[4,4,136,512]{3,2,1,0:T(8,128)(2,1)}, u32[]{:S(2)}, u32[]{:S(2)}) collective-permute-start(bf16[4,4,136,512]{3,2,1,0:T(8,128)(2,1)S(1)} %bitcast.26), channel_id=1, source_target_pairs={{0,4},{4,0},{1,5},{5,1},{2,6},{6,2},{3,7},{7,3},{8,12},{12,8},{9,1... | collective-permute-start | bytes 6684680 | tf_op jit(solution)/shard_map/ppermute | solution.py:28
  54.3 24.9 %collective-permute-start.3 = (bf16[176,256]{1,0:T(8,128)(2,1)S(1)}, bf16[176,256]{1,0:T(8,128)(2,1)S(1)}, u32[]{:S(2)}, u32[]{:S(2)}) collective-permute-start(bf16[176,256]{1,0:T(8,128)(2,1)S(1)} %pad_maximum_fusion.1.mine_ref), channel_id=1, source_target_pairs={{0,256},{32,288},{64,320},{96,352},{128,384},{160,416},{192,448},{... | collective-permute-start | bytes 270344 | tf_op jit(solution)/shard_map/ppermute | solution.py:529
  70.0 17.2 %collective-permute-start.2 = (bf16[176,256]{1,0:T(8,128)(2,1)S(1)}, bf16[176,256]{1,0:T(8,128)(2,1)S(1)}, u32[]{:S(2)}, u32[]{:S(2)}) collective-permute-start(bf16[176,256]{1,0:T(8,128)(2,1)S(1)} %pad_maximum_fusion.1.mine_ref), channel_id=1, source_target_pairs={{0,384},{32,416},{64,448},{96,480},{128,0},{160,32},{192,64},{224,... | collective-permute-start | bytes 270344 | tf_op jit(solution)/shard_map/ppermute | solution.py:529
  71.9 15.2 %collective-permute-start.1 = (bf16[176,256]{1,0:T(8,128)(2,1)S(1)}, bf16[176,256]{1,0:T(8,128)(2,1)S(1)}, u32[]{:S(2)}, u32[]{:S(2)}) collective-permute-start(bf16[176,256]{1,0:T(8,128)(2,1)S(1)} %pad_maximum_fusion.1.mine_ref), channel_id=1, source_target_pairs={{0,128},{32,160},{64,192},{96,224},{128,256},{160,288},{192,320},{... | collective-permute-start | bytes 270344 | tf_op jit(solution)/shard_map/ppermute | solution.py:529
  90.4 24.5 %collective-permute-start.5 = (bf16[4,176,256]{2,1,0:T(8,128)(2,1)}, bf16[4,176,256]{2,1,0:T(8,128)(2,1)S(1)}, u32[]{:S(2)}, u32[]{:S(2)}) collective-permute-start(bf16[4,176,256]{2,1,0:T(8,128)(2,1)} %get-tuple-element.23.w0_ref), channel_id=1, source_target_pairs={{0,32},{32,64},{64,96},{96,128},{128,160},{160,192},{192,224},{224... | collective-permute-start | bytes 1081352 | tf_op jit(solution)/shard_map/ppermute | solution.py:529
  92.9 22.0 %collective-permute-start.4 = (bf16[4,176,256]{2,1,0:T(8,128)(2,1)}, bf16[4,176,256]{2,1,0:T(8,128)(2,1)S(1)}, u32[]{:S(2)}, u32[]{:S(2)}) collective-permute-start(bf16[4,176,256]{2,1,0:T(8,128)(2,1)} %get-tuple-element.23.w0_ref), channel_id=1, source_target_pairs={{0,480},{32,0},{64,32},{96,64},{128,96},{160,128},{192,160},{224,1... | collective-permute-start | bytes 1081352 | tf_op jit(solution)/shard_map/ppermute | solution.py:529
  96.9 13.9 %collective-permute-start.6 = (bf16[2,176,256]{2,1,0:T(8,128)(2,1)}, bf16[2,176,256]{2,1,0:T(8,128)(2,1)}, u32[]{:S(2)}, u32[]{:S(2)}) collective-permute-start(bf16[2,176,256]{2,1,0:T(8,128)(2,1)} %get-tuple-element.24), channel_id=1, source_target_pairs={{0,448},{32,480},{64,0},{96,32},{128,64},{160,96},{192,128},{224,1... | collective-permute-start | bytes 540680 | tf_op jit(solution)/shard_map/ppermute | solution.py:529
  98.8 16.1 %collective-permute-start.7 = (bf16[2,176,256]{2,1,0:T(8,128)(2,1)}, bf16[2,176,256]{2,1,0:T(8,128)(2,1)}, u32[]{:S(2)}, u32[]{:S(2)}) collective-permute-start(bf16[2,176,256]{2,1,0:T(8,128)(2,1)} %get-tuple-element.25), channel_id=1, source_target_pairs={{0,64},{32,96},{64,128},{96,160},{128,192},{160,224},{192,256},{22... | collective-permute-start | bytes 540680 | tf_op jit(solution)/shard_map/ppermute | solution.py:529
  122.2 39.6 %copy-start.10 = (bf16[4,4,16,768]{3,2,1,0:T(8,128)(2,1)S(1)}, bf16[4,4,16,768]{3,2,1,0:T(8,128)(2,1)}, u32[]{:S(2)}) copy-start(bf16[4,4,16,768]{3,2,1,0:T(8,128)(2,1)} %get-tuple-element.35) | copy-start | bytes 1179652
  156.3 33.9 %all-to-all-start.4 = ((bf16[4,72,256]{2,1,0:T(8,128)(2,1)}), bf16[4,72,256]{2,1,0:T(8,128)(2,1)S(1)}, u32[]{:S(2)}, u32[]{:S(2)}) async-start(bf16[4,72,256]{2,1,0:T(8,128)(2,1)} %group.1), calls=%async_computation.4 | async-start | bytes 294912 | tf_op jit(solution)/shard_map/all_to_all | solution.py:24
  161.9 7.9 %collective-permute-start.10 = (bf16[4,16,768]{2,1,0:T(8,128)(2,1)S(1)}, bf16[4,16,768]{2,1,0:T(8,128)(2,1)S(1)}, u32[]{:S(2)}, u32[]{:S(2)}) collective-permute-start(bf16[4,16,768]{2,1,0:T(8,128)(2,1)S(1)} %get-tuple-element.38), channel_id=1, source_target_pairs={{0,3},{1,0},{2,1},{3,2},{4,7},{5,4},{6,5},{7,6},{8,11},{9,8},{10,9... | collective-permute-start | bytes 294920 | tf_op jit(solution)/shard_map/ppermute | solution.py:608
  164.8 6.9 %collective-permute-start.9 = (bf16[4,16,768]{2,1,0:T(8,128)(2,1)S(1)}, bf16[4,16,768]{2,1,0:T(8,128)(2,1)S(1)}, u32[]{:S(2)}, u32[]{:S(2)}) collective-permute-start(bf16[4,16,768]{2,1,0:T(8,128)(2,1)S(1)} %get-tuple-element.39), channel_id=1, source_target_pairs={{0,2},{1,3},{2,0},{3,1},{4,6},{5,7},{6,4},{7,5},{8,10},{9,11},{10,... | collective-permute-start | bytes 294920 | tf_op jit(solution)/shard_map/ppermute | solution.py:608
  167.7 6.9 %collective-permute-start.8 = (bf16[4,16,768]{2,1,0:T(8,128)(2,1)S(1)}, bf16[4,16,768]{2,1,0:T(8,128)(2,1)S(1)}, u32[]{:S(2)}, u32[]{:S(2)}) collective-permute-start(bf16[4,16,768]{2,1,0:T(8,128)(2,1)S(1)} %get-tuple-element.40), channel_id=1, source_target_pairs={{0,1},{1,2},{2,3},{3,0},{4,5},{5,6},{6,7},{7,4},{8,9},{9,10},{10,1... | collective-permute-start | bytes 294920 | tf_op jit(solution)/shard_map/ppermute | solution.py:608
  174.6 33.8 %collective-permute-start.13 = (bf16[4,4,16,768]{3,2,1,0:T(8,128)(2,1)S(1)}, bf16[4,4,16,768]{3,2,1,0:T(8,128)(2,1)S(1)}, u32[]{:S(2)}, u32[]{:S(2)}) collective-permute-start(bf16[4,4,16,768]{3,2,1,0:T(8,128)(2,1)S(1)} %pad_maximum_fusion.refs_0_), channel_id=1, source_target_pairs={{0,8},{8,16},{16,24},{24,0},{1,9},{9,17},{17,25},{25,1},{2,10},{10... | collective-permute-start | bytes 1179656 | tf_op jit(solution)/shard_map/ppermute | solution.py:613
  176.8 33.8 %collective-permute-start.12 = (bf16[4,4,16,768]{3,2,1,0:T(8,128)(2,1)S(1)}, bf16[4,4,16,768]{3,2,1,0:T(8,128)(2,1)S(1)}, u32[]{:S(2)}, u32[]{:S(2)}) collective-permute-start(bf16[4,4,16,768]{3,2,1,0:T(8,128)(2,1)S(1)} %pad_maximum_fusion.refs_0_), channel_id=1, source_target_pairs={{0,16},{8,24},{16,0},{24,8},{1,17},{9,25},{17,1},{25,9},{2,18},{10... | collective-permute-start | bytes 1179656 | tf_op jit(solution)/shard_map/ppermute | solution.py:613
  180.5 32.3 %collective-permute-start.11 = (bf16[4,4,16,768]{3,2,1,0:T(8,128)(2,1)S(1)}, bf16[4,4,16,768]{3,2,1,0:T(8,128)(2,1)S(1)}, u32[]{:S(2)}, u32[]{:S(2)}) collective-permute-start(bf16[4,4,16,768]{3,2,1,0:T(8,128)(2,1)S(1)} %pad_maximum_fusion.refs_0_), channel_id=1, source_target_pairs={{0,24},{8,0},{16,8},{24,16},{1,25},{9,1},{17,9},{25,17},{2,26},{10... | collective-permute-start | bytes 1179656 | tf_op jit(solution)/shard_map/ppermute | solution.py:613
  195.2 25.1 %all-to-all-start.5 = ((bf16[32,96,128]{2,1,0:T(8,128)(2,1)}), bf16[32,96,128]{2,1,0:T(8,128)(2,1)S(1)}, u32[]{:S(2)}, u32[]{:S(2)}) async-start(bf16[32,96,128]{2,1,0:T(8,128)(2,1)} %bitcast.28), calls=%async_computation.5 | async-start | bytes 1572864 | tf_op jit(solution)/shard_map/all_to_all | solution.py:24
  206.3 8.8 %collective-permute-start.14 = (bf16[4,4,16,768]{3,2,1,0:T(8,128)(2,1)S(1)}, bf16[4,4,16,768]{3,2,1,0:T(8,128)(2,1)S(1)}, u32[]{:S(2)}, u32[]{:S(2)}) collective-permute-start(bf16[4,4,16,768]{3,2,1,0:T(8,128)(2,1)S(1)} %pad_maximum_fusion.refs_0_), channel_id=1, source_target_pairs={{0,4},{4,0},{1,5},{5,1},{2,6},{6,2},{3,7},{7,3},{8,12},{12,8},{9,1... | collective-permute-start | bytes 1179656 | tf_op jit(solution)/shard_map/ppermute | solution.py:28
  208.5 6.6 %collective-permute-start.17 = (bf16[4,4,16,768]{3,2,1,0:T(8,128)(2,1)S(1)}, bf16[4,4,16,768]{3,2,1,0:T(8,128)(2,1)S(1)}, u32[]{:S(2)}, u32[]{:S(2)}) collective-permute-start(bf16[4,4,16,768]{3,2,1,0:T(8,128)(2,1)S(1)} %collective-permute-done.13.refs_3_), channel_id=1, source_target_pairs={{0,4},{4,0},{1,5},{5,1},{2,6},{6,2},{3,7},{7,3},{8,12},{12,8},{9,1... | collective-permute-start | bytes 1179656 | tf_op jit(solution)/shard_map/ppermute | solution.py:28
  210.7 4.4 %collective-permute-start.16 = (bf16[4,4,16,768]{3,2,1,0:T(8,128)(2,1)S(1)}, bf16[4,4,16,768]{3,2,1,0:T(8,128)(2,1)S(1)}, u32[]{:S(2)}, u32[]{:S(2)}) collective-permute-start(bf16[4,4,16,768]{3,2,1,0:T(8,128)(2,1)S(1)} %collective-permute-done.12.refs_2_), channel_id=1, source_target_pairs={{0,4},{4,0},{1,5},{5,1},{2,6},{6,2},{3,7},{7,3},{8,12},{12,8},{9,1... | collective-permute-start | bytes 1179656 | tf_op jit(solution)/shard_map/ppermute | solution.py:28
  212.8 3.7 %collective-permute-start.15 = (bf16[4,4,16,768]{3,2,1,0:T(8,128)(2,1)S(1)}, bf16[4,4,16,768]{3,2,1,0:T(8,128)(2,1)}, u32[]{:S(2)}, u32[]{:S(2)}) collective-permute-start(bf16[4,4,16,768]{3,2,1,0:T(8,128)(2,1)S(1)} %collective-permute-done.11.refs_1_), channel_id=1, source_target_pairs={{0,4},{4,0},{1,5},{5,1},{2,6},{6,2},{3,7},{7,3},{8,12},{12,8},{9,1... | collective-permute-start | bytes 1179656 | tf_op jit(solution)/shard_map/ppermute | solution.py:28
  (15 other events, 98.7 us)

commit v10 on v9

--- a/solution.py
+++ b/solution.py
@@ -88,12 +88,7 @@
 ):
     nx, nc = out_ref.shape[0], out_ref.shape[1]
     rows = memory_ref.shape[0]
-    width, chan = memory_ref.shape[1] // (nx * nc), conv_ref.shape[1] // (nx * nc)
-    parts = []
-    for at in range(nx * nc):
-        parts.append(memory_ref[:, at * width : (at + 1) * width])
-        parts.append(conv_ref[:, at * chan : (at + 1) * chan])
-    whole = jnp.concatenate(parts, axis=1)
+    whole = jnp.concatenate([memory_ref[...], conv_ref[...]], axis=1)
     wide = out_ref.shape[3]
     for j in range(whole.shape[1] // wide):
         turn_ref[j * rows : (j + 1) * rows] = whole[:, j * wide : (j + 1) * wide]
@@ -135,7 +130,7 @@
 def project_kernel(
     place_ref, own_ref, other_ref,
     w0_ref, w1_ref, w3_ref, low_ref, high_ref, gate_ref,
-    qk_ref, v_ref, glu_ref, gates_ref, gain_ref, out_weight_ref,
+    qk_ref, v_ref, glu_ref, gates_ref, memory_gain_ref, conv_gain_ref, out_weight_ref,
 ):
     nx, ny, _, part = own_ref.shape
     far, tall, wide = w0_ref.shape
@@ -216,65 +211,48 @@
             forget = jnp.where(at, forget_pre + offsets_f, forget)
     for b in range(ny):
         extra = own_ref[0, b, length : length + 8].astype(F32)
-        memory_gain = extra[3:4] + extra[4:5] + extra[5:6]
+        memory_gain_ref[b : b + 1] = extra[3:4] + extra[4:5] + extra[5:6]
         half = part // 2
-        conv_gain = extra[6:7, :half] + extra[6:7, half:] + extra[7:8, :half]
-        for at in range(2 * nx):
-            gain_ref[b, at : at + 1] = jnp.concatenate(
-                [
-                    memory_gain[:, at * width : (at + 1) * width],
-                    conv_gain[:, at * chan : (at + 1) * chan],
-                    jnp.zeros((1, width - chan), F32),
-                ],
-                axis=1,
-            )
+        conv_gain_ref[b : b + 1] = extra[6:7, :half] + extra[6:7, half:] + extra[7:8, :half]
     y = jnp.exp(-jnp.abs(forget))
     small = y * (1.0 - y * (1 / 2 - y * (1 / 3 - y * (1 / 4 - y * (1 / 5)))))
     gates_ref[0] = gate_in
     gates_ref[1] = jnp.minimum(forget, 0.0) - jnp.where(y < 0.03, small, jnp.log(1.0 + y))
 
 
-def finish_kernel(arrived_ref, weight_ref, gain_ref, out_ref):
+def finish_kernel(arrived_ref, weight_ref, memory_gain_ref, conv_gain_ref, out_ref):
     nx, nc, ny, _, lanes = arrived_ref.shape
     width = lanes // 2
     chan = width // 2
     length, part = out_ref.shape
-    lane = lax.broadcasted_iota(jnp.int32, (length, width + chan), 1)
-    is_memory = lane < width
     half = length // 2
-
-    def block(x, c, b):
-        got = arrived_ref[x, c, b].astype(F32)
-        memory = jnp.concatenate([got[:half, :width], got[:half, width:]], axis=0)
-        conv = [got[half:, k * chan : (k + 1) * chan] for k in range(4)]
-        return jnp.concatenate([memory, jnp.concatenate(conv, axis=0)], axis=1)
-
-    blocks = {
-        (x, c, b): block(x, c, b) for x in range(nx) for c in range(nc) for b in range(ny)
-    }
-    first = sum(blocks.values())
-    second = sum(got * got for got in blocks.values())
-    senders = nx * nc * ny
-    memory_mean = jnp.sum(jnp.where(is_memory, second, 0.0), axis=1, keepdims=True)
-    scale = lax.rsqrt(memory_mean / (senders * width) + EPS)
-    mean = jnp.sum(jnp.where(is_memory, 0.0, first), axis=1, keepdims=True) / (senders * chan)
-    power = jnp.sum(jnp.where(is_memory, 0.0, second), axis=1, keepdims=True) / (senders * chan)
-    spread = lax.rsqrt(power - mean * mean + EPS)
-    shift = jnp.where(is_memory, 0.0, mean)
-    factor = jnp.where(is_memory, scale, spread)
+    memory, conv = [], []
+    for b in range(ny):
+        blocks = [arrived_ref[x, c, b].astype(F32) for c in range(nc) for x in range(nx)]
+        upper = jnp.concatenate([got[:half, :width] for got in blocks], axis=1)
+        lower = jnp.concatenate([got[:half, width:] for got in blocks], axis=1)
+        memory.append(jnp.concatenate([upper, lower], axis=0))
+        quarters = [
+            jnp.concatenate([got[half:, k * chan : (k + 1) * chan] for got in blocks], axis=1)
+            for k in range(4)
+        ]
+        conv.append(jnp.concatenate(quarters, axis=0))
+
+    def mean_of(arrays):
+        each = sum(arrays)
+        return jnp.sum(each, axis=1, keepdims=True) / (ny * each.shape[1])
+
+    scale = lax.rsqrt(mean_of([m * m for m in memory]) + EPS)
+    mean = mean_of(conv)
+    spread = lax.rsqrt(mean_of([t * t for t in conv]) - mean * mean + EPS)
     deep = weight_ref.shape[5]
     total = jnp.zeros((length, part), F32)
     for b in range(ny):
-        left = []
-        for c in range(nc):
-            for x in range(nx):
-                gain = gain_ref[b, c * nx + x : c * nx + x + 1, : width + chan]
-                normed = (blocks[x, c, b] - shift) * factor * gain
-                branch = normed / (1.0 + jnp.exp(-normed))
-                left.append(jnp.where(is_memory, normed, branch).astype(BF16))
-        total = total + dot(
-            jnp.concatenate(left, axis=1), weight_ref[b].reshape(part, deep), NT
-        )
+        scaled = memory[b] * scale * memory_gain_ref[b : b + 1]
+        normed = (conv[b] - mean) * spread * conv_gain_ref[b : b + 1]
+        branch = normed / (1.0 + jnp.exp(-normed))
+        both = jnp.concatenate([scaled.astype(BF16), branch.astype(BF16)], axis=1)
+        total = total + dot(both, weight_ref[b].reshape(part, deep), NT)
     out_ref[...] = total.astype(BF16)
 
 
@@ -587,18 +565,19 @@
     )
     place = jnp.stack([zi, ci, yi, xi])
     smem = pl.BlockSpec(memory_space=pltpu.SMEM)
-    qk, value, packed, gates, gain, out_part = pl.pallas_call(
+    qk, value, packed, gates, memory_gain, conv_gain, out_part = pl.pallas_call(
         project_kernel,
         out_shape=(
             jax.ShapeDtypeStruct((nx, nx, nc, length, 2 * width), BF16),
             jax.ShapeDtypeStruct((nx, nc, length, 2 * width), BF16),
             jax.ShapeDtypeStruct((nc, length, nx * chan), BF16),
             jax.ShapeDtypeStruct((2, nx * nc, length), F32),
-            jax.ShapeDtypeStruct((ny, nc * nx, 2 * width), F32),
+            jax.ShapeDtypeStruct((ny, memory_norm_gain.shape[0]), F32),
+            jax.ShapeDtypeStruct((ny, conv_norm_gain.shape[0]), F32),
             jax.ShapeDtypeStruct((nzh, nzl, rows, deep), BF16),
         ),
         in_specs=[smem] + vmem(8),
-        out_specs=vmem(6),
+        out_specs=vmem(7),
         interpret=INTERPRET,
         name="project",
     )(place, own, other, *sets, gate_weight)
@@ -609,10 +588,12 @@
         for ahead in range(1, ny)
     ]
     out_part = jnp.stack(out_part, axis=0)
-    out_parts = [out_part] + [
-        lax.ppermute(out_part, "x", [(j, (j - ahead) % nx) for j in range(nx)])
-        for ahead in range(1, nx)
-    ]
+
+    def from_x(value, ahead):
+        return lax.ppermute(value, "x", [(j, (j - ahead) % nx) for j in range(nx)])
+
+    out_parts = [out_part] + [from_x(out_part, ahead) for ahead in (1, 3)]
+    out_parts.insert(2, from_x(out_part, 2))
     other_parts = [swapped(out, "c") for out in out_parts]
 
     state_rows = width + 8
@@ -675,11 +656,11 @@
     return pl.pallas_call(
         finish_kernel,
         out_shape=jax.ShapeDtypeStruct((length, part), BF16),
-        in_specs=vmem(3),
+        in_specs=vmem(4),
         out_specs=pl.BlockSpec(memory_space=pltpu.VMEM),
         interpret=INTERPRET,
         name="finish",
-    )(arrived, out_weight, gain)
+    )(arrived, out_weight, memory_gain, conv_gain)
 
 
 def solution(mesh):

time: 228 us -> 227 us (level)
  no operation moved by 1% of the time
where the time goes in v10:
time: 227 us; the launch traced here: 226 us
  starting transfers between devices  84.9 us (37%)
  blocking collectives  71.1 us (31%)
  Pallas kernels  37.3 us (16%)
  waiting for transfers between devices  23.4 us (10%)
  local copies, waits for them, and re-layouts  5.75 us (3%)
  other arithmetic  2.68 us (1%)
    all_to_all x4, blocking collectives, exchange(): return lax.all_to_all(pieces, axes, split_axis=0, concat_axis=0, tiled=True)  71.1 us
    ppermute x7, starting transfers between devices, from_z(): lax.ppermute(value, Z, [(j, (j - ahead) % members) for j in range(members)])  37.6 us
    ppermute x7, waiting for transfers between devices, from_z(): lax.ppermute(value, Z, [(j, (j - ahead) % members) for j in range(members)])  17.9 us
    all_to_all x2, starting transfers between devices, exchange(): return lax.all_to_all(pieces, axes, split_axis=0, concat_axis=0, tiled=True)  16.6 us
    ppermute x5, starting transfers between devices, swapped(): return lax.ppermute(value, axis, [(0, 1), (1, 0)])  14.5 us
    ppermute x3, starting transfers between devices, from_x(): return lax.ppermute(value, 'x', [(j, (j - ahead) % nx) for j in range(nx)])  8.41 us
    ppermute x3, starting transfers between devices, layer(): lax.ppermute(out_part[ahead], 'tp', [(j, (j + ahead) % ny) for j in range...  7.83 us
    pallas_call x1, Pallas kernels, layer(): call_local(place, query, key, value, gates, packed, conv_kernel)  7.2 us
  transfers between devices with their start and end apart: 20, of which 6 were waited for; matrix products, arithmetic and copies ran while one was open for 1% of the time, Pallas kernels for 8%

profile of v10, /device:TPU:1, one launch (start us, length us, event | category | flops | bytes accessed | tf_op | source)
XLA Modules:
  0.0 225.6 jit_solution(5427604450905798327)
XLA Ops:
  3.7 34.3 %all_to_all.30 = bf16[16,136,512]{2,1,0:T(8,128)(2,1)S(1)} all-to-all(bf16[16,136,512]{2,1,0:T(8,128)(2,1)} %pack.1), channel_id=1, replica_groups=mesh['zh'=4,'zl'=4,'x'=4,'c'=2,'tp'=4] {'x','tp'}, dimensions={0} | all-to-all | bytes 4456448 | tf_op jit(solution)/shard_map/all_to_all | solution.py:24
  38.0 5.9 %collective-permute-start = (bf16[4,4,136,512]{3,2,1,0:T(8,128)(2,1)S(1)}, bf16[4,4,136,512]{3,2,1,0:T(8,128)(2,1)}, u32[]{:S(2)}, u32[]{:S(2)}) collective-permute-start(bf16[4,4,136,512]{3,2,1,0:T(8,128)(2,1)S(1)} %bitcast.26), channel_id=1, source_target_pairs={{0,4},{4,0},{1,5},{5,1},{2,6},{6,2},{3,7},{7,3},{8,12},{12,8},{9,1... | collective-permute-start | bytes 6684680 | tf_op jit(solution)/shard_map/ppermute | solution.py:28
  45.4 8.1 %all_to_all.31 = bf16[8,16,256]{2,1,0:T(8,128)(2,1)S(1)} all-to-all(bf16[8,16,256]{2,1,0:T(8,128)(2,1)} %bitcast.37), channel_id=1, replica_groups=mesh['zh'=4,'zl'=4,'x'=4,'c'=2,'tp'=4] {'x','c'}, dimensions={0} | all-to-all | bytes 131072 | tf_op jit(solution)/shard_map/all_to_all | solution.py:24
  54.3 15.7 %collective-permute-start.3 = (bf16[176,256]{1,0:T(8,128)(2,1)S(1)}, bf16[176,256]{1,0:T(8,128)(2,1)S(1)}, u32[]{:S(2)}, u32[]{:S(2)}) collective-permute-start(bf16[176,256]{1,0:T(8,128)(2,1)S(1)} %pad_maximum_fusion.1.mine_ref), channel_id=1, source_target_pairs={{0,256},{32,288},{64,320},{96,352},{128,384},{160,416},{192,448},{... | collective-permute-start | bytes 270344 | tf_op jit(solution)/shard_map/ppermute | solution.py:507
  71.9 7.3 %collective-permute-start.1 = (bf16[176,256]{1,0:T(8,128)(2,1)S(1)}, bf16[176,256]{1,0:T(8,128)(2,1)S(1)}, u32[]{:S(2)}, u32[]{:S(2)}) collective-permute-start(bf16[176,256]{1,0:T(8,128)(2,1)S(1)} %pad_maximum_fusion.1.mine_ref), channel_id=1, source_target_pairs={{0,128},{32,160},{64,192},{96,224},{128,256},{160,288},{192,320},{... | collective-permute-start | bytes 270344 | tf_op jit(solution)/shard_map/ppermute | solution.py:507
  79.2 7.9 %collective-permute-done.2.after_ref = bf16[176,256]{1,0:T(8,128)(2,1)S(1)} collective-permute-done((bf16[176,256]{1,0:T(8,128)(2,1)S(1)}, bf16[176,256]{1,0:T(8,128)(2,1)S(1)}, u32[]{:S(2)}, u32[]{:S(2)}) %collective-permute-start.2) | collective-permute-done | bytes 90144 | tf_op jit(solution)/shard_map/ppermute | solution.py:507
  92.9 4.0 %collective-permute-start.4 = (bf16[4,176,256]{2,1,0:T(8,128)(2,1)}, bf16[4,176,256]{2,1,0:T(8,128)(2,1)S(1)}, u32[]{:S(2)}, u32[]{:S(2)}) collective-permute-start(bf16[4,176,256]{2,1,0:T(8,128)(2,1)} %get-tuple-element.24.w0_ref), channel_id=1, source_target_pairs={{0,480},{32,0},{64,32},{96,64},{128,96},{160,128},{192,160},{224,1... | collective-permute-start | bytes 1081352 | tf_op jit(solution)/shard_map/ppermute | solution.py:507
  98.8 4.3 %collective-permute-start.7 = (bf16[2,176,256]{2,1,0:T(8,128)(2,1)}, bf16[2,176,256]{2,1,0:T(8,128)(2,1)}, u32[]{:S(2)}, u32[]{:S(2)}) collective-permute-start(bf16[2,176,256]{2,1,0:T(8,128)(2,1)} %get-tuple-element.26), channel_id=1, source_target_pairs={{0,64},{32,96},{64,128},{96,160},{128,192},{160,224},{192,256},{22... | collective-permute-start | bytes 540680 | tf_op jit(solution)/shard_map/ppermute | solution.py:507
  105.0 5.8 %collective-permute-done.6.low_ref = bf16[2,176,256]{2,1,0:T(8,128)(2,1)} collective-permute-done((bf16[2,176,256]{2,1,0:T(8,128)(2,1)}, bf16[2,176,256]{2,1,0:T(8,128)(2,1)}, u32[]{:S(2)}, u32[]{:S(2)}) %collective-permute-start.6) | collective-permute-done | bytes 180256 | tf_op jit(solution)/shard_map/ppermute | solution.py:507
  110.8 4.1 %collective-permute-done.7.high_ref = bf16[2,176,256]{2,1,0:T(8,128)(2,1)} collective-permute-done((bf16[2,176,256]{2,1,0:T(8,128)(2,1)}, bf16[2,176,256]{2,1,0:T(8,128)(2,1)}, u32[]{:S(2)}, u32[]{:S(2)}) %collective-permute-start.7) | collective-permute-done | bytes 180256 | tf_op jit(solution)/shard_map/ppermute | solution.py:507
  115.8 6.4 %project.1 = (bf16[4,4,2,128,128]{4,3,2,1,0:T(8,128)(2,1)}, bf16[4,2,128,128]{3,2,1,0:T(8,128)(2,1)}, bf16[2,128,128]{2,1,0:T(8,128)(2,1)}, f32[2,8,128]{2,1,0:T...) custom-call(s32[4]{0:T(128)} %pad_add_fusion.place_ref, ...), custom_call_target="tpu_custom_call" | custom-call | tf_op jit(solution)/shard_map/project/pallas_call | solution.py:568
  122.2 19.2 %all_to_all.32.qk_ref = bf16[4,1024,128]{2,1,0:T(8,128)(2,1)} all-to-all(bf16[4,1024,128]{2,1,0:T(8,128)(2,1)} %bitcast.30), channel_id=1, replica_groups=mesh['zh'=4,'zl'=4,'x'=4,'c'=2,'tp'=4] {'x'}, dimensions={0} | all-to-all | bytes 2097152 | tf_op jit(solution)/shard_map/all_to_all | solution.py:24
  141.4 3.6 %slab_state.1 = (bf16[4,72,256]{2,1,0:T(8,128)(2,1)}, bf16[1024,256]{1,0:T(8,128)(2,1)}, bf16[1024,256]{1,0:T(8,128)(2,1)}) custom-call(bf16[4,1024,128]{2,1,0:T(8,128)(2,1)} %all_to_all.32.qk_ref, bf16[1024,128]{1,0:T(8,128)(2,1)} %bitcast.31, f32[2,8,128]{2,1,0:T(8,128)} %get-tuple-element.29.gate_ref, bf16[2,128,128]{2,1,0:T(8,128)(2,1)} %get-tuple-element.30.glu_ref), custom_call_target="tpu_custom_call" | custom-call | tf_op jit(solution)/shard_map/slab_state/pallas_call | solution.py:612
  145.0 9.5 %all_to_all.33.in_ref = bf16[4,72,256]{2,1,0:T(8,128)(2,1)} all-to-all(bf16[4,72,256]{2,1,0:T(8,128)(2,1)} %get-tuple-element.31), channel_id=1, replica_groups=mesh['zh'=4,'zl'=4,'x'=4,'c'=2,'tp'=4] {'zl'}, dimensions={0} | all-to-all | bytes 294912 | tf_op jit(solution)/shard_map/all_to_all | solution.py:24
  156.3 5.5 %all-to-all-start.4 = ((bf16[4,72,256]{2,1,0:T(8,128)(2,1)}), bf16[4,72,256]{2,1,0:T(8,128)(2,1)S(1)}, u32[]{:S(2)}, u32[]{:S(2)}) async-start(bf16[4,72,256]{2,1,0:T(8,128)(2,1)} %group.1), calls=%async_computation.4 | async-start | bytes 294912 | tf_op jit(solution)/shard_map/all_to_all | solution.py:24
  161.9 2.9 %collective-permute-start.10 = (bf16[4,16,768]{2,1,0:T(8,128)(2,1)S(1)}, bf16[4,16,768]{2,1,0:T(8,128)(2,1)S(1)}, u32[]{:S(2)}, u32[]{:S(2)}) collective-permute-start(bf16[4,16,768]{2,1,0:T(8,128)(2,1)S(1)} %get-tuple-element.40), channel_id=1, source_target_pairs={{0,3},{1,0},{2,1},{3,2},{4,7},{5,4},{6,5},{7,6},{8,11},{9,8},{10,9... | collective-permute-start | bytes 294920 | tf_op jit(solution)/shard_map/ppermute | solution.py:587
  164.8 2.9 %collective-permute-start.9 = (bf16[4,16,768]{2,1,0:T(8,128)(2,1)S(1)}, bf16[4,16,768]{2,1,0:T(8,128)(2,1)S(1)}, u32[]{:S(2)}, u32[]{:S(2)}) collective-permute-start(bf16[4,16,768]{2,1,0:T(8,128)(2,1)S(1)} %get-tuple-element.41), channel_id=1, source_target_pairs={{0,2},{1,3},{2,0},{3,1},{4,6},{5,7},{6,4},{7,5},{8,10},{9,11},{10,... | collective-permute-start | bytes 294920 | tf_op jit(solution)/shard_map/ppermute | solution.py:587
  171.7 2.9 %collective-permute-done.8 = bf16[4,16,768]{2,1,0:T(8,128)(2,1)S(1)} collective-permute-done((bf16[4,16,768]{2,1,0:T(8,128)(2,1)S(1)}, bf16[4,16,768]{2,1,0:T(8,128)(2,1)S(1)}, u32[]{:S(2)}, u32[]{:S(2)}) %collective-permute-start.8) | collective-permute-done | bytes 98336 | tf_op jit(solution)/shard_map/ppermute | solution.py:587
  176.8 3.7 %collective-permute-start.12 = (bf16[4,4,16,768]{3,2,1,0:T(8,128)(2,1)S(1)}, bf16[4,4,16,768]{3,2,1,0:T(8,128)(2,1)S(1)}, u32[]{:S(2)}, u32[]{:S(2)}) collective-permute-start(bf16[4,4,16,768]{3,2,1,0:T(8,128)(2,1)S(1)} %pad_maximum_fusion.refs_0_), channel_id=1, source_target_pairs={{0,16},{8,24},{16,0},{24,8},{1,17},{9,25},{17,1},{25,9},{2,18},{10... | collective-permute-start | bytes 1179656 | tf_op jit(solution)/shard_map/ppermute | solution.py:593
  183.0 7.2 %local.1 = (f32[1024,128]{1,0:T(8,128)}, f32[256,128]{1,0:T(8,128)}) custom-call(s32[4]{0:T(128)} %pad_add_fusion.place_ref, bf16[1024,256]{1,0:T(8,128)(2,1)} %get-tuple-element.32.q_ref, bf16[1024,256]{1,0:T(8,128)(2,1)} %get-tuple-element.33.k_ref, bf16[1024,128]{1,0:T(8,128)(2,1)} %bitcast.32, f32[2,8,128]{2,1,0:T(8,128)} %get-tuple-element.29.gate_ref, ...), custom_call_target="tpu_custom_call" | custom-call | tf_op jit(solution)/shard_map/local/pallas_call | solution.py:635
  190.9 4.3 %cell.1 = bf16[4,2,4,96,128]{4,3,2,1,0:T(8,128)(2,1)} custom-call(s32[4]{0:T(128)} %pad_add_fusion.place_ref, bf16[4,72,256]{2,1,0:T(8,128)(2,1)} %copy-done.3, bf16[4,72,256]{2,1,0:T(8,128)(2,1)} %all_to_all.33.in_ref, bf16[1024,256]{1,0:T(8,128)(2,1)} %get-tuple-element.32.q_ref, f32[1024,128]{1,0:T(8,128)} %get-tuple-element.34.local_ref, ...), custom_call_target="tpu_custom_call" | custom-call | tf_op jit(solution)/shard_map/cell/pallas_call | solution.py:644
  195.2 11.1 %all-to-all-start.5 = ((bf16[32,96,128]{2,1,0:T(8,128)(2,1)}), bf16[32,96,128]{2,1,0:T(8,128)(2,1)S(1)}, u32[]{:S(2)}, u32[]{:S(2)}) async-start(bf16[32,96,128]{2,1,0:T(8,128)(2,1)} %bitcast.29), calls=%async_computation.5 | async-start | bytes 1572864 | tf_op jit(solution)/shard_map/all_to_all | solution.py:24
  216.6 3.7 %assemble.1.weight_ref = bf16[4,4,4,2,16,768]{5,4,3,2,1,0:T(8,128)(2,1)} custom-call(s32[4]{0:T(128)} %pad_add_fusion.place_ref, bf16[4,4,16,768]{3,2,1,0:T(8,128)(2,1)} %copy-done.2, bf16[4,4,16,768]{3,2,1,0:T(8,128)(2,1)} %copy-done.6, bf16[4,4,16,768]{3,2,1,0:T(8,128)(2,1)} %copy-done.5, bf16[4,4,16,768]{3,2,1,0:T(8,128)(2,1)} %copy-done.4, ...), custom_call_target="tpu_custom_call" | custom-call | tf_op jit(solution)/shard_map/assemble/pallas_call | solution.py:655
  221.2 4.4 %finish.1 = bf16[128,512]{1,0:T(8,128)(2,1)} custom-call(bf16[4,2,4,96,128]{4,3,2,1,0:T(8,128)(2,1)} %bitcast.28, bf16[4,4,4,2,16,768]{5,4,3,2,1,0:T(8,128)(2,1)} %assemble.1.weight_ref, f32[4,512]{1,0:T(4,128)} %get-tuple-element.37.memory_gain_ref, f32[4,256]{1,0:T(4,128)} %get-tuple-element.38.conv_gain_ref), custom_call_target="tpu_custom_call" | custom-call | tf_op jit(solution)/shard_map/finish/pallas_call | solution.py:656
  (76 shorter events, 40.6 us)
Async XLA Ops:
  3.7 99.3 %copy-start.17 = (bf16[2048,2]{0,1:T(2,128)(2,1)S(1)}, bf16[2048,2]{0,1:T(2,128)(2,1)}, u32[]{:S(2)}) copy-start(bf16[2048,2]{0,1:T(2,128)(2,1)} %param.24) | copy-start | bytes 24580
  3.7 99.4 %copy-start.18 = (bf16[2048,2]{0,1:T(2,128)(2,1)S(1)}, bf16[2048,2]{0,1:T(2,128)(2,1)}, u32[]{:S(2)}) copy-start(bf16[2048,2]{0,1:T(2,128)(2,1)} %param.23) | copy-start | bytes 24580
  38.0 76.9 %copy-start = (bf16[16,136,512]{2,1,0:T(8,128)(2,1)}, bf16[16,136,512]{2,1,0:T(8,128)(2,1)S(1)}, u32[]{:S(2)}) copy-start(bf16[16,136,512]{2,1,0:T(8,128)(2,1)S(1)} %all_to_all.30) | copy-start | bytes 6684676
  38.0 76.9 %collective-permute-start = (bf16[4,4,136,512]{3,2,1,0:T(8,128)(2,1)S(1)}, bf16[4,4,136,512]{3,2,1,0:T(8,128)(2,1)}, u32[]{:S(2)}, u32[]{:S(2)}) collective-permute-start(bf16[4,4,136,512]{3,2,1,0:T(8,128)(2,1)S(1)} %bitcast.26), channel_id=1, source_target_pairs={{0,4},{4,0},{1,5},{5,1},{2,6},{6,2},{3,7},{7,3},{8,12},{12,8},{9,1... | collective-permute-start | bytes 6684680 | tf_op jit(solution)/shard_map/ppermute | solution.py:28
  54.3 24.9 %collective-permute-start.3 = (bf16[176,256]{1,0:T(8,128)(2,1)S(1)}, bf16[176,256]{1,0:T(8,128)(2,1)S(1)}, u32[]{:S(2)}, u32[]{:S(2)}) collective-permute-start(bf16[176,256]{1,0:T(8,128)(2,1)S(1)} %pad_maximum_fusion.1.mine_ref), channel_id=1, source_target_pairs={{0,256},{32,288},{64,320},{96,352},{128,384},{160,416},{192,448},{... | collective-permute-start | bytes 270344 | tf_op jit(solution)/shard_map/ppermute | solution.py:507
  70.0 17.2 %collective-permute-start.2 = (bf16[176,256]{1,0:T(8,128)(2,1)S(1)}, bf16[176,256]{1,0:T(8,128)(2,1)S(1)}, u32[]{:S(2)}, u32[]{:S(2)}) collective-permute-start(bf16[176,256]{1,0:T(8,128)(2,1)S(1)} %pad_maximum_fusion.1.mine_ref), channel_id=1, source_target_pairs={{0,384},{32,416},{64,448},{96,480},{128,0},{160,32},{192,64},{224,... | collective-permute-start | bytes 270344 | tf_op jit(solution)/shard_map/ppermute | solution.py:507
  71.9 15.2 %collective-permute-start.1 = (bf16[176,256]{1,0:T(8,128)(2,1)S(1)}, bf16[176,256]{1,0:T(8,128)(2,1)S(1)}, u32[]{:S(2)}, u32[]{:S(2)}) collective-permute-start(bf16[176,256]{1,0:T(8,128)(2,1)S(1)} %pad_maximum_fusion.1.mine_ref), channel_id=1, source_target_pairs={{0,128},{32,160},{64,192},{96,224},{128,256},{160,288},{192,320},{... | collective-permute-start | bytes 270344 | tf_op jit(solution)/shard_map/ppermute | solution.py:507
  90.4 24.5 %collective-permute-start.5 = (bf16[4,176,256]{2,1,0:T(8,128)(2,1)}, bf16[4,176,256]{2,1,0:T(8,128)(2,1)S(1)}, u32[]{:S(2)}, u32[]{:S(2)}) collective-permute-start(bf16[4,176,256]{2,1,0:T(8,128)(2,1)} %get-tuple-element.24.w0_ref), channel_id=1, source_target_pairs={{0,32},{32,64},{64,96},{96,128},{128,160},{160,192},{192,224},{224... | collective-permute-start | bytes 1081352 | tf_op jit(solution)/shard_map/ppermute | solution.py:507
  92.9 22.0 %collective-permute-start.4 = (bf16[4,176,256]{2,1,0:T(8,128)(2,1)}, bf16[4,176,256]{2,1,0:T(8,128)(2,1)S(1)}, u32[]{:S(2)}, u32[]{:S(2)}) collective-permute-start(bf16[4,176,256]{2,1,0:T(8,128)(2,1)} %get-tuple-element.24.w0_ref), channel_id=1, source_target_pairs={{0,480},{32,0},{64,32},{96,64},{128,96},{160,128},{192,160},{224,1... | collective-permute-start | bytes 1081352 | tf_op jit(solution)/shard_map/ppermute | solution.py:507
  96.9 13.9 %collective-permute-start.6 = (bf16[2,176,256]{2,1,0:T(8,128)(2,1)}, bf16[2,176,256]{2,1,0:T(8,128)(2,1)}, u32[]{:S(2)}, u32[]{:S(2)}) collective-permute-start(bf16[2,176,256]{2,1,0:T(8,128)(2,1)} %get-tuple-element.25), channel_id=1, source_target_pairs={{0,448},{32,480},{64,0},{96,32},{128,64},{160,96},{192,128},{224,1... | collective-permute-start | bytes 540680 | tf_op jit(solution)/shard_map/ppermute | solution.py:507
  98.8 16.1 %collective-permute-start.7 = (bf16[2,176,256]{2,1,0:T(8,128)(2,1)}, bf16[2,176,256]{2,1,0:T(8,128)(2,1)}, u32[]{:S(2)}, u32[]{:S(2)}) collective-permute-start(bf16[2,176,256]{2,1,0:T(8,128)(2,1)} %get-tuple-element.26), channel_id=1, source_target_pairs={{0,64},{32,96},{64,128},{96,160},{128,192},{160,224},{192,256},{22... | collective-permute-start | bytes 540680 | tf_op jit(solution)/shard_map/ppermute | solution.py:507
  122.2 39.6 %copy-start.10 = (bf16[4,4,16,768]{3,2,1,0:T(8,128)(2,1)S(1)}, bf16[4,4,16,768]{3,2,1,0:T(8,128)(2,1)}, u32[]{:S(2)}) copy-start(bf16[4,4,16,768]{3,2,1,0:T(8,128)(2,1)} %get-tuple-element.36) | copy-start | bytes 1179652
  156.3 33.9 %all-to-all-start.4 = ((bf16[4,72,256]{2,1,0:T(8,128)(2,1)}), bf16[4,72,256]{2,1,0:T(8,128)(2,1)S(1)}, u32[]{:S(2)}, u32[]{:S(2)}) async-start(bf16[4,72,256]{2,1,0:T(8,128)(2,1)} %group.1), calls=%async_computation.4 | async-start | bytes 294912 | tf_op jit(solution)/shard_map/all_to_all | solution.py:24
  161.9 7.9 %collective-permute-start.10 = (bf16[4,16,768]{2,1,0:T(8,128)(2,1)S(1)}, bf16[4,16,768]{2,1,0:T(8,128)(2,1)S(1)}, u32[]{:S(2)}, u32[]{:S(2)}) collective-permute-start(bf16[4,16,768]{2,1,0:T(8,128)(2,1)S(1)} %get-tuple-element.40), channel_id=1, source_target_pairs={{0,3},{1,0},{2,1},{3,2},{4,7},{5,4},{6,5},{7,6},{8,11},{9,8},{10,9... | collective-permute-start | bytes 294920 | tf_op jit(solution)/shard_map/ppermute | solution.py:587
  164.8 6.9 %collective-permute-start.9 = (bf16[4,16,768]{2,1,0:T(8,128)(2,1)S(1)}, bf16[4,16,768]{2,1,0:T(8,128)(2,1)S(1)}, u32[]{:S(2)}, u32[]{:S(2)}) collective-permute-start(bf16[4,16,768]{2,1,0:T(8,128)(2,1)S(1)} %get-tuple-element.41), channel_id=1, source_target_pairs={{0,2},{1,3},{2,0},{3,1},{4,6},{5,7},{6,4},{7,5},{8,10},{9,11},{10,... | collective-permute-start | bytes 294920 | tf_op jit(solution)/shard_map/ppermute | solution.py:587
  167.7 6.9 %collective-permute-start.8 = (bf16[4,16,768]{2,1,0:T(8,128)(2,1)S(1)}, bf16[4,16,768]{2,1,0:T(8,128)(2,1)S(1)}, u32[]{:S(2)}, u32[]{:S(2)}) collective-permute-start(bf16[4,16,768]{2,1,0:T(8,128)(2,1)S(1)} %get-tuple-element.42), channel_id=1, source_target_pairs={{0,1},{1,2},{2,3},{3,0},{4,5},{5,6},{6,7},{7,4},{8,9},{9,10},{10,1... | collective-permute-start | bytes 294920 | tf_op jit(solution)/shard_map/ppermute | solution.py:587
  174.6 33.8 %collective-permute-start.13 = (bf16[4,4,16,768]{3,2,1,0:T(8,128)(2,1)S(1)}, bf16[4,4,16,768]{3,2,1,0:T(8,128)(2,1)S(1)}, u32[]{:S(2)}, u32[]{:S(2)}) collective-permute-start(bf16[4,4,16,768]{3,2,1,0:T(8,128)(2,1)S(1)} %pad_maximum_fusion.refs_0_), channel_id=1, source_target_pairs={{0,8},{8,16},{16,24},{24,0},{1,9},{9,17},{17,25},{25,1},{2,10},{10... | collective-permute-start | bytes 1179656 | tf_op jit(solution)/shard_map/ppermute | solution.py:593
  176.8 33.8 %collective-permute-start.12 = (bf16[4,4,16,768]{3,2,1,0:T(8,128)(2,1)S(1)}, bf16[4,4,16,768]{3,2,1,0:T(8,128)(2,1)S(1)}, u32[]{:S(2)}, u32[]{:S(2)}) collective-permute-start(bf16[4,4,16,768]{3,2,1,0:T(8,128)(2,1)S(1)} %pad_maximum_fusion.refs_0_), channel_id=1, source_target_pairs={{0,16},{8,24},{16,0},{24,8},{1,17},{9,25},{17,1},{25,9},{2,18},{10... | collective-permute-start | bytes 1179656 | tf_op jit(solution)/shard_map/ppermute | solution.py:593
  180.5 32.3 %collective-permute-start.11 = (bf16[4,4,16,768]{3,2,1,0:T(8,128)(2,1)S(1)}, bf16[4,4,16,768]{3,2,1,0:T(8,128)(2,1)S(1)}, u32[]{:S(2)}, u32[]{:S(2)}) collective-permute-start(bf16[4,4,16,768]{3,2,1,0:T(8,128)(2,1)S(1)} %pad_maximum_fusion.refs_0_), channel_id=1, source_target_pairs={{0,24},{8,0},{16,8},{24,16},{1,25},{9,1},{17,9},{25,17},{2,26},{10... | collective-permute-start | bytes 1179656 | tf_op jit(solution)/shard_map/ppermute | solution.py:593
  195.2 25.1 %all-to-all-start.5 = ((bf16[32,96,128]{2,1,0:T(8,128)(2,1)}), bf16[32,96,128]{2,1,0:T(8,128)(2,1)S(1)}, u32[]{:S(2)}, u32[]{:S(2)}) async-start(bf16[32,96,128]{2,1,0:T(8,128)(2,1)} %bitcast.29), calls=%async_computation.5 | async-start | bytes 1572864 | tf_op jit(solution)/shard_map/all_to_all | solution.py:24
  206.3 8.8 %collective-permute-start.14 = (bf16[4,4,16,768]{3,2,1,0:T(8,128)(2,1)S(1)}, bf16[4,4,16,768]{3,2,1,0:T(8,128)(2,1)S(1)}, u32[]{:S(2)}, u32[]{:S(2)}) collective-permute-start(bf16[4,4,16,768]{3,2,1,0:T(8,128)(2,1)S(1)} %pad_maximum_fusion.refs_0_), channel_id=1, source_target_pairs={{0,4},{4,0},{1,5},{5,1},{2,6},{6,2},{3,7},{7,3},{8,12},{12,8},{9,1... | collective-permute-start | bytes 1179656 | tf_op jit(solution)/shard_map/ppermute | solution.py:28
  208.4 6.6 %collective-permute-start.17 = (bf16[4,4,16,768]{3,2,1,0:T(8,128)(2,1)S(1)}, bf16[4,4,16,768]{3,2,1,0:T(8,128)(2,1)S(1)}, u32[]{:S(2)}, u32[]{:S(2)}) collective-permute-start(bf16[4,4,16,768]{3,2,1,0:T(8,128)(2,1)S(1)} %collective-permute-done.13.refs_3_), channel_id=1, source_target_pairs={{0,4},{4,0},{1,5},{5,1},{2,6},{6,2},{3,7},{7,3},{8,12},{12,8},{9,1... | collective-permute-start | bytes 1179656 | tf_op jit(solution)/shard_map/ppermute | solution.py:28
  210.6 4.4 %collective-permute-start.16 = (bf16[4,4,16,768]{3,2,1,0:T(8,128)(2,1)S(1)}, bf16[4,4,16,768]{3,2,1,0:T(8,128)(2,1)S(1)}, u32[]{:S(2)}, u32[]{:S(2)}) collective-permute-start(bf16[4,4,16,768]{3,2,1,0:T(8,128)(2,1)S(1)} %collective-permute-done.12.refs_2_), channel_id=1, source_target_pairs={{0,4},{4,0},{1,5},{5,1},{2,6},{6,2},{3,7},{7,3},{8,12},{12,8},{9,1... | collective-permute-start | bytes 1179656 | tf_op jit(solution)/shard_map/ppermute | solution.py:28
  212.8 3.7 %collective-permute-start.15 = (bf16[4,4,16,768]{3,2,1,0:T(8,128)(2,1)S(1)}, bf16[4,4,16,768]{3,2,1,0:T(8,128)(2,1)}, u32[]{:S(2)}, u32[]{:S(2)}) collective-permute-start(bf16[4,4,16,768]{3,2,1,0:T(8,128)(2,1)S(1)} %collective-permute-done.11.refs_1_), channel_id=1, source_target_pairs={{0,4},{4,0},{1,5},{5,1},{2,6},{6,2},{3,7},{7,3},{8,12},{12,8},{9,1... | collective-permute-start | bytes 1179656 | tf_op jit(solution)/shard_map/ppermute | solution.py:28
  (15 other events, 98.7 us)

commit v11 on v10

--- a/solution.py
+++ b/solution.py
@@ -165,24 +165,19 @@
         out_weight_ref[pl.ds(behind, 1), pl.ds(homes[-1][1], 1)] = jnp.concatenate(
             [ref[i, rows + j * depth : rows + (j + 1) * depth] for j in range(chunks)], axis=1
         )[None, None]
+    right = []
+    for (w_ref, i, _), (y, z) in zip(blocks, homes):
+        start = pl.multiple_of(y * part + z * rows, rows)
+        right.append(jnp.concatenate([w_ref[i, :rows], gate_ref[pl.ds(start, rows)]], axis=1))
+    right = jnp.concatenate(right, axis=0)
     for half, ref in enumerate((own_ref, other_ref)):
         home = core if half == 0 else 1 - core
-        acc = jnp.zeros((tokens_rows, wide), F32)
-        pre = jnp.zeros((tokens_rows, gate_ref.shape[1]), F32)
-        for pair in range(0, len(blocks), 2):
-            left, right, gate_rows = [], [], []
-            for at in (pair, pair + 1):
-                w_ref, i, _ = blocks[at]
-                y, z = homes[at]
-                start = pl.multiple_of(z * rows, rows)
-                left.append(
-                    ref[:, pl.ds(y, 1), :length, pl.ds(start, rows)].reshape(tokens_rows, rows)
-                )
-                right.append(w_ref[i, :rows])
-                gate_rows.append(gate_ref[pl.ds(y * part + start, rows)])
-            lhs = jnp.concatenate(left, axis=1)
-            acc = acc + dot(lhs, jnp.concatenate(right, axis=0), NN)
-            pre = pre + dot(lhs, jnp.concatenate(gate_rows, axis=0), NN)
+        left = []
+        for y, z in homes:
+            lanes = pl.ds(pl.multiple_of(z * rows, rows), rows)
+            left.append(ref[:, pl.ds(y, 1), :length, lanes].reshape(tokens_rows, rows))
+        acc = dot(jnp.concatenate(left, axis=1), right, NN)
+        pre = acc[:, wide:]
         glu = []
         for x in range(nx):
             mine = acc[x * length : (x + 1) * length]
@@ -193,8 +188,8 @@
                 [mine[:, 2 * width : 3 * width].astype(BF16), ones], axis=1
             )[None]
             left = mine[:, 3 * width : 3 * width + chan]
-            right = mine[:, 3 * width + chan :]
-            glu.append(left / (1.0 + jnp.exp(-right)))
+            gates_side = mine[:, 3 * width + chan : wide]
+            glu.append(left / (1.0 + jnp.exp(-gates_side)))
         glu_ref[pl.ds(home, 1)] = jnp.concatenate(glu, axis=1).astype(BF16)[None]
         for x in range(nx):
             turned = pre[x * length : (x + 1) * length].T
@@ -592,9 +587,11 @@
     def from_x(value, ahead):
         return lax.ppermute(value, "x", [(j, (j - ahead) % nx) for j in range(nx)])
 
-    out_parts = [out_part] + [from_x(out_part, ahead) for ahead in (1, 3)]
-    out_parts.insert(2, from_x(out_part, 2))
-    other_parts = [swapped(out, "c") for out in out_parts]
+    out_parts = [out_part, from_x(out_part, 1)]
+    from_last = from_x(out_part, 3)
+    out_parts += [from_x(out_part, 2), from_last]
+    other_parts = [swapped(out, "c") for out in out_parts[:2]]
+    other_parts += [swapped(out, "c") for out in out_parts[2:]]
 
     state_rows = width + 8
     call_slab = pl.pallas_call(

time: 227 us -> 227 us (level)
  no operation moved by 1% of the time
where the time goes in v11:
time: 227 us; the launch traced here: 226 us
  starting transfers between devices  84.9 us (37%)
  blocking collectives  71.1 us (31%)
  Pallas kernels  37.3 us (16%)
  waiting for transfers between devices  23.4 us (10%)
  local copies, waits for them, and re-layouts  5.75 us (3%)
  other arithmetic  2.68 us (1%)
    all_to_all x4, blocking collectives, exchange(): return lax.all_to_all(pieces, axes, split_axis=0, concat_axis=0, tiled=True)  71.1 us
    ppermute x7, starting transfers between devices, from_z(): lax.ppermute(value, Z, [(j, (j - ahead) % members) for j in range(members)])  37.6 us
    ppermute x7, waiting for transfers between devices, from_z(): lax.ppermute(value, Z, [(j, (j - ahead) % members) for j in range(members)])  17.9 us
    all_to_all x2, starting transfers between devices, exchange(): return lax.all_to_all(pieces, axes, split_axis=0, concat_axis=0, tiled=True)  16.5 us
    ppermute x5, starting transfers between devices, swapped(): return lax.ppermute(value, axis, [(0, 1), (1, 0)])  14.5 us
    ppermute x3, starting transfers between devices, from_x(): return lax.ppermute(value, 'x', [(j, (j - ahead) % nx) for j in range(nx)])  8.43 us
    ppermute x3, starting transfers between devices, layer(): lax.ppermute(out_part[ahead], 'tp', [(j, (j + ahead) % ny) for j in range...  7.83 us
    pallas_call x1, Pallas kernels, layer(): call_local(place, query, key, value, gates, packed, conv_kernel)  7.2 us
  transfers between devices with their start and end apart: 20, of which 6 were waited for; matrix products, arithmetic and copies ran while one was open for 1% of the time, Pallas kernels for 8%

profile of v11, /device:TPU:1, one launch (start us, length us, event | category | flops | bytes accessed | tf_op | source)
XLA Modules:
  0.0 225.6 jit_solution(2982850568767505199)
XLA Ops:
  3.7 34.3 %all_to_all.30 = bf16[16,136,512]{2,1,0:T(8,128)(2,1)S(1)} all-to-all(bf16[16,136,512]{2,1,0:T(8,128)(2,1)} %pack.1), channel_id=1, replica_groups=mesh['zh'=4,'zl'=4,'x'=4,'c'=2,'tp'=4] {'x','tp'}, dimensions={0} | all-to-all | bytes 4456448 | tf_op jit(solution)/shard_map/all_to_all | solution.py:24
  38.0 5.9 %collective-permute-start = (bf16[4,4,136,512]{3,2,1,0:T(8,128)(2,1)S(1)}, bf16[4,4,136,512]{3,2,1,0:T(8,128)(2,1)}, u32[]{:S(2)}, u32[]{:S(2)}) collective-permute-start(bf16[4,4,136,512]{3,2,1,0:T(8,128)(2,1)S(1)} %bitcast.26), channel_id=1, source_target_pairs={{0,4},{4,0},{1,5},{5,1},{2,6},{6,2},{3,7},{7,3},{8,12},{12,8},{9,1... | collective-permute-start | bytes 6684680 | tf_op jit(solution)/shard_map/ppermute | solution.py:28
  45.4 8.1 %all_to_all.31 = bf16[8,16,256]{2,1,0:T(8,128)(2,1)S(1)} all-to-all(bf16[8,16,256]{2,1,0:T(8,128)(2,1)} %bitcast.37), channel_id=1, replica_groups=mesh['zh'=4,'zl'=4,'x'=4,'c'=2,'tp'=4] {'x','c'}, dimensions={0} | all-to-all | bytes 131072 | tf_op jit(solution)/shard_map/all_to_all | solution.py:24
  54.3 15.7 %collective-permute-start.3 = (bf16[176,256]{1,0:T(8,128)(2,1)S(1)}, bf16[176,256]{1,0:T(8,128)(2,1)S(1)}, u32[]{:S(2)}, u32[]{:S(2)}) collective-permute-start(bf16[176,256]{1,0:T(8,128)(2,1)S(1)} %pad_maximum_fusion.1.mine_ref), channel_id=1, source_target_pairs={{0,256},{32,288},{64,320},{96,352},{128,384},{160,416},{192,448},{... | collective-permute-start | bytes 270344 | tf_op jit(solution)/shard_map/ppermute | solution.py:502
  71.9 7.3 %collective-permute-start.1 = (bf16[176,256]{1,0:T(8,128)(2,1)S(1)}, bf16[176,256]{1,0:T(8,128)(2,1)S(1)}, u32[]{:S(2)}, u32[]{:S(2)}) collective-permute-start(bf16[176,256]{1,0:T(8,128)(2,1)S(1)} %pad_maximum_fusion.1.mine_ref), channel_id=1, source_target_pairs={{0,128},{32,160},{64,192},{96,224},{128,256},{160,288},{192,320},{... | collective-permute-start | bytes 270344 | tf_op jit(solution)/shard_map/ppermute | solution.py:502
  79.2 7.9 %collective-permute-done.2.after_ref = bf16[176,256]{1,0:T(8,128)(2,1)S(1)} collective-permute-done((bf16[176,256]{1,0:T(8,128)(2,1)S(1)}, bf16[176,256]{1,0:T(8,128)(2,1)S(1)}, u32[]{:S(2)}, u32[]{:S(2)}) %collective-permute-start.2) | collective-permute-done | bytes 90144 | tf_op jit(solution)/shard_map/ppermute | solution.py:502
  92.9 4.0 %collective-permute-start.4 = (bf16[4,176,256]{2,1,0:T(8,128)(2,1)}, bf16[4,176,256]{2,1,0:T(8,128)(2,1)S(1)}, u32[]{:S(2)}, u32[]{:S(2)}) collective-permute-start(bf16[4,176,256]{2,1,0:T(8,128)(2,1)} %get-tuple-element.24.w0_ref), channel_id=1, source_target_pairs={{0,480},{32,0},{64,32},{96,64},{128,96},{160,128},{192,160},{224,1... | collective-permute-start | bytes 1081352 | tf_op jit(solution)/shard_map/ppermute | solution.py:502
  98.8 4.3 %collective-permute-start.7 = (bf16[2,176,256]{2,1,0:T(8,128)(2,1)}, bf16[2,176,256]{2,1,0:T(8,128)(2,1)}, u32[]{:S(2)}, u32[]{:S(2)}) collective-permute-start(bf16[2,176,256]{2,1,0:T(8,128)(2,1)} %get-tuple-element.26), channel_id=1, source_target_pairs={{0,64},{32,96},{64,128},{96,160},{128,192},{160,224},{192,256},{22... | collective-permute-start | bytes 540680 | tf_op jit(solution)/shard_map/ppermute | solution.py:502
  105.0 5.8 %collective-permute-done.6.low_ref = bf16[2,176,256]{2,1,0:T(8,128)(2,1)} collective-permute-done((bf16[2,176,256]{2,1,0:T(8,128)(2,1)}, bf16[2,176,256]{2,1,0:T(8,128)(2,1)}, u32[]{:S(2)}, u32[]{:S(2)}) %collective-permute-start.6) | collective-permute-done | bytes 180256 | tf_op jit(solution)/shard_map/ppermute | solution.py:502
  110.8 4.1 %collective-permute-done.7.high_ref = bf16[2,176,256]{2,1,0:T(8,128)(2,1)} collective-permute-done((bf16[2,176,256]{2,1,0:T(8,128)(2,1)}, bf16[2,176,256]{2,1,0:T(8,128)(2,1)}, u32[]{:S(2)}, u32[]{:S(2)}) %collective-permute-start.7) | collective-permute-done | bytes 180256 | tf_op jit(solution)/shard_map/ppermute | solution.py:502
  115.8 6.4 %project.1 = (bf16[4,4,2,128,128]{4,3,2,1,0:T(8,128)(2,1)}, bf16[4,2,128,128]{3,2,1,0:T(8,128)(2,1)}, bf16[2,128,128]{2,1,0:T(8,128)(2,1)}, f32[2,8,128]{2,1,0:T...) custom-call(s32[4]{0:T(128)} %pad_add_fusion.place_ref, ...), custom_call_target="tpu_custom_call" | custom-call | tf_op jit(solution)/shard_map/project/pallas_call | solution.py:563
  122.2 19.2 %all_to_all.32.qk_ref = bf16[4,1024,128]{2,1,0:T(8,128)(2,1)} all-to-all(bf16[4,1024,128]{2,1,0:T(8,128)(2,1)} %bitcast.30), channel_id=1, replica_groups=mesh['zh'=4,'zl'=4,'x'=4,'c'=2,'tp'=4] {'x'}, dimensions={0} | all-to-all | bytes 2097152 | tf_op jit(solution)/shard_map/all_to_all | solution.py:24
  141.4 3.6 %slab_state.1 = (bf16[4,72,256]{2,1,0:T(8,128)(2,1)}, bf16[1024,256]{1,0:T(8,128)(2,1)}, bf16[1024,256]{1,0:T(8,128)(2,1)}) custom-call(bf16[4,1024,128]{2,1,0:T(8,128)(2,1)} %all_to_all.32.qk_ref, bf16[1024,128]{1,0:T(8,128)(2,1)} %bitcast.31, f32[2,8,128]{2,1,0:T(8,128)} %get-tuple-element.29.gate_ref, bf16[2,128,128]{2,1,0:T(8,128)(2,1)} %get-tuple-element.30.glu_ref), custom_call_target="tpu_custom_call" | custom-call | tf_op jit(solution)/shard_map/slab_state/pallas_call | solution.py:609
  145.0 9.5 %all_to_all.33.in_ref = bf16[4,72,256]{2,1,0:T(8,128)(2,1)} all-to-all(bf16[4,72,256]{2,1,0:T(8,128)(2,1)} %get-tuple-element.31), channel_id=1, replica_groups=mesh['zh'=4,'zl'=4,'x'=4,'c'=2,'tp'=4] {'zl'}, dimensions={0} | all-to-all | bytes 294912 | tf_op jit(solution)/shard_map/all_to_all | solution.py:24
  156.3 5.5 %all-to-all-start.4 = ((bf16[4,72,256]{2,1,0:T(8,128)(2,1)}), bf16[4,72,256]{2,1,0:T(8,128)(2,1)S(1)}, u32[]{:S(2)}, u32[]{:S(2)}) async-start(bf16[4,72,256]{2,1,0:T(8,128)(2,1)} %group.1), calls=%async_computation.4 | async-start | bytes 294912 | tf_op jit(solution)/shard_map/all_to_all | solution.py:24
  161.8 2.9 %collective-permute-start.10 = (bf16[4,16,768]{2,1,0:T(8,128)(2,1)S(1)}, bf16[4,16,768]{2,1,0:T(8,128)(2,1)S(1)}, u32[]{:S(2)}, u32[]{:S(2)}) collective-permute-start(bf16[4,16,768]{2,1,0:T(8,128)(2,1)S(1)} %get-tuple-element.40), channel_id=1, source_target_pairs={{0,3},{1,0},{2,1},{3,2},{4,7},{5,4},{6,5},{7,6},{8,11},{9,8},{10,9... | collective-permute-start | bytes 294920 | tf_op jit(solution)/shard_map/ppermute | solution.py:582
  164.8 2.9 %collective-permute-start.9 = (bf16[4,16,768]{2,1,0:T(8,128)(2,1)S(1)}, bf16[4,16,768]{2,1,0:T(8,128)(2,1)S(1)}, u32[]{:S(2)}, u32[]{:S(2)}) collective-permute-start(bf16[4,16,768]{2,1,0:T(8,128)(2,1)S(1)} %get-tuple-element.41), channel_id=1, source_target_pairs={{0,2},{1,3},{2,0},{3,1},{4,6},{5,7},{6,4},{7,5},{8,10},{9,11},{10,... | collective-permute-start | bytes 294920 | tf_op jit(solution)/shard_map/ppermute | solution.py:582
  171.6 2.9 %collective-permute-done.8 = bf16[4,16,768]{2,1,0:T(8,128)(2,1)S(1)} collective-permute-done((bf16[4,16,768]{2,1,0:T(8,128)(2,1)S(1)}, bf16[4,16,768]{2,1,0:T(8,128)(2,1)S(1)}, u32[]{:S(2)}, u32[]{:S(2)}) %collective-permute-start.8) | collective-permute-done | bytes 98336 | tf_op jit(solution)/shard_map/ppermute | solution.py:582
  176.8 3.7 %collective-permute-start.12 = (bf16[4,4,16,768]{3,2,1,0:T(8,128)(2,1)S(1)}, bf16[4,4,16,768]{3,2,1,0:T(8,128)(2,1)S(1)}, u32[]{:S(2)}, u32[]{:S(2)}) collective-permute-start(bf16[4,4,16,768]{3,2,1,0:T(8,128)(2,1)S(1)} %pad_maximum_fusion.refs_0_), channel_id=1, source_target_pairs={{0,16},{8,24},{16,0},{24,8},{1,17},{9,25},{17,1},{25,9},{2,18},{10... | collective-permute-start | bytes 1179656 | tf_op jit(solution)/shard_map/ppermute | solution.py:588
  183.0 7.2 %local.1 = (f32[1024,128]{1,0:T(8,128)}, f32[256,128]{1,0:T(8,128)}) custom-call(s32[4]{0:T(128)} %pad_add_fusion.place_ref, bf16[1024,256]{1,0:T(8,128)(2,1)} %get-tuple-element.32.q_ref, bf16[1024,256]{1,0:T(8,128)(2,1)} %get-tuple-element.33.k_ref, bf16[1024,128]{1,0:T(8,128)(2,1)} %bitcast.32, f32[2,8,128]{2,1,0:T(8,128)} %get-tuple-element.29.gate_ref, ...), custom_call_target="tpu_custom_call" | custom-call | tf_op jit(solution)/shard_map/local/pallas_call | solution.py:632
  190.9 4.3 %cell.1 = bf16[4,2,4,96,128]{4,3,2,1,0:T(8,128)(2,1)} custom-call(s32[4]{0:T(128)} %pad_add_fusion.place_ref, bf16[4,72,256]{2,1,0:T(8,128)(2,1)} %copy-done.3, bf16[4,72,256]{2,1,0:T(8,128)(2,1)} %all_to_all.33.in_ref, bf16[1024,256]{1,0:T(8,128)(2,1)} %get-tuple-element.32.q_ref, f32[1024,128]{1,0:T(8,128)} %get-tuple-element.34.local_ref, ...), custom_call_target="tpu_custom_call" | custom-call | tf_op jit(solution)/shard_map/cell/pallas_call | solution.py:641
  195.2 11.1 %all-to-all-start.5 = ((bf16[32,96,128]{2,1,0:T(8,128)(2,1)}), bf16[32,96,128]{2,1,0:T(8,128)(2,1)S(1)}, u32[]{:S(2)}, u32[]{:S(2)}) async-start(bf16[32,96,128]{2,1,0:T(8,128)(2,1)} %bitcast.29), calls=%async_computation.5 | async-start | bytes 1572864 | tf_op jit(solution)/shard_map/all_to_all | solution.py:24
  216.6 3.7 %assemble.1.weight_ref = bf16[4,4,4,2,16,768]{5,4,3,2,1,0:T(8,128)(2,1)} custom-call(s32[4]{0:T(128)} %pad_add_fusion.place_ref, bf16[4,4,16,768]{3,2,1,0:T(8,128)(2,1)} %copy-done.2, bf16[4,4,16,768]{3,2,1,0:T(8,128)(2,1)} %copy-done.6, bf16[4,4,16,768]{3,2,1,0:T(8,128)(2,1)} %copy-done.5, bf16[4,4,16,768]{3,2,1,0:T(8,128)(2,1)} %copy-done.4, ...), custom_call_target="tpu_custom_call" | custom-call | tf_op jit(solution)/shard_map/assemble/pallas_call | solution.py:652
  221.2 4.4 %finish.1 = bf16[128,512]{1,0:T(8,128)(2,1)} custom-call(bf16[4,2,4,96,128]{4,3,2,1,0:T(8,128)(2,1)} %bitcast.28, bf16[4,4,4,2,16,768]{5,4,3,2,1,0:T(8,128)(2,1)} %assemble.1.weight_ref, f32[4,512]{1,0:T(4,128)} %get-tuple-element.37.memory_gain_ref, f32[4,256]{1,0:T(4,128)} %get-tuple-element.38.conv_gain_ref), custom_call_target="tpu_custom_call" | custom-call | tf_op jit(solution)/shard_map/finish/pallas_call | solution.py:653
  (76 shorter events, 40.6 us)
Async XLA Ops:
  3.7 99.3 %copy-start.17 = (bf16[2048,2]{0,1:T(2,128)(2,1)S(1)}, bf16[2048,2]{0,1:T(2,128)(2,1)}, u32[]{:S(2)}) copy-start(bf16[2048,2]{0,1:T(2,128)(2,1)} %param.24) | copy-start | bytes 24580
  3.7 99.4 %copy-start.18 = (bf16[2048,2]{0,1:T(2,128)(2,1)S(1)}, bf16[2048,2]{0,1:T(2,128)(2,1)}, u32[]{:S(2)}) copy-start(bf16[2048,2]{0,1:T(2,128)(2,1)} %param.23) | copy-start | bytes 24580
  38.0 76.9 %copy-start = (bf16[16,136,512]{2,1,0:T(8,128)(2,1)}, bf16[16,136,512]{2,1,0:T(8,128)(2,1)S(1)}, u32[]{:S(2)}) copy-start(bf16[16,136,512]{2,1,0:T(8,128)(2,1)S(1)} %all_to_all.30) | copy-start | bytes 6684676
  38.0 76.9 %collective-permute-start = (bf16[4,4,136,512]{3,2,1,0:T(8,128)(2,1)S(1)}, bf16[4,4,136,512]{3,2,1,0:T(8,128)(2,1)}, u32[]{:S(2)}, u32[]{:S(2)}) collective-permute-start(bf16[4,4,136,512]{3,2,1,0:T(8,128)(2,1)S(1)} %bitcast.26), channel_id=1, source_target_pairs={{0,4},{4,0},{1,5},{5,1},{2,6},{6,2},{3,7},{7,3},{8,12},{12,8},{9,1... | collective-permute-start | bytes 6684680 | tf_op jit(solution)/shard_map/ppermute | solution.py:28
  54.3 24.9 %collective-permute-start.3 = (bf16[176,256]{1,0:T(8,128)(2,1)S(1)}, bf16[176,256]{1,0:T(8,128)(2,1)S(1)}, u32[]{:S(2)}, u32[]{:S(2)}) collective-permute-start(bf16[176,256]{1,0:T(8,128)(2,1)S(1)} %pad_maximum_fusion.1.mine_ref), channel_id=1, source_target_pairs={{0,256},{32,288},{64,320},{96,352},{128,384},{160,416},{192,448},{... | collective-permute-start | bytes 270344 | tf_op jit(solution)/shard_map/ppermute | solution.py:502
  70.0 17.2 %collective-permute-start.2 = (bf16[176,256]{1,0:T(8,128)(2,1)S(1)}, bf16[176,256]{1,0:T(8,128)(2,1)S(1)}, u32[]{:S(2)}, u32[]{:S(2)}) collective-permute-start(bf16[176,256]{1,0:T(8,128)(2,1)S(1)} %pad_maximum_fusion.1.mine_ref), channel_id=1, source_target_pairs={{0,384},{32,416},{64,448},{96,480},{128,0},{160,32},{192,64},{224,... | collective-permute-start | bytes 270344 | tf_op jit(solution)/shard_map/ppermute | solution.py:502
  71.9 15.2 %collective-permute-start.1 = (bf16[176,256]{1,0:T(8,128)(2,1)S(1)}, bf16[176,256]{1,0:T(8,128)(2,1)S(1)}, u32[]{:S(2)}, u32[]{:S(2)}) collective-permute-start(bf16[176,256]{1,0:T(8,128)(2,1)S(1)} %pad_maximum_fusion.1.mine_ref), channel_id=1, source_target_pairs={{0,128},{32,160},{64,192},{96,224},{128,256},{160,288},{192,320},{... | collective-permute-start | bytes 270344 | tf_op jit(solution)/shard_map/ppermute | solution.py:502
  90.4 24.5 %collective-permute-start.5 = (bf16[4,176,256]{2,1,0:T(8,128)(2,1)}, bf16[4,176,256]{2,1,0:T(8,128)(2,1)S(1)}, u32[]{:S(2)}, u32[]{:S(2)}) collective-permute-start(bf16[4,176,256]{2,1,0:T(8,128)(2,1)} %get-tuple-element.24.w0_ref), channel_id=1, source_target_pairs={{0,32},{32,64},{64,96},{96,128},{128,160},{160,192},{192,224},{224... | collective-permute-start | bytes 1081352 | tf_op jit(solution)/shard_map/ppermute | solution.py:502
  92.9 22.0 %collective-permute-start.4 = (bf16[4,176,256]{2,1,0:T(8,128)(2,1)}, bf16[4,176,256]{2,1,0:T(8,128)(2,1)S(1)}, u32[]{:S(2)}, u32[]{:S(2)}) collective-permute-start(bf16[4,176,256]{2,1,0:T(8,128)(2,1)} %get-tuple-element.24.w0_ref), channel_id=1, source_target_pairs={{0,480},{32,0},{64,32},{96,64},{128,96},{160,128},{192,160},{224,1... | collective-permute-start | bytes 1081352 | tf_op jit(solution)/shard_map/ppermute | solution.py:502
  96.9 13.9 %collective-permute-start.6 = (bf16[2,176,256]{2,1,0:T(8,128)(2,1)}, bf16[2,176,256]{2,1,0:T(8,128)(2,1)}, u32[]{:S(2)}, u32[]{:S(2)}) collective-permute-start(bf16[2,176,256]{2,1,0:T(8,128)(2,1)} %get-tuple-element.25), channel_id=1, source_target_pairs={{0,448},{32,480},{64,0},{96,32},{128,64},{160,96},{192,128},{224,1... | collective-permute-start | bytes 540680 | tf_op jit(solution)/shard_map/ppermute | solution.py:502
  98.8 16.1 %collective-permute-start.7 = (bf16[2,176,256]{2,1,0:T(8,128)(2,1)}, bf16[2,176,256]{2,1,0:T(8,128)(2,1)}, u32[]{:S(2)}, u32[]{:S(2)}) collective-permute-start(bf16[2,176,256]{2,1,0:T(8,128)(2,1)} %get-tuple-element.26), channel_id=1, source_target_pairs={{0,64},{32,96},{64,128},{96,160},{128,192},{160,224},{192,256},{22... | collective-permute-start | bytes 540680 | tf_op jit(solution)/shard_map/ppermute | solution.py:502
  122.2 39.6 %copy-start.10 = (bf16[4,4,16,768]{3,2,1,0:T(8,128)(2,1)S(1)}, bf16[4,4,16,768]{3,2,1,0:T(8,128)(2,1)}, u32[]{:S(2)}) copy-start(bf16[4,4,16,768]{3,2,1,0:T(8,128)(2,1)} %get-tuple-element.36) | copy-start | bytes 1179652
  156.3 33.9 %all-to-all-start.4 = ((bf16[4,72,256]{2,1,0:T(8,128)(2,1)}), bf16[4,72,256]{2,1,0:T(8,128)(2,1)S(1)}, u32[]{:S(2)}, u32[]{:S(2)}) async-start(bf16[4,72,256]{2,1,0:T(8,128)(2,1)} %group.1), calls=%async_computation.4 | async-start | bytes 294912 | tf_op jit(solution)/shard_map/all_to_all | solution.py:24
  161.8 7.9 %collective-permute-start.10 = (bf16[4,16,768]{2,1,0:T(8,128)(2,1)S(1)}, bf16[4,16,768]{2,1,0:T(8,128)(2,1)S(1)}, u32[]{:S(2)}, u32[]{:S(2)}) collective-permute-start(bf16[4,16,768]{2,1,0:T(8,128)(2,1)S(1)} %get-tuple-element.40), channel_id=1, source_target_pairs={{0,3},{1,0},{2,1},{3,2},{4,7},{5,4},{6,5},{7,6},{8,11},{9,8},{10,9... | collective-permute-start | bytes 294920 | tf_op jit(solution)/shard_map/ppermute | solution.py:582
  164.8 6.9 %collective-permute-start.9 = (bf16[4,16,768]{2,1,0:T(8,128)(2,1)S(1)}, bf16[4,16,768]{2,1,0:T(8,128)(2,1)S(1)}, u32[]{:S(2)}, u32[]{:S(2)}) collective-permute-start(bf16[4,16,768]{2,1,0:T(8,128)(2,1)S(1)} %get-tuple-element.41), channel_id=1, source_target_pairs={{0,2},{1,3},{2,0},{3,1},{4,6},{5,7},{6,4},{7,5},{8,10},{9,11},{10,... | collective-permute-start | bytes 294920 | tf_op jit(solution)/shard_map/ppermute | solution.py:582
  167.7 6.9 %collective-permute-start.8 = (bf16[4,16,768]{2,1,0:T(8,128)(2,1)S(1)}, bf16[4,16,768]{2,1,0:T(8,128)(2,1)S(1)}, u32[]{:S(2)}, u32[]{:S(2)}) collective-permute-start(bf16[4,16,768]{2,1,0:T(8,128)(2,1)S(1)} %get-tuple-element.42), channel_id=1, source_target_pairs={{0,1},{1,2},{2,3},{3,0},{4,5},{5,6},{6,7},{7,4},{8,9},{9,10},{10,1... | collective-permute-start | bytes 294920 | tf_op jit(solution)/shard_map/ppermute | solution.py:582
  174.6 33.8 %collective-permute-start.13 = (bf16[4,4,16,768]{3,2,1,0:T(8,128)(2,1)S(1)}, bf16[4,4,16,768]{3,2,1,0:T(8,128)(2,1)S(1)}, u32[]{:S(2)}, u32[]{:S(2)}) collective-permute-start(bf16[4,4,16,768]{3,2,1,0:T(8,128)(2,1)S(1)} %pad_maximum_fusion.refs_0_), channel_id=1, source_target_pairs={{0,8},{8,16},{16,24},{24,0},{1,9},{9,17},{17,25},{25,1},{2,10},{10... | collective-permute-start | bytes 1179656 | tf_op jit(solution)/shard_map/ppermute | solution.py:588
  176.8 33.8 %collective-permute-start.12 = (bf16[4,4,16,768]{3,2,1,0:T(8,128)(2,1)S(1)}, bf16[4,4,16,768]{3,2,1,0:T(8,128)(2,1)S(1)}, u32[]{:S(2)}, u32[]{:S(2)}) collective-permute-start(bf16[4,4,16,768]{3,2,1,0:T(8,128)(2,1)S(1)} %pad_maximum_fusion.refs_0_), channel_id=1, source_target_pairs={{0,16},{8,24},{16,0},{24,8},{1,17},{9,25},{17,1},{25,9},{2,18},{10... | collective-permute-start | bytes 1179656 | tf_op jit(solution)/shard_map/ppermute | solution.py:588
  180.5 32.3 %collective-permute-start.11 = (bf16[4,4,16,768]{3,2,1,0:T(8,128)(2,1)S(1)}, bf16[4,4,16,768]{3,2,1,0:T(8,128)(2,1)S(1)}, u32[]{:S(2)}, u32[]{:S(2)}) collective-permute-start(bf16[4,4,16,768]{3,2,1,0:T(8,128)(2,1)S(1)} %pad_maximum_fusion.refs_0_), channel_id=1, source_target_pairs={{0,24},{8,0},{16,8},{24,16},{1,25},{9,1},{17,9},{25,17},{2,26},{10... | collective-permute-start | bytes 1179656 | tf_op jit(solution)/shard_map/ppermute | solution.py:588
  195.2 25.1 %all-to-all-start.5 = ((bf16[32,96,128]{2,1,0:T(8,128)(2,1)}), bf16[32,96,128]{2,1,0:T(8,128)(2,1)S(1)}, u32[]{:S(2)}, u32[]{:S(2)}) async-start(bf16[32,96,128]{2,1,0:T(8,128)(2,1)} %bitcast.29), calls=%async_computation.5 | async-start | bytes 1572864 | tf_op jit(solution)/shard_map/all_to_all | solution.py:24
  206.3 8.8 %collective-permute-start.14 = (bf16[4,4,16,768]{3,2,1,0:T(8,128)(2,1)S(1)}, bf16[4,4,16,768]{3,2,1,0:T(8,128)(2,1)S(1)}, u32[]{:S(2)}, u32[]{:S(2)}) collective-permute-start(bf16[4,4,16,768]{3,2,1,0:T(8,128)(2,1)S(1)} %pad_maximum_fusion.refs_0_), channel_id=1, source_target_pairs={{0,4},{4,0},{1,5},{5,1},{2,6},{6,2},{3,7},{7,3},{8,12},{12,8},{9,1... | collective-permute-start | bytes 1179656 | tf_op jit(solution)/shard_map/ppermute | solution.py:28
  208.4 6.6 %collective-permute-start.17 = (bf16[4,4,16,768]{3,2,1,0:T(8,128)(2,1)S(1)}, bf16[4,4,16,768]{3,2,1,0:T(8,128)(2,1)S(1)}, u32[]{:S(2)}, u32[]{:S(2)}) collective-permute-start(bf16[4,4,16,768]{3,2,1,0:T(8,128)(2,1)S(1)} %collective-permute-done.13.refs_3_), channel_id=1, source_target_pairs={{0,4},{4,0},{1,5},{5,1},{2,6},{6,2},{3,7},{7,3},{8,12},{12,8},{9,1... | collective-permute-start | bytes 1179656 | tf_op jit(solution)/shard_map/ppermute | solution.py:28
  210.6 4.4 %collective-permute-start.16 = (bf16[4,4,16,768]{3,2,1,0:T(8,128)(2,1)S(1)}, bf16[4,4,16,768]{3,2,1,0:T(8,128)(2,1)S(1)}, u32[]{:S(2)}, u32[]{:S(2)}) collective-permute-start(bf16[4,4,16,768]{3,2,1,0:T(8,128)(2,1)S(1)} %collective-permute-done.12.refs_2_), channel_id=1, source_target_pairs={{0,4},{4,0},{1,5},{5,1},{2,6},{6,2},{3,7},{7,3},{8,12},{12,8},{9,1... | collective-permute-start | bytes 1179656 | tf_op jit(solution)/shard_map/ppermute | solution.py:28
  212.8 3.7 %collective-permute-start.15 = (bf16[4,4,16,768]{3,2,1,0:T(8,128)(2,1)S(1)}, bf16[4,4,16,768]{3,2,1,0:T(8,128)(2,1)}, u32[]{:S(2)}, u32[]{:S(2)}) collective-permute-start(bf16[4,4,16,768]{3,2,1,0:T(8,128)(2,1)S(1)} %collective-permute-done.11.refs_1_), channel_id=1, source_target_pairs={{0,4},{4,0},{1,5},{5,1},{2,6},{6,2},{3,7},{7,3},{8,12},{12,8},{9,1... | collective-permute-start | bytes 1179656 | tf_op jit(solution)/shard_map/ppermute | solution.py:28
  (15 other events, 98.8 us)

commit v12 on v11

--- a/solution.py
+++ b/solution.py
@@ -308,18 +308,6 @@
     return state, level, acc
 
 
-def group_kernel(in_ref, out_ref):
-    members, rows, _ = in_ref.shape
-    width = rows - 8
-    blocks = [in_ref[j] for j in range(members)]
-    state, level, total = merged(blocks, [True] * members, width)
-    last = blocks[-1].astype(F32)
-    kept = jnp.concatenate([state[: width + 2], last[width + 2 :]], axis=0)
-    kept = with_logs(kept, width, level, total).astype(BF16)
-    for j in range(out_ref.shape[0]):
-        out_ref[j] = kept
-
-
 def slab_kernel(
     qk_ref, v_ref, gate_ref, glu_ref, out_ref, q_ref, k_ref,
 ):
@@ -415,25 +403,22 @@
         level = new_level
 
 
-def cell_kernel(place_ref, far_ref, in_ref, q_ref, local_ref, conv_ref, taps_ref, out_ref):
+def cell_kernel(place_ref, in_ref, q_ref, local_ref, conv_ref, taps_ref, out_ref):
     members, rows, head = in_ref.shape
-    groups = far_ref.shape[0]
     nx, nc, ny, _, lanes = out_ref.shape
     width, chan = lanes // 2, lanes // nx
     length = q_ref.shape[0] // (nx * nc)
     scale = head ** (-0.5)
     place = place_ref[0]
-    at_far, at_close = lax.div(place, members), lax.rem(place, members)
-    blocks = [far_ref[j] for j in range(groups)] + [in_ref[j] for j in range(members)]
-    passed = [j < at_far for j in range(groups)] + [j < at_close for j in range(members)]
+    blocks = [in_ref[j] for j in range(members)]
+    passed = [j < place for j in range(members)]
     state, level, _ = merged(blocks, passed, width)
     state = jnp.concatenate([state, jnp.zeros((lanes - rows, head), F32)], axis=0).astype(BF16)
 
     group = head // chan
     each = HOLD // group
-    near_rows = in_ref[jnp.maximum(at_close - 1, 0), width : width + 8].astype(F32)
-    far_rows = far_ref[jnp.maximum(at_far - 1, 0), width : width + 8].astype(F32)
-    last_rows = jnp.where(at_close > 0, near_rows, jnp.where(at_far > 0, far_rows, 0.0))
+    last_rows = in_ref[jnp.maximum(place - 1, 0), width : width + 8].astype(F32)
+    last_rows = jnp.where(place > 0, last_rows, 0.0)
     last_rows = last_rows[2 : 2 + each]
     prior = jnp.concatenate([last_rows[:, g * chan : (g + 1) * chan] for g in range(group)], axis=0)
     prior = jnp.concatenate([prior, jnp.zeros((HOLD, lanes - chan), F32)], axis=1)
@@ -597,7 +582,7 @@
     call_slab = pl.pallas_call(
         slab_kernel,
         out_shape=(
-            jax.ShapeDtypeStruct((nzl, state_rows, head), BF16),
+            jax.ShapeDtypeStruct((members, state_rows, head), BF16),
             jax.ShapeDtypeStruct((slab, head), BF16),
             jax.ShapeDtypeStruct((slab, head), BF16),
         ),
@@ -607,17 +592,7 @@
         name="slab_state",
     )
     states, query, key = call_slab(all_qk, value, gates, packed)
-    states = exchange(states, "zl")
-    call_group = pl.pallas_call(
-        group_kernel,
-        out_shape=jax.ShapeDtypeStruct((nzh, state_rows, head), BF16),
-        in_specs=vmem(1),
-        out_specs=pl.BlockSpec(memory_space=pltpu.VMEM),
-        interpret=INTERPRET,
-        name="group",
-    )
-    groups = call_group(states)
-    groups = exchange(groups, "zh")
+    states = exchange(states, Z)
     call_local = pl.pallas_call(
         local_kernel,
         out_shape=(
@@ -633,12 +608,12 @@
     call_cell = pl.pallas_call(
         cell_kernel,
         out_shape=jax.ShapeDtypeStruct((nx, nc, ny, length // 4 * 3, 2 * width), BF16),
-        in_specs=[smem] + vmem(6),
+        in_specs=[smem] + vmem(5),
         out_specs=pl.BlockSpec(memory_space=pltpu.VMEM),
         interpret=INTERPRET,
         name="cell",
     )
-    last = call_cell(place, groups, states, query, local, conv, conv_kernel)
+    last = call_cell(place, states, query, local, conv, conv_kernel)
     arrived = exchange(last.reshape(nx * nc * ny, length // 4 * 3, -1), ("x", "c", "tp"))
     arrived = arrived.reshape(nx, nc, ny, length // 4 * 3, -1)
     call_assemble = pl.pallas_call(

time: 227 us -> 215 us (0.947)
  blocking collectives: 71.1 us -> 61.5 us
    all_to_all x4 -> x3, blocking collectives: 71.1 us -> 61.5 us  [exchange(): return lax.all_to_all(pieces, axes, split_axis=0, concat_axis=0, tiled=True)]
    pallas_call x2 -> x1, Pallas kernels: 6.08 us -> 4.43 us  [layer(): last = call_cell(place, states, query, local, conv, conv_kernel)]
  transfers between devices with their start and end apart: 20 -> 20, of which waited for: 6 -> 6; matrix products, arithmetic and copies ran while one was open for 1% -> 1% of each run, Pallas kernels for 8% -> 9%
where the time goes in v12:
time: 215 us; the launch traced here: 214 us
  starting transfers between devices  84.1 us (39%)
  blocking collectives  61.5 us (29%)
  Pallas kernels  35.9 us (17%)
  waiting for transfers between devices  23.5 us (11%)
  local copies, waits for them, and re-layouts  5.88 us (3%)
  other arithmetic  2.68 us (1%)
    all_to_all x3, blocking collectives, exchange(): return lax.all_to_all(pieces, axes, split_axis=0, concat_axis=0, tiled=True)  61.5 us
    ppermute x7, starting transfers between devices, from_z(): lax.ppermute(value, Z, [(j, (j - ahead) % members) for j in range(members)])  37.6 us
    ppermute x7, waiting for transfers between devices, from_z(): lax.ppermute(value, Z, [(j, (j - ahead) % members) for j in range(members)])  17.9 us
    all_to_all x2, starting transfers between devices, exchange(): return lax.all_to_all(pieces, axes, split_axis=0, concat_axis=0, tiled=True)  15.7 us
    ppermute x5, starting transfers between devices, swapped(): return lax.ppermute(value, axis, [(0, 1), (1, 0)])  14.5 us
    ppermute x3, starting transfers between devices, from_x(): return lax.ppermute(value, 'x', [(j, (j - ahead) % nx) for j in range(nx)])  8.45 us
    ppermute x3, starting transfers between devices, layer(): lax.ppermute(out_part[ahead], 'tp', [(j, (j + ahead) % ny) for j in range...  7.83 us
    pallas_call x1, Pallas kernels, layer(): call_local(place, query, key, value, gates, packed, conv_kernel)  7.22 us
  transfers between devices with their start and end apart: 20, of which 6 were waited for; matrix products, arithmetic and copies ran while one was open for 1% of the time, Pallas kernels for 9%

profile of v12, /device:TPU:1, one launch (start us, length us, event | category | flops | bytes accessed | tf_op | source)
XLA Modules:
  0.0 214.0 jit_solution(8673830507545604439)
XLA Ops:
  3.7 34.3 %all_to_all.25 = bf16[16,136,512]{2,1,0:T(8,128)(2,1)S(1)} all-to-all(bf16[16,136,512]{2,1,0:T(8,128)(2,1)} %pack.1), channel_id=1, replica_groups=mesh['zh'=4,'zl'=4,'x'=4,'c'=2,'tp'=4] {'x','tp'}, dimensions={0} | all-to-all | bytes 4456448 | tf_op jit(solution)/shard_map/all_to_all | solution.py:24
  38.0 5.9 %collective-permute-start = (bf16[4,4,136,512]{3,2,1,0:T(8,128)(2,1)S(1)}, bf16[4,4,136,512]{3,2,1,0:T(8,128)(2,1)}, u32[]{:S(2)}, u32[]{:S(2)}) collective-permute-start(bf16[4,4,136,512]{3,2,1,0:T(8,128)(2,1)S(1)} %bitcast.26), channel_id=1, source_target_pairs={{0,4},{4,0},{1,5},{5,1},{2,6},{6,2},{3,7},{7,3},{8,12},{12,8},{9,1... | collective-permute-start | bytes 6684680 | tf_op jit(solution)/shard_map/ppermute | solution.py:28
  45.4 8.1 %all_to_all.26 = bf16[8,16,256]{2,1,0:T(8,128)(2,1)S(1)} all-to-all(bf16[8,16,256]{2,1,0:T(8,128)(2,1)} %bitcast.37), channel_id=1, replica_groups=mesh['zh'=4,'zl'=4,'x'=4,'c'=2,'tp'=4] {'x','c'}, dimensions={0} | all-to-all | bytes 131072 | tf_op jit(solution)/shard_map/all_to_all | solution.py:24
  54.3 15.7 %collective-permute-start.3 = (bf16[176,256]{1,0:T(8,128)(2,1)S(1)}, bf16[176,256]{1,0:T(8,128)(2,1)S(1)}, u32[]{:S(2)}, u32[]{:S(2)}) collective-permute-start(bf16[176,256]{1,0:T(8,128)(2,1)S(1)} %pad_maximum_fusion.1.mine_ref), channel_id=1, source_target_pairs={{0,256},{32,288},{64,320},{96,352},{128,384},{160,416},{192,448},{... | collective-permute-start | bytes 270344 | tf_op jit(solution)/shard_map/ppermute | solution.py:487
  71.9 7.3 %collective-permute-start.1 = (bf16[176,256]{1,0:T(8,128)(2,1)S(1)}, bf16[176,256]{1,0:T(8,128)(2,1)S(1)}, u32[]{:S(2)}, u32[]{:S(2)}) collective-permute-start(bf16[176,256]{1,0:T(8,128)(2,1)S(1)} %pad_maximum_fusion.1.mine_ref), channel_id=1, source_target_pairs={{0,128},{32,160},{64,192},{96,224},{128,256},{160,288},{192,320},{... | collective-permute-start | bytes 270344 | tf_op jit(solution)/shard_map/ppermute | solution.py:487
  79.2 7.9 %collective-permute-done.2.after_ref = bf16[176,256]{1,0:T(8,128)(2,1)S(1)} collective-permute-done((bf16[176,256]{1,0:T(8,128)(2,1)S(1)}, bf16[176,256]{1,0:T(8,128)(2,1)S(1)}, u32[]{:S(2)}, u32[]{:S(2)}) %collective-permute-start.2) | collective-permute-done | bytes 90144 | tf_op jit(solution)/shard_map/ppermute | solution.py:487
  92.9 4.0 %collective-permute-start.4 = (bf16[4,176,256]{2,1,0:T(8,128)(2,1)}, bf16[4,176,256]{2,1,0:T(8,128)(2,1)S(1)}, u32[]{:S(2)}, u32[]{:S(2)}) collective-permute-start(bf16[4,176,256]{2,1,0:T(8,128)(2,1)} %get-tuple-element.24.w0_ref), channel_id=1, source_target_pairs={{0,480},{32,0},{64,32},{96,64},{128,96},{160,128},{192,160},{224,1... | collective-permute-start | bytes 1081352 | tf_op jit(solution)/shard_map/ppermute | solution.py:487
  98.8 4.3 %collective-permute-start.7 = (bf16[2,176,256]{2,1,0:T(8,128)(2,1)}, bf16[2,176,256]{2,1,0:T(8,128)(2,1)}, u32[]{:S(2)}, u32[]{:S(2)}) collective-permute-start(bf16[2,176,256]{2,1,0:T(8,128)(2,1)} %get-tuple-element.26), channel_id=1, source_target_pairs={{0,64},{32,96},{64,128},{96,160},{128,192},{160,224},{192,256},{22... | collective-permute-start | bytes 540680 | tf_op jit(solution)/shard_map/ppermute | solution.py:487
  105.0 5.8 %collective-permute-done.6.low_ref = bf16[2,176,256]{2,1,0:T(8,128)(2,1)} collective-permute-done((bf16[2,176,256]{2,1,0:T(8,128)(2,1)}, bf16[2,176,256]{2,1,0:T(8,128)(2,1)}, u32[]{:S(2)}, u32[]{:S(2)}) %collective-permute-start.6) | collective-permute-done | bytes 180256 | tf_op jit(solution)/shard_map/ppermute | solution.py:487
  110.8 4.1 %collective-permute-done.7.high_ref = bf16[2,176,256]{2,1,0:T(8,128)(2,1)} collective-permute-done((bf16[2,176,256]{2,1,0:T(8,128)(2,1)}, bf16[2,176,256]{2,1,0:T(8,128)(2,1)}, u32[]{:S(2)}, u32[]{:S(2)}) %collective-permute-start.7) | collective-permute-done | bytes 180256 | tf_op jit(solution)/shard_map/ppermute | solution.py:487
  115.8 6.4 %project.1 = (bf16[4,4,2,128,128]{4,3,2,1,0:T(8,128)(2,1)}, bf16[4,2,128,128]{3,2,1,0:T(8,128)(2,1)}, bf16[2,128,128]{2,1,0:T(8,128)(2,1)}, f32[2,8,128]{2,1,0:T...) custom-call(s32[4]{0:T(128)} %pad_add_fusion.place_ref, ...), custom_call_target="tpu_custom_call" | custom-call | tf_op jit(solution)/shard_map/project/pallas_call | solution.py:548
  122.2 19.2 %all_to_all.27.qk_ref = bf16[4,1024,128]{2,1,0:T(8,128)(2,1)} all-to-all(bf16[4,1024,128]{2,1,0:T(8,128)(2,1)} %bitcast.30), channel_id=1, replica_groups=mesh['zh'=4,'zl'=4,'x'=4,'c'=2,'tp'=4] {'x'}, dimensions={0} | all-to-all | bytes 2097152 | tf_op jit(solution)/shard_map/all_to_all | solution.py:24
  141.4 3.8 %slab_state.1 = (bf16[16,72,256]{2,1,0:T(8,128)(2,1)}, bf16[1024,256]{1,0:T(8,128)(2,1)}, bf16[1024,256]{1,0:T(8,128)(2,1)}) custom-call(bf16[4,1024,128]{2,1,0:T(8,128)(2,1)} %all_to_all.27.qk_ref, bf16[1024,128]{1,0:T(8,128)(2,1)} %bitcast.31, f32[2,8,128]{2,1,0:T(8,128)} %get-tuple-element.29.gate_ref, bf16[2,128,128]{2,1,0:T(8,128)(2,1)} %get-tuple-element.30.glu_ref), custom_call_target="tpu_custom_call" | custom-call | tf_op jit(solution)/shard_map/slab_state/pallas_call | solution.py:594
  145.1 6.2 %all-to-all-start.3 = ((bf16[16,72,256]{2,1,0:T(8,128)(2,1)}), bf16[16,72,256]{2,1,0:T(8,128)(2,1)S(1)}, u32[]{:S(2)}, u32[]{:S(2)}) async-start(bf16[16,72,256]{2,1,0:T(8,128)(2,1)} %get-tuple-element.31), calls=%async_computation.3 | async-start | bytes 1179648 | tf_op jit(solution)/shard_map/all_to_all | solution.py:24
  151.4 2.9 %collective-permute-start.10 = (bf16[4,16,768]{2,1,0:T(8,128)(2,1)S(1)}, bf16[4,16,768]{2,1,0:T(8,128)(2,1)S(1)}, u32[]{:S(2)}, u32[]{:S(2)}) collective-permute-start(bf16[4,16,768]{2,1,0:T(8,128)(2,1)S(1)} %get-tuple-element.40), channel_id=1, source_target_pairs={{0,3},{1,0},{2,1},{3,2},{4,7},{5,4},{6,5},{7,6},{8,11},{9,8},{10,9... | collective-permute-start | bytes 294920 | tf_op jit(solution)/shard_map/ppermute | solution.py:567
  154.3 2.9 %collective-permute-start.9 = (bf16[4,16,768]{2,1,0:T(8,128)(2,1)S(1)}, bf16[4,16,768]{2,1,0:T(8,128)(2,1)S(1)}, u32[]{:S(2)}, u32[]{:S(2)}) collective-permute-start(bf16[4,16,768]{2,1,0:T(8,128)(2,1)S(1)} %get-tuple-element.41), channel_id=1, source_target_pairs={{0,2},{1,3},{2,0},{3,1},{4,6},{5,7},{6,4},{7,5},{8,10},{9,11},{10,... | collective-permute-start | bytes 294920 | tf_op jit(solution)/shard_map/ppermute | solution.py:567
  161.2 3.0 %collective-permute-done.8 = bf16[4,16,768]{2,1,0:T(8,128)(2,1)S(1)} collective-permute-done((bf16[4,16,768]{2,1,0:T(8,128)(2,1)S(1)}, bf16[4,16,768]{2,1,0:T(8,128)(2,1)S(1)}, u32[]{:S(2)}, u32[]{:S(2)}) %collective-permute-start.8) | collective-permute-done | bytes 98336 | tf_op jit(solution)/shard_map/ppermute | solution.py:567
  166.4 3.7 %collective-permute-start.12 = (bf16[4,4,16,768]{3,2,1,0:T(8,128)(2,1)S(1)}, bf16[4,4,16,768]{3,2,1,0:T(8,128)(2,1)S(1)}, u32[]{:S(2)}, u32[]{:S(2)}) collective-permute-start(bf16[4,4,16,768]{3,2,1,0:T(8,128)(2,1)S(1)} %pad_maximum_fusion.refs_0_), channel_id=1, source_target_pairs={{0,16},{8,24},{16,0},{24,8},{1,17},{9,25},{17,1},{25,9},{2,18},{10... | collective-permute-start | bytes 1179656 | tf_op jit(solution)/shard_map/ppermute | solution.py:573
  170.1 2.6 %collective-permute-start.11 = (bf16[4,4,16,768]{3,2,1,0:T(8,128)(2,1)S(1)}, bf16[4,4,16,768]{3,2,1,0:T(8,128)(2,1)S(1)}, u32[]{:S(2)}, u32[]{:S(2)}) collective-permute-start(bf16[4,4,16,768]{3,2,1,0:T(8,128)(2,1)S(1)} %pad_maximum_fusion.refs_0_), channel_id=1, source_target_pairs={{0,24},{8,0},{16,8},{24,16},{1,25},{9,1},{17,9},{25,17},{2,26},{10... | collective-permute-start | bytes 1179656 | tf_op jit(solution)/shard_map/ppermute | solution.py:573
  172.7 7.2 %local.1 = (f32[1024,128]{1,0:T(8,128)}, f32[256,128]{1,0:T(8,128)}) custom-call(s32[4]{0:T(128)} %pad_add_fusion.place_ref, bf16[1024,256]{1,0:T(8,128)(2,1)} %get-tuple-element.32.q_ref, bf16[1024,256]{1,0:T(8,128)(2,1)} %get-tuple-element.33.k_ref, bf16[1024,128]{1,0:T(8,128)(2,1)} %bitcast.32, f32[2,8,128]{2,1,0:T(8,128)} %get-tuple-element.29.gate_ref, ...), custom_call_target="tpu_custom_call" | custom-call | tf_op jit(solution)/shard_map/local/pallas_call | solution.py:607
  180.7 4.4 %cell.1 = bf16[4,2,4,96,128]{4,3,2,1,0:T(8,128)(2,1)} custom-call(s32[4]{0:T(128)} %pad_add_fusion.place_ref, bf16[16,72,256]{2,1,0:T(8,128)(2,1)} %copy-done.2, bf16[1024,256]{1,0:T(8,128)(2,1)} %get-tuple-element.32.q_ref, f32[1024,128]{1,0:T(8,128)} %get-tuple-element.34.local_ref, f32[256,128]{1,0:T(8,128)} %get-tuple-element.35.conv_ref, ...), custom_call_target="tpu_custom_call" | custom-call | tf_op jit(solution)/shard_map/cell/pallas_call | solution.py:616
  185.1 9.5 %all-to-all-start.4 = ((bf16[32,96,128]{2,1,0:T(8,128)(2,1)}), bf16[32,96,128]{2,1,0:T(8,128)(2,1)S(1)}, u32[]{:S(2)}, u32[]{:S(2)}) async-start(bf16[32,96,128]{2,1,0:T(8,128)(2,1)} %bitcast.29), calls=%async_computation.4 | async-start | bytes 1572864 | tf_op jit(solution)/shard_map/all_to_all | solution.py:24
  205.0 3.7 %assemble.1.weight_ref = bf16[4,4,4,2,16,768]{5,4,3,2,1,0:T(8,128)(2,1)} custom-call(s32[4]{0:T(128)} %pad_add_fusion.place_ref, bf16[4,4,16,768]{3,2,1,0:T(8,128)(2,1)} %copy-done.3, bf16[4,4,16,768]{3,2,1,0:T(8,128)(2,1)} %copy-done.6, bf16[4,4,16,768]{3,2,1,0:T(8,128)(2,1)} %copy-done.5, bf16[4,4,16,768]{3,2,1,0:T(8,128)(2,1)} %copy-done.4, ...), custom_call_target="tpu_custom_call" | custom-call | tf_op jit(solution)/shard_map/assemble/pallas_call | solution.py:627
  209.6 4.4 %finish.1 = bf16[128,512]{1,0:T(8,128)(2,1)} custom-call(bf16[4,2,4,96,128]{4,3,2,1,0:T(8,128)(2,1)} %bitcast.28, bf16[4,4,4,2,16,768]{5,4,3,2,1,0:T(8,128)(2,1)} %assemble.1.weight_ref, f32[4,512]{1,0:T(4,128)} %get-tuple-element.37.memory_gain_ref, f32[4,256]{1,0:T(4,128)} %get-tuple-element.38.conv_gain_ref), custom_call_target="tpu_custom_call" | custom-call | tf_op jit(solution)/shard_map/finish/pallas_call | solution.py:628
  (74 shorter events, 36.4 us)
Async XLA Ops:
  3.7 99.3 %copy-start.17 = (bf16[2048,2]{0,1:T(2,128)(2,1)S(1)}, bf16[2048,2]{0,1:T(2,128)(2,1)}, u32[]{:S(2)}) copy-start(bf16[2048,2]{0,1:T(2,128)(2,1)} %param.24) | copy-start | bytes 24580
  3.7 99.4 %copy-start.18 = (bf16[2048,2]{0,1:T(2,128)(2,1)S(1)}, bf16[2048,2]{0,1:T(2,128)(2,1)}, u32[]{:S(2)}) copy-start(bf16[2048,2]{0,1:T(2,128)(2,1)} %param.23) | copy-start | bytes 24580
  38.0 76.9 %copy-start = (bf16[16,136,512]{2,1,0:T(8,128)(2,1)}, bf16[16,136,512]{2,1,0:T(8,128)(2,1)S(1)}, u32[]{:S(2)}) copy-start(bf16[16,136,512]{2,1,0:T(8,128)(2,1)S(1)} %all_to_all.25) | copy-start | bytes 6684676
  38.0 76.9 %collective-permute-start = (bf16[4,4,136,512]{3,2,1,0:T(8,128)(2,1)S(1)}, bf16[4,4,136,512]{3,2,1,0:T(8,128)(2,1)}, u32[]{:S(2)}, u32[]{:S(2)}) collective-permute-start(bf16[4,4,136,512]{3,2,1,0:T(8,128)(2,1)S(1)} %bitcast.26), channel_id=1, source_target_pairs={{0,4},{4,0},{1,5},{5,1},{2,6},{6,2},{3,7},{7,3},{8,12},{12,8},{9,1... | collective-permute-start | bytes 6684680 | tf_op jit(solution)/shard_map/ppermute | solution.py:28
  54.3 32.9 %copy-start.11 = (bf16[176,256]{1,0:T(8,128)(2,1)}, bf16[176,256]{1,0:T(8,128)(2,1)S(1)}, u32[]{:S(2)}) copy-start(bf16[176,256]{1,0:T(8,128)(2,1)S(1)} %pad_maximum_fusion.1.mine_ref) | copy-start | bytes 270340
  54.3 24.9 %collective-permute-start.3 = (bf16[176,256]{1,0:T(8,128)(2,1)S(1)}, bf16[176,256]{1,0:T(8,128)(2,1)S(1)}, u32[]{:S(2)}, u32[]{:S(2)}) collective-permute-start(bf16[176,256]{1,0:T(8,128)(2,1)S(1)} %pad_maximum_fusion.1.mine_ref), channel_id=1, source_target_pairs={{0,256},{32,288},{64,320},{96,352},{128,384},{160,416},{192,448},{... | collective-permute-start | bytes 270344 | tf_op jit(solution)/shard_map/ppermute | solution.py:487
  70.0 17.2 %collective-permute-start.2 = (bf16[176,256]{1,0:T(8,128)(2,1)S(1)}, bf16[176,256]{1,0:T(8,128)(2,1)S(1)}, u32[]{:S(2)}, u32[]{:S(2)}) collective-permute-start(bf16[176,256]{1,0:T(8,128)(2,1)S(1)} %pad_maximum_fusion.1.mine_ref), channel_id=1, source_target_pairs={{0,384},{32,416},{64,448},{96,480},{128,0},{160,32},{192,64},{224,... | collective-permute-start | bytes 270344 | tf_op jit(solution)/shard_map/ppermute | solution.py:487
  71.9 15.2 %collective-permute-start.1 = (bf16[176,256]{1,0:T(8,128)(2,1)S(1)}, bf16[176,256]{1,0:T(8,128)(2,1)S(1)}, u32[]{:S(2)}, u32[]{:S(2)}) collective-permute-start(bf16[176,256]{1,0:T(8,128)(2,1)S(1)} %pad_maximum_fusion.1.mine_ref), channel_id=1, source_target_pairs={{0,128},{32,160},{64,192},{96,224},{128,256},{160,288},{192,320},{... | collective-permute-start | bytes 270344 | tf_op jit(solution)/shard_map/ppermute | solution.py:487
  90.4 24.5 %collective-permute-start.5 = (bf16[4,176,256]{2,1,0:T(8,128)(2,1)}, bf16[4,176,256]{2,1,0:T(8,128)(2,1)S(1)}, u32[]{:S(2)}, u32[]{:S(2)}) collective-permute-start(bf16[4,176,256]{2,1,0:T(8,128)(2,1)} %get-tuple-element.24.w0_ref), channel_id=1, source_target_pairs={{0,32},{32,64},{64,96},{96,128},{128,160},{160,192},{192,224},{224... | collective-permute-start | bytes 1081352 | tf_op jit(solution)/shard_map/ppermute | solution.py:487
  92.9 22.0 %collective-permute-start.4 = (bf16[4,176,256]{2,1,0:T(8,128)(2,1)}, bf16[4,176,256]{2,1,0:T(8,128)(2,1)S(1)}, u32[]{:S(2)}, u32[]{:S(2)}) collective-permute-start(bf16[4,176,256]{2,1,0:T(8,128)(2,1)} %get-tuple-element.24.w0_ref), channel_id=1, source_target_pairs={{0,480},{32,0},{64,32},{96,64},{128,96},{160,128},{192,160},{224,1... | collective-permute-start | bytes 1081352 | tf_op jit(solution)/shard_map/ppermute | solution.py:487
  96.9 13.9 %collective-permute-start.6 = (bf16[2,176,256]{2,1,0:T(8,128)(2,1)}, bf16[2,176,256]{2,1,0:T(8,128)(2,1)}, u32[]{:S(2)}, u32[]{:S(2)}) collective-permute-start(bf16[2,176,256]{2,1,0:T(8,128)(2,1)} %get-tuple-element.25), channel_id=1, source_target_pairs={{0,448},{32,480},{64,0},{96,32},{128,64},{160,96},{192,128},{224,1... | collective-permute-start | bytes 540680 | tf_op jit(solution)/shard_map/ppermute | solution.py:487
  98.8 16.1 %collective-permute-start.7 = (bf16[2,176,256]{2,1,0:T(8,128)(2,1)}, bf16[2,176,256]{2,1,0:T(8,128)(2,1)}, u32[]{:S(2)}, u32[]{:S(2)}) collective-permute-start(bf16[2,176,256]{2,1,0:T(8,128)(2,1)} %get-tuple-element.26), channel_id=1, source_target_pairs={{0,64},{32,96},{64,128},{96,160},{128,192},{160,224},{192,256},{22... | collective-permute-start | bytes 540680 | tf_op jit(solution)/shard_map/ppermute | solution.py:487
  145.1 34.7 %all-to-all-start.3 = ((bf16[16,72,256]{2,1,0:T(8,128)(2,1)}), bf16[16,72,256]{2,1,0:T(8,128)(2,1)S(1)}, u32[]{:S(2)}, u32[]{:S(2)}) async-start(bf16[16,72,256]{2,1,0:T(8,128)(2,1)} %get-tuple-element.31), calls=%async_computation.3 | async-start | bytes 1179648 | tf_op jit(solution)/shard_map/all_to_all | solution.py:24
  151.4 7.9 %collective-permute-start.10 = (bf16[4,16,768]{2,1,0:T(8,128)(2,1)S(1)}, bf16[4,16,768]{2,1,0:T(8,128)(2,1)S(1)}, u32[]{:S(2)}, u32[]{:S(2)}) collective-permute-start(bf16[4,16,768]{2,1,0:T(8,128)(2,1)S(1)} %get-tuple-element.40), channel_id=1, source_target_pairs={{0,3},{1,0},{2,1},{3,2},{4,7},{5,4},{6,5},{7,6},{8,11},{9,8},{10,9... | collective-permute-start | bytes 294920 | tf_op jit(solution)/shard_map/ppermute | solution.py:567
  154.3 6.9 %collective-permute-start.9 = (bf16[4,16,768]{2,1,0:T(8,128)(2,1)S(1)}, bf16[4,16,768]{2,1,0:T(8,128)(2,1)S(1)}, u32[]{:S(2)}, u32[]{:S(2)}) collective-permute-start(bf16[4,16,768]{2,1,0:T(8,128)(2,1)S(1)} %get-tuple-element.41), channel_id=1, source_target_pairs={{0,2},{1,3},{2,0},{3,1},{4,6},{5,7},{6,4},{7,5},{8,10},{9,11},{10,... | collective-permute-start | bytes 294920 | tf_op jit(solution)/shard_map/ppermute | solution.py:567
  157.2 6.9 %collective-permute-start.8 = (bf16[4,16,768]{2,1,0:T(8,128)(2,1)S(1)}, bf16[4,16,768]{2,1,0:T(8,128)(2,1)S(1)}, u32[]{:S(2)}, u32[]{:S(2)}) collective-permute-start(bf16[4,16,768]{2,1,0:T(8,128)(2,1)S(1)} %get-tuple-element.42), channel_id=1, source_target_pairs={{0,1},{1,2},{2,3},{3,0},{4,5},{5,6},{6,7},{7,4},{8,9},{9,10},{10,1... | collective-permute-start | bytes 294920 | tf_op jit(solution)/shard_map/ppermute | solution.py:567
  164.2 32.7 %collective-permute-start.13 = (bf16[4,4,16,768]{3,2,1,0:T(8,128)(2,1)S(1)}, bf16[4,4,16,768]{3,2,1,0:T(8,128)(2,1)S(1)}, u32[]{:S(2)}, u32[]{:S(2)}) collective-permute-start(bf16[4,4,16,768]{3,2,1,0:T(8,128)(2,1)S(1)} %pad_maximum_fusion.refs_0_), channel_id=1, source_target_pairs={{0,8},{8,16},{16,24},{24,0},{1,9},{9,17},{17,25},{25,1},{2,10},{10... | collective-permute-start | bytes 1179656 | tf_op jit(solution)/shard_map/ppermute | solution.py:573
  166.4 32.6 %collective-permute-start.12 = (bf16[4,4,16,768]{3,2,1,0:T(8,128)(2,1)S(1)}, bf16[4,4,16,768]{3,2,1,0:T(8,128)(2,1)S(1)}, u32[]{:S(2)}, u32[]{:S(2)}) collective-permute-start(bf16[4,4,16,768]{3,2,1,0:T(8,128)(2,1)S(1)} %pad_maximum_fusion.refs_0_), channel_id=1, source_target_pairs={{0,16},{8,24},{16,0},{24,8},{1,17},{9,25},{17,1},{25,9},{2,18},{10... | collective-permute-start | bytes 1179656 | tf_op jit(solution)/shard_map/ppermute | solution.py:573
  170.1 31.1 %collective-permute-start.11 = (bf16[4,4,16,768]{3,2,1,0:T(8,128)(2,1)S(1)}, bf16[4,4,16,768]{3,2,1,0:T(8,128)(2,1)S(1)}, u32[]{:S(2)}, u32[]{:S(2)}) collective-permute-start(bf16[4,4,16,768]{3,2,1,0:T(8,128)(2,1)S(1)} %pad_maximum_fusion.refs_0_), channel_id=1, source_target_pairs={{0,24},{8,0},{16,8},{24,16},{1,25},{9,1},{17,9},{25,17},{2,26},{10... | collective-permute-start | bytes 1179656 | tf_op jit(solution)/shard_map/ppermute | solution.py:573
  185.1 23.6 %all-to-all-start.4 = ((bf16[32,96,128]{2,1,0:T(8,128)(2,1)}), bf16[32,96,128]{2,1,0:T(8,128)(2,1)S(1)}, u32[]{:S(2)}, u32[]{:S(2)}) async-start(bf16[32,96,128]{2,1,0:T(8,128)(2,1)} %bitcast.29), calls=%async_computation.4 | async-start | bytes 1572864 | tf_op jit(solution)/shard_map/all_to_all | solution.py:24
  194.7 8.8 %collective-permute-start.14 = (bf16[4,4,16,768]{3,2,1,0:T(8,128)(2,1)S(1)}, bf16[4,4,16,768]{3,2,1,0:T(8,128)(2,1)S(1)}, u32[]{:S(2)}, u32[]{:S(2)}) collective-permute-start(bf16[4,4,16,768]{3,2,1,0:T(8,128)(2,1)S(1)} %pad_maximum_fusion.refs_0_), channel_id=1, source_target_pairs={{0,4},{4,0},{1,5},{5,1},{2,6},{6,2},{3,7},{7,3},{8,12},{12,8},{9,1... | collective-permute-start | bytes 1179656 | tf_op jit(solution)/shard_map/ppermute | solution.py:28
  196.9 6.6 %collective-permute-start.17 = (bf16[4,4,16,768]{3,2,1,0:T(8,128)(2,1)S(1)}, bf16[4,4,16,768]{3,2,1,0:T(8,128)(2,1)S(1)}, u32[]{:S(2)}, u32[]{:S(2)}) collective-permute-start(bf16[4,4,16,768]{3,2,1,0:T(8,128)(2,1)S(1)} %collective-permute-done.13.refs_3_), channel_id=1, source_target_pairs={{0,4},{4,0},{1,5},{5,1},{2,6},{6,2},{3,7},{7,3},{8,12},{12,8},{9,1... | collective-permute-start | bytes 1179656 | tf_op jit(solution)/shard_map/ppermute | solution.py:28
  199.1 4.4 %collective-permute-start.16 = (bf16[4,4,16,768]{3,2,1,0:T(8,128)(2,1)S(1)}, bf16[4,4,16,768]{3,2,1,0:T(8,128)(2,1)S(1)}, u32[]{:S(2)}, u32[]{:S(2)}) collective-permute-start(bf16[4,4,16,768]{3,2,1,0:T(8,128)(2,1)S(1)} %collective-permute-done.12.refs_2_), channel_id=1, source_target_pairs={{0,4},{4,0},{1,5},{5,1},{2,6},{6,2},{3,7},{7,3},{8,12},{12,8},{9,1... | collective-permute-start | bytes 1179656 | tf_op jit(solution)/shard_map/ppermute | solution.py:28
  201.2 3.7 %collective-permute-start.15 = (bf16[4,4,16,768]{3,2,1,0:T(8,128)(2,1)S(1)}, bf16[4,4,16,768]{3,2,1,0:T(8,128)(2,1)}, u32[]{:S(2)}, u32[]{:S(2)}) collective-permute-start(bf16[4,4,16,768]{3,2,1,0:T(8,128)(2,1)S(1)} %collective-permute-done.11.refs_1_), channel_id=1, source_target_pairs={{0,4},{4,0},{1,5},{5,1},{2,6},{6,2},{3,7},{7,3},{8,12},{12,8},{9,1... | collective-permute-start | bytes 1179656 | tf_op jit(solution)/shard_map/ppermute | solution.py:28
  (15 other events, 93.9 us)

commit v13 on v11

--- a/solution.py
+++ b/solution.py
@@ -100,16 +100,6 @@
                 width = ref.shape[1] // (nx * nc)
                 parts.append(ref[:, at * width : (at + 1) * width])
             out_ref[x, c] = jnp.concatenate(parts, axis=1)
-
-
-def arrange_kernel(before_ref, mine_ref, after_ref, opposite_ref, near_ref, low_ref, high_ref):
-    for ref, at in ((near_ref, 0), (high_ref, 0)):
-        ref[at] = before_ref[...]
-    for ref, at in ((near_ref, 1), (high_ref, 1), (low_ref, 0)):
-        ref[at] = mine_ref[...]
-    for ref, at in ((near_ref, 2), (low_ref, 1)):
-        ref[at] = after_ref[...]
-    near_ref[3] = opposite_ref[...]
 
 
 def assemble_kernel(place_ref, *refs):
@@ -321,7 +311,7 @@
 
 
 def slab_kernel(
-    qk_ref, v_ref, gate_ref, glu_ref, out_ref, q_ref, k_ref,
+    qk_ref, v_ref, gate_ref, glu_ref, out_ref,
 ):
     chunks, length = gate_ref.shape[1], gate_ref.shape[2]
     width = qk_ref.shape[2] // 2
@@ -338,9 +328,7 @@
     fresh = columns_of(jnp.exp(end_log - level))
     state = jnp.zeros((2 * width, width * qk_ref.shape[0]), F32)
     for r in range(chunks):
-        q_ref[r * length : (r + 1) * length] = joined(qk_ref, 0, width, r, length)
         key = joined(qk_ref, width, width, r, length)
-        k_ref[r * length : (r + 1) * length] = key
         scaled = (fresh[:, r : r + 1] * key.astype(F32)).astype(BF16)
         state = state + dot(v_ref[r * length : (r + 1) * length], scaled, TN)
     rows, head_lanes = out_ref.shape[1], out_ref.shape[2]
@@ -358,7 +346,7 @@
         out_ref[j] = kept
 
 
-def local_kernel(place_ref, q_ref, k_ref, v_ref, gate_ref, glu_ref, taps_ref, out_ref, conv_ref):
+def local_kernel(place_ref, qk_ref, v_ref, gate_ref, glu_ref, taps_ref, out_ref, conv_ref, q_ref):
     chunks, length = gate_ref.shape[1], gate_ref.shape[2]
     head = q_ref.shape[1]
     lanes = v_ref.shape[1]
@@ -385,7 +373,10 @@
     passed = jnp.zeros((1, 1), F32)
     for r in range(chunks):
         here = slice(r * length, (r + 1) * length)
-        query, key, value = q_ref[here], k_ref[here], v_ref[here]
+        value = v_ref[here]
+        query = joined(qk_ref, 0, width, r, length)
+        key = joined(qk_ref, width, width, r, length)
+        q_ref[here] = query
         within_row, gate_row = within[r : r + 1], gate[r : r + 1]
         within_col = turned[:, r : r + 1]
         gate_col = turned[:, chunks + r : chunks + r + 1]
@@ -537,20 +528,8 @@
     opposite = from_z(mine, 2 * step)
     far = [from_z(mine, -step), mine, from_z(mine, step), opposite]
     own = exchange(sent, ("x", "tp")).reshape(nx, ny, length + 8, part)
-    half_shape = (nzh // 2, *mine.shape)
-    call_arrange = pl.pallas_call(
-        arrange_kernel,
-        out_shape=(
-            jax.ShapeDtypeStruct((nzh, *mine.shape), BF16),
-            jax.ShapeDtypeStruct(half_shape, BF16),
-            jax.ShapeDtypeStruct(half_shape, BF16),
-        ),
-        in_specs=vmem(4),
-        out_specs=vmem(3),
-        interpret=INTERPRET,
-        name="arrange",
-    )
-    near, *halves = call_arrange(*far)
+    near = jnp.stack(far, axis=0)
+    halves = near[1:3], near[:2]
     sets = [near, from_z(near, 1), from_z(near, -1)]
     sets += [from_z(halves[0], 2), from_z(halves[1], -2)]
     other = swapped(own, "c")
@@ -594,19 +573,16 @@
     other_parts += [swapped(out, "c") for out in out_parts[2:]]
 
     state_rows = width + 8
+    keys = all_qk.reshape(nx, slab, 2 * width)
     call_slab = pl.pallas_call(
         slab_kernel,
-        out_shape=(
-            jax.ShapeDtypeStruct((nzl, state_rows, head), BF16),
-            jax.ShapeDtypeStruct((slab, head), BF16),
-            jax.ShapeDtypeStruct((slab, head), BF16),
-        ),
+        out_shape=jax.ShapeDtypeStruct((nzl, state_rows, head), BF16),
         in_specs=vmem(4),
-        out_specs=vmem(3),
+        out_specs=pl.BlockSpec(memory_space=pltpu.VMEM),
         interpret=INTERPRET,
         name="slab_state",
     )
-    states, query, key = call_slab(all_qk, value, gates, packed)
+    states = call_slab(keys, value, gates, packed)
     states = exchange(states, "zl")
     call_group = pl.pallas_call(
         group_kernel,
@@ -623,13 +599,14 @@
         out_shape=(
             jax.ShapeDtypeStruct((slab, 2 * width), F32),
             jax.ShapeDtypeStruct((nc * length, nx * chan), F32),
+            jax.ShapeDtypeStruct((slab, head), BF16),
         ),
-        in_specs=[smem] + vmem(6),
-        out_specs=vmem(2),
+        in_specs=[smem] + vmem(5),
+        out_specs=vmem(3),
         interpret=INTERPRET,
         name="local",
     )
-    local, conv = call_local(place, query, key, value, gates, packed, conv_kernel)
+    local, conv, query = call_local(place, keys, value, gates, packed, conv_kernel)
     call_cell = pl.pallas_call(
         cell_kernel,
         out_shape=jax.ShapeDtypeStruct((nx, nc, ny, length // 4 * 3, 2 * width), BF16),

time: 227 us -> 228 us (level)
  starting transfers between devices: 84.9 us -> 93.8 us
  waiting for transfers between devices: 23.4 us -> 17.9 us
    ppermute x7, starting transfers between devices: 37.6 us -> 45.3 us  [from_z(): lax.ppermute(value, Z, [(j, (j - ahead) % members) for j in range(members)])]
    ppermute x7, waiting for transfers between devices: 17.9 us -> 12.4 us  [from_z(): lax.ppermute(value, Z, [(j, (j - ahead) % members) for j in range(members)])]
    pallas_call x3 -> x2, Pallas kernels: 12.7 us -> 11.1 us  [the longest x1 7.84 us: layer(): call_local(place, keys, value, gates, packed, conv_kernel)]
  transfers between devices with their start and end apart: 20 -> 20, of which waited for: 6 -> 8; matrix products, arithmetic and copies ran while one was open for 1% -> 2% of each run, Pallas kernels for 8% -> 8%
where the time goes in v13:
time: 228 us; the launch traced here: 226 us
  starting transfers between devices  93.8 us (41%)
  blocking collectives  70.5 us (31%)
  Pallas kernels  35.7 us (16%)
  waiting for transfers between devices  17.9 us (8%)
  local copies, waits for them, and re-layouts  4.33 us (2%)
  other arithmetic  3.53 us (2%)
    all_to_all x4, blocking collectives, exchange(): return lax.all_to_all(pieces, axes, split_axis=0, concat_axis=0, tiled=True)  70.5 us
    ppermute x7, starting transfers between devices, from_z(): lax.ppermute(value, Z, [(j, (j - ahead) % members) for j in range(members)])  45.3 us
    all_to_all x2, starting transfers between devices, exchange(): return lax.all_to_all(pieces, axes, split_axis=0, concat_axis=0, tiled=True)  17.7 us
    ppermute x5, starting transfers between devices, swapped(): return lax.ppermute(value, axis, [(0, 1), (1, 0)])  14.5 us
    ppermute x7, waiting for transfers between devices, from_z(): lax.ppermute(value, Z, [(j, (j - ahead) % members) for j in range(members)])  12.4 us
    ppermute x3, starting transfers between devices, from_x(): return lax.ppermute(value, 'x', [(j, (j - ahead) % nx) for j in range(nx)])  8.42 us
    pallas_call x1, Pallas kernels, layer(): call_local(place, keys, value, gates, packed, conv_kernel)  7.84 us
    ppermute x3, starting transfers between devices, layer(): lax.ppermute(out_part[ahead], 'tp', [(j, (j + ahead) % ny) for j in range...  7.83 us
  transfers between devices with their start and end apart: 20, of which 8 were waited for; matrix products, arithmetic and copies ran while one was open for 2% of the time, Pallas kernels for 8%

profile of v13, /device:TPU:1, one launch (start us, length us, event | category | flops | bytes accessed | tf_op | source)
XLA Modules:
  0.0 226.2 jit_solution(14662881762345091607)
XLA Ops:
  3.7 34.3 %all_to_all.30 = bf16[16,136,512]{2,1,0:T(8,128)(2,1)S(1)} all-to-all(bf16[16,136,512]{2,1,0:T(8,128)(2,1)} %pack.1), channel_id=1, replica_groups=mesh['zh'=4,'zl'=4,'x'=4,'c'=2,'tp'=4] {'x','tp'}, dimensions={0} | all-to-all | bytes 4456448 | tf_op jit(solution)/shard_map/all_to_all | solution.py:24
  38.0 5.9 %collective-permute-start = (bf16[4,4,136,512]{3,2,1,0:T(8,128)(2,1)S(1)}, bf16[4,4,136,512]{3,2,1,0:T(8,128)(2,1)}, u32[]{:S(2)}, u32[]{:S(2)}) collective-permute-start(bf16[4,4,136,512]{3,2,1,0:T(8,128)(2,1)S(1)} %bitcast.31), channel_id=1, source_target_pairs={{0,4},{4,0},{1,5},{5,1},{2,6},{6,2},{3,7},{7,3},{8,12},{12,8},{9,1... | collective-permute-start | bytes 6684680 | tf_op jit(solution)/shard_map/ppermute | solution.py:28
  45.4 8.1 %all_to_all.31 = bf16[8,16,256]{2,1,0:T(8,128)(2,1)S(1)} all-to-all(bf16[8,16,256]{2,1,0:T(8,128)(2,1)} %bitcast.47), channel_id=1, replica_groups=mesh['zh'=4,'zl'=4,'x'=4,'c'=2,'tp'=4] {'x','c'}, dimensions={0} | all-to-all | bytes 131072 | tf_op jit(solution)/shard_map/all_to_all | solution.py:24
  54.3 12.7 %collective-permute-start.2 = (bf16[176,256]{1,0:T(8,128)(2,1)S(1)}, bf16[176,256]{1,0:T(8,128)(2,1)S(1)}, u32[]{:S(2)}, u32[]{:S(2)}) collective-permute-start(bf16[176,256]{1,0:T(8,128)(2,1)S(1)} %get-tuple-element.36), channel_id=1, source_target_pairs={{0,384},{32,416},{64,448},{96,480},{128,0},{160,32},{192,64},{224,... | collective-permute-start | bytes 270344 | tf_op jit(solution)/shard_map/ppermute | solution.py:493
  67.0 4.9 %collective-permute-start.3 = (bf16[176,256]{1,0:T(8,128)(2,1)S(1)}, bf16[176,256]{1,0:T(8,128)(2,1)S(1)}, u32[]{:S(2)}, u32[]{:S(2)}) collective-permute-start(bf16[176,256]{1,0:T(8,128)(2,1)S(1)} %get-tuple-element.36), channel_id=1, source_target_pairs={{0,256},{32,288},{64,320},{96,352},{128,384},{160,416},{192,448},{... | collective-permute-start | bytes 270344 | tf_op jit(solution)/shard_map/ppermute | solution.py:493
  71.9 7.3 %collective-permute-start.1 = (bf16[176,256]{1,0:T(8,128)(2,1)S(1)}, bf16[176,256]{1,0:T(8,128)(2,1)S(1)}, u32[]{:S(2)}, u32[]{:S(2)}) collective-permute-start(bf16[176,256]{1,0:T(8,128)(2,1)S(1)} %get-tuple-element.36), channel_id=1, source_target_pairs={{0,128},{32,160},{64,192},{96,224},{128,256},{160,288},{192,320},{... | collective-permute-start | bytes 270344 | tf_op jit(solution)/shard_map/ppermute | solution.py:493
  81.5 4.4 %collective-permute-done.1 = bf16[176,256]{1,0:T(8,128)(2,1)S(1)} collective-permute-done((bf16[176,256]{1,0:T(8,128)(2,1)S(1)}, bf16[176,256]{1,0:T(8,128)(2,1)S(1)}, u32[]{:S(2)}, u32[]{:S(2)}) %collective-permute-start.1) | collective-permute-done | bytes 90144 | tf_op jit(solution)/shard_map/ppermute | solution.py:493
  86.0 8.3 %collective-permute-start.5 = (bf16[4,176,256]{2,1,0:T(8,128)(2,1)S(1)}, bf16[4,176,256]{2,1,0:T(8,128)(2,1)S(1)}, u32[]{:S(2)}, u32[]{:S(2)}) collective-permute-start(bf16[4,176,256]{2,1,0:T(8,128)(2,1)S(1)} %pad_maximum_fusion.1.w0_ref), channel_id=1, source_target_pairs={{0,32},{32,64},{64,96},{96,128},{128,160},{160,192},{192,224},{224... | collective-permute-start | bytes 1081352 | tf_op jit(solution)/shard_map/ppermute | solution.py:493
  94.3 4.7 %collective-permute-start.4 = (bf16[4,176,256]{2,1,0:T(8,128)(2,1)S(1)}, bf16[4,176,256]{2,1,0:T(8,128)(2,1)}, u32[]{:S(2)}, u32[]{:S(2)}) collective-permute-start(bf16[4,176,256]{2,1,0:T(8,128)(2,1)S(1)} %pad_maximum_fusion.1.w0_ref), channel_id=1, source_target_pairs={{0,480},{32,0},{64,32},{96,64},{128,96},{160,128},{192,160},{224,1... | collective-permute-start | bytes 1081352 | tf_op jit(solution)/shard_map/ppermute | solution.py:493
  101.7 5.5 %collective-permute-start.6 = (bf16[2,176,256]{2,1,0:T(8,128)(2,1)}, bf16[2,176,256]{2,1,0:T(8,128)(2,1)}, u32[]{:S(2)}, u32[]{:S(2)}) collective-permute-start(bf16[2,176,256]{2,1,0:T(8,128)(2,1)} %get-tuple-element.34), channel_id=1, source_target_pairs={{0,448},{32,480},{64,0},{96,32},{128,64},{160,96},{192,128},{224,1... | collective-permute-start | bytes 540680 | tf_op jit(solution)/shard_map/ppermute | solution.py:493
  109.1 5.3 %collective-permute-done.7.high_ref = bf16[2,176,256]{2,1,0:T(8,128)(2,1)} collective-permute-done((bf16[2,176,256]{2,1,0:T(8,128)(2,1)}, bf16[2,176,256]{2,1,0:T(8,128)(2,1)}, u32[]{:S(2)}, u32[]{:S(2)}) %collective-permute-start.7) | collective-permute-done | bytes 180256 | tf_op jit(solution)/shard_map/ppermute | solution.py:493
  115.5 6.5 %project.1 = (bf16[4,4,2,128,128]{4,3,2,1,0:T(8,128)(2,1)}, bf16[4,2,128,128]{3,2,1,0:T(8,128)(2,1)}, bf16[2,128,128]{2,1,0:T(8,128)(2,1)}, f32[2,8,128]{2,1,0:T...) custom-call(s32[4]{0:T(128)} %pad_add_fusion.place_ref, ...), custom_call_target="tpu_custom_call" | custom-call | tf_op jit(solution)/shard_map/project/pallas_call | solution.py:542
  122.0 18.6 %all_to_all.32.qk_ref = bf16[4,1024,128]{2,1,0:T(8,128)(2,1)} all-to-all(bf16[4,1024,128]{2,1,0:T(8,128)(2,1)} %bitcast.35), channel_id=1, replica_groups=mesh['zh'=4,'zl'=4,'x'=4,'c'=2,'tp'=4] {'x'}, dimensions={0} | all-to-all | bytes 2097152 | tf_op jit(solution)/shard_map/all_to_all | solution.py:24
  140.5 3.2 %slab_state.1 = bf16[4,72,256]{2,1,0:T(8,128)(2,1)} custom-call(bf16[4,1024,128]{2,1,0:T(8,128)(2,1)} %all_to_all.32.qk_ref, bf16[1024,128]{1,0:T(8,128)(2,1)} %bitcast.36, f32[2,8,128]{2,1,0:T(8,128)} %get-tuple-element.21.gate_ref, bf16[2,128,128]{2,1,0:T(8,128)(2,1)} %get-tuple-element.22.glu_ref), custom_call_target="tpu_custom_call" | custom-call | tf_op jit(solution)/shard_map/slab_state/pallas_call | solution.py:585
  143.8 9.6 %all_to_all.33.in_ref = bf16[4,72,256]{2,1,0:T(8,128)(2,1)} all-to-all(bf16[4,72,256]{2,1,0:T(8,128)(2,1)} %slab_state.1), channel_id=1, replica_groups=mesh['zh'=4,'zl'=4,'x'=4,'c'=2,'tp'=4] {'zl'}, dimensions={0} | all-to-all | bytes 294912 | tf_op jit(solution)/shard_map/all_to_all | solution.py:24
  155.2 7.3 %all-to-all-start.4 = ((bf16[4,72,256]{2,1,0:T(8,128)(2,1)}), bf16[4,72,256]{2,1,0:T(8,128)(2,1)S(1)}, u32[]{:S(2)}, u32[]{:S(2)}) async-start(bf16[4,72,256]{2,1,0:T(8,128)(2,1)} %group.1), calls=%async_computation.4 | async-start | bytes 294912 | tf_op jit(solution)/shard_map/all_to_all | solution.py:24
  162.5 2.9 %collective-permute-start.10 = (bf16[4,16,768]{2,1,0:T(8,128)(2,1)S(1)}, bf16[4,16,768]{2,1,0:T(8,128)(2,1)S(1)}, u32[]{:S(2)}, u32[]{:S(2)}) collective-permute-start(bf16[4,16,768]{2,1,0:T(8,128)(2,1)S(1)} %get-tuple-element.30), channel_id=1, source_target_pairs={{0,3},{1,0},{2,1},{3,2},{4,7},{5,4},{6,5},{7,6},{8,11},{9,8},{10,9... | collective-permute-start | bytes 294920 | tf_op jit(solution)/shard_map/ppermute | solution.py:561
  172.4 2.9 %collective-permute-done.8 = bf16[4,16,768]{2,1,0:T(8,128)(2,1)S(1)} collective-permute-done((bf16[4,16,768]{2,1,0:T(8,128)(2,1)S(1)}, bf16[4,16,768]{2,1,0:T(8,128)(2,1)S(1)}, u32[]{:S(2)}, u32[]{:S(2)}) %collective-permute-start.8) | collective-permute-done | bytes 98336 | tf_op jit(solution)/shard_map/ppermute | solution.py:561
  177.5 3.7 %collective-permute-start.12 = (bf16[4,4,16,768]{3,2,1,0:T(8,128)(2,1)S(1)}, bf16[4,4,16,768]{3,2,1,0:T(8,128)(2,1)S(1)}, u32[]{:S(2)}, u32[]{:S(2)}) collective-permute-start(bf16[4,4,16,768]{3,2,1,0:T(8,128)(2,1)S(1)} %pad_maximum_fusion.refs_0_), channel_id=1, source_target_pairs={{0,16},{8,24},{16,0},{24,8},{1,17},{9,25},{17,1},{25,9},{2,18},{10... | collective-permute-start | bytes 1179656 | tf_op jit(solution)/shard_map/ppermute | solution.py:567
  183.7 7.8 %local.1 = (f32[1024,128]{1,0:T(8,128)}, f32[256,128]{1,0:T(8,128)}, bf16[1024,256]{1,0:T(8,128)(2,1)}) custom-call(s32[4]{0:T(128)} %pad_add_fusion.place_ref, bf16[4,1024,128]{2,1,0:T(8,128)(2,1)} %all_to_all.32.qk_ref, bf16[1024,128]{1,0:T(8,128)(2,1)} %bitcast.37, f32[2,8,128]{2,1,0:T(8,128)} %get-tuple-element.21.gate_ref, ...), custom_call_target="tpu_custom_call" | custom-call | tf_op jit(solution)/shard_map/local/pallas_call | solution.py:609
  192.2 4.3 %cell.1 = bf16[4,2,4,96,128]{4,3,2,1,0:T(8,128)(2,1)} custom-call(s32[4]{0:T(128)} %pad_add_fusion.place_ref, bf16[4,72,256]{2,1,0:T(8,128)(2,1)} %copy-done.4, bf16[4,72,256]{2,1,0:T(8,128)(2,1)} %all_to_all.33.in_ref, bf16[1024,256]{1,0:T(8,128)(2,1)} %get-tuple-element.23.q_ref, f32[1024,128]{1,0:T(8,128)} %get-tuple-element.24.local_ref, ...), custom_call_target="tpu_custom_call" | custom-call | tf_op jit(solution)/shard_map/cell/pallas_call | solution.py:618
  196.5 10.4 %all-to-all-start.5 = ((bf16[32,96,128]{2,1,0:T(8,128)(2,1)}), bf16[32,96,128]{2,1,0:T(8,128)(2,1)S(1)}, u32[]{:S(2)}, u32[]{:S(2)}) async-start(bf16[32,96,128]{2,1,0:T(8,128)(2,1)} %bitcast.34), calls=%async_computation.5 | async-start | bytes 1572864 | tf_op jit(solution)/shard_map/all_to_all | solution.py:24
  217.2 3.7 %assemble.1.weight_ref = bf16[4,4,4,2,16,768]{5,4,3,2,1,0:T(8,128)(2,1)} custom-call(s32[4]{0:T(128)} %pad_add_fusion.place_ref, bf16[4,4,16,768]{3,2,1,0:T(8,128)(2,1)} %copy-done.2, bf16[4,4,16,768]{3,2,1,0:T(8,128)(2,1)} %copy-done.7, bf16[4,4,16,768]{3,2,1,0:T(8,128)(2,1)} %copy-done.6, bf16[4,4,16,768]{3,2,1,0:T(8,128)(2,1)} %copy-done.5, ...), custom_call_target="tpu_custom_call" | custom-call | tf_op jit(solution)/shard_map/assemble/pallas_call | solution.py:629
  221.8 4.4 %finish.1 = bf16[128,512]{1,0:T(8,128)(2,1)} custom-call(bf16[4,2,4,96,128]{4,3,2,1,0:T(8,128)(2,1)} %bitcast.33, bf16[4,4,4,2,16,768]{5,4,3,2,1,0:T(8,128)(2,1)} %assemble.1.weight_ref, f32[4,512]{1,0:T(4,128)} %get-tuple-element.27.memory_gain_ref, f32[4,256]{1,0:T(4,128)} %get-tuple-element.28.conv_gain_ref), custom_call_target="tpu_custom_call" | custom-call | tf_op jit(solution)/shard_map/finish/pallas_call | solution.py:630
  (69 shorter events, 39.2 us)
Async XLA Ops:
  3.7 103.4 %copy-start.13 = (bf16[2048,2]{0,1:T(2,128)(2,1)S(1)}, bf16[2048,2]{0,1:T(2,128)(2,1)}, u32[]{:S(2)}) copy-start(bf16[2048,2]{0,1:T(2,128)(2,1)} %param.24) | copy-start | bytes 24580
  3.7 103.5 %copy-start.14 = (bf16[2048,2]{0,1:T(2,128)(2,1)S(1)}, bf16[2048,2]{0,1:T(2,128)(2,1)}, u32[]{:S(2)}) copy-start(bf16[2048,2]{0,1:T(2,128)(2,1)} %param.23) | copy-start | bytes 24580
  38.0 76.8 %copy-start = (bf16[16,136,512]{2,1,0:T(8,128)(2,1)}, bf16[16,136,512]{2,1,0:T(8,128)(2,1)S(1)}, u32[]{:S(2)}) copy-start(bf16[16,136,512]{2,1,0:T(8,128)(2,1)S(1)} %all_to_all.30) | copy-start | bytes 6684676
  38.0 76.8 %collective-permute-start = (bf16[4,4,136,512]{3,2,1,0:T(8,128)(2,1)S(1)}, bf16[4,4,136,512]{3,2,1,0:T(8,128)(2,1)}, u32[]{:S(2)}, u32[]{:S(2)}) collective-permute-start(bf16[4,4,136,512]{3,2,1,0:T(8,128)(2,1)S(1)} %bitcast.31), channel_id=1, source_target_pairs={{0,4},{4,0},{1,5},{5,1},{2,6},{6,2},{3,7},{7,3},{8,12},{12,8},{9,1... | collective-permute-start | bytes 6684680 | tf_op jit(solution)/shard_map/ppermute | solution.py:28
  54.3 26.1 %collective-permute-start.2 = (bf16[176,256]{1,0:T(8,128)(2,1)S(1)}, bf16[176,256]{1,0:T(8,128)(2,1)S(1)}, u32[]{:S(2)}, u32[]{:S(2)}) collective-permute-start(bf16[176,256]{1,0:T(8,128)(2,1)S(1)} %get-tuple-element.36), channel_id=1, source_target_pairs={{0,384},{32,416},{64,448},{96,480},{128,0},{160,32},{192,64},{224,... | collective-permute-start | bytes 270344 | tf_op jit(solution)/shard_map/ppermute | solution.py:493
  67.0 14.5 %collective-permute-start.3 = (bf16[176,256]{1,0:T(8,128)(2,1)S(1)}, bf16[176,256]{1,0:T(8,128)(2,1)S(1)}, u32[]{:S(2)}, u32[]{:S(2)}) collective-permute-start(bf16[176,256]{1,0:T(8,128)(2,1)S(1)} %get-tuple-element.36), channel_id=1, source_target_pairs={{0,256},{32,288},{64,320},{96,352},{128,384},{160,416},{192,448},{... | collective-permute-start | bytes 270344 | tf_op jit(solution)/shard_map/ppermute | solution.py:493
  71.9 13.9 %collective-permute-start.1 = (bf16[176,256]{1,0:T(8,128)(2,1)S(1)}, bf16[176,256]{1,0:T(8,128)(2,1)S(1)}, u32[]{:S(2)}, u32[]{:S(2)}) collective-permute-start(bf16[176,256]{1,0:T(8,128)(2,1)S(1)} %get-tuple-element.36), channel_id=1, source_target_pairs={{0,128},{32,160},{64,192},{96,224},{128,256},{160,288},{192,320},{... | collective-permute-start | bytes 270344 | tf_op jit(solution)/shard_map/ppermute | solution.py:493
  86.0 28.8 %collective-permute-start.5 = (bf16[4,176,256]{2,1,0:T(8,128)(2,1)S(1)}, bf16[4,176,256]{2,1,0:T(8,128)(2,1)S(1)}, u32[]{:S(2)}, u32[]{:S(2)}) collective-permute-start(bf16[4,176,256]{2,1,0:T(8,128)(2,1)S(1)} %pad_maximum_fusion.1.w0_ref), channel_id=1, source_target_pairs={{0,32},{32,64},{64,96},{96,128},{128,160},{160,192},{192,224},{224... | collective-permute-start | bytes 1081352 | tf_op jit(solution)/shard_map/ppermute | solution.py:493
  94.3 20.5 %collective-permute-start.4 = (bf16[4,176,256]{2,1,0:T(8,128)(2,1)S(1)}, bf16[4,176,256]{2,1,0:T(8,128)(2,1)}, u32[]{:S(2)}, u32[]{:S(2)}) collective-permute-start(bf16[4,176,256]{2,1,0:T(8,128)(2,1)S(1)} %pad_maximum_fusion.1.w0_ref), channel_id=1, source_target_pairs={{0,480},{32,0},{64,32},{96,64},{128,96},{160,128},{192,160},{224,1... | collective-permute-start | bytes 1081352 | tf_op jit(solution)/shard_map/ppermute | solution.py:493
  99.8 14.6 %collective-permute-start.7 = (bf16[2,176,256]{2,1,0:T(8,128)(2,1)}, bf16[2,176,256]{2,1,0:T(8,128)(2,1)}, u32[]{:S(2)}, u32[]{:S(2)}) collective-permute-start(bf16[2,176,256]{2,1,0:T(8,128)(2,1)} %get-tuple-element.33), channel_id=1, source_target_pairs={{0,64},{32,96},{64,128},{96,160},{128,192},{160,224},{192,256},{22... | collective-permute-start | bytes 540680 | tf_op jit(solution)/shard_map/ppermute | solution.py:493
  101.7 13.1 %collective-permute-start.6 = (bf16[2,176,256]{2,1,0:T(8,128)(2,1)}, bf16[2,176,256]{2,1,0:T(8,128)(2,1)}, u32[]{:S(2)}, u32[]{:S(2)}) collective-permute-start(bf16[2,176,256]{2,1,0:T(8,128)(2,1)} %get-tuple-element.34), channel_id=1, source_target_pairs={{0,448},{32,480},{64,0},{96,32},{128,64},{160,96},{192,128},{224,1... | collective-permute-start | bytes 540680 | tf_op jit(solution)/shard_map/ppermute | solution.py:493
  122.0 40.5 %copy-start.11 = (bf16[4,4,16,768]{3,2,1,0:T(8,128)(2,1)S(1)}, bf16[4,4,16,768]{3,2,1,0:T(8,128)(2,1)}, u32[]{:S(2)}) copy-start(bf16[4,4,16,768]{3,2,1,0:T(8,128)(2,1)} %get-tuple-element.26) | copy-start | bytes 1179652
  155.2 36.4 %all-to-all-start.4 = ((bf16[4,72,256]{2,1,0:T(8,128)(2,1)}), bf16[4,72,256]{2,1,0:T(8,128)(2,1)S(1)}, u32[]{:S(2)}, u32[]{:S(2)}) async-start(bf16[4,72,256]{2,1,0:T(8,128)(2,1)} %group.1), calls=%async_computation.4 | async-start | bytes 294912 | tf_op jit(solution)/shard_map/all_to_all | solution.py:24
  162.5 7.9 %collective-permute-start.10 = (bf16[4,16,768]{2,1,0:T(8,128)(2,1)S(1)}, bf16[4,16,768]{2,1,0:T(8,128)(2,1)S(1)}, u32[]{:S(2)}, u32[]{:S(2)}) collective-permute-start(bf16[4,16,768]{2,1,0:T(8,128)(2,1)S(1)} %get-tuple-element.30), channel_id=1, source_target_pairs={{0,3},{1,0},{2,1},{3,2},{4,7},{5,4},{6,5},{7,6},{8,11},{9,8},{10,9... | collective-permute-start | bytes 294920 | tf_op jit(solution)/shard_map/ppermute | solution.py:561
  165.5 6.9 %collective-permute-start.9 = (bf16[4,16,768]{2,1,0:T(8,128)(2,1)S(1)}, bf16[4,16,768]{2,1,0:T(8,128)(2,1)S(1)}, u32[]{:S(2)}, u32[]{:S(2)}) collective-permute-start(bf16[4,16,768]{2,1,0:T(8,128)(2,1)S(1)} %get-tuple-element.31), channel_id=1, source_target_pairs={{0,2},{1,3},{2,0},{3,1},{4,6},{5,7},{6,4},{7,5},{8,10},{9,11},{10,... | collective-permute-start | bytes 294920 | tf_op jit(solution)/shard_map/ppermute | solution.py:561
  168.4 6.9 %collective-permute-start.8 = (bf16[4,16,768]{2,1,0:T(8,128)(2,1)S(1)}, bf16[4,16,768]{2,1,0:T(8,128)(2,1)S(1)}, u32[]{:S(2)}, u32[]{:S(2)}) collective-permute-start(bf16[4,16,768]{2,1,0:T(8,128)(2,1)S(1)} %get-tuple-element.32), channel_id=1, source_target_pairs={{0,1},{1,2},{2,3},{3,0},{4,5},{5,6},{6,7},{7,4},{8,9},{9,10},{10,1... | collective-permute-start | bytes 294920 | tf_op jit(solution)/shard_map/ppermute | solution.py:561
  175.3 33.7 %collective-permute-start.13 = (bf16[4,4,16,768]{3,2,1,0:T(8,128)(2,1)S(1)}, bf16[4,4,16,768]{3,2,1,0:T(8,128)(2,1)S(1)}, u32[]{:S(2)}, u32[]{:S(2)}) collective-permute-start(bf16[4,4,16,768]{3,2,1,0:T(8,128)(2,1)S(1)} %pad_maximum_fusion.refs_0_), channel_id=1, source_target_pairs={{0,8},{8,16},{16,24},{24,0},{1,9},{9,17},{17,25},{25,1},{2,10},{10... | collective-permute-start | bytes 1179656 | tf_op jit(solution)/shard_map/ppermute | solution.py:567
  177.5 33.7 %collective-permute-start.12 = (bf16[4,4,16,768]{3,2,1,0:T(8,128)(2,1)S(1)}, bf16[4,4,16,768]{3,2,1,0:T(8,128)(2,1)S(1)}, u32[]{:S(2)}, u32[]{:S(2)}) collective-permute-start(bf16[4,4,16,768]{3,2,1,0:T(8,128)(2,1)S(1)} %pad_maximum_fusion.refs_0_), channel_id=1, source_target_pairs={{0,16},{8,24},{16,0},{24,8},{1,17},{9,25},{17,1},{25,9},{2,18},{10... | collective-permute-start | bytes 1179656 | tf_op jit(solution)/shard_map/ppermute | solution.py:567
  181.2 32.2 %collective-permute-start.11 = (bf16[4,4,16,768]{3,2,1,0:T(8,128)(2,1)S(1)}, bf16[4,4,16,768]{3,2,1,0:T(8,128)(2,1)S(1)}, u32[]{:S(2)}, u32[]{:S(2)}) collective-permute-start(bf16[4,4,16,768]{3,2,1,0:T(8,128)(2,1)S(1)} %pad_maximum_fusion.refs_0_), channel_id=1, source_target_pairs={{0,24},{8,0},{16,8},{24,16},{1,25},{9,1},{17,9},{25,17},{2,26},{10... | collective-permute-start | bytes 1179656 | tf_op jit(solution)/shard_map/ppermute | solution.py:567
  196.5 24.4 %all-to-all-start.5 = ((bf16[32,96,128]{2,1,0:T(8,128)(2,1)}), bf16[32,96,128]{2,1,0:T(8,128)(2,1)S(1)}, u32[]{:S(2)}, u32[]{:S(2)}) async-start(bf16[32,96,128]{2,1,0:T(8,128)(2,1)} %bitcast.34), calls=%async_computation.5 | async-start | bytes 1572864 | tf_op jit(solution)/shard_map/all_to_all | solution.py:24
  206.9 8.8 %collective-permute-start.14 = (bf16[4,4,16,768]{3,2,1,0:T(8,128)(2,1)S(1)}, bf16[4,4,16,768]{3,2,1,0:T(8,128)(2,1)S(1)}, u32[]{:S(2)}, u32[]{:S(2)}) collective-permute-start(bf16[4,4,16,768]{3,2,1,0:T(8,128)(2,1)S(1)} %pad_maximum_fusion.refs_0_), channel_id=1, source_target_pairs={{0,4},{4,0},{1,5},{5,1},{2,6},{6,2},{3,7},{7,3},{8,12},{12,8},{9,1... | collective-permute-start | bytes 1179656 | tf_op jit(solution)/shard_map/ppermute | solution.py:28
  209.1 6.6 %collective-permute-start.17 = (bf16[4,4,16,768]{3,2,1,0:T(8,128)(2,1)S(1)}, bf16[4,4,16,768]{3,2,1,0:T(8,128)(2,1)S(1)}, u32[]{:S(2)}, u32[]{:S(2)}) collective-permute-start(bf16[4,4,16,768]{3,2,1,0:T(8,128)(2,1)S(1)} %collective-permute-done.13.refs_3_), channel_id=1, source_target_pairs={{0,4},{4,0},{1,5},{5,1},{2,6},{6,2},{3,7},{7,3},{8,12},{12,8},{9,1... | collective-permute-start | bytes 1179656 | tf_op jit(solution)/shard_map/ppermute | solution.py:28
  211.3 4.4 %collective-permute-start.16 = (bf16[4,4,16,768]{3,2,1,0:T(8,128)(2,1)S(1)}, bf16[4,4,16,768]{3,2,1,0:T(8,128)(2,1)S(1)}, u32[]{:S(2)}, u32[]{:S(2)}) collective-permute-start(bf16[4,4,16,768]{3,2,1,0:T(8,128)(2,1)S(1)} %collective-permute-done.12.refs_2_), channel_id=1, source_target_pairs={{0,4},{4,0},{1,5},{5,1},{2,6},{6,2},{3,7},{7,3},{8,12},{12,8},{9,1... | collective-permute-start | bytes 1179656 | tf_op jit(solution)/shard_map/ppermute | solution.py:28
  213.4 3.7 %collective-permute-start.15 = (bf16[4,4,16,768]{3,2,1,0:T(8,128)(2,1)S(1)}, bf16[4,4,16,768]{3,2,1,0:T(8,128)(2,1)}, u32[]{:S(2)}, u32[]{:S(2)}) collective-permute-start(bf16[4,4,16,768]{3,2,1,0:T(8,128)(2,1)S(1)} %collective-permute-done.11.refs_1_), channel_id=1, source_target_pairs={{0,4},{4,0},{1,5},{5,1},{2,6},{6,2},{3,7},{7,3},{8,12},{12,8},{9,1... | collective-permute-start | bytes 1179656 | tf_op jit(solution)/shard_map/ppermute | solution.py:28
  (11 other events, 84.5 us)

commit v14 on v13

--- a/solution.py
+++ b/solution.py
@@ -529,7 +529,7 @@
     far = [from_z(mine, -step), mine, from_z(mine, step), opposite]
     own = exchange(sent, ("x", "tp")).reshape(nx, ny, length + 8, part)
     near = jnp.stack(far, axis=0)
-    halves = near[1:3], near[:2]
+    halves = jnp.stack(far[1:3], axis=0), jnp.stack(far[:2], axis=0)
     sets = [near, from_z(near, 1), from_z(near, -1)]
     sets += [from_z(halves[0], 2), from_z(halves[1], -2)]
     other = swapped(own, "c")
@@ -569,8 +569,8 @@
     out_parts = [out_part, from_x(out_part, 1)]
     from_last = from_x(out_part, 3)
     out_parts += [from_x(out_part, 2), from_last]
-    other_parts = [swapped(out, "c") for out in out_parts[:2]]
-    other_parts += [swapped(out, "c") for out in out_parts[2:]]
+    other_parts = [swapped(out, "c") for out in out_parts[:1]]
+    other_parts += [swapped(out, "c") for out in out_parts[1:]]
 
     state_rows = width + 8
     keys = all_qk.reshape(nx, slab, 2 * width)

time: 228 us -> 228 us (level)
  no operation moved by 1% of the time
where the time goes in v14:
time: 228 us; the launch traced here: 226 us
  starting transfers between devices  93.8 us (41%)
  blocking collectives  70.5 us (31%)
  Pallas kernels  35.7 us (16%)
  waiting for transfers between devices  17.9 us (8%)
  local copies, waits for them, and re-layouts  4.33 us (2%)
  other arithmetic  3.53 us (2%)
    all_to_all x4, blocking collectives, exchange(): return lax.all_to_all(pieces, axes, split_axis=0, concat_axis=0, tiled=True)  70.5 us
    ppermute x7, starting transfers between devices, from_z(): lax.ppermute(value, Z, [(j, (j - ahead) % members) for j in range(members)])  45.3 us
    all_to_all x2, starting transfers between devices, exchange(): return lax.all_to_all(pieces, axes, split_axis=0, concat_axis=0, tiled=True)  17.7 us
    ppermute x5, starting transfers between devices, swapped(): return lax.ppermute(value, axis, [(0, 1), (1, 0)])  14.5 us
    ppermute x7, waiting for transfers between devices, from_z(): lax.ppermute(value, Z, [(j, (j - ahead) % members) for j in range(members)])  12.4 us
    ppermute x3, starting transfers between devices, from_x(): return lax.ppermute(value, 'x', [(j, (j - ahead) % nx) for j in range(nx)])  8.42 us
    pallas_call x1, Pallas kernels, layer(): call_local(place, keys, value, gates, packed, conv_kernel)  7.84 us
    ppermute x3, starting transfers between devices, layer(): lax.ppermute(out_part[ahead], 'tp', [(j, (j + ahead) % ny) for j in range...  7.83 us
  transfers between devices with their start and end apart: 20, of which 8 were waited for; matrix products, arithmetic and copies ran while one was open for 2% of the time, Pallas kernels for 8%

profile of v14, /device:TPU:1, one launch (start us, length us, event | category | flops | bytes accessed | tf_op | source)
XLA Modules:
  0.0 226.2 jit_solution(14662881762345091607)
XLA Ops:
  3.7 34.3 %all_to_all.30 = bf16[16,136,512]{2,1,0:T(8,128)(2,1)S(1)} all-to-all(bf16[16,136,512]{2,1,0:T(8,128)(2,1)} %pack.1), channel_id=1, replica_groups=mesh['zh'=4,'zl'=4,'x'=4,'c'=2,'tp'=4] {'x','tp'}, dimensions={0} | all-to-all | bytes 4456448 | tf_op jit(solution)/shard_map/all_to_all | solution.py:24
  38.0 5.9 %collective-permute-start = (bf16[4,4,136,512]{3,2,1,0:T(8,128)(2,1)S(1)}, bf16[4,4,136,512]{3,2,1,0:T(8,128)(2,1)}, u32[]{:S(2)}, u32[]{:S(2)}) collective-permute-start(bf16[4,4,136,512]{3,2,1,0:T(8,128)(2,1)S(1)} %bitcast.31), channel_id=1, source_target_pairs={{0,4},{4,0},{1,5},{5,1},{2,6},{6,2},{3,7},{7,3},{8,12},{12,8},{9,1... | collective-permute-start | bytes 6684680 | tf_op jit(solution)/shard_map/ppermute | solution.py:28
  45.4 8.1 %all_to_all.31 = bf16[8,16,256]{2,1,0:T(8,128)(2,1)S(1)} all-to-all(bf16[8,16,256]{2,1,0:T(8,128)(2,1)} %bitcast.47), channel_id=1, replica_groups=mesh['zh'=4,'zl'=4,'x'=4,'c'=2,'tp'=4] {'x','c'}, dimensions={0} | all-to-all | bytes 131072 | tf_op jit(solution)/shard_map/all_to_all | solution.py:24
  54.3 12.7 %collective-permute-start.2 = (bf16[176,256]{1,0:T(8,128)(2,1)S(1)}, bf16[176,256]{1,0:T(8,128)(2,1)S(1)}, u32[]{:S(2)}, u32[]{:S(2)}) collective-permute-start(bf16[176,256]{1,0:T(8,128)(2,1)S(1)} %get-tuple-element.36), channel_id=1, source_target_pairs={{0,384},{32,416},{64,448},{96,480},{128,0},{160,32},{192,64},{224,... | collective-permute-start | bytes 270344 | tf_op jit(solution)/shard_map/ppermute | solution.py:493
  67.0 4.9 %collective-permute-start.3 = (bf16[176,256]{1,0:T(8,128)(2,1)S(1)}, bf16[176,256]{1,0:T(8,128)(2,1)S(1)}, u32[]{:S(2)}, u32[]{:S(2)}) collective-permute-start(bf16[176,256]{1,0:T(8,128)(2,1)S(1)} %get-tuple-element.36), channel_id=1, source_target_pairs={{0,256},{32,288},{64,320},{96,352},{128,384},{160,416},{192,448},{... | collective-permute-start | bytes 270344 | tf_op jit(solution)/shard_map/ppermute | solution.py:493
  71.9 7.3 %collective-permute-start.1 = (bf16[176,256]{1,0:T(8,128)(2,1)S(1)}, bf16[176,256]{1,0:T(8,128)(2,1)S(1)}, u32[]{:S(2)}, u32[]{:S(2)}) collective-permute-start(bf16[176,256]{1,0:T(8,128)(2,1)S(1)} %get-tuple-element.36), channel_id=1, source_target_pairs={{0,128},{32,160},{64,192},{96,224},{128,256},{160,288},{192,320},{... | collective-permute-start | bytes 270344 | tf_op jit(solution)/shard_map/ppermute | solution.py:493
  81.5 4.4 %collective-permute-done.1 = bf16[176,256]{1,0:T(8,128)(2,1)S(1)} collective-permute-done((bf16[176,256]{1,0:T(8,128)(2,1)S(1)}, bf16[176,256]{1,0:T(8,128)(2,1)S(1)}, u32[]{:S(2)}, u32[]{:S(2)}) %collective-permute-start.1) | collective-permute-done | bytes 90144 | tf_op jit(solution)/shard_map/ppermute | solution.py:493
  86.0 8.3 %collective-permute-start.5 = (bf16[4,176,256]{2,1,0:T(8,128)(2,1)S(1)}, bf16[4,176,256]{2,1,0:T(8,128)(2,1)S(1)}, u32[]{:S(2)}, u32[]{:S(2)}) collective-permute-start(bf16[4,176,256]{2,1,0:T(8,128)(2,1)S(1)} %pad_maximum_fusion.1.w0_ref), channel_id=1, source_target_pairs={{0,32},{32,64},{64,96},{96,128},{128,160},{160,192},{192,224},{224... | collective-permute-start | bytes 1081352 | tf_op jit(solution)/shard_map/ppermute | solution.py:493
  94.3 4.7 %collective-permute-start.4 = (bf16[4,176,256]{2,1,0:T(8,128)(2,1)S(1)}, bf16[4,176,256]{2,1,0:T(8,128)(2,1)}, u32[]{:S(2)}, u32[]{:S(2)}) collective-permute-start(bf16[4,176,256]{2,1,0:T(8,128)(2,1)S(1)} %pad_maximum_fusion.1.w0_ref), channel_id=1, source_target_pairs={{0,480},{32,0},{64,32},{96,64},{128,96},{160,128},{192,160},{224,1... | collective-permute-start | bytes 1081352 | tf_op jit(solution)/shard_map/ppermute | solution.py:493
  101.7 5.5 %collective-permute-start.6 = (bf16[2,176,256]{2,1,0:T(8,128)(2,1)}, bf16[2,176,256]{2,1,0:T(8,128)(2,1)}, u32[]{:S(2)}, u32[]{:S(2)}) collective-permute-start(bf16[2,176,256]{2,1,0:T(8,128)(2,1)} %get-tuple-element.34), channel_id=1, source_target_pairs={{0,448},{32,480},{64,0},{96,32},{128,64},{160,96},{192,128},{224,1... | collective-permute-start | bytes 540680 | tf_op jit(solution)/shard_map/ppermute | solution.py:493
  109.1 5.3 %collective-permute-done.7.high_ref = bf16[2,176,256]{2,1,0:T(8,128)(2,1)} collective-permute-done((bf16[2,176,256]{2,1,0:T(8,128)(2,1)}, bf16[2,176,256]{2,1,0:T(8,128)(2,1)}, u32[]{:S(2)}, u32[]{:S(2)}) %collective-permute-start.7) | collective-permute-done | bytes 180256 | tf_op jit(solution)/shard_map/ppermute | solution.py:493
  115.5 6.5 %project.1 = (bf16[4,4,2,128,128]{4,3,2,1,0:T(8,128)(2,1)}, bf16[4,2,128,128]{3,2,1,0:T(8,128)(2,1)}, bf16[2,128,128]{2,1,0:T(8,128)(2,1)}, f32[2,8,128]{2,1,0:T...) custom-call(s32[4]{0:T(128)} %pad_add_fusion.place_ref, ...), custom_call_target="tpu_custom_call" | custom-call | tf_op jit(solution)/shard_map/project/pallas_call | solution.py:542
  122.0 18.6 %all_to_all.32.qk_ref = bf16[4,1024,128]{2,1,0:T(8,128)(2,1)} all-to-all(bf16[4,1024,128]{2,1,0:T(8,128)(2,1)} %bitcast.35), channel_id=1, replica_groups=mesh['zh'=4,'zl'=4,'x'=4,'c'=2,'tp'=4] {'x'}, dimensions={0} | all-to-all | bytes 2097152 | tf_op jit(solution)/shard_map/all_to_all | solution.py:24
  140.5 3.2 %slab_state.1 = bf16[4,72,256]{2,1,0:T(8,128)(2,1)} custom-call(bf16[4,1024,128]{2,1,0:T(8,128)(2,1)} %all_to_all.32.qk_ref, bf16[1024,128]{1,0:T(8,128)(2,1)} %bitcast.36, f32[2,8,128]{2,1,0:T(8,128)} %get-tuple-element.21.gate_ref, bf16[2,128,128]{2,1,0:T(8,128)(2,1)} %get-tuple-element.22.glu_ref), custom_call_target="tpu_custom_call" | custom-call | tf_op jit(solution)/shard_map/slab_state/pallas_call | solution.py:585
  143.8 9.6 %all_to_all.33.in_ref = bf16[4,72,256]{2,1,0:T(8,128)(2,1)} all-to-all(bf16[4,72,256]{2,1,0:T(8,128)(2,1)} %slab_state.1), channel_id=1, replica_groups=mesh['zh'=4,'zl'=4,'x'=4,'c'=2,'tp'=4] {'zl'}, dimensions={0} | all-to-all | bytes 294912 | tf_op jit(solution)/shard_map/all_to_all | solution.py:24
  155.2 7.3 %all-to-all-start.4 = ((bf16[4,72,256]{2,1,0:T(8,128)(2,1)}), bf16[4,72,256]{2,1,0:T(8,128)(2,1)S(1)}, u32[]{:S(2)}, u32[]{:S(2)}) async-start(bf16[4,72,256]{2,1,0:T(8,128)(2,1)} %group.1), calls=%async_computation.4 | async-start | bytes 294912 | tf_op jit(solution)/shard_map/all_to_all | solution.py:24
  162.5 2.9 %collective-permute-start.10 = (bf16[4,16,768]{2,1,0:T(8,128)(2,1)S(1)}, bf16[4,16,768]{2,1,0:T(8,128)(2,1)S(1)}, u32[]{:S(2)}, u32[]{:S(2)}) collective-permute-start(bf16[4,16,768]{2,1,0:T(8,128)(2,1)S(1)} %get-tuple-element.30), channel_id=1, source_target_pairs={{0,3},{1,0},{2,1},{3,2},{4,7},{5,4},{6,5},{7,6},{8,11},{9,8},{10,9... | collective-permute-start | bytes 294920 | tf_op jit(solution)/shard_map/ppermute | solution.py:561
  172.4 2.9 %collective-permute-done.8 = bf16[4,16,768]{2,1,0:T(8,128)(2,1)S(1)} collective-permute-done((bf16[4,16,768]{2,1,0:T(8,128)(2,1)S(1)}, bf16[4,16,768]{2,1,0:T(8,128)(2,1)S(1)}, u32[]{:S(2)}, u32[]{:S(2)}) %collective-permute-start.8) | collective-permute-done | bytes 98336 | tf_op jit(solution)/shard_map/ppermute | solution.py:561
  177.5 3.7 %collective-permute-start.12 = (bf16[4,4,16,768]{3,2,1,0:T(8,128)(2,1)S(1)}, bf16[4,4,16,768]{3,2,1,0:T(8,128)(2,1)S(1)}, u32[]{:S(2)}, u32[]{:S(2)}) collective-permute-start(bf16[4,4,16,768]{3,2,1,0:T(8,128)(2,1)S(1)} %pad_maximum_fusion.refs_0_), channel_id=1, source_target_pairs={{0,16},{8,24},{16,0},{24,8},{1,17},{9,25},{17,1},{25,9},{2,18},{10... | collective-permute-start | bytes 1179656 | tf_op jit(solution)/shard_map/ppermute | solution.py:567
  183.7 7.8 %local.1 = (f32[1024,128]{1,0:T(8,128)}, f32[256,128]{1,0:T(8,128)}, bf16[1024,256]{1,0:T(8,128)(2,1)}) custom-call(s32[4]{0:T(128)} %pad_add_fusion.place_ref, bf16[4,1024,128]{2,1,0:T(8,128)(2,1)} %all_to_all.32.qk_ref, bf16[1024,128]{1,0:T(8,128)(2,1)} %bitcast.37, f32[2,8,128]{2,1,0:T(8,128)} %get-tuple-element.21.gate_ref, ...), custom_call_target="tpu_custom_call" | custom-call | tf_op jit(solution)/shard_map/local/pallas_call | solution.py:609
  192.2 4.3 %cell.1 = bf16[4,2,4,96,128]{4,3,2,1,0:T(8,128)(2,1)} custom-call(s32[4]{0:T(128)} %pad_add_fusion.place_ref, bf16[4,72,256]{2,1,0:T(8,128)(2,1)} %copy-done.4, bf16[4,72,256]{2,1,0:T(8,128)(2,1)} %all_to_all.33.in_ref, bf16[1024,256]{1,0:T(8,128)(2,1)} %get-tuple-element.23.q_ref, f32[1024,128]{1,0:T(8,128)} %get-tuple-element.24.local_ref, ...), custom_call_target="tpu_custom_call" | custom-call | tf_op jit(solution)/shard_map/cell/pallas_call | solution.py:618
  196.5 10.4 %all-to-all-start.5 = ((bf16[32,96,128]{2,1,0:T(8,128)(2,1)}), bf16[32,96,128]{2,1,0:T(8,128)(2,1)S(1)}, u32[]{:S(2)}, u32[]{:S(2)}) async-start(bf16[32,96,128]{2,1,0:T(8,128)(2,1)} %bitcast.34), calls=%async_computation.5 | async-start | bytes 1572864 | tf_op jit(solution)/shard_map/all_to_all | solution.py:24
  217.2 3.7 %assemble.1.weight_ref = bf16[4,4,4,2,16,768]{5,4,3,2,1,0:T(8,128)(2,1)} custom-call(s32[4]{0:T(128)} %pad_add_fusion.place_ref, bf16[4,4,16,768]{3,2,1,0:T(8,128)(2,1)} %copy-done.2, bf16[4,4,16,768]{3,2,1,0:T(8,128)(2,1)} %copy-done.7, bf16[4,4,16,768]{3,2,1,0:T(8,128)(2,1)} %copy-done.6, bf16[4,4,16,768]{3,2,1,0:T(8,128)(2,1)} %copy-done.5, ...), custom_call_target="tpu_custom_call" | custom-call | tf_op jit(solution)/shard_map/assemble/pallas_call | solution.py:629
  221.8 4.4 %finish.1 = bf16[128,512]{1,0:T(8,128)(2,1)} custom-call(bf16[4,2,4,96,128]{4,3,2,1,0:T(8,128)(2,1)} %bitcast.33, bf16[4,4,4,2,16,768]{5,4,3,2,1,0:T(8,128)(2,1)} %assemble.1.weight_ref, f32[4,512]{1,0:T(4,128)} %get-tuple-element.27.memory_gain_ref, f32[4,256]{1,0:T(4,128)} %get-tuple-element.28.conv_gain_ref), custom_call_target="tpu_custom_call" | custom-call | tf_op jit(solution)/shard_map/finish/pallas_call | solution.py:630
  (69 shorter events, 39.2 us)
Async XLA Ops:
  3.7 103.4 %copy-start.13 = (bf16[2048,2]{0,1:T(2,128)(2,1)S(1)}, bf16[2048,2]{0,1:T(2,128)(2,1)}, u32[]{:S(2)}) copy-start(bf16[2048,2]{0,1:T(2,128)(2,1)} %param.24) | copy-start | bytes 24580
  3.7 103.5 %copy-start.14 = (bf16[2048,2]{0,1:T(2,128)(2,1)S(1)}, bf16[2048,2]{0,1:T(2,128)(2,1)}, u32[]{:S(2)}) copy-start(bf16[2048,2]{0,1:T(2,128)(2,1)} %param.23) | copy-start | bytes 24580
  38.0 76.8 %copy-start = (bf16[16,136,512]{2,1,0:T(8,128)(2,1)}, bf16[16,136,512]{2,1,0:T(8,128)(2,1)S(1)}, u32[]{:S(2)}) copy-start(bf16[16,136,512]{2,1,0:T(8,128)(2,1)S(1)} %all_to_all.30) | copy-start | bytes 6684676
  38.0 76.8 %collective-permute-start = (bf16[4,4,136,512]{3,2,1,0:T(8,128)(2,1)S(1)}, bf16[4,4,136,512]{3,2,1,0:T(8,128)(2,1)}, u32[]{:S(2)}, u32[]{:S(2)}) collective-permute-start(bf16[4,4,136,512]{3,2,1,0:T(8,128)(2,1)S(1)} %bitcast.31), channel_id=1, source_target_pairs={{0,4},{4,0},{1,5},{5,1},{2,6},{6,2},{3,7},{7,3},{8,12},{12,8},{9,1... | collective-permute-start | bytes 6684680 | tf_op jit(solution)/shard_map/ppermute | solution.py:28
  54.3 26.1 %collective-permute-start.2 = (bf16[176,256]{1,0:T(8,128)(2,1)S(1)}, bf16[176,256]{1,0:T(8,128)(2,1)S(1)}, u32[]{:S(2)}, u32[]{:S(2)}) collective-permute-start(bf16[176,256]{1,0:T(8,128)(2,1)S(1)} %get-tuple-element.36), channel_id=1, source_target_pairs={{0,384},{32,416},{64,448},{96,480},{128,0},{160,32},{192,64},{224,... | collective-permute-start | bytes 270344 | tf_op jit(solution)/shard_map/ppermute | solution.py:493
  67.0 14.5 %collective-permute-start.3 = (bf16[176,256]{1,0:T(8,128)(2,1)S(1)}, bf16[176,256]{1,0:T(8,128)(2,1)S(1)}, u32[]{:S(2)}, u32[]{:S(2)}) collective-permute-start(bf16[176,256]{1,0:T(8,128)(2,1)S(1)} %get-tuple-element.36), channel_id=1, source_target_pairs={{0,256},{32,288},{64,320},{96,352},{128,384},{160,416},{192,448},{... | collective-permute-start | bytes 270344 | tf_op jit(solution)/shard_map/ppermute | solution.py:493
  71.9 13.9 %collective-permute-start.1 = (bf16[176,256]{1,0:T(8,128)(2,1)S(1)}, bf16[176,256]{1,0:T(8,128)(2,1)S(1)}, u32[]{:S(2)}, u32[]{:S(2)}) collective-permute-start(bf16[176,256]{1,0:T(8,128)(2,1)S(1)} %get-tuple-element.36), channel_id=1, source_target_pairs={{0,128},{32,160},{64,192},{96,224},{128,256},{160,288},{192,320},{... | collective-permute-start | bytes 270344 | tf_op jit(solution)/shard_map/ppermute | solution.py:493
  86.0 28.8 %collective-permute-start.5 = (bf16[4,176,256]{2,1,0:T(8,128)(2,1)S(1)}, bf16[4,176,256]{2,1,0:T(8,128)(2,1)S(1)}, u32[]{:S(2)}, u32[]{:S(2)}) collective-permute-start(bf16[4,176,256]{2,1,0:T(8,128)(2,1)S(1)} %pad_maximum_fusion.1.w0_ref), channel_id=1, source_target_pairs={{0,32},{32,64},{64,96},{96,128},{128,160},{160,192},{192,224},{224... | collective-permute-start | bytes 1081352 | tf_op jit(solution)/shard_map/ppermute | solution.py:493
  94.3 20.5 %collective-permute-start.4 = (bf16[4,176,256]{2,1,0:T(8,128)(2,1)S(1)}, bf16[4,176,256]{2,1,0:T(8,128)(2,1)}, u32[]{:S(2)}, u32[]{:S(2)}) collective-permute-start(bf16[4,176,256]{2,1,0:T(8,128)(2,1)S(1)} %pad_maximum_fusion.1.w0_ref), channel_id=1, source_target_pairs={{0,480},{32,0},{64,32},{96,64},{128,96},{160,128},{192,160},{224,1... | collective-permute-start | bytes 1081352 | tf_op jit(solution)/shard_map/ppermute | solution.py:493
  99.8 14.6 %collective-permute-start.7 = (bf16[2,176,256]{2,1,0:T(8,128)(2,1)}, bf16[2,176,256]{2,1,0:T(8,128)(2,1)}, u32[]{:S(2)}, u32[]{:S(2)}) collective-permute-start(bf16[2,176,256]{2,1,0:T(8,128)(2,1)} %get-tuple-element.33), channel_id=1, source_target_pairs={{0,64},{32,96},{64,128},{96,160},{128,192},{160,224},{192,256},{22... | collective-permute-start | bytes 540680 | tf_op jit(solution)/shard_map/ppermute | solution.py:493
  101.7 13.1 %collective-permute-start.6 = (bf16[2,176,256]{2,1,0:T(8,128)(2,1)}, bf16[2,176,256]{2,1,0:T(8,128)(2,1)}, u32[]{:S(2)}, u32[]{:S(2)}) collective-permute-start(bf16[2,176,256]{2,1,0:T(8,128)(2,1)} %get-tuple-element.34), channel_id=1, source_target_pairs={{0,448},{32,480},{64,0},{96,32},{128,64},{160,96},{192,128},{224,1... | collective-permute-start | bytes 540680 | tf_op jit(solution)/shard_map/ppermute | solution.py:493
  122.0 40.5 %copy-start.11 = (bf16[4,4,16,768]{3,2,1,0:T(8,128)(2,1)S(1)}, bf16[4,4,16,768]{3,2,1,0:T(8,128)(2,1)}, u32[]{:S(2)}) copy-start(bf16[4,4,16,768]{3,2,1,0:T(8,128)(2,1)} %get-tuple-element.26) | copy-start | bytes 1179652
  155.2 36.4 %all-to-all-start.4 = ((bf16[4,72,256]{2,1,0:T(8,128)(2,1)}), bf16[4,72,256]{2,1,0:T(8,128)(2,1)S(1)}, u32[]{:S(2)}, u32[]{:S(2)}) async-start(bf16[4,72,256]{2,1,0:T(8,128)(2,1)} %group.1), calls=%async_computation.4 | async-start | bytes 294912 | tf_op jit(solution)/shard_map/all_to_all | solution.py:24
  162.5 7.9 %collective-permute-start.10 = (bf16[4,16,768]{2,1,0:T(8,128)(2,1)S(1)}, bf16[4,16,768]{2,1,0:T(8,128)(2,1)S(1)}, u32[]{:S(2)}, u32[]{:S(2)}) collective-permute-start(bf16[4,16,768]{2,1,0:T(8,128)(2,1)S(1)} %get-tuple-element.30), channel_id=1, source_target_pairs={{0,3},{1,0},{2,1},{3,2},{4,7},{5,4},{6,5},{7,6},{8,11},{9,8},{10,9... | collective-permute-start | bytes 294920 | tf_op jit(solution)/shard_map/ppermute | solution.py:561
  165.5 6.9 %collective-permute-start.9 = (bf16[4,16,768]{2,1,0:T(8,128)(2,1)S(1)}, bf16[4,16,768]{2,1,0:T(8,128)(2,1)S(1)}, u32[]{:S(2)}, u32[]{:S(2)}) collective-permute-start(bf16[4,16,768]{2,1,0:T(8,128)(2,1)S(1)} %get-tuple-element.31), channel_id=1, source_target_pairs={{0,2},{1,3},{2,0},{3,1},{4,6},{5,7},{6,4},{7,5},{8,10},{9,11},{10,... | collective-permute-start | bytes 294920 | tf_op jit(solution)/shard_map/ppermute | solution.py:561
  168.4 6.9 %collective-permute-start.8 = (bf16[4,16,768]{2,1,0:T(8,128)(2,1)S(1)}, bf16[4,16,768]{2,1,0:T(8,128)(2,1)S(1)}, u32[]{:S(2)}, u32[]{:S(2)}) collective-permute-start(bf16[4,16,768]{2,1,0:T(8,128)(2,1)S(1)} %get-tuple-element.32), channel_id=1, source_target_pairs={{0,1},{1,2},{2,3},{3,0},{4,5},{5,6},{6,7},{7,4},{8,9},{9,10},{10,1... | collective-permute-start | bytes 294920 | tf_op jit(solution)/shard_map/ppermute | solution.py:561
  175.3 33.7 %collective-permute-start.13 = (bf16[4,4,16,768]{3,2,1,0:T(8,128)(2,1)S(1)}, bf16[4,4,16,768]{3,2,1,0:T(8,128)(2,1)S(1)}, u32[]{:S(2)}, u32[]{:S(2)}) collective-permute-start(bf16[4,4,16,768]{3,2,1,0:T(8,128)(2,1)S(1)} %pad_maximum_fusion.refs_0_), channel_id=1, source_target_pairs={{0,8},{8,16},{16,24},{24,0},{1,9},{9,17},{17,25},{25,1},{2,10},{10... | collective-permute-start | bytes 1179656 | tf_op jit(solution)/shard_map/ppermute | solution.py:567
  177.5 33.7 %collective-permute-start.12 = (bf16[4,4,16,768]{3,2,1,0:T(8,128)(2,1)S(1)}, bf16[4,4,16,768]{3,2,1,0:T(8,128)(2,1)S(1)}, u32[]{:S(2)}, u32[]{:S(2)}) collective-permute-start(bf16[4,4,16,768]{3,2,1,0:T(8,128)(2,1)S(1)} %pad_maximum_fusion.refs_0_), channel_id=1, source_target_pairs={{0,16},{8,24},{16,0},{24,8},{1,17},{9,25},{17,1},{25,9},{2,18},{10... | collective-permute-start | bytes 1179656 | tf_op jit(solution)/shard_map/ppermute | solution.py:567
  181.2 32.2 %collective-permute-start.11 = (bf16[4,4,16,768]{3,2,1,0:T(8,128)(2,1)S(1)}, bf16[4,4,16,768]{3,2,1,0:T(8,128)(2,1)S(1)}, u32[]{:S(2)}, u32[]{:S(2)}) collective-permute-start(bf16[4,4,16,768]{3,2,1,0:T(8,128)(2,1)S(1)} %pad_maximum_fusion.refs_0_), channel_id=1, source_target_pairs={{0,24},{8,0},{16,8},{24,16},{1,25},{9,1},{17,9},{25,17},{2,26},{10... | collective-permute-start | bytes 1179656 | tf_op jit(solution)/shard_map/ppermute | solution.py:567
  196.5 24.4 %all-to-all-start.5 = ((bf16[32,96,128]{2,1,0:T(8,128)(2,1)}), bf16[32,96,128]{2,1,0:T(8,128)(2,1)S(1)}, u32[]{:S(2)}, u32[]{:S(2)}) async-start(bf16[32,96,128]{2,1,0:T(8,128)(2,1)} %bitcast.34), calls=%async_computation.5 | async-start | bytes 1572864 | tf_op jit(solution)/shard_map/all_to_all | solution.py:24
  206.9 8.8 %collective-permute-start.14 = (bf16[4,4,16,768]{3,2,1,0:T(8,128)(2,1)S(1)}, bf16[4,4,16,768]{3,2,1,0:T(8,128)(2,1)S(1)}, u32[]{:S(2)}, u32[]{:S(2)}) collective-permute-start(bf16[4,4,16,768]{3,2,1,0:T(8,128)(2,1)S(1)} %pad_maximum_fusion.refs_0_), channel_id=1, source_target_pairs={{0,4},{4,0},{1,5},{5,1},{2,6},{6,2},{3,7},{7,3},{8,12},{12,8},{9,1... | collective-permute-start | bytes 1179656 | tf_op jit(solution)/shard_map/ppermute | solution.py:28
  209.1 6.6 %collective-permute-start.17 = (bf16[4,4,16,768]{3,2,1,0:T(8,128)(2,1)S(1)}, bf16[4,4,16,768]{3,2,1,0:T(8,128)(2,1)S(1)}, u32[]{:S(2)}, u32[]{:S(2)}) collective-permute-start(bf16[4,4,16,768]{3,2,1,0:T(8,128)(2,1)S(1)} %collective-permute-done.13.refs_3_), channel_id=1, source_target_pairs={{0,4},{4,0},{1,5},{5,1},{2,6},{6,2},{3,7},{7,3},{8,12},{12,8},{9,1... | collective-permute-start | bytes 1179656 | tf_op jit(solution)/shard_map/ppermute | solution.py:28
  211.3 4.4 %collective-permute-start.16 = (bf16[4,4,16,768]{3,2,1,0:T(8,128)(2,1)S(1)}, bf16[4,4,16,768]{3,2,1,0:T(8,128)(2,1)S(1)}, u32[]{:S(2)}, u32[]{:S(2)}) collective-permute-start(bf16[4,4,16,768]{3,2,1,0:T(8,128)(2,1)S(1)} %collective-permute-done.12.refs_2_), channel_id=1, source_target_pairs={{0,4},{4,0},{1,5},{5,1},{2,6},{6,2},{3,7},{7,3},{8,12},{12,8},{9,1... | collective-permute-start | bytes 1179656 | tf_op jit(solution)/shard_map/ppermute | solution.py:28
  213.4 3.7 %collective-permute-start.15 = (bf16[4,4,16,768]{3,2,1,0:T(8,128)(2,1)S(1)}, bf16[4,4,16,768]{3,2,1,0:T(8,128)(2,1)}, u32[]{:S(2)}, u32[]{:S(2)}) collective-permute-start(bf16[4,4,16,768]{3,2,1,0:T(8,128)(2,1)S(1)} %collective-permute-done.11.refs_1_), channel_id=1, source_target_pairs={{0,4},{4,0},{1,5},{5,1},{2,6},{6,2},{3,7},{7,3},{8,12},{12,8},{9,1... | collective-permute-start | bytes 1179656 | tf_op jit(solution)/shard_map/ppermute | solution.py:28
  (11 other events, 84.5 us)
